TPU v7x, 32 devices: a whole 2x2x4 slice. The times are simulated.
32 devices in a mesh: sp: 8 (over z, y), tp: 4 (over x, core).
Axes of the slice: x: 2, y: 2, z: 4, core: 2. Of those that a mesh axis runs over, the one named last changes fastest.
Arguments:
- latent: bfloat16 [4096, 2048], P(('sp', 'tp')), may hold values from -6 to 6
- context: bfloat16 [512, 2048], P('sp'), may hold values from -6 to 6
- condition: float32 [2048], replicated, may hold values from -6 to 6
- context_condition: float32 [2048], replicated, may hold values from -6 to 6
- norm_gain: float32 [2048], replicated, may hold values from 0.1 to 1.9
- shift_weight: bfloat16 [2048, 2048], P('sp', 'tp'), may hold values from -0.21875 to 0.21875
- scale_weight: bfloat16 [2048, 2048], P('sp', 'tp'), may hold values from -0.21875 to 0.21875
- gate_weight: bfloat16 [2048, 2048], P('sp', 'tp'), may hold values from -0.21875 to 0.21875
- query_weight: bfloat16 [2048, 1024], P(None, 'tp'), may hold values from -1 to 1
- key_weight: bfloat16 [2048, 512], P(None, 'tp'), may hold values from -1 to 1
- value_weight: bfloat16 [2048, 512], P(None, 'tp'), may hold values from -0.125 to 0.125
- query_gain: float32 [64], replicated, may hold values from 0.1 to 7.8
- key_gain: float32 [64], replicated, may hold values from 0.1 to 7.8
- output_weight: bfloat16 [1024, 2048], replicated, may hold values from -1 to 1
Outputs:
- updated: bfloat16 [4096, 2048], P(('sp', 'tp'))
All inputs are finite; a program needn't handle non-finite values.
Results may differ from a plain program's by a relative error of at most 0.012.
The roundings to bfloat16 on the way count: a program that leaves them out, or rounds other values in their place, can miss the bound.
Values may be sent and summed in bfloat16 or wider, within the bound.
No kernel may reach another device: no remote copies, remote signals or barrier semaphores. Data moves between devices by JAX's collectives and lax.ppermute only.
A program may use at most 64 MiB of HBM per device.

v0:
```python
import math

import jax
import jax.numpy as jnp
from jax import lax
from jax.experimental import pallas as pl
from jax.experimental.pallas import tpu as pltpu
from jax.sharding import PartitionSpec as P


CHANNEL_SPAN = 64
GRID_W = 64


epsilon = 1e-06
rope_base = 10000.0


def modulate(tok_rows, norm_gain, shift_row, scale_row):
    wide = tok_rows.astype(jnp.float32)
    normed = wide * lax.rsqrt(jnp.mean(wide * wide, axis=-1, keepdims=True) + epsilon)
    return (normed * norm_gain * (1.0 + scale_row) + shift_row).astype(jnp.bfloat16)


def headnorm(raw, gain, heads):
    field = raw.reshape(raw.shape[0], heads, -1)
    return field * lax.rsqrt(jnp.mean(field * field, axis=-1, keepdims=True) + epsilon) * gain


def rotate(field, places):
    count = field.shape[0]
    heads = field.shape[1]
    quarter = field.shape[2] // 4
    grid_row = (places // GRID_W).astype(jnp.float32)
    grid_col = (places % GRID_W).astype(jnp.float32)
    inverse = rope_base ** (-jnp.arange(quarter, dtype=jnp.float32) / quarter)
    angles = jnp.stack([grid_row[:, None] * inverse, grid_col[:, None] * inverse], axis=1)[:, None]
    cosine = jnp.cos(angles)
    sine = jnp.sin(angles)
    matcher_content_couples = field.reshape(count, heads, 2, 2, quarter)
    first = matcher_content_couples[:, :, :, 0]
    second = matcher_content_couples[:, :, :, 1]
    turned = jnp.stack([first * cosine - second * sine, second * cosine + first * sine], axis=3)
    return turned.reshape(count, heads, 4 * quarter)


def process_probe_group(
    accumulator_carry, probe_entries, matcher_content_couples, similarity_offset
):
    row_peak, row_total, weighted = accumulator_carry
    kv_heads = probe_entries.shape[1]
    head_size = probe_entries.shape[3]
    pair_width = kv_heads * head_size
    matcher_pieces = matcher_content_couples[:, :pair_width].reshape(
        matcher_content_couples.shape[0], kv_heads, head_size
    )
    value_rows = matcher_content_couples[:, pair_width:].reshape(
        matcher_content_couples.shape[0], kv_heads, head_size
    )
    similarity_matrix = (
        jnp.einsum(
            "dmvk,hmk->dmvh", probe_entries, matcher_pieces, preferred_element_type=jnp.float32
        )
        * head_size ** (-0.5)
        + similarity_offset
    )
    new_peak = jnp.maximum(row_peak, jnp.max(similarity_matrix, axis=-1))
    shares = jnp.exp(similarity_matrix - new_peak[..., None])
    shrink = jnp.exp(row_peak - new_peak)
    row_total = row_total * shrink + jnp.sum(shares, axis=-1)
    weighted = weighted * shrink[..., None] + jnp.einsum(
        "qkgn,nkd->qkgd",
        shares.astype(jnp.bfloat16),
        value_rows,
        preferred_element_type=jnp.float32,
    )
    return (new_peak, row_total, weighted)


def group_walker(accumulator_carry, probe_entries, matcher_content_couples, similarity_offset):
    pair_count = matcher_content_couples.shape[0]
    probe_group_total = -(-pair_count // 2048)
    while pair_count % probe_group_total:
        probe_group_total += 1
    if probe_group_total == 1:
        return process_probe_group(
            accumulator_carry, probe_entries, matcher_content_couples, similarity_offset
        )
    group_extent = pair_count // probe_group_total

    def scan_step(inner, slices):
        return (process_probe_group(inner, probe_entries, slices[0], slices[1]), None)

    result, _ = lax.scan(
        scan_step,
        accumulator_carry,
        (
            matcher_content_couples.reshape(
                probe_group_total, group_extent, matcher_content_couples.shape[1]
            ),
            similarity_offset.reshape(probe_group_total, group_extent),
        ),
    )
    return result


def general_device(
    latent,
    context,
    condition,
    context_condition,
    norm_gain,
    shift_weight,
    scale_weight,
    gate_weight,
    query_weight,
    key_weight,
    value_weight,
    query_gain,
    key_gain,
    output_weight,
):
    head_split = lax.axis_size("tp")
    seq_index = lax.axis_index("sp")
    head_index = lax.axis_index("tp")
    row_slab = shift_weight.shape[0]
    columns = shift_weight.shape[1]
    conditions = jnp.stack([condition, context_condition])
    activated = jax.nn.silu(
        lax.dynamic_slice_in_dim(conditions, seq_index * row_slab, row_slab, 1)
    ).astype(jnp.bfloat16)
    part_shift = jnp.dot(activated, shift_weight, preferred_element_type=jnp.float32)
    part_scale = jnp.dot(activated, scale_weight, preferred_element_type=jnp.float32)
    part_gate = jnp.dot(activated, gate_weight, preferred_element_type=jnp.float32)

    def widen(member):
        blank = jnp.zeros((2, columns * head_split), jnp.float32)
        return lax.dynamic_update_slice_in_dim(blank, member, head_index * columns, 1)

    shifts, scales, gates = lax.psum(
        (widen(part_shift), widen(part_scale), widen(part_gate)), ("sp", "tp")
    )
    own_rows = latent.shape[0]
    tok_count = own_rows * head_split
    ctx_rows = context.shape[0]
    hidden = modulate(latent, norm_gain, shifts[0], scales[0])
    context_hidden = modulate(context, norm_gain, shifts[1], scales[1])
    q_heads = query_weight.shape[1] // CHANNEL_SPAN
    kv_heads = key_weight.shape[1] // CHANNEL_SPAN
    group_size = q_heads // kv_heads
    q_width = q_heads * CHANNEL_SPAN
    kv_width = kv_heads * CHANNEL_SPAN
    joined_weight = jnp.concatenate([query_weight, key_weight, value_weight], axis=1)
    projected = jnp.dot(
        lax.all_gather(hidden, "tp", axis=0, tiled=True),
        joined_weight,
        preferred_element_type=jnp.float32,
    )
    places = seq_index * tok_count + jnp.arange(tok_count, dtype=jnp.int32)
    probe_entries = rotate(headnorm(projected[:, :q_width], query_gain, q_heads), places).astype(
        jnp.bfloat16
    )
    probe_entries = probe_entries.reshape(tok_count, kv_heads, group_size, CHANNEL_SPAN)
    latent_keys = rotate(
        headnorm(projected[:, q_width : q_width + kv_width], key_gain, kv_heads), places
    ).astype(jnp.bfloat16)
    latent_values = projected[:, q_width + kv_width :].astype(jnp.bfloat16)
    own_pairs = jnp.concatenate([latent_keys.reshape(tok_count, kv_width), latent_values], axis=1)
    ctx_projected = jnp.dot(
        context_hidden, joined_weight[:, q_width:], preferred_element_type=jnp.float32
    )
    ctx_keys = (
        headnorm(ctx_projected[:, :kv_width], key_gain, kv_heads)
        .astype(jnp.bfloat16)
        .reshape(ctx_rows, kv_width)
    )
    ctx_pairs = jnp.concatenate(
        [ctx_keys, ctx_projected[:, kv_width:].astype(jnp.bfloat16)], axis=1
    )
    prefix_mapped = math.log(tok_count / (2.0 * ctx_rows))
    stat_shape = (tok_count, kv_heads, group_size)
    start_state = (
        jnp.full(stat_shape, -jnp.inf, jnp.float32),
        jnp.zeros(stat_shape, jnp.float32),
        jnp.zeros(stat_shape + (CHANNEL_SPAN,), jnp.float32),
    )
    ctx_whole = lax.all_gather(ctx_pairs, "sp", axis=0, tiled=True)
    ctx_state = group_walker(
        start_state,
        probe_entries,
        ctx_whole,
        jnp.full((ctx_whole.shape[0],), prefix_mapped, jnp.float32),
    )
    key_piece = lax.all_gather(own_pairs, "sp", axis=0, tiled=True)
    final_state = group_walker(
        ctx_state, probe_entries, key_piece, jnp.zeros((key_piece.shape[0],), jnp.float32)
    )
    _, row_total, weighted = final_state
    attended = (weighted / row_total[..., None]).astype(jnp.bfloat16).reshape(tok_count, q_width)
    branch = jnp.dot(
        lax.all_to_all(attended, "tp", split_axis=0, concat_axis=1, tiled=True),
        output_weight,
        preferred_element_type=jnp.float32,
    )
    return (latent.astype(jnp.float32) + gates[0] * branch).astype(jnp.bfloat16)


LOG2E = math.log2(math.e)


def whole_spec():
    return pl.BlockSpec(memory_space=pltpu.VMEM)


def kernel_call(body, out_shape, count, flops, scratch=()):
    return pl.pallas_call(
        body,
        out_shape=out_shape,
        in_specs=[whole_spec()] * count,
        out_specs=jax.tree.map(lambda unused: whole_spec(), out_shape),
        scratch_shapes=list(scratch),
        cost_estimate=pl.CostEstimate(flops=flops, transcendentals=0, bytes_accessed=0),
        compiler_params=pltpu.CompilerParams(vmem_limit_bytes=48 * 1024 * 1024),
    )


ROOMY = 60 * 1024 * 1024


def hbm_spec():
    return pl.BlockSpec(memory_space=pltpu.HBM)


def start_loads(pairs, sems):
    copies = []
    for i, (source, target) in enumerate(pairs):
        copies.append(pltpu.make_async_copy(source, target, sems.at[i]))
        copies[-1].start()
    return copies


def opening_body(first_hbm, second_hbm, shift_hbm, scale_hbm, gate_hbm, out_ref, *scratch):
    first, second, *targets, sems = scratch
    row_slab = shift_hbm.shape[0]
    cut = pl.ds(pl.multiple_of(lax.axis_index("sp") * row_slab, row_slab), row_slab)
    copies = start_loads(
        [(first_hbm.at[:, cut], first), (second_hbm.at[:, cut], second)]
        + list(zip((shift_hbm, scale_hbm, gate_hbm), targets)),
        sems,
    )
    copies[0].wait()
    copies[1].wait()
    rows = lax.broadcasted_iota(jnp.int32, (16, row_slab), 0)
    pair = jnp.where(rows == 0, first[...], second[...])
    activated = (pair / (1.0 + jnp.exp(-pair))).astype(jnp.bfloat16)
    out_ref[6:8, :] = jnp.zeros((2, out_ref.shape[1]), jnp.float32)
    for i in range(3):
        copies[2 + i].wait()
        part = jnp.dot(activated, targets[i][...], preferred_element_type=jnp.float32)
        out_ref[2 * i : 2 * i + 2, :] = part[0:2]


def combine_body(one_ref, other_ref, out_ref):
    out_ref[...] = one_ref[...] + other_ref[...]


def combine(one, other, flops):
    return kernel_call(combine_body, jax.ShapeDtypeStruct(one.shape, one.dtype), 2, flops)(
        one, other
    )


def opening(first, second, *weights):
    row_slab, columns = weights[0].shape
    return pl.pallas_call(
        opening_body,
        out_shape=jax.ShapeDtypeStruct((8, columns), jnp.float32),
        in_specs=[hbm_spec()] * 5,
        out_specs=whole_spec(),
        scratch_shapes=[pltpu.VMEM((1, row_slab), jnp.float32)] * 2
        + [pltpu.VMEM((row_slab, columns), jnp.bfloat16)] * 3
        + [pltpu.SemaphoreType.DMA((5,))],
        cost_estimate=pl.CostEstimate(flops=10**8, transcendentals=0, bytes_accessed=0),
        compiler_params=pltpu.CompilerParams(vmem_limit_bytes=ROOMY),
    )(first, second, *weights)


def turn(field, cosine, sine):
    quarter = field.shape[0] // 4
    pieces = [field[i * quarter : (i + 1) * quarter] for i in range(4)]
    swapped = jnp.concatenate([pieces[1], pieces[0], pieces[3], pieces[2]], axis=0)
    return field * cosine + swapped * sine


def projection_body(
    heads,
    kv_heads,
    own_ref,
    context_ref,
    query_ref,
    key_ref,
    value_ref,
    core_ref,
    far_ref,
    both_ref,
    mod_ref,
    gain_ref,
    query_gain_ref,
    key_gain_ref,
    cosine_ref,
    sine_ref,
    q_out,
    kv_out,
):
    span = CHANNEL_SPAN
    group = heads // kv_heads

    def vector(row):
        return jnp.concatenate([mod_ref[i, row : row + 1, :] for i in range(mod_ref.shape[0])], axis=1)

    gain = gain_ref[...]

    def hidden_of(ref, row):
        wide = ref[...].astype(jnp.float32)
        scaled = wide * lax.rsqrt(jnp.mean(wide * wide, axis=-1, keepdims=True) + epsilon)
        return (scaled * (gain * (1.0 + vector(2 + row))) + vector(row)).astype(jnp.bfloat16)

    def normed(raw, head_gain):
        return raw * lax.rsqrt(jnp.mean(raw * raw, axis=0, keepdims=True) + epsilon) * head_gain

    q_out[...] = jnp.zeros_like(q_out)

    def upright(ref):
        return jnp.broadcast_to(ref[...], (8, span)).T[:, 0:1]

    query_gain = upright(query_gain_ref)
    key_gain = upright(key_gain_ref)
    blocks = (own_ref, core_ref, far_ref, both_ref)
    own_rows = own_ref.shape[0]
    tok_count = own_rows * len(blocks)
    for j in (1, 2, 3, 0):
        hidden = hidden_of(blocks[j], 0)
        cosine = cosine_ref[j]
        sine = sine_ref[j]
        queries = jnp.dot(hidden, query_ref[...], preferred_element_type=jnp.float32).T
        for h in range(heads):
            turned = turn(normed(queries[h * span : (h + 1) * span], query_gain), cosine, sine)
            kv, g = h // group, h % group
            lane = g * tok_count + j * own_rows
            q_out[kv, kv * span : (kv + 1) * span, lane : lane + own_rows] = turned.astype(jnp.bfloat16)
        keys = jnp.dot(hidden, key_ref[...], preferred_element_type=jnp.float32).T
        made = [
            turn(normed(keys[h * span : (h + 1) * span], key_gain), cosine, sine)
            for h in range(kv_heads)
        ]
        kv_out[j] = jnp.concatenate(made, axis=0).T.astype(jnp.bfloat16)
        values = jnp.dot(hidden, value_ref[...], preferred_element_type=jnp.float32)
        kv_out[len(blocks) + j] = values.T.astype(jnp.bfloat16)
    hidden = hidden_of(context_ref, 1)
    ctx_rows = context_ref.shape[0]
    keys = jnp.dot(hidden, key_ref[...], preferred_element_type=jnp.float32).T
    made = [normed(keys[h * span : (h + 1) * span], key_gain) for h in range(kv_heads)]
    kv_out[2 * len(blocks), 0:ctx_rows, :] = jnp.concatenate(made, axis=0).T.astype(jnp.bfloat16)
    kv_out[2 * len(blocks), ctx_rows : 2 * ctx_rows, :] = jnp.dot(
        hidden, value_ref[...], preferred_element_type=jnp.float32
    ).astype(jnp.bfloat16)


def attention_body(blocks, first, last, offset, q_tile, *refs):
    q_ref = refs[0]
    kv_refs = refs[1 : 1 + blocks]
    refs = refs[1 + blocks :]
    if not first:
        peak_in, total_in, sum_in = refs[:3]
        refs = refs[3:]
    kv_heads, width, lanes = q_ref.shape
    span = width // kv_heads
    scale = span ** (-0.5) * LOG2E
    parts = (kv_refs[0].shape[0] - 1) // 2
    ctx_rows = kv_refs[0].shape[1] // 2
    chunks = []
    for ref in kv_refs:
        half = parts // 2
        chunks += [(ref, range(half), False), (ref, range(half, parts), True)]
    tiles = [
        (h, lane, chunk)
        for chunk in chunks
        for h in range(kv_heads)
        for lane in range(0, lanes, q_tile)
    ]
    states = {}

    def scores(tile):
        h, lane, (ref, places, context) = tile
        keys = [ref[j] for j in places]
        if context:
            keys.append(ref[2 * parts, 0:ctx_rows, :])
        query = q_ref[h, :, lane : lane + q_tile]
        found = jnp.dot(jnp.concatenate(keys, axis=0), query, preferred_element_type=jnp.float32)
        found = found * scale
        if context:
            rows = found.shape[0] - ctx_rows
            found = jnp.concatenate([found[:rows], found[rows:] + offset * LOG2E], axis=0)
        return found

    def soften(tile, found):
        h, lane, _ = tile
        peak = jnp.max(found, axis=0, keepdims=True)
        old = states.get((h, lane))
        if old is None and not first:
            cut = slice(lane, lane + q_tile)
            old = (peak_in[h, :, cut], total_in[h, :, cut], sum_in[h, :, cut])
        if old is not None:
            peak = jnp.maximum(peak, old[0])
        shares = jnp.exp2(found - peak)
        total = jnp.sum(shares, axis=0, keepdims=True)
        shrink = None
        if old is not None:
            shrink = jnp.exp2(old[0] - peak)
            total = total + old[1] * shrink
        states[(h, lane)] = (peak, total, old[2] if old is not None else None)
        return shares.astype(jnp.bfloat16), shrink

    def gather(tile, shares, shrink):
        h, lane, (ref, places, context) = tile
        rows = slice(h * span, (h + 1) * span)
        values = [ref[parts + j, rows, :] for j in places]
        if context:
            values.append(ref[2 * parts, ctx_rows : 2 * ctx_rows, :].T[rows])
        weighted = jnp.dot(
            jnp.concatenate(values, axis=1), shares, preferred_element_type=jnp.float32
        )
        peak, total, old = states[(h, lane)]
        if shrink is not None:
            weighted = weighted + old * shrink
        states[(h, lane)] = (peak, total, weighted)

    following = scores(tiles[0])
    waiting = None
    for i, tile in enumerate(tiles):
        found = following
        if i + 1 < len(tiles):
            following = scores(tiles[i + 1])
        shares, shrink = soften(tile, found)
        if waiting:
            gather(*waiting)
        waiting = (tile, shares, shrink)
    gather(*waiting)
    for (h, lane), (peak, total, weighted) in states.items():
        cut = slice(lane, lane + q_tile)
        if last:
            (out_ref,) = refs
            attended = (weighted / total).astype(jnp.bfloat16)
            own_rows = out_ref.shape[2]
            group_lanes = own_rows * out_ref.shape[0]
            for at in range(0, q_tile, own_rows):
                g, j = (lane + at) // group_lanes, (lane + at) % group_lanes // own_rows
                head = h * (lanes // group_lanes) + g
                out_ref[j, head * span : (head + 1) * span, :] = attended[:, at : at + own_rows]
        else:
            peak_out, total_out, sum_out = refs
            peak_out[h, :, cut] = peak
            total_out[h, :, cut] = total
            sum_out[h, :, cut] = weighted


def attend(state, probes, pairs, offset, last):
    kv_heads, width, lanes = probes.shape
    span = width // kv_heads
    keys = sum(p.shape[0] // 2 * p.shape[1] + p.shape[1] // 2 for p in pairs)
    inputs = [probes, *pairs] + list(state or ())
    if last:
        out = jax.ShapeDtypeStruct(last, jnp.bfloat16)
    else:
        stat = jax.ShapeDtypeStruct((kv_heads, 1, lanes), jnp.float32)
        out = [stat, stat, jax.ShapeDtypeStruct((kv_heads, span, lanes), jnp.float32)]

    def body(*refs):
        attention_body(len(pairs), state is None, bool(last), offset, 512, *refs)

    return kernel_call(body, out, len(inputs), 40 * kv_heads * lanes * keys * span)(*inputs)


def output_body(latent_ref, mod_ref, weight_ref, *refs):
    out_ref, lhs_ref = refs[-2:]
    parts = refs[:-2]
    head_index = lax.axis_index("tp")
    rows = parts[0].shape[0]
    for j, ref in enumerate(parts):
        at = pl.multiple_of(jnp.bitwise_xor(head_index, j) * rows, rows)
        lhs_ref[pl.ds(at, rows), :] = ref[...]
    lhs = lhs_ref[...].T
    columns = mod_ref.shape[2]
    for i in range(mod_ref.shape[0]):
        cut = slice(i * columns, (i + 1) * columns)
        branch = jnp.dot(lhs, weight_ref[:, cut], preferred_element_type=jnp.float32)
        gate = mod_ref[i, 4:5, :]
        out_ref[:, cut] = (latent_ref[:, cut].astype(jnp.float32) + gate * branch).astype(
            jnp.bfloat16
        )


def fast_device(*args):
    return inner_device(*args)


def xor_move(member, axis, mask):
    size = lax.axis_size(axis)
    return lax.ppermute(member, axis, [(i, i ^ mask) for i in range(size)])


def ring_move(member, step):
    size = lax.axis_size("sp")
    return lax.ppermute(member, "sp", [(i, (i + step) % size) for i in range(size)])


def tables(seq_index, head_index, own_rows, head_split):
    quarter = CHANNEL_SPAN // 4
    blocks = jnp.bitwise_xor(jnp.arange(head_split, dtype=jnp.int32), head_index)
    places = (
        seq_index * own_rows * head_split
        + blocks[:, None] * own_rows
        + jnp.arange(own_rows, dtype=jnp.int32)
    )
    inverse = rope_base ** (-jnp.arange(quarter, dtype=jnp.float32) / quarter)
    grid_row = (places // GRID_W).astype(jnp.float32)[:, None, :] * inverse[:, None]
    grid_col = (places % GRID_W).astype(jnp.float32)[:, None, :] * inverse[:, None]
    row_sine, col_sine = jnp.sin(grid_row), jnp.sin(grid_col)
    row_cosine, col_cosine = jnp.cos(grid_row), jnp.cos(grid_col)
    cosine = jnp.concatenate([row_cosine, row_cosine, col_cosine, col_cosine], axis=1)
    sine = jnp.concatenate([-row_sine, row_sine, -col_sine, col_sine], axis=1)
    return cosine, sine


def inner_device(
    latent,
    context,
    condition,
    context_condition,
    norm_gain,
    shift_weight,
    scale_weight,
    gate_weight,
    query_weight,
    key_weight,
    value_weight,
    query_gain,
    key_gain,
    output_weight,
):
    head_split = lax.axis_size("tp")
    seq_split = lax.axis_size("sp")
    seq_index = lax.axis_index("sp")
    head_index = lax.axis_index("tp")
    own_rows, depth = latent.shape
    ctx_rows = context.shape[0]
    tok_count = own_rows * head_split
    q_heads = query_weight.shape[1] // CHANNEL_SPAN
    kv_heads = key_weight.shape[1] // CHANNEL_SPAN

    part = opening(
        condition.reshape(1, depth),
        context_condition.reshape(1, depth),
        shift_weight,
        scale_weight,
        gate_weight,
    )
    far = xor_move(latent, "tp", 2)
    near = xor_move(latent, "tp", 1)
    mask = seq_split // 2
    while mask:
        other = xor_move(part, "sp", mask)
        part = combine(part, other, 10**11 if 2 * mask == seq_split else 10**6)
        mask //= 2
    both = xor_move(far, "tp", 1)
    modulation = lax.all_gather(part, "tp", axis=0, tiled=False)
    cosine, sine = tables(seq_index, head_index, own_rows, head_split)
    probes, own_pairs = pl.pallas_call(
        lambda *refs: projection_body(q_heads, kv_heads, *refs),
        out_shape=[
            jax.ShapeDtypeStruct(
                (kv_heads, kv_heads * CHANNEL_SPAN, q_heads // kv_heads * tok_count), jnp.bfloat16
            ),
            jax.ShapeDtypeStruct((2 * head_split + 1, own_rows, own_rows), jnp.bfloat16),
        ],
        in_specs=[whole_spec()] * 14,
        out_specs=[whole_spec()] * 2,
        cost_estimate=pl.CostEstimate(
            flops=4 * tok_count * depth * (q_heads + 2 * kv_heads) * CHANNEL_SPAN,
            transcendentals=0,
            bytes_accessed=0,
        ),
        compiler_params=pltpu.CompilerParams(vmem_limit_bytes=48 * 1024 * 1024),
    )(
        latent,
        context,
        query_weight,
        key_weight,
        value_weight,
        near,
        far,
        both,
        modulation,
        norm_gain.reshape(1, depth),
        query_gain.reshape(1, CHANNEL_SPAN),
        key_gain.reshape(1, CHANNEL_SPAN),
        cosine,
        sine,
    )
    offset = math.log(tok_count / (2.0 * ctx_rows))
    near_pairs = xor_move(own_pairs, "sp", 1)
    up = ring_move(own_pairs, 2)
    down = ring_move(own_pairs, -2)
    near_up = xor_move(up, "sp", 1)
    near_down = xor_move(down, "sp", 1)
    across = ring_move(up, 2)
    near_across = xor_move(across, "sp", 1)
    state = attend(None, probes, [own_pairs], offset, None)
    state = attend(state, probes, [near_pairs], offset, None)
    state = attend(state, probes, [up], offset, None)
    state = attend(state, probes, [down, near_up], offset, None)
    state = attend(state, probes, [across, near_down], offset, None)
    attended = attend(
        state, probes, [near_across], offset, (head_split, q_heads * CHANNEL_SPAN, own_rows)
    )
    parts = [attended[0]] + [xor_move(attended[j], "tp", j) for j in range(1, head_split)]
    width = q_heads * CHANNEL_SPAN
    return kernel_call(
        output_body,
        jax.ShapeDtypeStruct(latent.shape, jnp.bfloat16),
        3 + head_split,
        2 * own_rows * depth * width * head_split,
        [pltpu.VMEM((width * head_split, own_rows), jnp.bfloat16)],
    )(latent, modulation, output_weight, *parts)


def suits(mesh, latent, context, query_weight, key_weight):
    seq_split, head_split = mesh.shape["sp"], mesh.shape["tp"]
    own_rows = latent.shape[0] // (seq_split * head_split)
    ctx_rows = context.shape[0] // seq_split
    kv_heads = key_weight.shape[1] // CHANNEL_SPAN // head_split
    return (
        seq_split == 8
        and head_split == 4
        and own_rows == 2 * CHANNEL_SPAN
        and ctx_rows == CHANNEL_SPAN
        and kv_heads == 2
        and query_weight.shape[1] == 2 * key_weight.shape[1]
    )


def solution(mesh):
    in_specs = (
        P(("sp", "tp"), None),
        P("sp", None),
        P(),
        P(),
        P(),
        P("sp", "tp"),
        P("sp", "tp"),
        P("sp", "tp"),
        P(None, "tp"),
        P(None, "tp"),
        P(None, "tp"),
        P(),
        P(),
        P(),
    )
    out_specs = P(("sp", "tp"), None)

    def program(*args):
        fast = suits(mesh, args[0], args[1], args[8], args[9])
        step = jax.shard_map(
            fast_device if fast else general_device,
            mesh=mesh,
            in_specs=in_specs,
            out_specs=out_specs,
            check_vma=False,
        )
        return step(*args)

    return program
```

profile of v0, /device:TPU:0, one launch (start us, length us, event | category | flops | bytes accessed | tf_op | source)
XLA Modules:
  0.0 73.3 jit_solution(10524684458142121992)
XLA Ops:
  0.0 3.0 %collective-permute-start.4 = (bf16[128,2048]{1,0:T(8,128)(2,1)}, bf16[128,2048]{1,0:T(8,128)(2,1)S(1)}, u32[]{:S(2)}, u32[]{:S(2)}) collective-permute-start(bf16[128,2048]{1,0:T(8,128)(2,1)} %latent_ref.1), channel_id=1, source_target_pairs={{0,2},{1,3},{2,0},{3,1},{4,6},{5,7},{6,4},{7,5},{8,10},{9,11},{10,... | collective-permute-start | bytes 1572872 | tf_op jit(solution)/shard_map/ppermute | solution.py:509
  3.0 0.0 collective-permute-start.3
  3.0 2.1 %shard_map.136.one_ref = f32[8,512]{1,0:T(8,128)} custom-call(f32[1,2048]{1,0:T(1,128)} %bitcast.19, f32[1,2048]{1,0:T(1,128)} %bitcast.20, bf16[256,512]{1,0:T(8,128)(2,1)} %shift_hbm.1, bf16[256,512]{1,0:T(8,128)(2,1)} %scale_hbm.1, bf16[256,512]{1,0:T(8,128)(2,1)} %gate_hbm.1), custom_call_target="tpu_custom_call" | custom-call | flops 100000000 | tf_op jit(solution)/shard_map/pallas_call | solution.py:275
  5.1 2.7 %collective-permute-start = (f32[8,512]{1,0:T(8,128)}, f32[8,512]{1,0:T(8,128)S(1)}, u32[]{:S(2)}, u32[]{:S(2)}) collective-permute-start(f32[8,512]{1,0:T(8,128)} %shard_map.136.one_ref), channel_id=1, source_target_pairs={{0,16},{4,20},{8,24},{12,28},{16,0},{20,4},{24,8},{28,12},{1,17},{... | collective-permute-start | bytes 49160 | tf_op jit(solution)/shard_map/ppermute | solution.py:509
  7.7 0.1 fusion.2
  7.8 0.0 copy-start.8
  7.8 0.0 copy-start.9
  7.8 0.0 copy-start.1
  7.8 7.3 %collective-permute-done.4.refs_6_ = bf16[128,2048]{1,0:T(8,128)(2,1)S(1)} collective-permute-done((bf16[128,2048]{1,0:T(8,128)(2,1)}, bf16[128,2048]{1,0:T(8,128)(2,1)S(1)}, u32[]{:S(2)}, u32[]{:S(2)}) %collective-permute-start.4) | collective-permute-done | bytes 524320 | tf_op jit(solution)/shard_map/ppermute | solution.py:509
  15.1 0.0 collective-permute-start.5
  15.1 0.0 collective-permute-done.other_ref
  15.1 0.0 copy-start.2
  15.1 0.7 copy-done.2
  15.8 0.0 copy-start.3
  15.8 0.0 copy-start.4
  15.8 0.0 copy-start.5
  15.8 0.0 copy-start.6
  15.8 0.0 copy-start.7
  15.9 1.9 %collective-permute-start.1 = (f32[8,512]{1,0:T(8,128)S(1)}, f32[8,512]{1,0:T(8,128)S(1)}, u32[]{:S(2)}, u32[]{:S(2)}) collective-permute-start(f32[8,512]{1,0:T(8,128)S(1)} %shard_map.137.one_ref), channel_id=1, source_target_pairs={{0,8},{4,12},{8,0},{12,4},{16,24},{20,28},{24,16},{28,20},{1,9},{5... | collective-permute-start | bytes 49160 | tf_op jit(solution)/shard_map/ppermute | solution.py:509
  17.8 0.3 fusion
  18.1 1.6 %collective-permute-done.1.other_ref = f32[8,512]{1,0:T(8,128)S(1)} collective-permute-done((f32[8,512]{1,0:T(8,128)S(1)}, f32[8,512]{1,0:T(8,128)S(1)}, u32[]{:S(2)}, u32[]{:S(2)}) %collective-permute-start.1) | collective-permute-done | bytes 16416 | tf_op jit(solution)/shard_map/ppermute | solution.py:509
  19.7 1.8 %collective-permute-start.2 = (f32[8,512]{1,0:T(8,128)S(1)}, f32[8,512]{1,0:T(8,128)S(1)}, u32[]{:S(2)}, u32[]{:S(2)}) collective-permute-start(f32[8,512]{1,0:T(8,128)S(1)} %shard_map.138.one_ref), channel_id=1, source_target_pairs={{0,4},{4,0},{8,12},{12,8},{16,20},{20,16},{24,28},{28,24},{1,5},{5... | collective-permute-start | bytes 49160 | tf_op jit(solution)/shard_map/ppermute | solution.py:509
  21.5 1.9 %collective-permute-done.2.other_ref = f32[8,512]{1,0:T(8,128)S(1)} collective-permute-done((f32[8,512]{1,0:T(8,128)S(1)}, f32[8,512]{1,0:T(8,128)S(1)}, u32[]{:S(2)}, u32[]{:S(2)}) %collective-permute-start.2) | collective-permute-done | bytes 16416 | tf_op jit(solution)/shard_map/ppermute | solution.py:509
  23.4 5.2 %all-gather = f32[32,512]{1,0:T(8,128)S(1)} all-gather(f32[8,512]{1,0:T(8,128)S(1)} %shard_map.139), channel_id=2, replica_groups=mesh['sp'=8,'tp'=4] {'tp'}, dimensions={0}, use_global_device_ids=true | all-gather | bytes 81920 | tf_op jit(solution)/shard_map/all_gather | solution.py:576
  28.6 0.0 collective-permute-done.3.refs_5_
  28.6 0.0 collective-permute-done.5.refs_7_
  28.6 0.0 copy-done.8
  28.6 0.0 copy-done.9
  28.7 0.0 copy-done.1
  28.7 0.0 copy-done.3
  28.7 0.0 copy-done.4
  28.7 0.0 copy-done.5
  28.7 0.0 copy-done.6
  28.7 0.0 copy-done.7
  28.7 2.5 %shard_map.140 = (bf16[2,128,1024]{2,1,0:T(8,128)(2,1)S(1)}, bf16[9,128,128]{2,1,0:T(8,128)(2,1)S(1)}) custom-call(bf16[128,2048]{1,0:T(8,128)(2,1)S(1)} %copy-done.1, bf16[64,2048]{1,0:T(8,128)(2,1)S(1)} %copy-done.6, bf16[2048,256]{1,0:T(8,128)(2,1)S(1)} %copy-done.3, bf16[2048,128]{1,0:T(8,128)(2,1)S(1)} %copy-done.4, bf16[2048,128]{1,0:T(8,128)(2,1)S(1)} %copy-done.5, ...), custom_call_target="tpu_custom_call" | custom-call | flops 2147483648 | tf_op jit(solution)/shard_map/pallas_call | solution.py:578
  31.3 1.9 %collective-permute-start.6 = (bf16[9,128,128]{2,1,0:T(8,128)(2,1)S(1)}, bf16[9,128,128]{2,1,0:T(8,128)(2,1)S(1)}, u32[]{:S(2)}, u32[]{:S(2)}) collective-permute-start(bf16[9,128,128]{2,1,0:T(8,128)(2,1)S(1)} %get-tuple-element.23.refs_1_), channel_id=1, source_target_pairs={{0,8},{4,12},{8,16},{12,20},{16,24},{20,28},{24,0},{28,4},{1,9},{5... | collective-permute-start | bytes 884744 | tf_op jit(solution)/shard_map/ppermute | solution.py:514
  33.2 2.1 %collective-permute-start.9 = (bf16[9,128,128]{2,1,0:T(8,128)(2,1)S(1)}, bf16[9,128,128]{2,1,0:T(8,128)(2,1)S(1)}, u32[]{:S(2)}, u32[]{:S(2)}) collective-permute-start(bf16[9,128,128]{2,1,0:T(8,128)(2,1)S(1)} %get-tuple-element.23.refs_1_), channel_id=1, source_target_pairs={{0,24},{4,28},{8,0},{12,4},{16,8},{20,12},{24,16},{28,20},{1,25},{... | collective-permute-start | bytes 884744 | tf_op jit(solution)/shard_map/ppermute | solution.py:514
  35.3 1.7 %collective-permute-start.12 = (bf16[9,128,128]{2,1,0:T(8,128)(2,1)S(1)}, bf16[9,128,128]{2,1,0:T(8,128)(2,1)S(1)}, u32[]{:S(2)}, u32[]{:S(2)}) collective-permute-start(bf16[9,128,128]{2,1,0:T(8,128)(2,1)S(1)} %get-tuple-element.23.refs_1_), channel_id=1, source_target_pairs={{0,4},{4,0},{8,12},{12,8},{16,20},{20,16},{24,28},{28,24},{1,5},{5... | collective-permute-start | bytes 884744 | tf_op jit(solution)/shard_map/ppermute | solution.py:509
  36.9 1.7 %shard_map.141 = (f32[2,1,1024]{2,1,0:T(1,128)S(1)}, f32[2,1,1024]{2,1,0:T(1,128)S(1)}, f32[2,64,1024]{2,1,0:T(8,128)S(1)}) custom-call(bf16[2,128,1024]{2,1,0:T(8,128)(2,1)S(1)} %get-tuple-element.22.refs_0_, bf16[9,128,128]{2,1,0:T(8,128)(2,1)S(1)} %get-tuple-element.23.refs_1_), custom_call_target="tpu_custom_call" | custom-call | flops 3019898880 | tf_op jit(solution)/shard_map/pallas_call | solution.py:481
  38.6 4.5 %collective-permute-done.6.refs_1_ = bf16[9,128,128]{2,1,0:T(8,128)(2,1)S(1)} collective-permute-done((bf16[9,128,128]{2,1,0:T(8,128)(2,1)S(1)}, bf16[9,128,128]{2,1,0:T(8,128)(2,1)S(1)}, u32[]{:S(2)}, u32[]{:S(2)}) %collective-permute-start.6) | collective-permute-done | bytes 294944 | tf_op jit(solution)/shard_map/ppermute | solution.py:514
  43.1 1.7 %collective-permute-start.11 = (bf16[9,128,128]{2,1,0:T(8,128)(2,1)S(1)}, bf16[9,128,128]{2,1,0:T(8,128)(2,1)S(1)}, u32[]{:S(2)}, u32[]{:S(2)}) collective-permute-start(bf16[9,128,128]{2,1,0:T(8,128)(2,1)S(1)} %collective-permute-done.6.refs_1_), channel_id=1, source_target_pairs={{0,4},{4,0},{8,12},{12,8},{16,20},{20,16},{24,28},{28,24},{1,5},{5... | collective-permute-start | bytes 884744 | tf_op jit(solution)/shard_map/ppermute | solution.py:509
  44.8 0.0 collective-permute-start.7
  44.8 3.6 %collective-permute-done.9.refs_1_ = bf16[9,128,128]{2,1,0:T(8,128)(2,1)S(1)} collective-permute-done((bf16[9,128,128]{2,1,0:T(8,128)(2,1)S(1)}, bf16[9,128,128]{2,1,0:T(8,128)(2,1)S(1)}, u32[]{:S(2)}, u32[]{:S(2)}) %collective-permute-start.9) | collective-permute-done | bytes 294944 | tf_op jit(solution)/shard_map/ppermute | solution.py:514
  48.4 1.5 %collective-permute-start.10 = (bf16[9,128,128]{2,1,0:T(8,128)(2,1)S(1)}, bf16[9,128,128]{2,1,0:T(8,128)(2,1)S(1)}, u32[]{:S(2)}, u32[]{:S(2)}) collective-permute-start(bf16[9,128,128]{2,1,0:T(8,128)(2,1)S(1)} %collective-permute-done.9.refs_1_), channel_id=1, source_target_pairs={{0,4},{4,0},{8,12},{12,8},{16,20},{20,16},{24,28},{28,24},{1,5},{5... | collective-permute-start | bytes 884744 | tf_op jit(solution)/shard_map/ppermute | solution.py:509
  50.0 0.0 collective-permute-done.12.refs_1_
  50.0 1.8 %shard_map.142 = (f32[2,1,1024]{2,1,0:T(1,128)S(1)}, f32[2,1,1024]{2,1,0:T(1,128)S(1)}, f32[2,64,1024]{2,1,0:T(8,128)S(1)}) custom-call(bf16[2,128,1024]{2,1,0:T(8,128)(2,1)S(1)} %get-tuple-element.22.refs_0_, bf16[9,128,128]{2,1,0:T(8,128)(2,1)S(1)} %collective-permute-done.12.refs_1_, f32[2,1,1024]{2,1,0:T(1,128)S(1)} %get-tuple-element.24.refs_2_, ...), custom_call_target="tpu_custom_call" | custom-call | flops 3019898880 | tf_op jit(solution)/shard_map/pallas_call | solution.py:481
  51.8 1.8 %shard_map.143 = (f32[2,1,1024]{2,1,0:T(1,128)S(1)}, f32[2,1,1024]{2,1,0:T(1,128)S(1)}, f32[2,64,1024]{2,1,0:T(8,128)S(1)}) custom-call(bf16[2,128,1024]{2,1,0:T(8,128)(2,1)S(1)} %get-tuple-element.22.refs_0_, bf16[9,128,128]{2,1,0:T(8,128)(2,1)S(1)} %collective-permute-done.6.refs_1_, f32[2,1,1024]{2,1,0:T(1,128)S(1)} %get-tuple-element.27.refs_2_, ...), custom_call_target="tpu_custom_call" | custom-call | flops 3019898880 | tf_op jit(solution)/shard_map/pallas_call | solution.py:481
  53.6 3.1 %collective-permute-done.7.refs_1_ = bf16[9,128,128]{2,1,0:T(8,128)(2,1)S(1)} collective-permute-done((bf16[9,128,128]{2,1,0:T(8,128)(2,1)S(1)}, bf16[9,128,128]{2,1,0:T(8,128)(2,1)S(1)}, u32[]{:S(2)}, u32[]{:S(2)}) %collective-permute-start.7) | collective-permute-done | bytes 294944 | tf_op jit(solution)/shard_map/ppermute | solution.py:514
  56.7 0.6 collective-permute-start.8
  57.3 0.0 collective-permute-done.11.refs_2_
  57.3 3.4 %shard_map.144 = (f32[2,1,1024]{2,1,0:T(1,128)S(1)}, f32[2,1,1024]{2,1,0:T(1,128)S(1)}, f32[2,64,1024]{2,1,0:T(8,128)S(1)}) custom-call(bf16[2,128,1024]{2,1,0:T(8,128)(2,1)S(1)} %get-tuple-element.22.refs_0_, bf16[9,128,128]{2,1,0:T(8,128)(2,1)S(1)} %collective-permute-done.9.refs_1_, bf16[9,128,128]{2,1,0:T(8,128)(2,1)S(1)} %collective-permute-done.11.refs_2_, ...), custom_call_target="tpu_custom_call" | custom-call | flops 6039797760 | tf_op jit(solution)/shard_map/pallas_call | solution.py:481
  60.7 0.0 collective-permute-done.10.refs_2_
  60.7 3.4 %shard_map.145 = (f32[2,1,1024]{2,1,0:T(1,128)S(1)}, f32[2,1,1024]{2,1,0:T(1,128)S(1)}, f32[2,64,1024]{2,1,0:T(8,128)S(1)}) custom-call(bf16[2,128,1024]{2,1,0:T(8,128)(2,1)S(1)} %get-tuple-element.22.refs_0_, bf16[9,128,128]{2,1,0:T(8,128)(2,1)S(1)} %collective-permute-done.7.refs_1_, bf16[9,128,128]{2,1,0:T(8,128)(2,1)S(1)} %collective-permute-done.10.refs_2_, ...), custom_call_target="tpu_custom_call" | custom-call | flops 6039797760 | tf_op jit(solution)/shard_map/pallas_call | solution.py:481
  64.1 0.0 collective-permute-done.8.refs_1_
  64.1 0.0 copy-start
  64.2 1.8 %shard_map.146 = bf16[4,256,128]{2,1,0:T(8,128)(2,1)S(1)} custom-call(bf16[2,128,1024]{2,1,0:T(8,128)(2,1)S(1)} %get-tuple-element.22.refs_0_, bf16[9,128,128]{2,1,0:T(8,128)(2,1)S(1)} %collective-permute-done.8.refs_1_, f32[2,1,1024]{2,1,0:T(1,128)S(1)} %get-tuple-element.36.refs_2_, f32[2,1,1024]{2,1,0:T(1,128)S(1)} %get-tuple-element.37.refs_3_, ...), custom_call_target="tpu_custom_call" | custom-call | flops 3019898880 | tf_op jit(solution)/shard_map/pallas_call | solution.py:481
  66.0 0.1 collective-permute-start.13
  66.1 1.5 %collective-permute-start.14 = (bf16[256,128]{1,0:T(8,128)(2,1)S(1)}, bf16[256,128]{1,0:T(8,128)(2,1)S(1)}, u32[]{:S(2)}, u32[]{:S(2)}) collective-permute-start(bf16[256,128]{1,0:T(8,128)(2,1)S(1)} %get-tuple-element.40), channel_id=1, source_target_pairs={{0,2},{1,3},{2,0},{3,1},{4,6},{5,7},{6,4},{7,5},{8,10},{9,11},{10,... | collective-permute-start | bytes 196616 | tf_op jit(solution)/shard_map/ppermute | solution.py:509
  67.7 0.3 collective-permute-start.15
  68.0 0.0 collective-permute-done.13.refs_1_
  68.0 2.6 %collective-permute-done.14.refs_2_ = bf16[256,128]{1,0:T(8,128)(2,1)S(1)} collective-permute-done((bf16[256,128]{1,0:T(8,128)(2,1)S(1)}, bf16[256,128]{1,0:T(8,128)(2,1)S(1)}, u32[]{:S(2)}, u32[]{:S(2)}) %collective-permute-start.14) | collective-permute-done | bytes 65568 | tf_op jit(solution)/shard_map/ppermute | solution.py:509
  70.6 1.1 %collective-permute-done.15.refs_3_ = bf16[256,128]{1,0:T(8,128)(2,1)S(1)} collective-permute-done((bf16[256,128]{1,0:T(8,128)(2,1)S(1)}, bf16[256,128]{1,0:T(8,128)(2,1)S(1)}, u32[]{:S(2)}, u32[]{:S(2)}) %collective-permute-start.15) | collective-permute-done | bytes 65568 | tf_op jit(solution)/shard_map/ppermute | solution.py:509
  71.7 0.0 copy-done
  71.7 1.6 %shard_map.147 = bf16[128,2048]{1,0:T(8,128)(2,1)} custom-call(bf16[128,2048]{1,0:T(8,128)(2,1)S(1)} %copy-done.1, f32[4,8,512]{2,1,0:T(8,128)S(1)} %bitcast.15, bf16[1024,2048]{1,0:T(8,128)(2,1)S(1)} %copy-done, bf16[256,128]{1,0:T(8,128)(2,1)S(1)} %get-tuple-element.42.refs_0_, bf16[256,128]{1,0:T(8,128)(2,1)S(1)} %collective-permute-done.13.refs_1_, ...), custom_call_target="tpu_custom_call" | custom-call | flops 536870912 | tf_op jit(solution)/shard_map/pallas_call | solution.py:628
  (7 shorter events, 0.1 us)
Async XLA Ops:
  0.0 15.1 %collective-permute-start.4 = (bf16[128,2048]{1,0:T(8,128)(2,1)}, bf16[128,2048]{1,0:T(8,128)(2,1)S(1)}, u32[]{:S(2)}, u32[]{:S(2)}) collective-permute-start(bf16[128,2048]{1,0:T(8,128)(2,1)} %latent_ref.1), channel_id=1, source_target_pairs={{0,2},{1,3},{2,0},{3,1},{4,6},{5,7},{6,4},{7,5},{8,10},{9,11},{10,... | collective-permute-start | bytes 1572872 | tf_op jit(solution)/shard_map/ppermute | solution.py:509
  3.0 25.7 %collective-permute-start.3 = (bf16[128,2048]{1,0:T(8,128)(2,1)}, bf16[128,2048]{1,0:T(8,128)(2,1)S(1)}, u32[]{:S(2)}, u32[]{:S(2)}) collective-permute-start(bf16[128,2048]{1,0:T(8,128)(2,1)} %latent_ref.1), channel_id=1, source_target_pairs={{0,1},{1,0},{2,3},{3,2},{4,5},{5,4},{6,7},{7,6},{8,9},{9,8},{10,11... | collective-permute-start | bytes 1572872 | tf_op jit(solution)/shard_map/ppermute | solution.py:509
  5.1 10.0 %collective-permute-start = (f32[8,512]{1,0:T(8,128)}, f32[8,512]{1,0:T(8,128)S(1)}, u32[]{:S(2)}, u32[]{:S(2)}) collective-permute-start(f32[8,512]{1,0:T(8,128)} %shard_map.136.one_ref), channel_id=1, source_target_pairs={{0,16},{4,20},{8,24},{12,28},{16,0},{20,4},{24,8},{28,12},{1,17},{... | collective-permute-start | bytes 49160 | tf_op jit(solution)/shard_map/ppermute | solution.py:509
  7.8 20.8 %copy-start.8 = (f32[64]{0:T(128)S(1)}, f32[64]{0:T(128)}, u32[]{:S(2)}) copy-start(f32[64]{0:T(128)} %param.25) | copy-start | bytes 772
  7.8 20.8 %copy-start.9 = (f32[64]{0:T(128)S(1)}, f32[64]{0:T(128)}, u32[]{:S(2)}) copy-start(f32[64]{0:T(128)} %param.26) | copy-start | bytes 772
  7.8 20.8 %copy-start.1 = (bf16[128,2048]{1,0:T(8,128)(2,1)S(1)}, bf16[128,2048]{1,0:T(8,128)(2,1)}, u32[]{:S(2)}) copy-start(bf16[128,2048]{1,0:T(8,128)(2,1)} %latent_ref.1) | copy-start | bytes 1572868
  15.1 13.5 %collective-permute-start.5 = (bf16[128,2048]{1,0:T(8,128)(2,1)S(1)}, bf16[128,2048]{1,0:T(8,128)(2,1)S(1)}, u32[]{:S(2)}, u32[]{:S(2)}) collective-permute-start(bf16[128,2048]{1,0:T(8,128)(2,1)S(1)} %collective-permute-done.4.refs_6_), channel_id=1, source_target_pairs={{0,1},{1,0},{2,3},{3,2},{4,5},{5,4},{6,7},{7,6},{8,9},{9,8},{10,11... | collective-permute-start | bytes 1572872 | tf_op jit(solution)/shard_map/ppermute | solution.py:509
  15.1 0.7 copy-start.2
  15.8 12.8 %copy-start.3 = (bf16[2048,256]{1,0:T(8,128)(2,1)S(1)}, bf16[2048,256]{1,0:T(8,128)(2,1)}, u32[]{:S(2)}) copy-start(bf16[2048,256]{1,0:T(8,128)(2,1)} %refs_2_.1) | copy-start | bytes 3145732
  15.8 12.9 %copy-start.4 = (bf16[2048,128]{1,0:T(8,128)(2,1)S(1)}, bf16[2048,128]{1,0:T(8,128)(2,1)}, u32[]{:S(2)}) copy-start(bf16[2048,128]{1,0:T(8,128)(2,1)} %refs_3_.1) | copy-start | bytes 1572868
  15.8 12.9 %copy-start.5 = (bf16[2048,128]{1,0:T(8,128)(2,1)S(1)}, bf16[2048,128]{1,0:T(8,128)(2,1)}, u32[]{:S(2)}) copy-start(bf16[2048,128]{1,0:T(8,128)(2,1)} %refs_4_.1) | copy-start | bytes 1572868
  15.8 12.9 %copy-start.6 = (bf16[64,2048]{1,0:T(8,128)(2,1)S(1)}, bf16[64,2048]{1,0:T(8,128)(2,1)}, u32[]{:S(2)}) copy-start(bf16[64,2048]{1,0:T(8,128)(2,1)} %refs_1_.1) | copy-start | bytes 786436
  15.8 12.9 %copy-start.7 = (f32[2048]{0:T(1024)S(1)}, f32[2048]{0:T(1024)}, u32[]{:S(2)}) copy-start(f32[2048]{0:T(1024)} %param.18) | copy-start | bytes 24580
  15.9 3.8 %collective-permute-start.1 = (f32[8,512]{1,0:T(8,128)S(1)}, f32[8,512]{1,0:T(8,128)S(1)}, u32[]{:S(2)}, u32[]{:S(2)}) collective-permute-start(f32[8,512]{1,0:T(8,128)S(1)} %shard_map.137.one_ref), channel_id=1, source_target_pairs={{0,8},{4,12},{8,0},{12,4},{16,24},{20,28},{24,16},{28,20},{1,9},{5... | collective-permute-start | bytes 49160 | tf_op jit(solution)/shard_map/ppermute | solution.py:509
  19.7 3.7 %collective-permute-start.2 = (f32[8,512]{1,0:T(8,128)S(1)}, f32[8,512]{1,0:T(8,128)S(1)}, u32[]{:S(2)}, u32[]{:S(2)}) collective-permute-start(f32[8,512]{1,0:T(8,128)S(1)} %shard_map.138.one_ref), channel_id=1, source_target_pairs={{0,4},{4,0},{8,12},{12,8},{16,20},{20,16},{24,28},{28,24},{1,5},{5... | collective-permute-start | bytes 49160 | tf_op jit(solution)/shard_map/ppermute | solution.py:509
  31.3 11.8 %collective-permute-start.6 = (bf16[9,128,128]{2,1,0:T(8,128)(2,1)S(1)}, bf16[9,128,128]{2,1,0:T(8,128)(2,1)S(1)}, u32[]{:S(2)}, u32[]{:S(2)}) collective-permute-start(bf16[9,128,128]{2,1,0:T(8,128)(2,1)S(1)} %get-tuple-element.23.refs_1_), channel_id=1, source_target_pairs={{0,8},{4,12},{8,16},{12,20},{16,24},{20,28},{24,0},{28,4},{1,9},{5... | collective-permute-start | bytes 884744 | tf_op jit(solution)/shard_map/ppermute | solution.py:514
  33.2 15.3 %collective-permute-start.9 = (bf16[9,128,128]{2,1,0:T(8,128)(2,1)S(1)}, bf16[9,128,128]{2,1,0:T(8,128)(2,1)S(1)}, u32[]{:S(2)}, u32[]{:S(2)}) collective-permute-start(bf16[9,128,128]{2,1,0:T(8,128)(2,1)S(1)} %get-tuple-element.23.refs_1_), channel_id=1, source_target_pairs={{0,24},{4,28},{8,0},{12,4},{16,8},{20,12},{24,16},{28,20},{1,25},{... | collective-permute-start | bytes 884744 | tf_op jit(solution)/shard_map/ppermute | solution.py:514
  35.3 14.7 %collective-permute-start.12 = (bf16[9,128,128]{2,1,0:T(8,128)(2,1)S(1)}, bf16[9,128,128]{2,1,0:T(8,128)(2,1)S(1)}, u32[]{:S(2)}, u32[]{:S(2)}) collective-permute-start(bf16[9,128,128]{2,1,0:T(8,128)(2,1)S(1)} %get-tuple-element.23.refs_1_), channel_id=1, source_target_pairs={{0,4},{4,0},{8,12},{12,8},{16,20},{20,16},{24,28},{28,24},{1,5},{5... | collective-permute-start | bytes 884744 | tf_op jit(solution)/shard_map/ppermute | solution.py:509
  43.1 14.2 %collective-permute-start.11 = (bf16[9,128,128]{2,1,0:T(8,128)(2,1)S(1)}, bf16[9,128,128]{2,1,0:T(8,128)(2,1)S(1)}, u32[]{:S(2)}, u32[]{:S(2)}) collective-permute-start(bf16[9,128,128]{2,1,0:T(8,128)(2,1)S(1)} %collective-permute-done.6.refs_1_), channel_id=1, source_target_pairs={{0,4},{4,0},{8,12},{12,8},{16,20},{20,16},{24,28},{28,24},{1,5},{5... | collective-permute-start | bytes 884744 | tf_op jit(solution)/shard_map/ppermute | solution.py:509
  44.8 11.9 %collective-permute-start.7 = (bf16[9,128,128]{2,1,0:T(8,128)(2,1)S(1)}, bf16[9,128,128]{2,1,0:T(8,128)(2,1)S(1)}, u32[]{:S(2)}, u32[]{:S(2)}) collective-permute-start(bf16[9,128,128]{2,1,0:T(8,128)(2,1)S(1)} %collective-permute-done.6.refs_1_), channel_id=1, source_target_pairs={{0,8},{4,12},{8,16},{12,20},{16,24},{20,28},{24,0},{28,4},{1,9},{5... | collective-permute-start | bytes 884744 | tf_op jit(solution)/shard_map/ppermute | solution.py:514
  48.4 12.3 %collective-permute-start.10 = (bf16[9,128,128]{2,1,0:T(8,128)(2,1)S(1)}, bf16[9,128,128]{2,1,0:T(8,128)(2,1)S(1)}, u32[]{:S(2)}, u32[]{:S(2)}) collective-permute-start(bf16[9,128,128]{2,1,0:T(8,128)(2,1)S(1)} %collective-permute-done.9.refs_1_), channel_id=1, source_target_pairs={{0,4},{4,0},{8,12},{12,8},{16,20},{20,16},{24,28},{28,24},{1,5},{5... | collective-permute-start | bytes 884744 | tf_op jit(solution)/shard_map/ppermute | solution.py:509
  56.7 7.4 %collective-permute-start.8 = (bf16[9,128,128]{2,1,0:T(8,128)(2,1)S(1)}, bf16[9,128,128]{2,1,0:T(8,128)(2,1)S(1)}, u32[]{:S(2)}, u32[]{:S(2)}) collective-permute-start(bf16[9,128,128]{2,1,0:T(8,128)(2,1)S(1)} %collective-permute-done.7.refs_1_), channel_id=1, source_target_pairs={{0,4},{4,0},{8,12},{12,8},{16,20},{20,16},{24,28},{28,24},{1,5},{5... | collective-permute-start | bytes 884744 | tf_op jit(solution)/shard_map/ppermute | solution.py:509
  64.1 7.6 %copy-start = (bf16[1024,2048]{1,0:T(8,128)(2,1)S(1)}, bf16[1024,2048]{1,0:T(8,128)(2,1)}, u32[]{:S(2)}) copy-start(bf16[1024,2048]{1,0:T(8,128)(2,1)} %weight_ref.1) | copy-start | bytes 12582916
  66.0 1.9 %collective-permute-start.13 = (bf16[256,128]{1,0:T(8,128)(2,1)S(1)}, bf16[256,128]{1,0:T(8,128)(2,1)S(1)}, u32[]{:S(2)}, u32[]{:S(2)}) collective-permute-start(bf16[256,128]{1,0:T(8,128)(2,1)S(1)} %get-tuple-element.41), channel_id=1, source_target_pairs={{0,1},{1,0},{2,3},{3,2},{4,5},{5,4},{6,7},{7,6},{8,9},{9,8},{10,11... | collective-permute-start | bytes 196616 | tf_op jit(solution)/shard_map/ppermute | solution.py:509
  66.1 4.5 %collective-permute-start.14 = (bf16[256,128]{1,0:T(8,128)(2,1)S(1)}, bf16[256,128]{1,0:T(8,128)(2,1)S(1)}, u32[]{:S(2)}, u32[]{:S(2)}) collective-permute-start(bf16[256,128]{1,0:T(8,128)(2,1)S(1)} %get-tuple-element.40), channel_id=1, source_target_pairs={{0,2},{1,3},{2,0},{3,1},{4,6},{5,7},{6,4},{7,5},{8,10},{9,11},{10,... | collective-permute-start | bytes 196616 | tf_op jit(solution)/shard_map/ppermute | solution.py:509
  67.7 4.1 %collective-permute-start.15 = (bf16[256,128]{1,0:T(8,128)(2,1)S(1)}, bf16[256,128]{1,0:T(8,128)(2,1)S(1)}, u32[]{:S(2)}, u32[]{:S(2)}) collective-permute-start(bf16[256,128]{1,0:T(8,128)(2,1)S(1)} %get-tuple-element.39), channel_id=1, source_target_pairs={{0,3},{1,2},{2,1},{3,0},{4,7},{5,6},{6,5},{7,4},{8,11},{9,10},{10,... | collective-permute-start | bytes 196616 | tf_op jit(solution)/shard_map/ppermute | solution.py:509
where the time goes:
time: 73.8 us; the launch traced here: 73.3 us
  waiting for transfers between devices  25.8 us (35%)
  starting transfers between devices  20.7 us (28%)
  Pallas kernels  20.2 us (27%)
  blocking collectives  5.22 us (7%)
  local copies, waits for them, and re-layouts  0.78 us (1%)
    ppermute x13, starting transfers between devices, xor_move(): return lax.ppermute(member, axis, [(i, i ^ mask) for i in range(size)])  16.7 us
    ppermute x13, waiting for transfers between devices, xor_move(): return lax.ppermute(member, axis, [(i, i ^ mask) for i in range(size)])  14.6 us
    pallas_call x6, Pallas kernels, attend(): kernel_call(body, out, len(inputs), 40 * kv_heads * lanes * keys * span)  14 us
    ppermute x3, waiting for transfers between devices, ring_move(): lax.ppermute(member, 'sp', [(i, (i + step) % size) for i in range(size)])  11.2 us
    all_gather x1, blocking collectives, inner_device(): modulation = lax.all_gather(part, 'tp', axis=0, tiled=False)  5.22 us
    ppermute x3, starting transfers between devices, ring_move(): lax.ppermute(member, 'sp', [(i, (i + step) % size) for i in range(size)])  3.99 us
    pallas_call x1, Pallas kernels, inner_device(): pl.pallas_call(lambda *refs: projection_body(q_heads, kv_heads, *refs), o...  2.55 us
    pallas_call x1, Pallas kernels, opening(): pl.pallas_call(opening_body, out_shape=jax.ShapeDtypeStruct((8, columns),...  2.08 us
  transfers between devices with their start and end apart: 16, of which 8 were waited for; matrix products, arithmetic and copies ran while one was open for 1% of the time, Pallas kernels for 19%

commit v1 on v0

--- a/solution.py
+++ b/solution.py
@@ -309,8 +309,10 @@
     key_gain_ref,
     cosine_ref,
     sine_ref,
-    q_out,
-    kv_out,
+    keep_q,
+    keep_kv,
+    give,
+    made,
 ):
     span = CHANNEL_SPAN
     group = heads // kv_heads
@@ -328,88 +330,100 @@
     def normed(raw, head_gain):
         return raw * lax.rsqrt(jnp.mean(raw * raw, axis=0, keepdims=True) + epsilon) * head_gain
 
-    q_out[...] = jnp.zeros_like(q_out)
-
     def upright(ref):
         return jnp.broadcast_to(ref[...], (8, span)).T[:, 0:1]
 
     query_gain = upright(query_gain_ref)
     key_gain = upright(key_gain_ref)
     blocks = (own_ref, core_ref, far_ref, both_ref)
-    own_rows = own_ref.shape[0]
-    tok_count = own_rows * len(blocks)
-    for j in (1, 2, 3, 0):
-        hidden = hidden_of(blocks[j], 0)
+    q_tiles = group * len(blocks) // 2
+    waiting = {}
+    for j, ref in enumerate(blocks):
+        hidden = hidden_of(ref, 0)
         cosine = cosine_ref[j]
         sine = sine_ref[j]
+        rows = slice(j % 2 * span, (j % 2 + 1) * span)
         queries = jnp.dot(hidden, query_ref[...], preferred_element_type=jnp.float32).T
         for h in range(heads):
             turned = turn(normed(queries[h * span : (h + 1) * span], query_gain), cosine, sine)
             kv, g = h // group, h % group
-            lane = g * tok_count + j * own_rows
-            q_out[kv, kv * span : (kv + 1) * span, lane : lane + own_rows] = turned.astype(jnp.bfloat16)
+            made[kv, g * len(blocks) // 2 + j // 2, rows, :] = turned.astype(jnp.bfloat16)
         keys = jnp.dot(hidden, key_ref[...], preferred_element_type=jnp.float32).T
-        made = [
-            turn(normed(keys[h * span : (h + 1) * span], key_gain), cosine, sine)
-            for h in range(kv_heads)
-        ]
-        kv_out[j] = jnp.concatenate(made, axis=0).T.astype(jnp.bfloat16)
-        values = jnp.dot(hidden, value_ref[...], preferred_element_type=jnp.float32)
-        kv_out[len(blocks) + j] = values.T.astype(jnp.bfloat16)
+        values = jnp.dot(hidden, value_ref[...], preferred_element_type=jnp.float32).T
+        for h in range(kv_heads):
+            cut = slice(h * span, (h + 1) * span)
+            turned = turn(normed(keys[cut], key_gain), cosine, sine)
+            if j % 2:
+                pair = jnp.concatenate([waiting[h], turned], axis=0)
+                made[h, q_tiles + j // 2] = pair.T.astype(jnp.bfloat16)
+            waiting[h] = turned
+            made[h, q_tiles + len(blocks) // 2 + j // 2, rows, :] = values[cut].astype(jnp.bfloat16)
     hidden = hidden_of(context_ref, 1)
-    ctx_rows = context_ref.shape[0]
     keys = jnp.dot(hidden, key_ref[...], preferred_element_type=jnp.float32).T
-    made = [normed(keys[h * span : (h + 1) * span], key_gain) for h in range(kv_heads)]
-    kv_out[2 * len(blocks), 0:ctx_rows, :] = jnp.concatenate(made, axis=0).T.astype(jnp.bfloat16)
-    kv_out[2 * len(blocks), ctx_rows : 2 * ctx_rows, :] = jnp.dot(
-        hidden, value_ref[...], preferred_element_type=jnp.float32
-    ).astype(jnp.bfloat16)
-
-
-def attention_body(blocks, first, last, offset, q_tile, *refs):
+    values = jnp.dot(hidden, value_ref[...], preferred_element_type=jnp.float32).T
+    for h in range(kv_heads):
+        cut = slice(h * span, (h + 1) * span)
+        both = jnp.concatenate([normed(keys[cut], key_gain).T, values[cut]], axis=0)
+        made[h, q_tiles + len(blocks)] = jnp.concatenate([both, jnp.zeros_like(both)], axis=1).astype(
+            jnp.bfloat16
+        )
+    side = lax.rem(lax.axis_index("sp"), kv_heads)
+    for i in range(q_tiles):
+        keep_q[i] = made[side, i]
+    for i in range(keep_kv.shape[0]):
+        keep_kv[i] = made[side, q_tiles + i]
+    for i in range(give.shape[0]):
+        give[i] = made[1 - side, i]
+
+
+def attention_body(bases, first, last, offset, *refs):
     q_ref = refs[0]
-    kv_refs = refs[1 : 1 + blocks]
-    refs = refs[1 + blocks :]
+    kv_refs = refs[1 : 1 + len(bases)]
+    refs = refs[1 + len(bases) :]
     if not first:
         peak_in, total_in, sum_in = refs[:3]
         refs = refs[3:]
-    kv_heads, width, lanes = q_ref.shape
-    span = width // kv_heads
+    span = q_ref.shape[1] // 2
     scale = span ** (-0.5) * LOG2E
-    parts = (kv_refs[0].shape[0] - 1) // 2
-    ctx_rows = kv_refs[0].shape[1] // 2
-    chunks = []
-    for ref in kv_refs:
-        half = parts // 2
-        chunks += [(ref, range(half), False), (ref, range(half, parts), True)]
-    tiles = [
-        (h, lane, chunk)
-        for chunk in chunks
-        for h in range(kv_heads)
-        for lane in range(0, lanes, q_tile)
-    ]
+    groups = 2
+    pairs = 2
+    chunks = [(ref, base, part) for ref, base in zip(kv_refs, bases) for part in (0, 1)]
+    tiles = [(g, chunk) for chunk in chunks for g in range(groups)]
     states = {}
+    queries = {}
+    for g in range(groups):
+        found = jnp.concatenate(
+            [
+                q_ref[g * pairs + p, half * span : (half + 1) * span, :]
+                for p in range(pairs)
+                for half in (0, 1)
+            ],
+            axis=1,
+        )
+        blank = jnp.zeros_like(found)
+        queries[g, 0] = jnp.concatenate([found, blank], axis=0)
+        queries[g, 1] = jnp.concatenate([blank, found], axis=0)
 
     def scores(tile):
-        h, lane, (ref, places, context) = tile
-        keys = [ref[j] for j in places]
-        if context:
-            keys.append(ref[2 * parts, 0:ctx_rows, :])
-        query = q_ref[h, :, lane : lane + q_tile]
-        found = jnp.dot(jnp.concatenate(keys, axis=0), query, preferred_element_type=jnp.float32)
+        g, (ref, base, part) = tile
+        keys = [ref[base + p] for p in range(pairs)]
+        if part == 0:
+            keys.append(ref[base + 2 * pairs, 0:span, :])
+        found = jnp.dot(
+            jnp.concatenate(keys, axis=0), queries[g, part], preferred_element_type=jnp.float32
+        )
         found = found * scale
-        if context:
-            rows = found.shape[0] - ctx_rows
+        if part == 0:
+            rows = found.shape[0] - span
             found = jnp.concatenate([found[:rows], found[rows:] + offset * LOG2E], axis=0)
         return found
 
     def soften(tile, found):
-        h, lane, _ = tile
+        g = tile[0]
         peak = jnp.max(found, axis=0, keepdims=True)
-        old = states.get((h, lane))
+        old = states.get(g)
         if old is None and not first:
-            cut = slice(lane, lane + q_tile)
-            old = (peak_in[h, :, cut], total_in[h, :, cut], sum_in[h, :, cut])
+            old = (peak_in[g], total_in[g], sum_in[g])
         if old is not None:
             peak = jnp.maximum(peak, old[0])
         shares = jnp.exp2(found - peak)
@@ -418,22 +432,22 @@
         if old is not None:
             shrink = jnp.exp2(old[0] - peak)
             total = total + old[1] * shrink
-        states[(h, lane)] = (peak, total, old[2] if old is not None else None)
+        states[g] = (peak, total, old[2] if old is not None else None)
         return shares.astype(jnp.bfloat16), shrink
 
     def gather(tile, shares, shrink):
-        h, lane, (ref, places, context) = tile
-        rows = slice(h * span, (h + 1) * span)
-        values = [ref[parts + j, rows, :] for j in places]
-        if context:
-            values.append(ref[2 * parts, ctx_rows : 2 * ctx_rows, :].T[rows])
+        g, (ref, base, part) = tile
+        rows = slice(part * span, (part + 1) * span)
+        values = [ref[base + pairs + p, rows, :] for p in range(pairs)]
+        if part == 0:
+            values.append(ref[base + 2 * pairs, span : 2 * span, 0:span])
         weighted = jnp.dot(
             jnp.concatenate(values, axis=1), shares, preferred_element_type=jnp.float32
         )
-        peak, total, old = states[(h, lane)]
+        peak, total, old = states[g]
         if shrink is not None:
             weighted = weighted + old * shrink
-        states[(h, lane)] = (peak, total, weighted)
+        states[g] = (peak, total, weighted)
 
     following = scores(tiles[0])
     waiting = None
@@ -446,49 +460,49 @@
             gather(*waiting)
         waiting = (tile, shares, shrink)
     gather(*waiting)
-    for (h, lane), (peak, total, weighted) in states.items():
-        cut = slice(lane, lane + q_tile)
+    for g, (peak, total, weighted) in states.items():
         if last:
             (out_ref,) = refs
             attended = (weighted / total).astype(jnp.bfloat16)
             own_rows = out_ref.shape[2]
-            group_lanes = own_rows * out_ref.shape[0]
-            for at in range(0, q_tile, own_rows):
-                g, j = (lane + at) // group_lanes, (lane + at) % group_lanes // own_rows
-                head = h * (lanes // group_lanes) + g
-                out_ref[j, head * span : (head + 1) * span, :] = attended[:, at : at + own_rows]
+            for j in range(out_ref.shape[0]):
+                out_ref[j, g * span : (g + 1) * span, :] = attended[
+                    :, j * own_rows : (j + 1) * own_rows
+                ]
         else:
             peak_out, total_out, sum_out = refs
-            peak_out[h, :, cut] = peak
-            total_out[h, :, cut] = total
-            sum_out[h, :, cut] = weighted
-
-
-def attend(state, probes, pairs, offset, last):
-    kv_heads, width, lanes = probes.shape
-    span = width // kv_heads
-    keys = sum(p.shape[0] // 2 * p.shape[1] + p.shape[1] // 2 for p in pairs)
-    inputs = [probes, *pairs] + list(state or ())
+            peak_out[g] = peak
+            total_out[g] = total
+            sum_out[g] = weighted
+
+
+def attend(state, probes, pairs, offset, last=False):
+    lanes = 2 * 2 * probes.shape[2]
+    span = probes.shape[1] // 2
+    keys = sum(lanes + span for unused in pairs)
+    inputs = [probes, *(ref for ref, unused in pairs)] + list(state or ())
     if last:
-        out = jax.ShapeDtypeStruct(last, jnp.bfloat16)
+        out = jax.ShapeDtypeStruct((4, 2 * span, probes.shape[2]), jnp.bfloat16)
     else:
-        stat = jax.ShapeDtypeStruct((kv_heads, 1, lanes), jnp.float32)
-        out = [stat, stat, jax.ShapeDtypeStruct((kv_heads, span, lanes), jnp.float32)]
+        stat = jax.ShapeDtypeStruct((2, 1, lanes), jnp.float32)
+        out = [stat, stat, jax.ShapeDtypeStruct((2, span, lanes), jnp.float32)]
 
     def body(*refs):
-        attention_body(len(pairs), state is None, bool(last), offset, 512, *refs)
-
-    return kernel_call(body, out, len(inputs), 40 * kv_heads * lanes * keys * span)(*inputs)
+        attention_body([base for unused, base in pairs], state is None, last, offset, *refs)
+
+    return kernel_call(body, out, len(inputs), 40 * 2 * lanes * keys * span)(*inputs)
 
 
 def output_body(latent_ref, mod_ref, weight_ref, *refs):
     out_ref, lhs_ref = refs[-2:]
     parts = refs[:-2]
     head_index = lax.axis_index("tp")
+    side = lax.rem(lax.axis_index("sp"), 2)
     rows = parts[0].shape[0]
-    for j, ref in enumerate(parts):
-        at = pl.multiple_of(jnp.bitwise_xor(head_index, j) * rows, rows)
-        lhs_ref[pl.ds(at, rows), :] = ref[...]
+    for i, ref in enumerate(parts):
+        j, flip = i % (len(parts) // 2), i // (len(parts) // 2)
+        place = jnp.bitwise_xor(head_index, j) * 2 + jnp.bitwise_xor(side, flip)
+        lhs_ref[pl.ds(pl.multiple_of(place * rows, rows), rows), :] = ref[...]
     lhs = lhs_ref[...].T
     columns = mod_ref.shape[2]
     for i in range(mod_ref.shape[0]):
@@ -507,6 +521,16 @@
 def xor_move(member, axis, mask):
     size = lax.axis_size(axis)
     return lax.ppermute(member, axis, [(i, i ^ mask) for i in range(size)])
+
+
+def cross_move(member, mask):
+    seq_split, head_split = lax.axis_size("sp"), lax.axis_size("tp")
+    pairs = [
+        (i * head_split + j, (i ^ 1) * head_split + (j ^ mask))
+        for i in range(seq_split)
+        for j in range(head_split)
+    ]
+    return lax.ppermute(member, ("sp", "tp"), pairs)
 
 
 def ring_move(member, step):
@@ -575,16 +599,18 @@
     both = xor_move(far, "tp", 1)
     modulation = lax.all_gather(part, "tp", axis=0, tiled=False)
     cosine, sine = tables(seq_index, head_index, own_rows, head_split)
-    probes, own_pairs = pl.pallas_call(
+    q_tiles = q_heads // kv_heads * head_split // 2
+    kv_tiles = head_split + 1
+    tile = (own_rows, own_rows)
+    keep_q, keep_kv, give = pl.pallas_call(
         lambda *refs: projection_body(q_heads, kv_heads, *refs),
         out_shape=[
-            jax.ShapeDtypeStruct(
-                (kv_heads, kv_heads * CHANNEL_SPAN, q_heads // kv_heads * tok_count), jnp.bfloat16
-            ),
-            jax.ShapeDtypeStruct((2 * head_split + 1, own_rows, own_rows), jnp.bfloat16),
+            jax.ShapeDtypeStruct((count, *tile), jnp.bfloat16)
+            for count in (q_tiles, kv_tiles, q_tiles + kv_tiles)
         ],
         in_specs=[whole_spec()] * 14,
-        out_specs=[whole_spec()] * 2,
+        out_specs=[whole_spec()] * 3,
+        scratch_shapes=[pltpu.VMEM((kv_heads, q_tiles + kv_tiles, *tile), jnp.bfloat16)],
         cost_estimate=pl.CostEstimate(
             flops=4 * tok_count * depth * (q_heads + 2 * kv_heads) * CHANNEL_SPAN,
             transcendentals=0,
@@ -608,27 +634,30 @@
         sine,
     )
     offset = math.log(tok_count / (2.0 * ctx_rows))
-    near_pairs = xor_move(own_pairs, "sp", 1)
-    up = ring_move(own_pairs, 2)
-    down = ring_move(own_pairs, -2)
-    near_up = xor_move(up, "sp", 1)
-    near_down = xor_move(down, "sp", 1)
+    near = xor_move(give, "sp", 1)
+    up = ring_move(keep_kv, 2)
+    down = ring_move(keep_kv, -2)
+    near_kv = near[q_tiles:]
+    near_up = ring_move(near_kv, 2)
+    near_down = ring_move(near_kv, -2)
     across = ring_move(up, 2)
-    near_across = xor_move(across, "sp", 1)
-    state = attend(None, probes, [own_pairs], offset, None)
-    state = attend(state, probes, [near_pairs], offset, None)
-    state = attend(state, probes, [up], offset, None)
-    state = attend(state, probes, [down, near_up], offset, None)
-    state = attend(state, probes, [across, near_down], offset, None)
-    attended = attend(
-        state, probes, [near_across], offset, (head_split, q_heads * CHANNEL_SPAN, own_rows)
-    )
-    parts = [attended[0]] + [xor_move(attended[j], "tp", j) for j in range(1, head_split)]
+    near_across = ring_move(near_up, 2)
+    own = attend(None, keep_q, [(keep_kv, 0)], offset)
+    other = attend(None, near, [(keep_kv, 0), (near, q_tiles)], offset)
+    own = attend(own, keep_q, [(near, q_tiles)], offset)
+    for group in ([up, down], [across, near_up], [near_down]):
+        pieces = [(piece, 0) for piece in group]
+        other = attend(other, near, pieces, offset)
+        own = attend(own, keep_q, pieces, offset)
+    other = attend(other, near, [(near_across, 0)], offset, True)
+    own = attend(own, keep_q, [(near_across, 0)], offset, True)
+    sent = [cross_move(other[j], j) for j in range(head_split)]
+    parts = [own[0]] + [xor_move(own[j], "tp", j) for j in range(1, head_split)] + sent
     width = q_heads * CHANNEL_SPAN
     return kernel_call(
         output_body,
         jax.ShapeDtypeStruct(latent.shape, jnp.bfloat16),
-        3 + head_split,
+        3 + len(parts),
         2 * own_rows * depth * width * head_split,
         [pltpu.VMEM((width * head_split, own_rows), jnp.bfloat16)],
     )(latent, modulation, output_weight, *parts)

time: 73.8 us -> 75.2 us (1.019)
  starting transfers between devices: 20.7 us -> 25.3 us
  waiting for transfers between devices: 25.8 us -> 21.4 us
  Pallas kernels: 20.2 us -> 21.6 us
    ppermute x0 -> x4, starting transfers between devices: none -> 4.51 us  [cross_move(): return lax.ppermute(member, ('sp', 'tp'), pairs)]
    ppermute x3 -> x6, starting transfers between devices: 3.99 us -> 7.85 us  [ring_move(): lax.ppermute(member, 'sp', [(i, (i + step) % size) for i in range(size)])]
    ppermute x13 -> x10, starting transfers between devices: 16.7 us -> 13 us  [xor_move(): return lax.ppermute(member, axis, [(i, i ^ mask) for i in range(size)])]
    ppermute x3 -> x6, waiting for transfers between devices: 11.2 us -> 8.38 us  [ring_move(): lax.ppermute(member, 'sp', [(i, (i + step) % size) for i in range(size)])]
    ppermute x13 -> x10, waiting for transfers between devices: 14.6 us -> 12.3 us  [xor_move(): return lax.ppermute(member, axis, [(i, i ^ mask) for i in range(size)])]
    pallas_call x6 -> x11, Pallas kernels: 14 us -> 15.3 us  [attend(): kernel_call(body, out, len(inputs), 40 * 2 * lanes * keys * span)(*inputs)]
  transfers between devices with their start and end apart: 16 -> 20, of which waited for: 8 -> 9; matrix products, arithmetic and copies ran while one was open for 1% -> 1% of each run, Pallas kernels for 19% -> 22%
where the time goes in v1:
time: 75.2 us; the launch traced here: 75 us
  starting transfers between devices  25.3 us (34%)
  Pallas kernels  21.6 us (29%)
  waiting for transfers between devices  21.4 us (28%)
  blocking collectives  5.22 us (7%)
  local copies, waits for them, and re-layouts  0.79 us (1%)
    pallas_call x11, Pallas kernels, attend(): kernel_call(body, out, len(inputs), 40 * 2 * lanes * keys * span)(*inputs)  15.3 us
    ppermute x10, starting transfers between devices, xor_move(): return lax.ppermute(member, axis, [(i, i ^ mask) for i in range(size)])  13 us
    ppermute x10, waiting for transfers between devices, xor_move(): return lax.ppermute(member, axis, [(i, i ^ mask) for i in range(size)])  12.3 us
    ppermute x6, waiting for transfers between devices, ring_move(): lax.ppermute(member, 'sp', [(i, (i + step) % size) for i in range(size)])  8.38 us
    ppermute x6, starting transfers between devices, ring_move(): lax.ppermute(member, 'sp', [(i, (i + step) % size) for i in range(size)])  7.85 us
    all_gather x1, blocking collectives, inner_device(): modulation = lax.all_gather(part, 'tp', axis=0, tiled=False)  5.22 us
    ppermute x4, starting transfers between devices, cross_move(): return lax.ppermute(member, ('sp', 'tp'), pairs)  4.51 us
    pallas_call x1, Pallas kernels, inner_device(): pl.pallas_call(lambda *refs: projection_body(q_heads, kv_heads, *refs), o...  2.64 us
  transfers between devices with their start and end apart: 20, of which 9 were waited for; matrix products, arithmetic and copies ran while one was open for 1% of the time, Pallas kernels for 22%

profile of v1, /device:TPU:0, one launch (start us, length us, event | category | flops | bytes accessed | tf_op | source)
XLA Modules:
  0.0 75.0 jit_solution(2429176231108842047)
XLA Ops:
  0.0 3.0 %collective-permute-start.4 = (bf16[128,2048]{1,0:T(8,128)(2,1)}, bf16[128,2048]{1,0:T(8,128)(2,1)S(1)}, u32[]{:S(2)}, u32[]{:S(2)}) collective-permute-start(bf16[128,2048]{1,0:T(8,128)(2,1)} %latent_ref.1), channel_id=1, source_target_pairs={{0,2},{1,3},{2,0},{3,1},{4,6},{5,7},{6,4},{7,5},{8,10},{9,11},{10,... | collective-permute-start | bytes 1572872 | tf_op jit(solution)/shard_map/ppermute | solution.py:523
  3.0 0.0 collective-permute-start.3
  3.0 2.1 %shard_map.136.one_ref = f32[8,512]{1,0:T(8,128)} custom-call(f32[1,2048]{1,0:T(1,128)} %bitcast.27, f32[1,2048]{1,0:T(1,128)} %bitcast.28, bf16[256,512]{1,0:T(8,128)(2,1)} %shift_hbm.1, bf16[256,512]{1,0:T(8,128)(2,1)} %scale_hbm.1, bf16[256,512]{1,0:T(8,128)(2,1)} %gate_hbm.1), custom_call_target="tpu_custom_call" | custom-call | flops 100000000 | tf_op jit(solution)/shard_map/pallas_call | solution.py:275
  5.1 2.7 %collective-permute-start = (f32[8,512]{1,0:T(8,128)}, f32[8,512]{1,0:T(8,128)S(1)}, u32[]{:S(2)}, u32[]{:S(2)}) collective-permute-start(f32[8,512]{1,0:T(8,128)} %shard_map.136.one_ref), channel_id=1, source_target_pairs={{0,16},{4,20},{8,24},{12,28},{16,0},{20,4},{24,8},{28,12},{1,17},{... | collective-permute-start | bytes 49160 | tf_op jit(solution)/shard_map/ppermute | solution.py:523
  7.7 0.1 fusion.2
  7.8 0.0 copy-start.9
  7.8 0.0 copy-start.1
  7.8 7.3 %collective-permute-done.4.refs_6_ = bf16[128,2048]{1,0:T(8,128)(2,1)S(1)} collective-permute-done((bf16[128,2048]{1,0:T(8,128)(2,1)}, bf16[128,2048]{1,0:T(8,128)(2,1)S(1)}, u32[]{:S(2)}, u32[]{:S(2)}) %collective-permute-start.4) | collective-permute-done | bytes 524320 | tf_op jit(solution)/shard_map/ppermute | solution.py:523
  15.1 0.0 collective-permute-start.5
  15.1 0.0 collective-permute-done.other_ref
  15.1 0.7 copy-done.2
  15.8 0.0 copy-start.7
  15.9 1.9 %collective-permute-start.1 = (f32[8,512]{1,0:T(8,128)S(1)}, f32[8,512]{1,0:T(8,128)S(1)}, u32[]{:S(2)}, u32[]{:S(2)}) collective-permute-start(f32[8,512]{1,0:T(8,128)S(1)} %shard_map.137.one_ref), channel_id=1, source_target_pairs={{0,8},{4,12},{8,0},{12,4},{16,24},{20,28},{24,16},{28,20},{1,9},{5... | collective-permute-start | bytes 49160 | tf_op jit(solution)/shard_map/ppermute | solution.py:523
  17.8 0.3 fusion
  18.1 1.6 %collective-permute-done.1.other_ref = f32[8,512]{1,0:T(8,128)S(1)} collective-permute-done((f32[8,512]{1,0:T(8,128)S(1)}, f32[8,512]{1,0:T(8,128)S(1)}, u32[]{:S(2)}, u32[]{:S(2)}) %collective-permute-start.1) | collective-permute-done | bytes 16416 | tf_op jit(solution)/shard_map/ppermute | solution.py:523
  19.7 1.8 %collective-permute-start.2 = (f32[8,512]{1,0:T(8,128)S(1)}, f32[8,512]{1,0:T(8,128)S(1)}, u32[]{:S(2)}, u32[]{:S(2)}) collective-permute-start(f32[8,512]{1,0:T(8,128)S(1)} %shard_map.138.one_ref), channel_id=1, source_target_pairs={{0,4},{4,0},{8,12},{12,8},{16,20},{20,16},{24,28},{28,24},{1,5},{5... | collective-permute-start | bytes 49160 | tf_op jit(solution)/shard_map/ppermute | solution.py:523
  21.5 1.9 %collective-permute-done.2.other_ref = f32[8,512]{1,0:T(8,128)S(1)} collective-permute-done((f32[8,512]{1,0:T(8,128)S(1)}, f32[8,512]{1,0:T(8,128)S(1)}, u32[]{:S(2)}, u32[]{:S(2)}) %collective-permute-start.2) | collective-permute-done | bytes 16416 | tf_op jit(solution)/shard_map/ppermute | solution.py:523
  23.4 5.2 %all-gather = f32[32,512]{1,0:T(8,128)S(1)} all-gather(f32[8,512]{1,0:T(8,128)S(1)} %shard_map.139), channel_id=2, replica_groups=mesh['sp'=8,'tp'=4] {'tp'}, dimensions={0}, use_global_device_ids=true | all-gather | bytes 81920 | tf_op jit(solution)/shard_map/all_gather | solution.py:600
  28.6 0.0 collective-permute-done.3.refs_5_
  28.6 0.0 collective-permute-done.5.refs_7_
  28.6 0.0 copy-done.8
  28.6 0.0 copy-done.9
  28.7 2.6 %shard_map.140 = (bf16[4,128,128]{2,1,0:T(8,128)(2,1)S(1)}, bf16[5,128,128]{2,1,0:T(8,128)(2,1)S(1)}, bf16[9,128,128]{2,1,0:T(8,128)(2,1)S(1)}) custom-call(bf16[128,2048]{1,0:T(8,128)(2,1)S(1)} %copy-done.1, bf16[64,2048]{1,0:T(8,128)(2,1)S(1)} %copy-done.6, bf16[2048,256]{1,0:T(8,128)(2,1)S(1)} %copy-done.3, bf16[2048,128]{1,0:T(8,128)(2,1)S(1)} %copy-done.4, ...), custom_call_target="tpu_custom_call" | custom-call | flops 2147483648 | tf_op jit(solution)/shard_map/pallas_call | solution.py:605
  31.4 1.8 %collective-permute-start.6 = (bf16[9,128,128]{2,1,0:T(8,128)(2,1)S(1)}, bf16[9,128,128]{2,1,0:T(8,128)(2,1)S(1)}, u32[]{:S(2)}, u32[]{:S(2)}) collective-permute-start(bf16[9,128,128]{2,1,0:T(8,128)(2,1)S(1)} %get-tuple-element.36), channel_id=1, source_target_pairs={{0,4},{4,0},{8,12},{12,8},{16,20},{20,16},{24,28},{28,24},{1,5},{5... | collective-permute-start | bytes 884744 | tf_op jit(solution)/shard_map/ppermute | solution.py:523
  33.2 1.6 %collective-permute-start.10 = (bf16[5,128,128]{2,1,0:T(8,128)(2,1)S(1)}, bf16[5,128,128]{2,1,0:T(8,128)(2,1)S(1)}, u32[]{:S(2)}, u32[]{:S(2)}) collective-permute-start(bf16[5,128,128]{2,1,0:T(8,128)(2,1)S(1)} %get-tuple-element.37.refs_1_), channel_id=1, source_target_pairs={{0,8},{4,12},{8,16},{12,20},{16,24},{20,28},{24,0},{28,4},{1,9},{5... | collective-permute-start | bytes 491528 | tf_op jit(solution)/shard_map/ppermute | solution.py:538
  34.8 2.2 %collective-permute-start.12 = (bf16[5,128,128]{2,1,0:T(8,128)(2,1)S(1)}, bf16[5,128,128]{2,1,0:T(8,128)(2,1)S(1)}, u32[]{:S(2)}, u32[]{:S(2)}) collective-permute-start(bf16[5,128,128]{2,1,0:T(8,128)(2,1)S(1)} %get-tuple-element.37.refs_1_), channel_id=1, source_target_pairs={{0,24},{4,28},{8,0},{12,4},{16,8},{20,12},{24,16},{28,20},{1,25},{... | collective-permute-start | bytes 491528 | tf_op jit(solution)/shard_map/ppermute | solution.py:538
  37.0 1.0 %shard_map.141 = (f32[2,1,512]{2,1,0:T(1,128)S(1)}, f32[2,1,512]{2,1,0:T(1,128)S(1)}, f32[2,64,512]{2,1,0:T(8,128)S(1)}) custom-call(bf16[4,128,128]{2,1,0:T(8,128)(2,1)S(1)} %get-tuple-element.35.refs_0_, bf16[5,128,128]{2,1,0:T(8,128)(2,1)S(1)} %get-tuple-element.37.refs_1_), custom_call_target="tpu_custom_call" | custom-call | flops 1509949440 | tf_op jit(solution)/shard_map/pallas_call | solution.py:493
  38.0 4.1 %collective-permute-done.10.refs_1_ = bf16[5,128,128]{2,1,0:T(8,128)(2,1)S(1)} collective-permute-done((bf16[5,128,128]{2,1,0:T(8,128)(2,1)S(1)}, bf16[5,128,128]{2,1,0:T(8,128)(2,1)S(1)}, u32[]{:S(2)}, u32[]{:S(2)}) %collective-permute-start.10) | collective-permute-done | bytes 163872 | tf_op jit(solution)/shard_map/ppermute | solution.py:538
  42.1 0.0 collective-permute-start.11
  42.1 0.0 collective-permute-done.6.refs_1_.refs_0_.refs_2_
  42.1 4.0 %collective-permute-start.9 = (bf16[5,128,128]{2,1,0:T(8,128)(2,1)S(1)}, bf16[5,128,128]{2,1,0:T(8,128)(2,1)S(1)}, u32[]{:S(2)}, u32[]{:S(2)}) collective-permute-start(bf16[5,128,128]{2,1,0:T(8,128)(2,1)S(1)} %slice.36), channel_id=1, source_target_pairs={{0,24},{4,28},{8,0},{12,4},{16,8},{20,12},{24,16},{28,20},{1,25},{... | collective-permute-start | bytes 491528 | tf_op jit(solution)/shard_map/ppermute | solution.py:538
  46.2 0.0 collective-permute-start.7
  46.2 1.8 %shard_map.147 = (f32[2,1,512]{2,1,0:T(1,128)S(1)}, f32[2,1,512]{2,1,0:T(1,128)S(1)}, f32[2,64,512]{2,1,0:T(8,128)S(1)}) custom-call(bf16[9,128,128]{2,1,0:T(8,128)(2,1)S(1)} %collective-permute-done.6.refs_1_.refs_0_.refs_2_, bf16[5,128,128]{2,1,0:T(8,128)(2,1)S(1)} %get-tuple-element.37.refs_1_, ...), custom_call_target="tpu_custom_call" | custom-call | flops 3019898880 | tf_op jit(solution)/shard_map/pallas_call | solution.py:493
  47.9 1.0 %shard_map.142 = (f32[2,1,512]{2,1,0:T(1,128)S(1)}, f32[2,1,512]{2,1,0:T(1,128)S(1)}, f32[2,64,512]{2,1,0:T(8,128)S(1)}) custom-call(bf16[4,128,128]{2,1,0:T(8,128)(2,1)S(1)} %get-tuple-element.35.refs_0_, bf16[9,128,128]{2,1,0:T(8,128)(2,1)S(1)} %collective-permute-done.6.refs_1_.refs_0_.refs_2_, f32[2,1,512]{2,1,0:T(1,128)S(1)} %get-tuple-element.38.refs_2_, ...), custom_call_target="tpu_custom_call" | custom-call | flops 1509949440 | tf_op jit(solution)/shard_map/pallas_call | solution.py:493
  48.9 0.0 collective-permute-done.12.refs_2_
  49.0 1.9 %shard_map.143 = (f32[2,1,512]{2,1,0:T(1,128)S(1)}, f32[2,1,512]{2,1,0:T(1,128)S(1)}, f32[2,64,512]{2,1,0:T(8,128)S(1)}) custom-call(bf16[4,128,128]{2,1,0:T(8,128)(2,1)S(1)} %get-tuple-element.35.refs_0_, bf16[5,128,128]{2,1,0:T(8,128)(2,1)S(1)} %collective-permute-done.10.refs_1_, bf16[5,128,128]{2,1,0:T(8,128)(2,1)S(1)} %collective-permute-done.12.refs_2_, ...), custom_call_target="tpu_custom_call" | custom-call | flops 3019898880 | tf_op jit(solution)/shard_map/pallas_call | solution.py:493
  50.8 1.9 %shard_map.148 = (f32[2,1,512]{2,1,0:T(1,128)S(1)}, f32[2,1,512]{2,1,0:T(1,128)S(1)}, f32[2,64,512]{2,1,0:T(8,128)S(1)}) custom-call(bf16[9,128,128]{2,1,0:T(8,128)(2,1)S(1)} %collective-permute-done.6.refs_1_.refs_0_.refs_2_, bf16[5,128,128]{2,1,0:T(8,128)(2,1)S(1)} %collective-permute-done.10.refs_1_, ...), custom_call_target="tpu_custom_call" | custom-call | flops 3019898880 | tf_op jit(solution)/shard_map/pallas_call | solution.py:493
  52.7 2.9 %collective-permute-done.7.refs_2_ = bf16[5,128,128]{2,1,0:T(8,128)(2,1)S(1)} collective-permute-done((bf16[5,128,128]{2,1,0:T(8,128)(2,1)S(1)}, bf16[5,128,128]{2,1,0:T(8,128)(2,1)S(1)}, u32[]{:S(2)}, u32[]{:S(2)}) %collective-permute-start.7) | collective-permute-done | bytes 163872 | tf_op jit(solution)/shard_map/ppermute | solution.py:538
  55.6 0.0 collective-permute-start.8
  55.6 0.0 collective-permute-done.11.refs_1_
  55.6 1.9 %shard_map.149 = (f32[2,1,512]{2,1,0:T(1,128)S(1)}, f32[2,1,512]{2,1,0:T(1,128)S(1)}, f32[2,64,512]{2,1,0:T(8,128)S(1)}) custom-call(bf16[9,128,128]{2,1,0:T(8,128)(2,1)S(1)} %collective-permute-done.6.refs_1_.refs_0_.refs_2_, bf16[5,128,128]{2,1,0:T(8,128)(2,1)S(1)} %collective-permute-done.11.refs_1_, ...), custom_call_target="tpu_custom_call" | custom-call | flops 3019898880 | tf_op jit(solution)/shard_map/pallas_call | solution.py:493
  57.5 1.9 %shard_map.144 = (f32[2,1,512]{2,1,0:T(1,128)S(1)}, f32[2,1,512]{2,1,0:T(1,128)S(1)}, f32[2,64,512]{2,1,0:T(8,128)S(1)}) custom-call(bf16[4,128,128]{2,1,0:T(8,128)(2,1)S(1)} %get-tuple-element.35.refs_0_, bf16[5,128,128]{2,1,0:T(8,128)(2,1)S(1)} %collective-permute-done.11.refs_1_, bf16[5,128,128]{2,1,0:T(8,128)(2,1)S(1)} %collective-permute-done.7.refs_2_, ...), custom_call_target="tpu_custom_call" | custom-call | flops 3019898880 | tf_op jit(solution)/shard_map/pallas_call | solution.py:493
  59.3 0.0 collective-permute-done.9.refs_1_
  59.3 1.0 %shard_map.150 = (f32[2,1,512]{2,1,0:T(1,128)S(1)}, f32[2,1,512]{2,1,0:T(1,128)S(1)}, f32[2,64,512]{2,1,0:T(8,128)S(1)}) custom-call(bf16[9,128,128]{2,1,0:T(8,128)(2,1)S(1)} %collective-permute-done.6.refs_1_.refs_0_.refs_2_, bf16[5,128,128]{2,1,0:T(8,128)(2,1)S(1)} %collective-permute-done.9.refs_1_, f32[2,1,512]{2,1,0:T(1,128)S(1)} %get-tuple-element.59.refs_2_, ...), custom_call_target="tpu_custom_call" | custom-call | flops 1509949440 | tf_op jit(solution)/shard_map/pallas_call | solution.py:493
  60.4 1.0 %shard_map.145 = (f32[2,1,512]{2,1,0:T(1,128)S(1)}, f32[2,1,512]{2,1,0:T(1,128)S(1)}, f32[2,64,512]{2,1,0:T(8,128)S(1)}) custom-call(bf16[4,128,128]{2,1,0:T(8,128)(2,1)S(1)} %get-tuple-element.35.refs_0_, bf16[5,128,128]{2,1,0:T(8,128)(2,1)S(1)} %collective-permute-done.9.refs_1_, f32[2,1,512]{2,1,0:T(1,128)S(1)} %get-tuple-element.47.refs_2_, ...), custom_call_target="tpu_custom_call" | custom-call | flops 1509949440 | tf_op jit(solution)/shard_map/pallas_call | solution.py:493
  61.4 1.3 %collective-permute-done.8.refs_1_ = bf16[5,128,128]{2,1,0:T(8,128)(2,1)S(1)} collective-permute-done((bf16[5,128,128]{2,1,0:T(8,128)(2,1)S(1)}, bf16[5,128,128]{2,1,0:T(8,128)(2,1)S(1)}, u32[]{:S(2)}, u32[]{:S(2)}) %collective-permute-start.8) | collective-permute-done | bytes 163872 | tf_op jit(solution)/shard_map/ppermute | solution.py:538
  62.7 1.0 %shard_map.151 = bf16[4,128,128]{2,1,0:T(8,128)(2,1)S(1)} custom-call(bf16[9,128,128]{2,1,0:T(8,128)(2,1)S(1)} %collective-permute-done.6.refs_1_.refs_0_.refs_2_, bf16[5,128,128]{2,1,0:T(8,128)(2,1)S(1)} %collective-permute-done.8.refs_1_, f32[2,1,512]{2,1,0:T(1,128)S(1)} %get-tuple-element.62.refs_2_, f32[2,1,512]{2,1,0:T(1,128)S(1)} %get-tuple-element.63.refs_3_, ...), custom_call_target="tpu_custom_call" | custom-call | flops 1509949440 | tf_op jit(solution)/shard_map/pallas_call | solution.py:493
  63.7 0.0 copy-start
  63.8 0.1 collective-permute-start.19
  63.9 1.4 %collective-permute-start.18 = (bf16[128,128]{1,0:T(8,128)(2,1)S(1)}, bf16[128,128]{1,0:T(8,128)(2,1)S(1)}, u32[]{:S(2)}, u32[]{:S(2)}) collective-permute-start(bf16[128,128]{1,0:T(8,128)(2,1)S(1)} %get-tuple-element.66), channel_id=1, source_target_pairs={{0,6},{1,7},{2,4},{3,5},{4,2},{5,3},{6,0},{7,1},{8,14},{9,15},{10,... | collective-permute-start | bytes 98312 | tf_op jit(solution)/shard_map/ppermute | solution.py:533
  65.2 1.0 %shard_map.146 = bf16[4,128,128]{2,1,0:T(8,128)(2,1)S(1)} custom-call(bf16[4,128,128]{2,1,0:T(8,128)(2,1)S(1)} %get-tuple-element.35.refs_0_, bf16[5,128,128]{2,1,0:T(8,128)(2,1)S(1)} %collective-permute-done.8.refs_1_, f32[2,1,512]{2,1,0:T(1,128)S(1)} %get-tuple-element.50.refs_2_, f32[2,1,512]{2,1,0:T(1,128)S(1)} %get-tuple-element.51.refs_3_, ...), custom_call_target="tpu_custom_call" | custom-call | flops 1509949440 | tf_op jit(solution)/shard_map/pallas_call | solution.py:493
  66.3 1.7 %collective-permute-start.17 = (bf16[128,128]{1,0:T(8,128)(2,1)S(1)}, bf16[128,128]{1,0:T(8,128)(2,1)S(1)}, u32[]{:S(2)}, u32[]{:S(2)}) collective-permute-start(bf16[128,128]{1,0:T(8,128)(2,1)S(1)} %get-tuple-element.67), channel_id=1, source_target_pairs={{0,5},{1,4},{2,7},{3,6},{4,1},{5,0},{6,3},{7,2},{8,13},{9,12},{10,... | collective-permute-start | bytes 98312 | tf_op jit(solution)/shard_map/ppermute | solution.py:533
  68.0 1.3 %collective-permute-start.16 = (bf16[128,128]{1,0:T(8,128)(2,1)S(1)}, bf16[128,128]{1,0:T(8,128)(2,1)S(1)}, u32[]{:S(2)}, u32[]{:S(2)}) collective-permute-start(bf16[128,128]{1,0:T(8,128)(2,1)S(1)} %get-tuple-element.68), channel_id=1, source_target_pairs={{0,4},{1,5},{2,6},{3,7},{4,0},{5,1},{6,2},{7,3},{8,12},{9,13},{10,... | collective-permute-start | bytes 98312 | tf_op jit(solution)/shard_map/ppermute | solution.py:533
  69.3 0.0 collective-permute-start.15
  69.3 0.0 collective-permute-done.19.refs_7_
  69.4 1.4 %collective-permute-start.14 = (bf16[128,128]{1,0:T(8,128)(2,1)S(1)}, bf16[128,128]{1,0:T(8,128)(2,1)S(1)}, u32[]{:S(2)}, u32[]{:S(2)}) collective-permute-start(bf16[128,128]{1,0:T(8,128)(2,1)S(1)} %get-tuple-element.70), channel_id=1, source_target_pairs={{0,2},{1,3},{2,0},{3,1},{4,6},{5,7},{6,4},{7,5},{8,10},{9,11},{10,... | collective-permute-start | bytes 98312 | tf_op jit(solution)/shard_map/ppermute | solution.py:523
  70.8 0.0 collective-permute-done.18.refs_6_
  70.8 0.4 collective-permute-start.13
  71.2 0.0 collective-permute-done.17.refs_5_
  71.2 0.7 collective-permute-done.16.refs_4_
  71.9 1.1 %collective-permute-done.15.refs_3_ = bf16[128,128]{1,0:T(8,128)(2,1)S(1)} collective-permute-done((bf16[128,128]{1,0:T(8,128)(2,1)S(1)}, bf16[128,128]{1,0:T(8,128)(2,1)S(1)}, u32[]{:S(2)}, u32[]{:S(2)}) %collective-permute-start.15) | collective-permute-done | bytes 32800 | tf_op jit(solution)/shard_map/ppermute | solution.py:523
  73.0 0.3 collective-permute-done.14.refs_2_
  73.4 0.0 collective-permute-done.13.refs_1_
  73.4 1.6 %shard_map.152 = bf16[128,2048]{1,0:T(8,128)(2,1)} custom-call(bf16[128,2048]{1,0:T(8,128)(2,1)S(1)} %copy-done.1, f32[4,8,512]{2,1,0:T(8,128)S(1)} %bitcast.23, bf16[1024,2048]{1,0:T(8,128)(2,1)S(1)} %copy-done, bf16[128,128]{1,0:T(8,128)(2,1)S(1)} %get-tuple-element.72.refs_0_, bf16[128,128]{1,0:T(8,128)(2,1)S(1)} %collective-permute-done.13.refs_1_, ...), custom_call_target="tpu_custom_call" | custom-call | flops 536870912 | tf_op jit(solution)/shard_map/pallas_call | solution.py:657
  (22 shorter events, 0.1 us)
Async XLA Ops:
  0.0 15.1 %collective-permute-start.4 = (bf16[128,2048]{1,0:T(8,128)(2,1)}, bf16[128,2048]{1,0:T(8,128)(2,1)S(1)}, u32[]{:S(2)}, u32[]{:S(2)}) collective-permute-start(bf16[128,2048]{1,0:T(8,128)(2,1)} %latent_ref.1), channel_id=1, source_target_pairs={{0,2},{1,3},{2,0},{3,1},{4,6},{5,7},{6,4},{7,5},{8,10},{9,11},{10,... | collective-permute-start | bytes 1572872 | tf_op jit(solution)/shard_map/ppermute | solution.py:523
  3.0 25.7 %collective-permute-start.3 = (bf16[128,2048]{1,0:T(8,128)(2,1)}, bf16[128,2048]{1,0:T(8,128)(2,1)S(1)}, u32[]{:S(2)}, u32[]{:S(2)}) collective-permute-start(bf16[128,2048]{1,0:T(8,128)(2,1)} %latent_ref.1), channel_id=1, source_target_pairs={{0,1},{1,0},{2,3},{3,2},{4,5},{5,4},{6,7},{7,6},{8,9},{9,8},{10,11... | collective-permute-start | bytes 1572872 | tf_op jit(solution)/shard_map/ppermute | solution.py:523
  5.1 10.0 %collective-permute-start = (f32[8,512]{1,0:T(8,128)}, f32[8,512]{1,0:T(8,128)S(1)}, u32[]{:S(2)}, u32[]{:S(2)}) collective-permute-start(f32[8,512]{1,0:T(8,128)} %shard_map.136.one_ref), channel_id=1, source_target_pairs={{0,16},{4,20},{8,24},{12,28},{16,0},{20,4},{24,8},{28,12},{1,17},{... | collective-permute-start | bytes 49160 | tf_op jit(solution)/shard_map/ppermute | solution.py:523
  7.8 20.8 %copy-start.8 = (f32[64]{0:T(128)S(1)}, f32[64]{0:T(128)}, u32[]{:S(2)}) copy-start(f32[64]{0:T(128)} %param.25) | copy-start | bytes 772
  7.8 20.8 %copy-start.9 = (f32[64]{0:T(128)S(1)}, f32[64]{0:T(128)}, u32[]{:S(2)}) copy-start(f32[64]{0:T(128)} %param.26) | copy-start | bytes 772
  7.8 20.8 %copy-start.1 = (bf16[128,2048]{1,0:T(8,128)(2,1)S(1)}, bf16[128,2048]{1,0:T(8,128)(2,1)}, u32[]{:S(2)}) copy-start(bf16[128,2048]{1,0:T(8,128)(2,1)} %latent_ref.1) | copy-start | bytes 1572868
  15.1 13.5 %collective-permute-start.5 = (bf16[128,2048]{1,0:T(8,128)(2,1)S(1)}, bf16[128,2048]{1,0:T(8,128)(2,1)S(1)}, u32[]{:S(2)}, u32[]{:S(2)}) collective-permute-start(bf16[128,2048]{1,0:T(8,128)(2,1)S(1)} %collective-permute-done.4.refs_6_), channel_id=1, source_target_pairs={{0,1},{1,0},{2,3},{3,2},{4,5},{5,4},{6,7},{7,6},{8,9},{9,8},{10,11... | collective-permute-start | bytes 1572872 | tf_op jit(solution)/shard_map/ppermute | solution.py:523
  15.1 0.7 copy-start.2
  15.8 12.8 %copy-start.3 = (bf16[2048,256]{1,0:T(8,128)(2,1)S(1)}, bf16[2048,256]{1,0:T(8,128)(2,1)}, u32[]{:S(2)}) copy-start(bf16[2048,256]{1,0:T(8,128)(2,1)} %refs_2_.1) | copy-start | bytes 3145732
  15.8 12.9 %copy-start.4 = (bf16[2048,128]{1,0:T(8,128)(2,1)S(1)}, bf16[2048,128]{1,0:T(8,128)(2,1)}, u32[]{:S(2)}) copy-start(bf16[2048,128]{1,0:T(8,128)(2,1)} %refs_3_.1) | copy-start | bytes 1572868
  15.8 12.9 %copy-start.5 = (bf16[2048,128]{1,0:T(8,128)(2,1)S(1)}, bf16[2048,128]{1,0:T(8,128)(2,1)}, u32[]{:S(2)}) copy-start(bf16[2048,128]{1,0:T(8,128)(2,1)} %refs_4_.1) | copy-start | bytes 1572868
  15.8 12.9 %copy-start.6 = (bf16[64,2048]{1,0:T(8,128)(2,1)S(1)}, bf16[64,2048]{1,0:T(8,128)(2,1)}, u32[]{:S(2)}) copy-start(bf16[64,2048]{1,0:T(8,128)(2,1)} %refs_1_.1) | copy-start | bytes 786436
  15.8 12.9 %copy-start.7 = (f32[2048]{0:T(1024)S(1)}, f32[2048]{0:T(1024)}, u32[]{:S(2)}) copy-start(f32[2048]{0:T(1024)} %param.18) | copy-start | bytes 24580
  15.9 3.8 %collective-permute-start.1 = (f32[8,512]{1,0:T(8,128)S(1)}, f32[8,512]{1,0:T(8,128)S(1)}, u32[]{:S(2)}, u32[]{:S(2)}) collective-permute-start(f32[8,512]{1,0:T(8,128)S(1)} %shard_map.137.one_ref), channel_id=1, source_target_pairs={{0,8},{4,12},{8,0},{12,4},{16,24},{20,28},{24,16},{28,20},{1,9},{5... | collective-permute-start | bytes 49160 | tf_op jit(solution)/shard_map/ppermute | solution.py:523
  19.7 3.7 %collective-permute-start.2 = (f32[8,512]{1,0:T(8,128)S(1)}, f32[8,512]{1,0:T(8,128)S(1)}, u32[]{:S(2)}, u32[]{:S(2)}) collective-permute-start(f32[8,512]{1,0:T(8,128)S(1)} %shard_map.138.one_ref), channel_id=1, source_target_pairs={{0,4},{4,0},{8,12},{12,8},{16,20},{20,16},{24,28},{28,24},{1,5},{5... | collective-permute-start | bytes 49160 | tf_op jit(solution)/shard_map/ppermute | solution.py:523
  31.4 10.8 %collective-permute-start.6 = (bf16[9,128,128]{2,1,0:T(8,128)(2,1)S(1)}, bf16[9,128,128]{2,1,0:T(8,128)(2,1)S(1)}, u32[]{:S(2)}, u32[]{:S(2)}) collective-permute-start(bf16[9,128,128]{2,1,0:T(8,128)(2,1)S(1)} %get-tuple-element.36), channel_id=1, source_target_pairs={{0,4},{4,0},{8,12},{12,8},{16,20},{20,16},{24,28},{28,24},{1,5},{5... | collective-permute-start | bytes 884744 | tf_op jit(solution)/shard_map/ppermute | solution.py:523
  33.2 8.9 %collective-permute-start.10 = (bf16[5,128,128]{2,1,0:T(8,128)(2,1)S(1)}, bf16[5,128,128]{2,1,0:T(8,128)(2,1)S(1)}, u32[]{:S(2)}, u32[]{:S(2)}) collective-permute-start(bf16[5,128,128]{2,1,0:T(8,128)(2,1)S(1)} %get-tuple-element.37.refs_1_), channel_id=1, source_target_pairs={{0,8},{4,12},{8,16},{12,20},{16,24},{20,28},{24,0},{28,4},{1,9},{5... | collective-permute-start | bytes 491528 | tf_op jit(solution)/shard_map/ppermute | solution.py:538
  34.8 14.2 %collective-permute-start.12 = (bf16[5,128,128]{2,1,0:T(8,128)(2,1)S(1)}, bf16[5,128,128]{2,1,0:T(8,128)(2,1)S(1)}, u32[]{:S(2)}, u32[]{:S(2)}) collective-permute-start(bf16[5,128,128]{2,1,0:T(8,128)(2,1)S(1)} %get-tuple-element.37.refs_1_), channel_id=1, source_target_pairs={{0,24},{4,28},{8,0},{12,4},{16,8},{20,12},{24,16},{28,20},{1,25},{... | collective-permute-start | bytes 491528 | tf_op jit(solution)/shard_map/ppermute | solution.py:538
  42.1 13.5 %collective-permute-start.11 = (bf16[5,128,128]{2,1,0:T(8,128)(2,1)S(1)}, bf16[5,128,128]{2,1,0:T(8,128)(2,1)S(1)}, u32[]{:S(2)}, u32[]{:S(2)}) collective-permute-start(bf16[5,128,128]{2,1,0:T(8,128)(2,1)S(1)} %collective-permute-done.10.refs_1_), channel_id=1, source_target_pairs={{0,8},{4,12},{8,16},{12,20},{16,24},{20,28},{24,0},{28,4},{1,9},{5... | collective-permute-start | bytes 491528 | tf_op jit(solution)/shard_map/ppermute | solution.py:538
  42.1 17.2 %collective-permute-start.9 = (bf16[5,128,128]{2,1,0:T(8,128)(2,1)S(1)}, bf16[5,128,128]{2,1,0:T(8,128)(2,1)S(1)}, u32[]{:S(2)}, u32[]{:S(2)}) collective-permute-start(bf16[5,128,128]{2,1,0:T(8,128)(2,1)S(1)} %slice.36), channel_id=1, source_target_pairs={{0,24},{4,28},{8,0},{12,4},{16,8},{20,12},{24,16},{28,20},{1,25},{... | collective-permute-start | bytes 491528 | tf_op jit(solution)/shard_map/ppermute | solution.py:538
  46.2 9.4 %collective-permute-start.7 = (bf16[5,128,128]{2,1,0:T(8,128)(2,1)S(1)}, bf16[5,128,128]{2,1,0:T(8,128)(2,1)S(1)}, u32[]{:S(2)}, u32[]{:S(2)}) collective-permute-start(bf16[5,128,128]{2,1,0:T(8,128)(2,1)S(1)} %slice.36), channel_id=1, source_target_pairs={{0,8},{4,12},{8,16},{12,20},{16,24},{20,28},{24,0},{28,4},{1,9},{5... | collective-permute-start | bytes 491528 | tf_op jit(solution)/shard_map/ppermute | solution.py:538
  55.6 7.1 %collective-permute-start.8 = (bf16[5,128,128]{2,1,0:T(8,128)(2,1)S(1)}, bf16[5,128,128]{2,1,0:T(8,128)(2,1)S(1)}, u32[]{:S(2)}, u32[]{:S(2)}) collective-permute-start(bf16[5,128,128]{2,1,0:T(8,128)(2,1)S(1)} %collective-permute-done.7.refs_2_), channel_id=1, source_target_pairs={{0,8},{4,12},{8,16},{12,20},{16,24},{20,28},{24,0},{28,4},{1,9},{5... | collective-permute-start | bytes 491528 | tf_op jit(solution)/shard_map/ppermute | solution.py:538
  63.7 9.6 %copy-start = (bf16[1024,2048]{1,0:T(8,128)(2,1)S(1)}, bf16[1024,2048]{1,0:T(8,128)(2,1)}, u32[]{:S(2)}) copy-start(bf16[1024,2048]{1,0:T(8,128)(2,1)} %weight_ref.1) | copy-start | bytes 12582916
  63.8 5.6 %collective-permute-start.19 = (bf16[128,128]{1,0:T(8,128)(2,1)S(1)}, bf16[128,128]{1,0:T(8,128)(2,1)S(1)}, u32[]{:S(2)}, u32[]{:S(2)}) collective-permute-start(bf16[128,128]{1,0:T(8,128)(2,1)S(1)} %get-tuple-element.65), channel_id=1, source_target_pairs={{0,7},{1,6},{2,5},{3,4},{4,3},{5,2},{6,1},{7,0},{8,15},{9,14},{10,... | collective-permute-start | bytes 98312 | tf_op jit(solution)/shard_map/ppermute | solution.py:533
  63.9 6.9 %collective-permute-start.18 = (bf16[128,128]{1,0:T(8,128)(2,1)S(1)}, bf16[128,128]{1,0:T(8,128)(2,1)S(1)}, u32[]{:S(2)}, u32[]{:S(2)}) collective-permute-start(bf16[128,128]{1,0:T(8,128)(2,1)S(1)} %get-tuple-element.66), channel_id=1, source_target_pairs={{0,6},{1,7},{2,4},{3,5},{4,2},{5,3},{6,0},{7,1},{8,14},{9,15},{10,... | collective-permute-start | bytes 98312 | tf_op jit(solution)/shard_map/ppermute | solution.py:533
  66.3 4.9 %collective-permute-start.17 = (bf16[128,128]{1,0:T(8,128)(2,1)S(1)}, bf16[128,128]{1,0:T(8,128)(2,1)S(1)}, u32[]{:S(2)}, u32[]{:S(2)}) collective-permute-start(bf16[128,128]{1,0:T(8,128)(2,1)S(1)} %get-tuple-element.67), channel_id=1, source_target_pairs={{0,5},{1,4},{2,7},{3,6},{4,1},{5,0},{6,3},{7,2},{8,13},{9,12},{10,... | collective-permute-start | bytes 98312 | tf_op jit(solution)/shard_map/ppermute | solution.py:533
  68.0 3.9 %collective-permute-start.16 = (bf16[128,128]{1,0:T(8,128)(2,1)S(1)}, bf16[128,128]{1,0:T(8,128)(2,1)S(1)}, u32[]{:S(2)}, u32[]{:S(2)}) collective-permute-start(bf16[128,128]{1,0:T(8,128)(2,1)S(1)} %get-tuple-element.68), channel_id=1, source_target_pairs={{0,4},{1,5},{2,6},{3,7},{4,0},{5,1},{6,2},{7,3},{8,12},{9,13},{10,... | collective-permute-start | bytes 98312 | tf_op jit(solution)/shard_map/ppermute | solution.py:533
  69.3 3.7 %collective-permute-start.15 = (bf16[128,128]{1,0:T(8,128)(2,1)S(1)}, bf16[128,128]{1,0:T(8,128)(2,1)S(1)}, u32[]{:S(2)}, u32[]{:S(2)}) collective-permute-start(bf16[128,128]{1,0:T(8,128)(2,1)S(1)} %get-tuple-element.69), channel_id=1, source_target_pairs={{0,3},{1,2},{2,1},{3,0},{4,7},{5,6},{6,5},{7,4},{8,11},{9,10},{10,... | collective-permute-start | bytes 98312 | tf_op jit(solution)/shard_map/ppermute | solution.py:523
  69.4 4.0 %collective-permute-start.14 = (bf16[128,128]{1,0:T(8,128)(2,1)S(1)}, bf16[128,128]{1,0:T(8,128)(2,1)S(1)}, u32[]{:S(2)}, u32[]{:S(2)}) collective-permute-start(bf16[128,128]{1,0:T(8,128)(2,1)S(1)} %get-tuple-element.70), channel_id=1, source_target_pairs={{0,2},{1,3},{2,0},{3,1},{4,6},{5,7},{6,4},{7,5},{8,10},{9,11},{10,... | collective-permute-start | bytes 98312 | tf_op jit(solution)/shard_map/ppermute | solution.py:523
  70.8 2.6 %collective-permute-start.13 = (bf16[128,128]{1,0:T(8,128)(2,1)S(1)}, bf16[128,128]{1,0:T(8,128)(2,1)S(1)}, u32[]{:S(2)}, u32[]{:S(2)}) collective-permute-start(bf16[128,128]{1,0:T(8,128)(2,1)S(1)} %get-tuple-element.71), channel_id=1, source_target_pairs={{0,1},{1,0},{2,3},{3,2},{4,5},{5,4},{6,7},{7,6},{8,9},{9,8},{10,11... | collective-permute-start | bytes 98312 | tf_op jit(solution)/shard_map/ppermute | solution.py:523

commit v2 on v1

--- a/solution.py
+++ b/solution.py
@@ -311,7 +311,9 @@
     sine_ref,
     keep_q,
     keep_kv,
-    give,
+    keep_ctx,
+    give_q,
+    give_kv,
     made,
 ):
     span = CHANNEL_SPAN
@@ -368,18 +370,30 @@
             jnp.bfloat16
         )
     side = lax.rem(lax.axis_index("sp"), kv_heads)
-    for i in range(q_tiles):
-        keep_q[i] = made[side, i]
-    for i in range(keep_kv.shape[0]):
-        keep_kv[i] = made[side, q_tiles + i]
-    for i in range(give.shape[0]):
-        give[i] = made[1 - side, i]
-
-
-def attention_body(bases, first, last, offset, *refs):
+    for head, q_ref, kv_ref in ((1 - side, give_q, give_kv), (side, keep_q, keep_kv)):
+        for i in range(q_tiles):
+            q_ref[i] = made[head, i]
+        for i in range(kv_ref.shape[0]):
+            kv_ref[i] = made[head, q_tiles + i]
+    keep_ctx[...] = made[side, q_tiles + len(blocks)]
+
+
+def merge_body(near_ref, ctx_ref, out_ref):
+    last = near_ref.shape[0] - 1
+    span = ctx_ref.shape[1] // 2
+    for i in range(last):
+        out_ref[i] = near_ref[i]
+    out_ref[last] = jnp.concatenate([near_ref[last, :, 0:span], ctx_ref[:, 0:span]], axis=1)
+
+
+def merge(near, ctx):
+    return kernel_call(merge_body, jax.ShapeDtypeStruct(near.shape, near.dtype), 2, 10**6)(near, ctx)
+
+
+def attention_body(count, first, last, offset, *refs):
     q_ref = refs[0]
-    kv_refs = refs[1 : 1 + len(bases)]
-    refs = refs[1 + len(bases) :]
+    kv_refs = refs[1 : 1 + count]
+    refs = refs[1 + count :]
     if not first:
         peak_in, total_in, sum_in = refs[:3]
         refs = refs[3:]
@@ -387,7 +401,7 @@
     scale = span ** (-0.5) * LOG2E
     groups = 2
     pairs = 2
-    chunks = [(ref, base, part) for ref, base in zip(kv_refs, bases) for part in (0, 1)]
+    chunks = [(ref, part, ref.shape[0] > 2 * pairs) for ref in kv_refs for part in (0, 1)]
     tiles = [(g, chunk) for chunk in chunks for g in range(groups)]
     states = {}
     queries = {}
@@ -405,15 +419,15 @@
         queries[g, 1] = jnp.concatenate([blank, found], axis=0)
 
     def scores(tile):
-        g, (ref, base, part) = tile
-        keys = [ref[base + p] for p in range(pairs)]
-        if part == 0:
-            keys.append(ref[base + 2 * pairs, 0:span, :])
+        g, (ref, part, context) = tile
+        keys = [ref[p] for p in range(pairs)]
+        if context:
+            keys.append(ref[2 * pairs, 0:span, :])
         found = jnp.dot(
             jnp.concatenate(keys, axis=0), queries[g, part], preferred_element_type=jnp.float32
         )
         found = found * scale
-        if part == 0:
+        if context:
             rows = found.shape[0] - span
             found = jnp.concatenate([found[:rows], found[rows:] + offset * LOG2E], axis=0)
         return found
@@ -436,11 +450,11 @@
         return shares.astype(jnp.bfloat16), shrink
 
     def gather(tile, shares, shrink):
-        g, (ref, base, part) = tile
+        g, (ref, part, context) = tile
         rows = slice(part * span, (part + 1) * span)
-        values = [ref[base + pairs + p, rows, :] for p in range(pairs)]
-        if part == 0:
-            values.append(ref[base + 2 * pairs, span : 2 * span, 0:span])
+        values = [ref[pairs + p, rows, :] for p in range(pairs)]
+        if context:
+            values.append(ref[2 * pairs, span : 2 * span, rows])
         weighted = jnp.dot(
             jnp.concatenate(values, axis=1), shares, preferred_element_type=jnp.float32
         )
@@ -479,8 +493,8 @@
 def attend(state, probes, pairs, offset, last=False):
     lanes = 2 * 2 * probes.shape[2]
     span = probes.shape[1] // 2
-    keys = sum(lanes + span for unused in pairs)
-    inputs = [probes, *(ref for ref, unused in pairs)] + list(state or ())
+    keys = sum(p.shape[0] * p.shape[1] // 2 for p in pairs)
+    inputs = [probes, *pairs] + list(state or ())
     if last:
         out = jax.ShapeDtypeStruct((4, 2 * span, probes.shape[2]), jnp.bfloat16)
     else:
@@ -488,7 +502,7 @@
         out = [stat, stat, jax.ShapeDtypeStruct((2, span, lanes), jnp.float32)]
 
     def body(*refs):
-        attention_body([base for unused, base in pairs], state is None, last, offset, *refs)
+        attention_body(len(pairs), state is None, last, offset, *refs)
 
     return kernel_call(body, out, len(inputs), 40 * 2 * lanes * keys * span)(*inputs)
 
@@ -600,17 +614,17 @@
     modulation = lax.all_gather(part, "tp", axis=0, tiled=False)
     cosine, sine = tables(seq_index, head_index, own_rows, head_split)
     q_tiles = q_heads // kv_heads * head_split // 2
-    kv_tiles = head_split + 1
+    kv_tiles = head_split
     tile = (own_rows, own_rows)
-    keep_q, keep_kv, give = pl.pallas_call(
+    keep_q, keep_kv, keep_ctx, give_q, give_kv = pl.pallas_call(
         lambda *refs: projection_body(q_heads, kv_heads, *refs),
         out_shape=[
-            jax.ShapeDtypeStruct((count, *tile), jnp.bfloat16)
-            for count in (q_tiles, kv_tiles, q_tiles + kv_tiles)
+            jax.ShapeDtypeStruct((*count, *tile), jnp.bfloat16)
+            for count in ((q_tiles,), (kv_tiles,), (), (q_tiles,), (kv_tiles + 1,))
         ],
         in_specs=[whole_spec()] * 14,
-        out_specs=[whole_spec()] * 3,
-        scratch_shapes=[pltpu.VMEM((kv_heads, q_tiles + kv_tiles, *tile), jnp.bfloat16)],
+        out_specs=[whole_spec()] * 5,
+        scratch_shapes=[pltpu.VMEM((kv_heads, q_tiles + kv_tiles + 1, *tile), jnp.bfloat16)],
         cost_estimate=pl.CostEstimate(
             flops=4 * tok_count * depth * (q_heads + 2 * kv_heads) * CHANNEL_SPAN,
             transcendentals=0,
@@ -634,23 +648,23 @@
         sine,
     )
     offset = math.log(tok_count / (2.0 * ctx_rows))
-    near = xor_move(give, "sp", 1)
+    near = xor_move(give_kv, "sp", 1)
     up = ring_move(keep_kv, 2)
     down = ring_move(keep_kv, -2)
-    near_kv = near[q_tiles:]
-    near_up = ring_move(near_kv, 2)
-    near_down = ring_move(near_kv, -2)
+    near_q = xor_move(give_q, "sp", 1)
+    near = merge(near, keep_ctx)
+    near_up = ring_move(near, 2)
+    near_down = ring_move(near, -2)
     across = ring_move(up, 2)
     near_across = ring_move(near_up, 2)
-    own = attend(None, keep_q, [(keep_kv, 0)], offset)
-    other = attend(None, near, [(keep_kv, 0), (near, q_tiles)], offset)
-    own = attend(own, keep_q, [(near, q_tiles)], offset)
-    for group in ([up, down], [across, near_up], [near_down]):
-        pieces = [(piece, 0) for piece in group]
-        other = attend(other, near, pieces, offset)
+    own = attend(None, keep_q, [keep_kv], offset)
+    own = attend(own, keep_q, [near], offset)
+    other = attend(None, near_q, [keep_kv, near], offset)
+    for pieces in ([up, down], [near_up, across], [near_down]):
+        other = attend(other, near_q, pieces, offset)
         own = attend(own, keep_q, pieces, offset)
-    other = attend(other, near, [(near_across, 0)], offset, True)
-    own = attend(own, keep_q, [(near_across, 0)], offset, True)
+    other = attend(other, near_q, [near_across], offset, True)
+    own = attend(own, keep_q, [near_across], offset, True)
     sent = [cross_move(other[j], j) for j in range(head_split)]
     parts = [own[0]] + [xor_move(own[j], "tp", j) for j in range(1, head_split)] + sent
     width = q_heads * CHANNEL_SPAN

time: 75.2 us -> 73.9 us (0.983)
  waiting for transfers between devices: 21.4 us -> 20 us
    ppermute x6, waiting for transfers between devices: 8.38 us -> 7.01 us  [ring_move(): lax.ppermute(member, 'sp', [(i, (i + step) % size) for i in range(size)])]
    ppermute x10 -> x11, waiting for transfers between devices: 12.3 us -> 13 us  [xor_move(): return lax.ppermute(member, axis, [(i, i ^ mask) for i in range(size)])]
    ppermute x10 -> x11, starting transfers between devices: 13 us -> 13.6 us  [xor_move(): return lax.ppermute(member, axis, [(i, i ^ mask) for i in range(size)])]
  transfers between devices with their start and end apart: 20 -> 21, of which waited for: 9 -> 8; matrix products, arithmetic and copies ran while one was open for 1% -> 1% of each run, Pallas kernels for 22% -> 22%
where the time goes in v2:
time: 73.9 us; the launch traced here: 73.6 us
  starting transfers between devices  25.4 us (34%)
  Pallas kernels  21.5 us (29%)
  waiting for transfers between devices  20 us (27%)
  blocking collectives  5.22 us (7%)
  local copies, waits for them, and re-layouts  0.78 us (1%)
    pallas_call x11, Pallas kernels, attend(): kernel_call(body, out, len(inputs), 40 * 2 * lanes * keys * span)(*inputs)  15.1 us
    ppermute x11, starting transfers between devices, xor_move(): return lax.ppermute(member, axis, [(i, i ^ mask) for i in range(size)])  13.6 us
    ppermute x11, waiting for transfers between devices, xor_move(): return lax.ppermute(member, axis, [(i, i ^ mask) for i in range(size)])  13 us
    ppermute x6, starting transfers between devices, ring_move(): lax.ppermute(member, 'sp', [(i, (i + step) % size) for i in range(size)])  7.4 us
    ppermute x6, waiting for transfers between devices, ring_move(): lax.ppermute(member, 'sp', [(i, (i + step) % size) for i in range(size)])  7.01 us
    all_gather x1, blocking collectives, inner_device(): modulation = lax.all_gather(part, 'tp', axis=0, tiled=False)  5.22 us
    ppermute x4, starting transfers between devices, cross_move(): return lax.ppermute(member, ('sp', 'tp'), pairs)  4.45 us
    pallas_call x1, Pallas kernels, inner_device(): pl.pallas_call(lambda *refs: projection_body(q_heads, kv_heads, *refs), o...  2.66 us
  transfers between devices with their start and end apart: 21, of which 8 were waited for; matrix products, arithmetic and copies ran while one was open for 1% of the time, Pallas kernels for 22%

profile of v2, /device:TPU:0, one launch (start us, length us, event | category | flops | bytes accessed | tf_op | source)
XLA Modules:
  0.0 73.6 jit_solution(2075050614295462746)
XLA Ops:
  0.0 3.0 %collective-permute-start.4 = (bf16[128,2048]{1,0:T(8,128)(2,1)}, bf16[128,2048]{1,0:T(8,128)(2,1)S(1)}, u32[]{:S(2)}, u32[]{:S(2)}) collective-permute-start(bf16[128,2048]{1,0:T(8,128)(2,1)} %latent_ref.1), channel_id=1, source_target_pairs={{0,2},{1,3},{2,0},{3,1},{4,6},{5,7},{6,4},{7,5},{8,10},{9,11},{10,... | collective-permute-start | bytes 1572872 | tf_op jit(solution)/shard_map/ppermute | solution.py:537
  3.0 0.0 collective-permute-start.3
  3.0 2.1 %shard_map.136.one_ref = f32[8,512]{1,0:T(8,128)} custom-call(f32[1,2048]{1,0:T(1,128)} %bitcast.27, f32[1,2048]{1,0:T(1,128)} %bitcast.28, bf16[256,512]{1,0:T(8,128)(2,1)} %shift_hbm.1, bf16[256,512]{1,0:T(8,128)(2,1)} %scale_hbm.1, bf16[256,512]{1,0:T(8,128)(2,1)} %gate_hbm.1), custom_call_target="tpu_custom_call" | custom-call | flops 100000000 | tf_op jit(solution)/shard_map/pallas_call | solution.py:275
  5.1 2.7 %collective-permute-start = (f32[8,512]{1,0:T(8,128)}, f32[8,512]{1,0:T(8,128)S(1)}, u32[]{:S(2)}, u32[]{:S(2)}) collective-permute-start(f32[8,512]{1,0:T(8,128)} %shard_map.136.one_ref), channel_id=1, source_target_pairs={{0,16},{4,20},{8,24},{12,28},{16,0},{20,4},{24,8},{28,12},{1,17},{... | collective-permute-start | bytes 49160 | tf_op jit(solution)/shard_map/ppermute | solution.py:537
  7.7 0.1 fusion.2
  7.8 0.0 copy-start.9
  7.8 0.0 copy-start.1
  7.8 7.3 %collective-permute-done.4.refs_6_ = bf16[128,2048]{1,0:T(8,128)(2,1)S(1)} collective-permute-done((bf16[128,2048]{1,0:T(8,128)(2,1)}, bf16[128,2048]{1,0:T(8,128)(2,1)S(1)}, u32[]{:S(2)}, u32[]{:S(2)}) %collective-permute-start.4) | collective-permute-done | bytes 524320 | tf_op jit(solution)/shard_map/ppermute | solution.py:537
  15.1 0.0 collective-permute-start.5
  15.1 0.0 collective-permute-done.other_ref
  15.1 0.7 copy-done.2
  15.8 0.0 copy-start.7
  15.9 1.9 %collective-permute-start.1 = (f32[8,512]{1,0:T(8,128)S(1)}, f32[8,512]{1,0:T(8,128)S(1)}, u32[]{:S(2)}, u32[]{:S(2)}) collective-permute-start(f32[8,512]{1,0:T(8,128)S(1)} %shard_map.137.one_ref), channel_id=1, source_target_pairs={{0,8},{4,12},{8,0},{12,4},{16,24},{20,28},{24,16},{28,20},{1,9},{5... | collective-permute-start | bytes 49160 | tf_op jit(solution)/shard_map/ppermute | solution.py:537
  17.8 0.3 fusion
  18.1 1.6 %collective-permute-done.1.other_ref = f32[8,512]{1,0:T(8,128)S(1)} collective-permute-done((f32[8,512]{1,0:T(8,128)S(1)}, f32[8,512]{1,0:T(8,128)S(1)}, u32[]{:S(2)}, u32[]{:S(2)}) %collective-permute-start.1) | collective-permute-done | bytes 16416 | tf_op jit(solution)/shard_map/ppermute | solution.py:537
  19.7 1.8 %collective-permute-start.2 = (f32[8,512]{1,0:T(8,128)S(1)}, f32[8,512]{1,0:T(8,128)S(1)}, u32[]{:S(2)}, u32[]{:S(2)}) collective-permute-start(f32[8,512]{1,0:T(8,128)S(1)} %shard_map.138.one_ref), channel_id=1, source_target_pairs={{0,4},{4,0},{8,12},{12,8},{16,20},{20,16},{24,28},{28,24},{1,5},{5... | collective-permute-start | bytes 49160 | tf_op jit(solution)/shard_map/ppermute | solution.py:537
  21.5 1.9 %collective-permute-done.2.other_ref = f32[8,512]{1,0:T(8,128)S(1)} collective-permute-done((f32[8,512]{1,0:T(8,128)S(1)}, f32[8,512]{1,0:T(8,128)S(1)}, u32[]{:S(2)}, u32[]{:S(2)}) %collective-permute-start.2) | collective-permute-done | bytes 16416 | tf_op jit(solution)/shard_map/ppermute | solution.py:537
  23.4 5.2 %all-gather = f32[32,512]{1,0:T(8,128)S(1)} all-gather(f32[8,512]{1,0:T(8,128)S(1)} %shard_map.139), channel_id=2, replica_groups=mesh['sp'=8,'tp'=4] {'tp'}, dimensions={0}, use_global_device_ids=true | all-gather | bytes 81920 | tf_op jit(solution)/shard_map/all_gather | solution.py:614
  28.6 0.0 collective-permute-done.3.refs_5_
  28.6 0.0 collective-permute-done.5.refs_7_
  28.7 2.7 %shard_map.140 = (bf16[4,128,128]{2,1,0:T(8,128)(2,1)S(1)}, bf16[4,128,128]{2,1,0:T(8,128)(2,1)S(1)}, bf16[128,128]{1,0:T(8,128)(2,1)S(1)}, bf16[4,128,128]{2,1,0:T(8,128)(2,1)S(1)}, bf16[5,128,128]{2,1,0:T(8,128)(2,1)S(1)}) custom-call(bf16[128,2048]{1,0:T(8,128)(2,1)S(1)} %copy-done.1, bf16[64,2048]{1,0:T(8,128)(2,1)S(1)} %copy-done.6, ...), custom_call_target="tpu_custom_call" | custom-call | flops 2147483648 | tf_op jit(solution)/shard_map/pallas_call | solution.py:619
  31.4 1.8 %collective-permute-start.6 = (bf16[5,128,128]{2,1,0:T(8,128)(2,1)S(1)}, bf16[5,128,128]{2,1,0:T(8,128)(2,1)S(1)}, u32[]{:S(2)}, u32[]{:S(2)}) collective-permute-start(bf16[5,128,128]{2,1,0:T(8,128)(2,1)S(1)} %get-tuple-element.38), channel_id=1, source_target_pairs={{0,4},{4,0},{8,12},{12,8},{16,20},{20,16},{24,28},{28,24},{1,5},{5... | collective-permute-start | bytes 491528 | tf_op jit(solution)/shard_map/ppermute | solution.py:537
  33.2 1.6 %collective-permute-start.10 = (bf16[4,128,128]{2,1,0:T(8,128)(2,1)S(1)}, bf16[4,128,128]{2,1,0:T(8,128)(2,1)S(1)}, u32[]{:S(2)}, u32[]{:S(2)}) collective-permute-start(bf16[4,128,128]{2,1,0:T(8,128)(2,1)S(1)} %get-tuple-element.40.refs_1_), channel_id=1, source_target_pairs={{0,8},{4,12},{8,16},{12,20},{16,24},{20,28},{24,0},{28,4},{1,9},{5... | collective-permute-start | bytes 393224 | tf_op jit(solution)/shard_map/ppermute | solution.py:552
  34.8 0.6 collective-permute-start.16
  35.3 2.0 %collective-permute-start.12 = (bf16[4,128,128]{2,1,0:T(8,128)(2,1)S(1)}, bf16[4,128,128]{2,1,0:T(8,128)(2,1)S(1)}, u32[]{:S(2)}, u32[]{:S(2)}) collective-permute-start(bf16[4,128,128]{2,1,0:T(8,128)(2,1)S(1)} %get-tuple-element.40.refs_1_), channel_id=1, source_target_pairs={{0,24},{4,28},{8,0},{12,4},{16,8},{20,12},{24,16},{28,20},{1,25},{... | collective-permute-start | bytes 393224 | tf_op jit(solution)/shard_map/ppermute | solution.py:552
  37.3 0.9 %shard_map.142 = (f32[2,1,512]{2,1,0:T(1,128)S(1)}, f32[2,1,512]{2,1,0:T(1,128)S(1)}, f32[2,64,512]{2,1,0:T(8,128)S(1)}) custom-call(bf16[4,128,128]{2,1,0:T(8,128)(2,1)S(1)} %get-tuple-element.37.refs_0_, bf16[4,128,128]{2,1,0:T(8,128)(2,1)S(1)} %get-tuple-element.40.refs_1_), custom_call_target="tpu_custom_call" | custom-call | flops 671088640 | tf_op jit(solution)/shard_map/pallas_call | solution.py:507
  38.2 3.1 %collective-permute-done.10.refs_1_ = bf16[4,128,128]{2,1,0:T(8,128)(2,1)S(1)} collective-permute-done((bf16[4,128,128]{2,1,0:T(8,128)(2,1)S(1)}, bf16[4,128,128]{2,1,0:T(8,128)(2,1)S(1)}, u32[]{:S(2)}, u32[]{:S(2)}) %collective-permute-start.10) | collective-permute-done | bytes 131104 | tf_op jit(solution)/shard_map/ppermute | solution.py:552
  41.4 0.0 collective-permute-start.11
  41.4 0.0 collective-permute-done.6.near_ref
  41.4 0.1 shard_map.141.refs_1_.refs_2_
  41.4 3.8 %collective-permute-start.9 = (bf16[5,128,128]{2,1,0:T(8,128)(2,1)S(1)}, bf16[5,128,128]{2,1,0:T(8,128)(2,1)S(1)}, u32[]{:S(2)}, u32[]{:S(2)}) collective-permute-start(bf16[5,128,128]{2,1,0:T(8,128)(2,1)S(1)} %shard_map.141.refs_1_.refs_2_), channel_id=1, source_target_pairs={{0,24},{4,28},{8,0},{12,4},{16,8},{20,12},{24,16},{28,20},{1,25},{... | collective-permute-start | bytes 491528 | tf_op jit(solution)/shard_map/ppermute | solution.py:552
  45.3 0.0 collective-permute-start.7
  45.3 0.0 collective-permute-done.16.refs_0_
  45.3 1.8 %shard_map.148 = (f32[2,1,512]{2,1,0:T(1,128)S(1)}, f32[2,1,512]{2,1,0:T(1,128)S(1)}, f32[2,64,512]{2,1,0:T(8,128)S(1)}) custom-call(bf16[4,128,128]{2,1,0:T(8,128)(2,1)S(1)} %collective-permute-done.16.refs_0_, bf16[4,128,128]{2,1,0:T(8,128)(2,1)S(1)} %get-tuple-element.40.refs_1_, bf16[5,128,128]{2,1,0:T(8,128)(2,1)S(1)} %shard_map.141.refs_1_.refs_2_), custom_call_target="tpu_custom_call" | custom-call | flops 1509949440 | tf_op jit(solution)/shard_map/pallas_call | solution.py:507
  47.0 0.0 collective-permute-done.12.refs_2_
  47.0 1.7 %shard_map.149 = (f32[2,1,512]{2,1,0:T(1,128)S(1)}, f32[2,1,512]{2,1,0:T(1,128)S(1)}, f32[2,64,512]{2,1,0:T(8,128)S(1)}) custom-call(bf16[4,128,128]{2,1,0:T(8,128)(2,1)S(1)} %collective-permute-done.16.refs_0_, bf16[4,128,128]{2,1,0:T(8,128)(2,1)S(1)} %collective-permute-done.10.refs_1_, bf16[4,128,128]{2,1,0:T(8,128)(2,1)S(1)} %collective-permute-done.12.refs_2_, ...), custom_call_target="tpu_custom_call" | custom-call | flops 1342177280 | tf_op jit(solution)/shard_map/pallas_call | solution.py:507
  48.7 1.1 %shard_map.143 = (f32[2,1,512]{2,1,0:T(1,128)S(1)}, f32[2,1,512]{2,1,0:T(1,128)S(1)}, f32[2,64,512]{2,1,0:T(8,128)S(1)}) custom-call(bf16[4,128,128]{2,1,0:T(8,128)(2,1)S(1)} %get-tuple-element.37.refs_0_, bf16[5,128,128]{2,1,0:T(8,128)(2,1)S(1)} %shard_map.141.refs_1_.refs_2_, f32[2,1,512]{2,1,0:T(1,128)S(1)} %get-tuple-element.41.refs_2_, ...), custom_call_target="tpu_custom_call" | custom-call | flops 838860800 | tf_op jit(solution)/shard_map/pallas_call | solution.py:507
  49.8 1.7 %shard_map.144 = (f32[2,1,512]{2,1,0:T(1,128)S(1)}, f32[2,1,512]{2,1,0:T(1,128)S(1)}, f32[2,64,512]{2,1,0:T(8,128)S(1)}) custom-call(bf16[4,128,128]{2,1,0:T(8,128)(2,1)S(1)} %get-tuple-element.37.refs_0_, bf16[4,128,128]{2,1,0:T(8,128)(2,1)S(1)} %collective-permute-done.10.refs_1_, bf16[4,128,128]{2,1,0:T(8,128)(2,1)S(1)} %collective-permute-done.12.refs_2_, ...), custom_call_target="tpu_custom_call" | custom-call | flops 1342177280 | tf_op jit(solution)/shard_map/pallas_call | solution.py:507
  51.5 2.5 %collective-permute-done.7.refs_1_ = bf16[5,128,128]{2,1,0:T(8,128)(2,1)S(1)} collective-permute-done((bf16[5,128,128]{2,1,0:T(8,128)(2,1)S(1)}, bf16[5,128,128]{2,1,0:T(8,128)(2,1)S(1)}, u32[]{:S(2)}, u32[]{:S(2)}) %collective-permute-start.7) | collective-permute-done | bytes 163872 | tf_op jit(solution)/shard_map/ppermute | solution.py:552
  54.1 0.0 collective-permute-start.8
  54.1 0.0 collective-permute-done.11.refs_2_
  54.1 1.8 %shard_map.150 = (f32[2,1,512]{2,1,0:T(1,128)S(1)}, f32[2,1,512]{2,1,0:T(1,128)S(1)}, f32[2,64,512]{2,1,0:T(8,128)S(1)}) custom-call(bf16[4,128,128]{2,1,0:T(8,128)(2,1)S(1)} %collective-permute-done.16.refs_0_, bf16[5,128,128]{2,1,0:T(8,128)(2,1)S(1)} %collective-permute-done.7.refs_1_, bf16[4,128,128]{2,1,0:T(8,128)(2,1)S(1)} %collective-permute-done.11.refs_2_, ...), custom_call_target="tpu_custom_call" | custom-call | flops 1509949440 | tf_op jit(solution)/shard_map/pallas_call | solution.py:507
  55.9 1.8 %shard_map.145 = (f32[2,1,512]{2,1,0:T(1,128)S(1)}, f32[2,1,512]{2,1,0:T(1,128)S(1)}, f32[2,64,512]{2,1,0:T(8,128)S(1)}) custom-call(bf16[4,128,128]{2,1,0:T(8,128)(2,1)S(1)} %get-tuple-element.37.refs_0_, bf16[5,128,128]{2,1,0:T(8,128)(2,1)S(1)} %collective-permute-done.7.refs_1_, bf16[4,128,128]{2,1,0:T(8,128)(2,1)S(1)} %collective-permute-done.11.refs_2_, ...), custom_call_target="tpu_custom_call" | custom-call | flops 1509949440 | tf_op jit(solution)/shard_map/pallas_call | solution.py:507
  57.7 0.0 collective-permute-done.9.refs_1_
  57.7 1.1 %shard_map.151 = (f32[2,1,512]{2,1,0:T(1,128)S(1)}, f32[2,1,512]{2,1,0:T(1,128)S(1)}, f32[2,64,512]{2,1,0:T(8,128)S(1)}) custom-call(bf16[4,128,128]{2,1,0:T(8,128)(2,1)S(1)} %collective-permute-done.16.refs_0_, bf16[5,128,128]{2,1,0:T(8,128)(2,1)S(1)} %collective-permute-done.9.refs_1_, f32[2,1,512]{2,1,0:T(1,128)S(1)} %get-tuple-element.63.refs_2_, ...), custom_call_target="tpu_custom_call" | custom-call | flops 838860800 | tf_op jit(solution)/shard_map/pallas_call | solution.py:507
  58.8 0.0 copy-start
  58.8 1.1 %shard_map.146 = (f32[2,1,512]{2,1,0:T(1,128)S(1)}, f32[2,1,512]{2,1,0:T(1,128)S(1)}, f32[2,64,512]{2,1,0:T(8,128)S(1)}) custom-call(bf16[4,128,128]{2,1,0:T(8,128)(2,1)S(1)} %get-tuple-element.37.refs_0_, bf16[5,128,128]{2,1,0:T(8,128)(2,1)S(1)} %collective-permute-done.9.refs_1_, f32[2,1,512]{2,1,0:T(1,128)S(1)} %get-tuple-element.50.refs_2_, ...), custom_call_target="tpu_custom_call" | custom-call | flops 838860800 | tf_op jit(solution)/shard_map/pallas_call | solution.py:507
  59.9 1.3 %collective-permute-done.8.refs_1_ = bf16[5,128,128]{2,1,0:T(8,128)(2,1)S(1)} collective-permute-done((bf16[5,128,128]{2,1,0:T(8,128)(2,1)S(1)}, bf16[5,128,128]{2,1,0:T(8,128)(2,1)S(1)}, u32[]{:S(2)}, u32[]{:S(2)}) %collective-permute-start.8) | collective-permute-done | bytes 163872 | tf_op jit(solution)/shard_map/ppermute | solution.py:552
  61.2 1.1 %shard_map.152 = bf16[4,128,128]{2,1,0:T(8,128)(2,1)S(1)} custom-call(bf16[4,128,128]{2,1,0:T(8,128)(2,1)S(1)} %collective-permute-done.16.refs_0_, bf16[5,128,128]{2,1,0:T(8,128)(2,1)S(1)} %collective-permute-done.8.refs_1_, f32[2,1,512]{2,1,0:T(1,128)S(1)} %get-tuple-element.66.refs_2_, f32[2,1,512]{2,1,0:T(1,128)S(1)} %get-tuple-element.67.refs_3_, ...), custom_call_target="tpu_custom_call" | custom-call | flops 838860800 | tf_op jit(solution)/shard_map/pallas_call | solution.py:507
  62.3 0.1 collective-permute-start.20
  62.4 1.5 %collective-permute-start.19 = (bf16[128,128]{1,0:T(8,128)(2,1)S(1)}, bf16[128,128]{1,0:T(8,128)(2,1)S(1)}, u32[]{:S(2)}, u32[]{:S(2)}) collective-permute-start(bf16[128,128]{1,0:T(8,128)(2,1)S(1)} %get-tuple-element.70), channel_id=1, source_target_pairs={{0,6},{1,7},{2,4},{3,5},{4,2},{5,3},{6,0},{7,1},{8,14},{9,15},{10,... | collective-permute-start | bytes 98312 | tf_op jit(solution)/shard_map/ppermute | solution.py:547
  63.9 1.6 %collective-permute-start.18 = (bf16[128,128]{1,0:T(8,128)(2,1)S(1)}, bf16[128,128]{1,0:T(8,128)(2,1)S(1)}, u32[]{:S(2)}, u32[]{:S(2)}) collective-permute-start(bf16[128,128]{1,0:T(8,128)(2,1)S(1)} %get-tuple-element.71), channel_id=1, source_target_pairs={{0,5},{1,4},{2,7},{3,6},{4,1},{5,0},{6,3},{7,2},{8,13},{9,12},{10,... | collective-permute-start | bytes 98312 | tf_op jit(solution)/shard_map/ppermute | solution.py:547
  65.5 1.3 %collective-permute-start.17 = (bf16[128,128]{1,0:T(8,128)(2,1)S(1)}, bf16[128,128]{1,0:T(8,128)(2,1)S(1)}, u32[]{:S(2)}, u32[]{:S(2)}) collective-permute-start(bf16[128,128]{1,0:T(8,128)(2,1)S(1)} %get-tuple-element.72), channel_id=1, source_target_pairs={{0,4},{1,5},{2,6},{3,7},{4,0},{5,1},{6,2},{7,3},{8,12},{9,13},{10,... | collective-permute-start | bytes 98312 | tf_op jit(solution)/shard_map/ppermute | solution.py:547
  66.8 1.1 %shard_map.147 = bf16[4,128,128]{2,1,0:T(8,128)(2,1)S(1)} custom-call(bf16[4,128,128]{2,1,0:T(8,128)(2,1)S(1)} %get-tuple-element.37.refs_0_, bf16[5,128,128]{2,1,0:T(8,128)(2,1)S(1)} %collective-permute-done.8.refs_1_, f32[2,1,512]{2,1,0:T(1,128)S(1)} %get-tuple-element.53.refs_2_, f32[2,1,512]{2,1,0:T(1,128)S(1)} %get-tuple-element.54.refs_3_, ...), custom_call_target="tpu_custom_call" | custom-call | flops 838860800 | tf_op jit(solution)/shard_map/pallas_call | solution.py:507
  67.9 0.1 collective-permute-start.15
  68.0 0.0 collective-permute-done.20.refs_7_
  68.0 1.6 %collective-permute-start.14 = (bf16[128,128]{1,0:T(8,128)(2,1)S(1)}, bf16[128,128]{1,0:T(8,128)(2,1)S(1)}, u32[]{:S(2)}, u32[]{:S(2)}) collective-permute-start(bf16[128,128]{1,0:T(8,128)(2,1)S(1)} %get-tuple-element.74), channel_id=1, source_target_pairs={{0,2},{1,3},{2,0},{3,1},{4,6},{5,7},{6,4},{7,5},{8,10},{9,11},{10,... | collective-permute-start | bytes 98312 | tf_op jit(solution)/shard_map/ppermute | solution.py:537
  69.6 0.0 collective-permute-done.19.refs_6_
  69.6 0.3 collective-permute-start.13
  69.8 0.0 collective-permute-done.18.refs_5_
  69.8 0.0 collective-permute-done.17.refs_4_
  69.8 1.8 %collective-permute-done.15.refs_3_ = bf16[128,128]{1,0:T(8,128)(2,1)S(1)} collective-permute-done((bf16[128,128]{1,0:T(8,128)(2,1)S(1)}, bf16[128,128]{1,0:T(8,128)(2,1)S(1)}, u32[]{:S(2)}, u32[]{:S(2)}) %collective-permute-start.15) | collective-permute-done | bytes 32800 | tf_op jit(solution)/shard_map/ppermute | solution.py:537
  71.6 0.4 collective-permute-done.14.refs_2_
  72.0 1.6 %shard_map.153 = bf16[128,2048]{1,0:T(8,128)(2,1)} custom-call(bf16[128,2048]{1,0:T(8,128)(2,1)S(1)} %copy-done.1, f32[4,8,512]{2,1,0:T(8,128)S(1)} %bitcast.23, bf16[1024,2048]{1,0:T(8,128)(2,1)S(1)} %copy-done, bf16[128,128]{1,0:T(8,128)(2,1)S(1)} %get-tuple-element.76.refs_0_, bf16[128,128]{1,0:T(8,128)(2,1)S(1)} %collective-permute-done.13.refs_1_, ...), custom_call_target="tpu_custom_call" | custom-call | flops 536870912 | tf_op jit(solution)/shard_map/pallas_call | solution.py:671
  (24 shorter events, 0.1 us)
Async XLA Ops:
  0.0 15.1 %collective-permute-start.4 = (bf16[128,2048]{1,0:T(8,128)(2,1)}, bf16[128,2048]{1,0:T(8,128)(2,1)S(1)}, u32[]{:S(2)}, u32[]{:S(2)}) collective-permute-start(bf16[128,2048]{1,0:T(8,128)(2,1)} %latent_ref.1), channel_id=1, source_target_pairs={{0,2},{1,3},{2,0},{3,1},{4,6},{5,7},{6,4},{7,5},{8,10},{9,11},{10,... | collective-permute-start | bytes 1572872 | tf_op jit(solution)/shard_map/ppermute | solution.py:537
  3.0 25.7 %collective-permute-start.3 = (bf16[128,2048]{1,0:T(8,128)(2,1)}, bf16[128,2048]{1,0:T(8,128)(2,1)S(1)}, u32[]{:S(2)}, u32[]{:S(2)}) collective-permute-start(bf16[128,2048]{1,0:T(8,128)(2,1)} %latent_ref.1), channel_id=1, source_target_pairs={{0,1},{1,0},{2,3},{3,2},{4,5},{5,4},{6,7},{7,6},{8,9},{9,8},{10,11... | collective-permute-start | bytes 1572872 | tf_op jit(solution)/shard_map/ppermute | solution.py:537
  5.1 10.0 %collective-permute-start = (f32[8,512]{1,0:T(8,128)}, f32[8,512]{1,0:T(8,128)S(1)}, u32[]{:S(2)}, u32[]{:S(2)}) collective-permute-start(f32[8,512]{1,0:T(8,128)} %shard_map.136.one_ref), channel_id=1, source_target_pairs={{0,16},{4,20},{8,24},{12,28},{16,0},{20,4},{24,8},{28,12},{1,17},{... | collective-permute-start | bytes 49160 | tf_op jit(solution)/shard_map/ppermute | solution.py:537
  7.8 20.8 %copy-start.8 = (f32[64]{0:T(128)S(1)}, f32[64]{0:T(128)}, u32[]{:S(2)}) copy-start(f32[64]{0:T(128)} %param.25) | copy-start | bytes 772
  7.8 20.8 %copy-start.9 = (f32[64]{0:T(128)S(1)}, f32[64]{0:T(128)}, u32[]{:S(2)}) copy-start(f32[64]{0:T(128)} %param.26) | copy-start | bytes 772
  7.8 20.8 %copy-start.1 = (bf16[128,2048]{1,0:T(8,128)(2,1)S(1)}, bf16[128,2048]{1,0:T(8,128)(2,1)}, u32[]{:S(2)}) copy-start(bf16[128,2048]{1,0:T(8,128)(2,1)} %latent_ref.1) | copy-start | bytes 1572868
  15.1 13.5 %collective-permute-start.5 = (bf16[128,2048]{1,0:T(8,128)(2,1)S(1)}, bf16[128,2048]{1,0:T(8,128)(2,1)S(1)}, u32[]{:S(2)}, u32[]{:S(2)}) collective-permute-start(bf16[128,2048]{1,0:T(8,128)(2,1)S(1)} %collective-permute-done.4.refs_6_), channel_id=1, source_target_pairs={{0,1},{1,0},{2,3},{3,2},{4,5},{5,4},{6,7},{7,6},{8,9},{9,8},{10,11... | collective-permute-start | bytes 1572872 | tf_op jit(solution)/shard_map/ppermute | solution.py:537
  15.1 0.7 copy-start.2
  15.8 12.8 %copy-start.3 = (bf16[2048,256]{1,0:T(8,128)(2,1)S(1)}, bf16[2048,256]{1,0:T(8,128)(2,1)}, u32[]{:S(2)}) copy-start(bf16[2048,256]{1,0:T(8,128)(2,1)} %refs_2_.1) | copy-start | bytes 3145732
  15.8 12.9 %copy-start.4 = (bf16[2048,128]{1,0:T(8,128)(2,1)S(1)}, bf16[2048,128]{1,0:T(8,128)(2,1)}, u32[]{:S(2)}) copy-start(bf16[2048,128]{1,0:T(8,128)(2,1)} %refs_3_.1) | copy-start | bytes 1572868
  15.8 12.9 %copy-start.5 = (bf16[2048,128]{1,0:T(8,128)(2,1)S(1)}, bf16[2048,128]{1,0:T(8,128)(2,1)}, u32[]{:S(2)}) copy-start(bf16[2048,128]{1,0:T(8,128)(2,1)} %refs_4_.1) | copy-start | bytes 1572868
  15.8 12.9 %copy-start.6 = (bf16[64,2048]{1,0:T(8,128)(2,1)S(1)}, bf16[64,2048]{1,0:T(8,128)(2,1)}, u32[]{:S(2)}) copy-start(bf16[64,2048]{1,0:T(8,128)(2,1)} %refs_1_.1) | copy-start | bytes 786436
  15.8 12.9 %copy-start.7 = (f32[2048]{0:T(1024)S(1)}, f32[2048]{0:T(1024)}, u32[]{:S(2)}) copy-start(f32[2048]{0:T(1024)} %param.18) | copy-start | bytes 24580
  15.9 3.8 %collective-permute-start.1 = (f32[8,512]{1,0:T(8,128)S(1)}, f32[8,512]{1,0:T(8,128)S(1)}, u32[]{:S(2)}, u32[]{:S(2)}) collective-permute-start(f32[8,512]{1,0:T(8,128)S(1)} %shard_map.137.one_ref), channel_id=1, source_target_pairs={{0,8},{4,12},{8,0},{12,4},{16,24},{20,28},{24,16},{28,20},{1,9},{5... | collective-permute-start | bytes 49160 | tf_op jit(solution)/shard_map/ppermute | solution.py:537
  19.7 3.7 %collective-permute-start.2 = (f32[8,512]{1,0:T(8,128)S(1)}, f32[8,512]{1,0:T(8,128)S(1)}, u32[]{:S(2)}, u32[]{:S(2)}) collective-permute-start(f32[8,512]{1,0:T(8,128)S(1)} %shard_map.138.one_ref), channel_id=1, source_target_pairs={{0,4},{4,0},{8,12},{12,8},{16,20},{20,16},{24,28},{28,24},{1,5},{5... | collective-permute-start | bytes 49160 | tf_op jit(solution)/shard_map/ppermute | solution.py:537
  31.4 10.0 %collective-permute-start.6 = (bf16[5,128,128]{2,1,0:T(8,128)(2,1)S(1)}, bf16[5,128,128]{2,1,0:T(8,128)(2,1)S(1)}, u32[]{:S(2)}, u32[]{:S(2)}) collective-permute-start(bf16[5,128,128]{2,1,0:T(8,128)(2,1)S(1)} %get-tuple-element.38), channel_id=1, source_target_pairs={{0,4},{4,0},{8,12},{12,8},{16,20},{20,16},{24,28},{28,24},{1,5},{5... | collective-permute-start | bytes 491528 | tf_op jit(solution)/shard_map/ppermute | solution.py:537
  33.2 8.2 %collective-permute-start.10 = (bf16[4,128,128]{2,1,0:T(8,128)(2,1)S(1)}, bf16[4,128,128]{2,1,0:T(8,128)(2,1)S(1)}, u32[]{:S(2)}, u32[]{:S(2)}) collective-permute-start(bf16[4,128,128]{2,1,0:T(8,128)(2,1)S(1)} %get-tuple-element.40.refs_1_), channel_id=1, source_target_pairs={{0,8},{4,12},{8,16},{12,20},{16,24},{20,28},{24,0},{28,4},{1,9},{5... | collective-permute-start | bytes 393224 | tf_op jit(solution)/shard_map/ppermute | solution.py:552
  34.8 10.5 %collective-permute-start.16 = (bf16[4,128,128]{2,1,0:T(8,128)(2,1)S(1)}, bf16[4,128,128]{2,1,0:T(8,128)(2,1)S(1)}, u32[]{:S(2)}, u32[]{:S(2)}) collective-permute-start(bf16[4,128,128]{2,1,0:T(8,128)(2,1)S(1)} %get-tuple-element.56), channel_id=1, source_target_pairs={{0,4},{4,0},{8,12},{12,8},{16,20},{20,16},{24,28},{28,24},{1,5},{5... | collective-permute-start | bytes 393224 | tf_op jit(solution)/shard_map/ppermute | solution.py:537
  35.3 11.7 %collective-permute-start.12 = (bf16[4,128,128]{2,1,0:T(8,128)(2,1)S(1)}, bf16[4,128,128]{2,1,0:T(8,128)(2,1)S(1)}, u32[]{:S(2)}, u32[]{:S(2)}) collective-permute-start(bf16[4,128,128]{2,1,0:T(8,128)(2,1)S(1)} %get-tuple-element.40.refs_1_), channel_id=1, source_target_pairs={{0,24},{4,28},{8,0},{12,4},{16,8},{20,12},{24,16},{28,20},{1,25},{... | collective-permute-start | bytes 393224 | tf_op jit(solution)/shard_map/ppermute | solution.py:552
  41.4 12.7 %collective-permute-start.11 = (bf16[4,128,128]{2,1,0:T(8,128)(2,1)S(1)}, bf16[4,128,128]{2,1,0:T(8,128)(2,1)S(1)}, u32[]{:S(2)}, u32[]{:S(2)}) collective-permute-start(bf16[4,128,128]{2,1,0:T(8,128)(2,1)S(1)} %collective-permute-done.10.refs_1_), channel_id=1, source_target_pairs={{0,8},{4,12},{8,16},{12,20},{16,24},{20,28},{24,0},{28,4},{1,9},{5... | collective-permute-start | bytes 393224 | tf_op jit(solution)/shard_map/ppermute | solution.py:552
  41.4 16.2 %collective-permute-start.9 = (bf16[5,128,128]{2,1,0:T(8,128)(2,1)S(1)}, bf16[5,128,128]{2,1,0:T(8,128)(2,1)S(1)}, u32[]{:S(2)}, u32[]{:S(2)}) collective-permute-start(bf16[5,128,128]{2,1,0:T(8,128)(2,1)S(1)} %shard_map.141.refs_1_.refs_2_), channel_id=1, source_target_pairs={{0,24},{4,28},{8,0},{12,4},{16,8},{20,12},{24,16},{28,20},{1,25},{... | collective-permute-start | bytes 491528 | tf_op jit(solution)/shard_map/ppermute | solution.py:552
  45.3 8.8 %collective-permute-start.7 = (bf16[5,128,128]{2,1,0:T(8,128)(2,1)S(1)}, bf16[5,128,128]{2,1,0:T(8,128)(2,1)S(1)}, u32[]{:S(2)}, u32[]{:S(2)}) collective-permute-start(bf16[5,128,128]{2,1,0:T(8,128)(2,1)S(1)} %shard_map.141.refs_1_.refs_2_), channel_id=1, source_target_pairs={{0,8},{4,12},{8,16},{12,20},{16,24},{20,28},{24,0},{28,4},{1,9},{5... | collective-permute-start | bytes 491528 | tf_op jit(solution)/shard_map/ppermute | solution.py:552
  54.1 7.1 %collective-permute-start.8 = (bf16[5,128,128]{2,1,0:T(8,128)(2,1)S(1)}, bf16[5,128,128]{2,1,0:T(8,128)(2,1)S(1)}, u32[]{:S(2)}, u32[]{:S(2)}) collective-permute-start(bf16[5,128,128]{2,1,0:T(8,128)(2,1)S(1)} %collective-permute-done.7.refs_1_), channel_id=1, source_target_pairs={{0,8},{4,12},{8,16},{12,20},{16,24},{20,28},{24,0},{28,4},{1,9},{5... | collective-permute-start | bytes 491528 | tf_op jit(solution)/shard_map/ppermute | solution.py:552
  58.8 13.2 %copy-start = (bf16[1024,2048]{1,0:T(8,128)(2,1)S(1)}, bf16[1024,2048]{1,0:T(8,128)(2,1)}, u32[]{:S(2)}) copy-start(bf16[1024,2048]{1,0:T(8,128)(2,1)} %weight_ref.1) | copy-start | bytes 12582916
  62.3 5.7 %collective-permute-start.20 = (bf16[128,128]{1,0:T(8,128)(2,1)S(1)}, bf16[128,128]{1,0:T(8,128)(2,1)S(1)}, u32[]{:S(2)}, u32[]{:S(2)}) collective-permute-start(bf16[128,128]{1,0:T(8,128)(2,1)S(1)} %get-tuple-element.69), channel_id=1, source_target_pairs={{0,7},{1,6},{2,5},{3,4},{4,3},{5,2},{6,1},{7,0},{8,15},{9,14},{10,... | collective-permute-start | bytes 98312 | tf_op jit(solution)/shard_map/ppermute | solution.py:547
  62.4 7.2 %collective-permute-start.19 = (bf16[128,128]{1,0:T(8,128)(2,1)S(1)}, bf16[128,128]{1,0:T(8,128)(2,1)S(1)}, u32[]{:S(2)}, u32[]{:S(2)}) collective-permute-start(bf16[128,128]{1,0:T(8,128)(2,1)S(1)} %get-tuple-element.70), channel_id=1, source_target_pairs={{0,6},{1,7},{2,4},{3,5},{4,2},{5,3},{6,0},{7,1},{8,14},{9,15},{10,... | collective-permute-start | bytes 98312 | tf_op jit(solution)/shard_map/ppermute | solution.py:547
  63.9 6.0 %collective-permute-start.18 = (bf16[128,128]{1,0:T(8,128)(2,1)S(1)}, bf16[128,128]{1,0:T(8,128)(2,1)S(1)}, u32[]{:S(2)}, u32[]{:S(2)}) collective-permute-start(bf16[128,128]{1,0:T(8,128)(2,1)S(1)} %get-tuple-element.71), channel_id=1, source_target_pairs={{0,5},{1,4},{2,7},{3,6},{4,1},{5,0},{6,3},{7,2},{8,13},{9,12},{10,... | collective-permute-start | bytes 98312 | tf_op jit(solution)/shard_map/ppermute | solution.py:547
  65.5 4.4 %collective-permute-start.17 = (bf16[128,128]{1,0:T(8,128)(2,1)S(1)}, bf16[128,128]{1,0:T(8,128)(2,1)S(1)}, u32[]{:S(2)}, u32[]{:S(2)}) collective-permute-start(bf16[128,128]{1,0:T(8,128)(2,1)S(1)} %get-tuple-element.72), channel_id=1, source_target_pairs={{0,4},{1,5},{2,6},{3,7},{4,0},{5,1},{6,2},{7,3},{8,12},{9,13},{10,... | collective-permute-start | bytes 98312 | tf_op jit(solution)/shard_map/ppermute | solution.py:547
  67.9 3.7 %collective-permute-start.15 = (bf16[128,128]{1,0:T(8,128)(2,1)S(1)}, bf16[128,128]{1,0:T(8,128)(2,1)S(1)}, u32[]{:S(2)}, u32[]{:S(2)}) collective-permute-start(bf16[128,128]{1,0:T(8,128)(2,1)S(1)} %get-tuple-element.73), channel_id=1, source_target_pairs={{0,3},{1,2},{2,1},{3,0},{4,7},{5,6},{6,5},{7,4},{8,11},{9,10},{10,... | collective-permute-start | bytes 98312 | tf_op jit(solution)/shard_map/ppermute | solution.py:537
  68.0 4.0 %collective-permute-start.14 = (bf16[128,128]{1,0:T(8,128)(2,1)S(1)}, bf16[128,128]{1,0:T(8,128)(2,1)S(1)}, u32[]{:S(2)}, u32[]{:S(2)}) collective-permute-start(bf16[128,128]{1,0:T(8,128)(2,1)S(1)} %get-tuple-element.74), channel_id=1, source_target_pairs={{0,2},{1,3},{2,0},{3,1},{4,6},{5,7},{6,4},{7,5},{8,10},{9,11},{10,... | collective-permute-start | bytes 98312 | tf_op jit(solution)/shard_map/ppermute | solution.py:537
  69.6 2.5 %collective-permute-start.13 = (bf16[128,128]{1,0:T(8,128)(2,1)S(1)}, bf16[128,128]{1,0:T(8,128)(2,1)S(1)}, u32[]{:S(2)}, u32[]{:S(2)}) collective-permute-start(bf16[128,128]{1,0:T(8,128)(2,1)S(1)} %get-tuple-element.75), channel_id=1, source_target_pairs={{0,1},{1,0},{2,3},{3,2},{4,5},{5,4},{6,7},{7,6},{8,9},{9,8},{10,11... | collective-permute-start | bytes 98312 | tf_op jit(solution)/shard_map/ppermute | solution.py:537

commit v3 on v2

--- a/solution.py
+++ b/solution.py
@@ -390,54 +390,59 @@
     return kernel_call(merge_body, jax.ShapeDtypeStruct(near.shape, near.dtype), 2, 10**6)(near, ctx)
 
 
-def attention_body(count, first, last, offset, *refs):
-    q_ref = refs[0]
-    kv_refs = refs[1 : 1 + count]
-    refs = refs[1 + count :]
-    if not first:
-        peak_in, total_in, sum_in = refs[:3]
-        refs = refs[3:]
-    span = q_ref.shape[1] // 2
+def attention_body(plan, pieces, last, offset, *refs):
+    q_refs, refs = refs[: len(plan)], refs[len(plan) :]
+    kv_refs, refs = refs[:pieces], refs[pieces:]
+    pairs = 2
+    groups = 2
+    span = q_refs[0].shape[1] // 2
     scale = span ** (-0.5) * LOG2E
-    groups = 2
-    pairs = 2
-    chunks = [(ref, part, ref.shape[0] > 2 * pairs) for ref in kv_refs for part in (0, 1)]
-    tiles = [(g, chunk) for chunk in chunks for g in range(groups)]
+    halves = (0, 1)
     states = {}
     queries = {}
-    for g in range(groups):
-        found = jnp.concatenate(
-            [
-                q_ref[g * pairs + p, half * span : (half + 1) * span, :]
-                for p in range(pairs)
-                for half in (0, 1)
-            ],
-            axis=1,
-        )
-        blank = jnp.zeros_like(found)
-        queries[g, 0] = jnp.concatenate([found, blank], axis=0)
-        queries[g, 1] = jnp.concatenate([blank, found], axis=0)
+    tiles = []
+    for i, (q_ref, (started, wanted)) in enumerate(zip(q_refs, plan)):
+        if started:
+            old, refs = refs[:3], refs[3:]
+        for g in range(groups):
+            found = jnp.concatenate(
+                [
+                    q_ref[g * pairs + p, half * span : (half + 1) * span, :]
+                    for p in range(pairs)
+                    for half in halves
+                ],
+                axis=1,
+            )
+            blank = jnp.zeros_like(found)
+            queries[i, g, 0] = jnp.concatenate([found, blank], axis=0)
+            queries[i, g, 1] = jnp.concatenate([blank, found], axis=0)
+            if started:
+                states[i, g] = tuple(ref[g] for ref in old)
+            tiles += [(i, g, place) for place in wanted]
+    tiles.sort(key=lambda tile: tile[2])
 
     def scores(tile):
-        g, (ref, part, context) = tile
+        i, g, place = tile
+        ref = kv_refs[place]
+        context = ref.shape[0] > 2 * pairs
         keys = [ref[p] for p in range(pairs)]
         if context:
             keys.append(ref[2 * pairs, 0:span, :])
-        found = jnp.dot(
-            jnp.concatenate(keys, axis=0), queries[g, part], preferred_element_type=jnp.float32
-        )
-        found = found * scale
-        if context:
-            rows = found.shape[0] - span
-            found = jnp.concatenate([found[:rows], found[rows:] + offset * LOG2E], axis=0)
-        return found
+        keys = jnp.concatenate(keys, axis=0)
+        made = []
+        for half in halves:
+            found = jnp.dot(keys, queries[i, g, half], preferred_element_type=jnp.float32) * scale
+            if context:
+                rows = found.shape[0] - span
+                made += [found[:rows], found[rows:] + offset * LOG2E]
+            else:
+                made.append(found)
+        return jnp.concatenate(made, axis=0)
 
     def soften(tile, found):
-        g = tile[0]
+        place = tile[:2]
         peak = jnp.max(found, axis=0, keepdims=True)
-        old = states.get(g)
-        if old is None and not first:
-            old = (peak_in[g], total_in[g], sum_in[g])
+        old = states.get(place)
         if old is not None:
             peak = jnp.maximum(peak, old[0])
         shares = jnp.exp2(found - peak)
@@ -446,22 +451,24 @@
         if old is not None:
             shrink = jnp.exp2(old[0] - peak)
             total = total + old[1] * shrink
-        states[g] = (peak, total, old[2] if old is not None else None)
+        states[place] = (peak, total, old[2] if old is not None else None)
         return shares.astype(jnp.bfloat16), shrink
 
     def gather(tile, shares, shrink):
-        g, (ref, part, context) = tile
-        rows = slice(part * span, (part + 1) * span)
-        values = [ref[pairs + p, rows, :] for p in range(pairs)]
-        if context:
-            values.append(ref[2 * pairs, span : 2 * span, rows])
+        ref = kv_refs[tile[2]]
+        values = []
+        for half in halves:
+            rows = slice(half * span, (half + 1) * span)
+            values += [ref[pairs + p, rows, :] for p in range(pairs)]
+            if ref.shape[0] > 2 * pairs:
+                values.append(ref[2 * pairs, span : 2 * span, rows])
         weighted = jnp.dot(
             jnp.concatenate(values, axis=1), shares, preferred_element_type=jnp.float32
         )
-        peak, total, old = states[g]
+        peak, total, old = states[tile[:2]]
         if shrink is not None:
             weighted = weighted + old * shrink
-        states[g] = (peak, total, weighted)
+        states[tile[:2]] = (peak, total, weighted)
 
     following = scores(tiles[0])
     waiting = None
@@ -474,9 +481,9 @@
             gather(*waiting)
         waiting = (tile, shares, shrink)
     gather(*waiting)
-    for g, (peak, total, weighted) in states.items():
+    for (i, g), (peak, total, weighted) in states.items():
         if last:
-            (out_ref,) = refs
+            out_ref = refs[i]
             attended = (weighted / total).astype(jnp.bfloat16)
             own_rows = out_ref.shape[2]
             for j in range(out_ref.shape[0]):
@@ -484,27 +491,33 @@
                     :, j * own_rows : (j + 1) * own_rows
                 ]
         else:
-            peak_out, total_out, sum_out = refs
-            peak_out[g] = peak
-            total_out[g] = total
-            sum_out[g] = weighted
-
-
-def attend(state, probes, pairs, offset, last=False):
-    lanes = 2 * 2 * probes.shape[2]
-    span = probes.shape[1] // 2
-    keys = sum(p.shape[0] * p.shape[1] // 2 for p in pairs)
-    inputs = [probes, *pairs] + list(state or ())
+            for ref, value in zip(refs[3 * i : 3 * i + 3], (peak, total, weighted)):
+                ref[g] = value
+
+
+def attend(sources, pieces, offset, last=False):
+    probes = [source[0] for source in sources]
+    lanes = 2 * 2 * probes[0].shape[2]
+    span = probes[0].shape[1] // 2
+    plan = [(source[1] is not None, source[2]) for source in sources]
+    keys = sum(pieces[i].shape[0] * pieces[i].shape[1] // 2 for source in sources for i in source[2])
+    inputs = probes + pieces
+    for source in sources:
+        inputs += list(source[1] or ())
     if last:
-        out = jax.ShapeDtypeStruct((4, 2 * span, probes.shape[2]), jnp.bfloat16)
+        out = [jax.ShapeDtypeStruct((4, 2 * span, probes[0].shape[2]), jnp.bfloat16)]
     else:
         stat = jax.ShapeDtypeStruct((2, 1, lanes), jnp.float32)
         out = [stat, stat, jax.ShapeDtypeStruct((2, span, lanes), jnp.float32)]
 
     def body(*refs):
-        attention_body(len(pairs), state is None, last, offset, *refs)
-
-    return kernel_call(body, out, len(inputs), 40 * 2 * lanes * keys * span)(*inputs)
+        attention_body(plan, len(pieces), last, offset, *refs)
+
+    found = kernel_call(
+        body, out * len(sources), len(inputs), 40 * 2 * lanes * keys * span
+    )(*inputs)
+    size = len(out)
+    return [found[size * i : size * (i + 1)] for i in range(len(sources))]
 
 
 def output_body(latent_ref, mod_ref, weight_ref, *refs):
@@ -545,11 +558,6 @@
         for j in range(head_split)
     ]
     return lax.ppermute(member, ("sp", "tp"), pairs)
-
-
-def ring_move(member, step):
-    size = lax.axis_size("sp")
-    return lax.ppermute(member, "sp", [(i, (i + step) % size) for i in range(size)])
 
 
 def tables(seq_index, head_index, own_rows, head_split):
@@ -649,22 +657,21 @@
     )
     offset = math.log(tok_count / (2.0 * ctx_rows))
     near = xor_move(give_kv, "sp", 1)
-    up = ring_move(keep_kv, 2)
-    down = ring_move(keep_kv, -2)
+    up = xor_move(keep_kv, "sp", 2)
+    down = xor_move(keep_kv, "sp", 6)
     near_q = xor_move(give_q, "sp", 1)
     near = merge(near, keep_ctx)
-    near_up = ring_move(near, 2)
-    near_down = ring_move(near, -2)
-    across = ring_move(up, 2)
-    near_across = ring_move(near_up, 2)
-    own = attend(None, keep_q, [keep_kv], offset)
-    own = attend(own, keep_q, [near], offset)
-    other = attend(None, near_q, [keep_kv, near], offset)
-    for pieces in ([up, down], [near_up, across], [near_down]):
-        other = attend(other, near_q, pieces, offset)
-        own = attend(own, keep_q, pieces, offset)
-    other = attend(other, near_q, [near_across], offset, True)
-    own = attend(own, keep_q, [near_across], offset, True)
+    near_down = xor_move(near, "sp", 6)
+    near_up = xor_move(near, "sp", 2)
+    across = xor_move(down, "sp", 2)
+    near_across = xor_move(near_down, "sp", 2)
+    (own,) = attend([(keep_q, None, [0])], [keep_kv], offset)
+    own, other = attend([(keep_q, own, [1]), (near_q, None, [0, 1])], [keep_kv, near], offset)
+    for piece in (up, down, near_up, across, near_down):
+        own, other = attend([(keep_q, own, [0]), (near_q, other, [0])], [piece], offset)
+    (own,), (other,) = attend(
+        [(keep_q, own, [0]), (near_q, other, [0])], [near_across], offset, True
+    )
     sent = [cross_move(other[j], j) for j in range(head_split)]
     parts = [own[0]] + [xor_move(own[j], "tp", j) for j in range(1, head_split)] + sent
     width = q_heads * CHANNEL_SPAN

time: 73.9 us -> 73 us (0.988)
  waiting for transfers between devices: 20 us -> 18.1 us
  starting transfers between devices: 25.4 us -> 27.2 us
  Pallas kernels: 21.5 us -> 20.5 us
    ppermute x11 -> x17, starting transfers between devices: 13.6 us -> 22.8 us  [xor_move(): return lax.ppermute(member, axis, [(i, i ^ mask) for i in range(size)])]
    ppermute x6 -> x0, starting transfers between devices: 7.4 us -> none  [ring_move(): lax.ppermute(member, 'sp', [(i, (i + step) % size) for i in range(size)])]
    ppermute x6 -> x0, waiting for transfers between devices: 7.01 us -> none  [ring_move(): lax.ppermute(member, 'sp', [(i, (i + step) % size) for i in range(size)])]
    ppermute x4, waiting for transfers between devices: 0.01 us -> 2.82 us  [cross_move(): return lax.ppermute(member, ('sp', 'tp'), pairs)]
    ppermute x11 -> x17, waiting for transfers between devices: 13 us -> 15.3 us  [xor_move(): return lax.ppermute(member, axis, [(i, i ^ mask) for i in range(size)])]
    pallas_call x11 -> x8, Pallas kernels: 15.1 us -> 14.1 us  [attend(): kernel_call(body, out * len(sources), len(inputs), 40 * 2 * lanes * keys...]
  transfers between devices with their start and end apart: 21 -> 21, of which waited for: 8 -> 8; matrix products, arithmetic and copies ran while one was open for 1% -> 1% of each run, Pallas kernels for 22% -> 20%
where the time goes in v3:
time: 73 us; the launch traced here: 72.6 us
  starting transfers between devices  27.2 us (37%)
  Pallas kernels  20.5 us (28%)
  waiting for transfers between devices  18.1 us (25%)
  blocking collectives  5.22 us (7%)
  local copies, waits for them, and re-layouts  0.78 us (1%)
    ppermute x17, starting transfers between devices, xor_move(): return lax.ppermute(member, axis, [(i, i ^ mask) for i in range(size)])  22.8 us
    ppermute x17, waiting for transfers between devices, xor_move(): return lax.ppermute(member, axis, [(i, i ^ mask) for i in range(size)])  15.3 us
    pallas_call x8, Pallas kernels, attend(): kernel_call(body, out * len(sources), len(inputs), 40 * 2 * lanes * keys...  14.1 us
    all_gather x1, blocking collectives, inner_device(): modulation = lax.all_gather(part, 'tp', axis=0, tiled=False)  5.22 us
    ppermute x4, starting transfers between devices, cross_move(): return lax.ppermute(member, ('sp', 'tp'), pairs)  4.46 us
    ppermute x4, waiting for transfers between devices, cross_move(): return lax.ppermute(member, ('sp', 'tp'), pairs)  2.82 us
    pallas_call x1, Pallas kernels, inner_device(): pl.pallas_call(lambda *refs: projection_body(q_heads, kv_heads, *refs), o...  2.66 us
    pallas_call x1, Pallas kernels, opening(): pl.pallas_call(opening_body, out_shape=jax.ShapeDtypeStruct((8, columns),...  2.08 us
  transfers between devices with their start and end apart: 21, of which 8 were waited for; matrix products, arithmetic and copies ran while one was open for 1% of the time, Pallas kernels for 20%

profile of v3, /device:TPU:0, one launch (start us, length us, event | category | flops | bytes accessed | tf_op | source)
XLA Modules:
  0.0 72.6 jit_solution(5057275284155694201)
XLA Ops:
  0.0 3.0 %collective-permute-start.4 = (bf16[128,2048]{1,0:T(8,128)(2,1)}, bf16[128,2048]{1,0:T(8,128)(2,1)S(1)}, u32[]{:S(2)}, u32[]{:S(2)}) collective-permute-start(bf16[128,2048]{1,0:T(8,128)(2,1)} %latent_ref.1), channel_id=1, source_target_pairs={{0,2},{1,3},{2,0},{3,1},{4,6},{5,7},{6,4},{7,5},{8,10},{9,11},{10,... | collective-permute-start | bytes 1572872 | tf_op jit(solution)/shard_map/ppermute | solution.py:550
  3.0 0.0 collective-permute-start.3
  3.0 2.1 %shard_map.136.one_ref = f32[8,512]{1,0:T(8,128)} custom-call(f32[1,2048]{1,0:T(1,128)} %bitcast.27, f32[1,2048]{1,0:T(1,128)} %bitcast.28, bf16[256,512]{1,0:T(8,128)(2,1)} %shift_hbm.1, bf16[256,512]{1,0:T(8,128)(2,1)} %scale_hbm.1, bf16[256,512]{1,0:T(8,128)(2,1)} %gate_hbm.1), custom_call_target="tpu_custom_call" | custom-call | flops 100000000 | tf_op jit(solution)/shard_map/pallas_call | solution.py:275
  5.1 2.7 %collective-permute-start = (f32[8,512]{1,0:T(8,128)}, f32[8,512]{1,0:T(8,128)S(1)}, u32[]{:S(2)}, u32[]{:S(2)}) collective-permute-start(f32[8,512]{1,0:T(8,128)} %shard_map.136.one_ref), channel_id=1, source_target_pairs={{0,16},{4,20},{8,24},{12,28},{16,0},{20,4},{24,8},{28,12},{1,17},{... | collective-permute-start | bytes 49160 | tf_op jit(solution)/shard_map/ppermute | solution.py:550
  7.7 0.1 fusion.2
  7.8 0.0 copy-start.9
  7.8 0.0 copy-start.1
  7.8 7.3 %collective-permute-done.4.refs_6_ = bf16[128,2048]{1,0:T(8,128)(2,1)S(1)} collective-permute-done((bf16[128,2048]{1,0:T(8,128)(2,1)}, bf16[128,2048]{1,0:T(8,128)(2,1)S(1)}, u32[]{:S(2)}, u32[]{:S(2)}) %collective-permute-start.4) | collective-permute-done | bytes 524320 | tf_op jit(solution)/shard_map/ppermute | solution.py:550
  15.1 0.0 collective-permute-start.5
  15.1 0.0 collective-permute-done.other_ref
  15.1 0.7 copy-done.2
  15.8 0.0 copy-start.7
  15.9 1.9 %collective-permute-start.1 = (f32[8,512]{1,0:T(8,128)S(1)}, f32[8,512]{1,0:T(8,128)S(1)}, u32[]{:S(2)}, u32[]{:S(2)}) collective-permute-start(f32[8,512]{1,0:T(8,128)S(1)} %shard_map.137.one_ref), channel_id=1, source_target_pairs={{0,8},{4,12},{8,0},{12,4},{16,24},{20,28},{24,16},{28,20},{1,9},{5... | collective-permute-start | bytes 49160 | tf_op jit(solution)/shard_map/ppermute | solution.py:550
  17.8 0.3 fusion
  18.1 1.6 %collective-permute-done.1.other_ref = f32[8,512]{1,0:T(8,128)S(1)} collective-permute-done((f32[8,512]{1,0:T(8,128)S(1)}, f32[8,512]{1,0:T(8,128)S(1)}, u32[]{:S(2)}, u32[]{:S(2)}) %collective-permute-start.1) | collective-permute-done | bytes 16416 | tf_op jit(solution)/shard_map/ppermute | solution.py:550
  19.7 1.8 %collective-permute-start.2 = (f32[8,512]{1,0:T(8,128)S(1)}, f32[8,512]{1,0:T(8,128)S(1)}, u32[]{:S(2)}, u32[]{:S(2)}) collective-permute-start(f32[8,512]{1,0:T(8,128)S(1)} %shard_map.138.one_ref), channel_id=1, source_target_pairs={{0,4},{4,0},{8,12},{12,8},{16,20},{20,16},{24,28},{28,24},{1,5},{5... | collective-permute-start | bytes 49160 | tf_op jit(solution)/shard_map/ppermute | solution.py:550
  21.5 1.9 %collective-permute-done.2.other_ref = f32[8,512]{1,0:T(8,128)S(1)} collective-permute-done((f32[8,512]{1,0:T(8,128)S(1)}, f32[8,512]{1,0:T(8,128)S(1)}, u32[]{:S(2)}, u32[]{:S(2)}) %collective-permute-start.2) | collective-permute-done | bytes 16416 | tf_op jit(solution)/shard_map/ppermute | solution.py:550
  23.4 5.2 %all-gather = f32[32,512]{1,0:T(8,128)S(1)} all-gather(f32[8,512]{1,0:T(8,128)S(1)} %shard_map.139), channel_id=2, replica_groups=mesh['sp'=8,'tp'=4] {'tp'}, dimensions={0}, use_global_device_ids=true | all-gather | bytes 81920 | tf_op jit(solution)/shard_map/all_gather | solution.py:622
  28.6 0.0 collective-permute-done.3.refs_5_
  28.6 0.0 collective-permute-done.5.refs_7_
  28.6 0.0 copy-done.8
  28.6 0.0 copy-done.9
  28.7 2.7 %shard_map.140 = (bf16[4,128,128]{2,1,0:T(8,128)(2,1)S(1)}, bf16[4,128,128]{2,1,0:T(8,128)(2,1)S(1)}, bf16[128,128]{1,0:T(8,128)(2,1)S(1)}, bf16[4,128,128]{2,1,0:T(8,128)(2,1)S(1)}, bf16[5,128,128]{2,1,0:T(8,128)(2,1)S(1)}) custom-call(bf16[128,2048]{1,0:T(8,128)(2,1)S(1)} %copy-done.1, bf16[64,2048]{1,0:T(8,128)(2,1)S(1)} %copy-done.6, ...), custom_call_target="tpu_custom_call" | custom-call | flops 2147483648 | tf_op jit(solution)/shard_map/pallas_call | solution.py:627
  31.4 1.8 %collective-permute-start.7 = (bf16[5,128,128]{2,1,0:T(8,128)(2,1)S(1)}, bf16[5,128,128]{2,1,0:T(8,128)(2,1)S(1)}, u32[]{:S(2)}, u32[]{:S(2)}) collective-permute-start(bf16[5,128,128]{2,1,0:T(8,128)(2,1)S(1)} %get-tuple-element.53), channel_id=1, source_target_pairs={{0,4},{4,0},{8,12},{12,8},{16,20},{20,16},{24,28},{28,24},{1,5},{5... | collective-permute-start | bytes 491528 | tf_op jit(solution)/shard_map/ppermute | solution.py:550
  33.2 3.6 %collective-permute-start.10 = (bf16[4,128,128]{2,1,0:T(8,128)(2,1)S(1)}, bf16[4,128,128]{2,1,0:T(8,128)(2,1)S(1)}, u32[]{:S(2)}, u32[]{:S(2)}) collective-permute-start(bf16[4,128,128]{2,1,0:T(8,128)(2,1)S(1)} %get-tuple-element.55.refs_1_.refs_2_), channel_id=1, source_target_pairs={{0,24},{4,28},{8,16},{12,20},{16,8},{20,12},{24,0},{28,4},{1,25},{... | collective-permute-start | bytes 393224 | tf_op jit(solution)/shard_map/ppermute | solution.py:550
  36.8 0.5 collective-permute-start.6
  37.3 0.0 collective-permute-start.13
  37.3 0.9 %shard_map.142 = (f32[2,1,512]{2,1,0:T(1,128)S(1)}, f32[2,1,512]{2,1,0:T(1,128)S(1)}, f32[2,64,512]{2,1,0:T(8,128)S(1)}) custom-call(bf16[4,128,128]{2,1,0:T(8,128)(2,1)S(1)} %get-tuple-element.51.refs_0_, bf16[4,128,128]{2,1,0:T(8,128)(2,1)S(1)} %get-tuple-element.55.refs_1_.refs_2_), custom_call_target="tpu_custom_call" | custom-call | flops 671088640 | tf_op jit(solution)/shard_map/pallas_call | solution.py:516
  38.2 3.2 %collective-permute-done.10.refs_2_ = bf16[4,128,128]{2,1,0:T(8,128)(2,1)S(1)} collective-permute-done((bf16[4,128,128]{2,1,0:T(8,128)(2,1)S(1)}, bf16[4,128,128]{2,1,0:T(8,128)(2,1)S(1)}, u32[]{:S(2)}, u32[]{:S(2)}) %collective-permute-start.10) | collective-permute-done | bytes 131104 | tf_op jit(solution)/shard_map/ppermute | solution.py:550
  41.4 1.6 %collective-permute-start.11 = (bf16[4,128,128]{2,1,0:T(8,128)(2,1)S(1)}, bf16[4,128,128]{2,1,0:T(8,128)(2,1)S(1)}, u32[]{:S(2)}, u32[]{:S(2)}) collective-permute-start(bf16[4,128,128]{2,1,0:T(8,128)(2,1)S(1)} %collective-permute-done.10.refs_2_), channel_id=1, source_target_pairs={{0,8},{4,12},{8,0},{12,4},{16,24},{20,28},{24,16},{28,20},{1,9},{5... | collective-permute-start | bytes 393224 | tf_op jit(solution)/shard_map/ppermute | solution.py:550
  43.0 0.0 collective-permute-done.7.near_ref
  43.0 0.1 shard_map.141.refs_3_
  43.1 0.4 collective-permute-start.12
  43.5 3.6 %collective-permute-start.8 = (bf16[5,128,128]{2,1,0:T(8,128)(2,1)S(1)}, bf16[5,128,128]{2,1,0:T(8,128)(2,1)S(1)}, u32[]{:S(2)}, u32[]{:S(2)}) collective-permute-start(bf16[5,128,128]{2,1,0:T(8,128)(2,1)S(1)} %shard_map.141.refs_3_), channel_id=1, source_target_pairs={{0,24},{4,28},{8,16},{12,20},{16,8},{20,12},{24,0},{28,4},{1,25},{... | collective-permute-start | bytes 491528 | tf_op jit(solution)/shard_map/ppermute | solution.py:550
  47.1 0.0 collective-permute-done.6.refs_1_
  47.1 2.6 %shard_map.143 = (f32[2,1,512]{2,1,0:T(1,128)S(1)}, f32[2,1,512]{2,1,0:T(1,128)S(1)}, f32[2,64,512]{2,1,0:T(8,128)S(1)}, f32[2,1,512]{2,1,0:T(1,128)S(1)}, f32[2...) custom-call(bf16[4,128,128]{2,1,0:T(8,128)(2,1)S(1)} %get-tuple-element.51.refs_0_, ...), custom_call_target="tpu_custom_call" | custom-call | flops 2348810240 | tf_op jit(solution)/shard_map/pallas_call | solution.py:516
  49.7 0.0 collective-permute-done.13.refs_2_
  49.7 1.6 %shard_map.144 = (f32[2,1,512]{2,1,0:T(1,128)S(1)}, f32[2,1,512]{2,1,0:T(1,128)S(1)}, f32[2,64,512]{2,1,0:T(8,128)S(1)}, f32[2,1,512]{2,1,0:T(1,128)S(1)}, f32[2...) custom-call(bf16[4,128,128]{2,1,0:T(8,128)(2,1)S(1)} %get-tuple-element.51.refs_0_, ...), custom_call_target="tpu_custom_call" | custom-call | flops 1342177280 | tf_op jit(solution)/shard_map/pallas_call | solution.py:516
  51.3 1.6 %shard_map.145 = (f32[2,1,512]{2,1,0:T(1,128)S(1)}, f32[2,1,512]{2,1,0:T(1,128)S(1)}, f32[2,64,512]{2,1,0:T(8,128)S(1)}, f32[2,1,512]{2,1,0:T(1,128)S(1)}, f32[2...) custom-call(bf16[4,128,128]{2,1,0:T(8,128)(2,1)S(1)} %get-tuple-element.51.refs_0_, ...), custom_call_target="tpu_custom_call" | custom-call | flops 1342177280 | tf_op jit(solution)/shard_map/pallas_call | solution.py:516
  52.9 1.3 %collective-permute-done.8.refs_2_ = bf16[5,128,128]{2,1,0:T(8,128)(2,1)S(1)} collective-permute-done((bf16[5,128,128]{2,1,0:T(8,128)(2,1)S(1)}, bf16[5,128,128]{2,1,0:T(8,128)(2,1)S(1)}, u32[]{:S(2)}, u32[]{:S(2)}) %collective-permute-start.8) | collective-permute-done | bytes 163872 | tf_op jit(solution)/shard_map/ppermute | solution.py:550
  54.2 0.0 collective-permute-start.9
  54.2 0.0 collective-permute-done.12.refs_2_
  54.2 1.9 %shard_map.146 = (f32[2,1,512]{2,1,0:T(1,128)S(1)}, f32[2,1,512]{2,1,0:T(1,128)S(1)}, f32[2,64,512]{2,1,0:T(8,128)S(1)}, f32[2,1,512]{2,1,0:T(1,128)S(1)}, f32[2...) custom-call(bf16[4,128,128]{2,1,0:T(8,128)(2,1)S(1)} %get-tuple-element.51.refs_0_, ...), custom_call_target="tpu_custom_call" | custom-call | flops 1677721600 | tf_op jit(solution)/shard_map/pallas_call | solution.py:516
  56.1 0.0 collective-permute-done.11.refs_2_
  56.1 1.8 %shard_map.147 = (f32[2,1,512]{2,1,0:T(1,128)S(1)}, f32[2,1,512]{2,1,0:T(1,128)S(1)}, f32[2,64,512]{2,1,0:T(8,128)S(1)}, f32[2,1,512]{2,1,0:T(1,128)S(1)}, f32[2...) custom-call(bf16[4,128,128]{2,1,0:T(8,128)(2,1)S(1)} %get-tuple-element.51.refs_0_, ...), custom_call_target="tpu_custom_call" | custom-call | flops 1342177280 | tf_op jit(solution)/shard_map/pallas_call | solution.py:516
  57.8 1.9 %shard_map.148 = (f32[2,1,512]{2,1,0:T(1,128)S(1)}, f32[2,1,512]{2,1,0:T(1,128)S(1)}, f32[2,64,512]{2,1,0:T(8,128)S(1)}, f32[2,1,512]{2,1,0:T(1,128)S(1)}, f32[2...) custom-call(bf16[4,128,128]{2,1,0:T(8,128)(2,1)S(1)} %get-tuple-element.51.refs_0_, ...), custom_call_target="tpu_custom_call" | custom-call | flops 1677721600 | tf_op jit(solution)/shard_map/pallas_call | solution.py:516
  59.7 0.0 copy-start
  59.7 0.0 collective-permute-done.9.refs_2_
  59.8 2.0 %shard_map.149 = (bf16[4,128,128]{2,1,0:T(8,128)(2,1)S(1)}, bf16[4,128,128]{2,1,0:T(8,128)(2,1)S(1)}) custom-call(bf16[4,128,128]{2,1,0:T(8,128)(2,1)S(1)} %get-tuple-element.51.refs_0_, bf16[4,128,128]{2,1,0:T(8,128)(2,1)S(1)} %collective-permute-done.6.refs_1_, bf16[5,128,128]{2,1,0:T(8,128)(2,1)S(1)} %collective-permute-done.9.refs_2_, ...), custom_call_target="tpu_custom_call" | custom-call | flops 1677721600 | tf_op jit(solution)/shard_map/pallas_call | solution.py:516
  61.7 0.1 collective-permute-start.16
  61.8 1.6 %collective-permute-start.15 = (bf16[128,128]{1,0:T(8,128)(2,1)S(1)}, bf16[128,128]{1,0:T(8,128)(2,1)S(1)}, u32[]{:S(2)}, u32[]{:S(2)}) collective-permute-start(bf16[128,128]{1,0:T(8,128)(2,1)S(1)} %get-tuple-element.102), channel_id=1, source_target_pairs={{0,2},{1,3},{2,0},{3,1},{4,6},{5,7},{6,4},{7,5},{8,10},{9,11},{10,... | collective-permute-start | bytes 98312 | tf_op jit(solution)/shard_map/ppermute | solution.py:550
  63.4 0.3 collective-permute-start.14
  63.7 1.1 %collective-permute-start.20 = (bf16[128,128]{1,0:T(8,128)(2,1)S(1)}, bf16[128,128]{1,0:T(8,128)(2,1)S(1)}, u32[]{:S(2)}, u32[]{:S(2)}) collective-permute-start(bf16[128,128]{1,0:T(8,128)(2,1)S(1)} %get-tuple-element.97), channel_id=1, source_target_pairs={{0,7},{1,6},{2,5},{3,4},{4,3},{5,2},{6,1},{7,0},{8,15},{9,14},{10,... | collective-permute-start | bytes 98312 | tf_op jit(solution)/shard_map/ppermute | solution.py:560
  64.8 1.7 %collective-permute-start.19 = (bf16[128,128]{1,0:T(8,128)(2,1)S(1)}, bf16[128,128]{1,0:T(8,128)(2,1)S(1)}, u32[]{:S(2)}, u32[]{:S(2)}) collective-permute-start(bf16[128,128]{1,0:T(8,128)(2,1)S(1)} %get-tuple-element.98), channel_id=1, source_target_pairs={{0,6},{1,7},{2,4},{3,5},{4,2},{5,3},{6,0},{7,1},{8,14},{9,15},{10,... | collective-permute-start | bytes 98312 | tf_op jit(solution)/shard_map/ppermute | solution.py:560
  66.5 0.0 collective-permute-done.16.refs_3_
  66.5 0.1 collective-permute-start.18
  66.6 0.0 collective-permute-done.15.refs_2_
  66.6 1.5 %collective-permute-start.17 = (bf16[128,128]{1,0:T(8,128)(2,1)S(1)}, bf16[128,128]{1,0:T(8,128)(2,1)S(1)}, u32[]{:S(2)}, u32[]{:S(2)}) collective-permute-start(bf16[128,128]{1,0:T(8,128)(2,1)S(1)} %get-tuple-element.100), channel_id=1, source_target_pairs={{0,4},{1,5},{2,6},{3,7},{4,0},{5,1},{6,2},{7,3},{8,12},{9,13},{10,... | collective-permute-start | bytes 98312 | tf_op jit(solution)/shard_map/ppermute | solution.py:560
  68.1 0.0 collective-permute-done.14.refs_1_
  68.2 0.0 collective-permute-done.20.refs_7_
  68.2 1.4 %collective-permute-done.19.refs_6_ = bf16[128,128]{1,0:T(8,128)(2,1)S(1)} collective-permute-done((bf16[128,128]{1,0:T(8,128)(2,1)S(1)}, bf16[128,128]{1,0:T(8,128)(2,1)S(1)}, u32[]{:S(2)}, u32[]{:S(2)}) %collective-permute-start.19) | collective-permute-done | bytes 32800 | tf_op jit(solution)/shard_map/ppermute | solution.py:560
  69.6 0.6 collective-permute-done.18.refs_5_
  70.2 0.8 %collective-permute-done.17.refs_4_ = bf16[128,128]{1,0:T(8,128)(2,1)S(1)} collective-permute-done((bf16[128,128]{1,0:T(8,128)(2,1)S(1)}, bf16[128,128]{1,0:T(8,128)(2,1)S(1)}, u32[]{:S(2)}, u32[]{:S(2)}) %collective-permute-start.17) | collective-permute-done | bytes 32800 | tf_op jit(solution)/shard_map/ppermute | solution.py:560
  71.0 1.6 %shard_map.150 = bf16[128,2048]{1,0:T(8,128)(2,1)} custom-call(bf16[128,2048]{1,0:T(8,128)(2,1)S(1)} %copy-done.1, f32[4,8,512]{2,1,0:T(8,128)S(1)} %bitcast.23, bf16[1024,2048]{1,0:T(8,128)(2,1)S(1)} %copy-done, bf16[128,128]{1,0:T(8,128)(2,1)S(1)} %get-tuple-element.104.refs_0_, bf16[128,128]{1,0:T(8,128)(2,1)S(1)} %collective-permute-done.14.refs_1_, ...), custom_call_target="tpu_custom_call" | custom-call | flops 536870912 | tf_op jit(solution)/shard_map/pallas_call | solution.py:678
  (21 shorter events, 0.1 us)
Async XLA Ops:
  0.0 15.1 %collective-permute-start.4 = (bf16[128,2048]{1,0:T(8,128)(2,1)}, bf16[128,2048]{1,0:T(8,128)(2,1)S(1)}, u32[]{:S(2)}, u32[]{:S(2)}) collective-permute-start(bf16[128,2048]{1,0:T(8,128)(2,1)} %latent_ref.1), channel_id=1, source_target_pairs={{0,2},{1,3},{2,0},{3,1},{4,6},{5,7},{6,4},{7,5},{8,10},{9,11},{10,... | collective-permute-start | bytes 1572872 | tf_op jit(solution)/shard_map/ppermute | solution.py:550
  3.0 25.7 %collective-permute-start.3 = (bf16[128,2048]{1,0:T(8,128)(2,1)}, bf16[128,2048]{1,0:T(8,128)(2,1)S(1)}, u32[]{:S(2)}, u32[]{:S(2)}) collective-permute-start(bf16[128,2048]{1,0:T(8,128)(2,1)} %latent_ref.1), channel_id=1, source_target_pairs={{0,1},{1,0},{2,3},{3,2},{4,5},{5,4},{6,7},{7,6},{8,9},{9,8},{10,11... | collective-permute-start | bytes 1572872 | tf_op jit(solution)/shard_map/ppermute | solution.py:550
  5.1 10.0 %collective-permute-start = (f32[8,512]{1,0:T(8,128)}, f32[8,512]{1,0:T(8,128)S(1)}, u32[]{:S(2)}, u32[]{:S(2)}) collective-permute-start(f32[8,512]{1,0:T(8,128)} %shard_map.136.one_ref), channel_id=1, source_target_pairs={{0,16},{4,20},{8,24},{12,28},{16,0},{20,4},{24,8},{28,12},{1,17},{... | collective-permute-start | bytes 49160 | tf_op jit(solution)/shard_map/ppermute | solution.py:550
  7.8 20.8 %copy-start.8 = (f32[64]{0:T(128)S(1)}, f32[64]{0:T(128)}, u32[]{:S(2)}) copy-start(f32[64]{0:T(128)} %param.25) | copy-start | bytes 772
  7.8 20.8 %copy-start.9 = (f32[64]{0:T(128)S(1)}, f32[64]{0:T(128)}, u32[]{:S(2)}) copy-start(f32[64]{0:T(128)} %param.26) | copy-start | bytes 772
  7.8 20.8 %copy-start.1 = (bf16[128,2048]{1,0:T(8,128)(2,1)S(1)}, bf16[128,2048]{1,0:T(8,128)(2,1)}, u32[]{:S(2)}) copy-start(bf16[128,2048]{1,0:T(8,128)(2,1)} %latent_ref.1) | copy-start | bytes 1572868
  15.1 13.5 %collective-permute-start.5 = (bf16[128,2048]{1,0:T(8,128)(2,1)S(1)}, bf16[128,2048]{1,0:T(8,128)(2,1)S(1)}, u32[]{:S(2)}, u32[]{:S(2)}) collective-permute-start(bf16[128,2048]{1,0:T(8,128)(2,1)S(1)} %collective-permute-done.4.refs_6_), channel_id=1, source_target_pairs={{0,1},{1,0},{2,3},{3,2},{4,5},{5,4},{6,7},{7,6},{8,9},{9,8},{10,11... | collective-permute-start | bytes 1572872 | tf_op jit(solution)/shard_map/ppermute | solution.py:550
  15.1 0.7 copy-start.2
  15.8 12.8 %copy-start.3 = (bf16[2048,256]{1,0:T(8,128)(2,1)S(1)}, bf16[2048,256]{1,0:T(8,128)(2,1)}, u32[]{:S(2)}) copy-start(bf16[2048,256]{1,0:T(8,128)(2,1)} %refs_2_.1) | copy-start | bytes 3145732
  15.8 12.9 %copy-start.4 = (bf16[2048,128]{1,0:T(8,128)(2,1)S(1)}, bf16[2048,128]{1,0:T(8,128)(2,1)}, u32[]{:S(2)}) copy-start(bf16[2048,128]{1,0:T(8,128)(2,1)} %refs_3_.1) | copy-start | bytes 1572868
  15.8 12.9 %copy-start.5 = (bf16[2048,128]{1,0:T(8,128)(2,1)S(1)}, bf16[2048,128]{1,0:T(8,128)(2,1)}, u32[]{:S(2)}) copy-start(bf16[2048,128]{1,0:T(8,128)(2,1)} %refs_4_.1) | copy-start | bytes 1572868
  15.8 12.9 %copy-start.6 = (bf16[64,2048]{1,0:T(8,128)(2,1)S(1)}, bf16[64,2048]{1,0:T(8,128)(2,1)}, u32[]{:S(2)}) copy-start(bf16[64,2048]{1,0:T(8,128)(2,1)} %refs_1_.1) | copy-start | bytes 786436
  15.8 12.9 %copy-start.7 = (f32[2048]{0:T(1024)S(1)}, f32[2048]{0:T(1024)}, u32[]{:S(2)}) copy-start(f32[2048]{0:T(1024)} %param.18) | copy-start | bytes 24580
  15.9 3.8 %collective-permute-start.1 = (f32[8,512]{1,0:T(8,128)S(1)}, f32[8,512]{1,0:T(8,128)S(1)}, u32[]{:S(2)}, u32[]{:S(2)}) collective-permute-start(f32[8,512]{1,0:T(8,128)S(1)} %shard_map.137.one_ref), channel_id=1, source_target_pairs={{0,8},{4,12},{8,0},{12,4},{16,24},{20,28},{24,16},{28,20},{1,9},{5... | collective-permute-start | bytes 49160 | tf_op jit(solution)/shard_map/ppermute | solution.py:550
  19.7 3.7 %collective-permute-start.2 = (f32[8,512]{1,0:T(8,128)S(1)}, f32[8,512]{1,0:T(8,128)S(1)}, u32[]{:S(2)}, u32[]{:S(2)}) collective-permute-start(f32[8,512]{1,0:T(8,128)S(1)} %shard_map.138.one_ref), channel_id=1, source_target_pairs={{0,4},{4,0},{8,12},{12,8},{16,20},{20,16},{24,28},{28,24},{1,5},{5... | collective-permute-start | bytes 49160 | tf_op jit(solution)/shard_map/ppermute | solution.py:550
  31.4 11.7 %collective-permute-start.7 = (bf16[5,128,128]{2,1,0:T(8,128)(2,1)S(1)}, bf16[5,128,128]{2,1,0:T(8,128)(2,1)S(1)}, u32[]{:S(2)}, u32[]{:S(2)}) collective-permute-start(bf16[5,128,128]{2,1,0:T(8,128)(2,1)S(1)} %get-tuple-element.53), channel_id=1, source_target_pairs={{0,4},{4,0},{8,12},{12,8},{16,20},{20,16},{24,28},{28,24},{1,5},{5... | collective-permute-start | bytes 491528 | tf_op jit(solution)/shard_map/ppermute | solution.py:550
  33.2 8.2 %collective-permute-start.10 = (bf16[4,128,128]{2,1,0:T(8,128)(2,1)S(1)}, bf16[4,128,128]{2,1,0:T(8,128)(2,1)S(1)}, u32[]{:S(2)}, u32[]{:S(2)}) collective-permute-start(bf16[4,128,128]{2,1,0:T(8,128)(2,1)S(1)} %get-tuple-element.55.refs_1_.refs_2_), channel_id=1, source_target_pairs={{0,24},{4,28},{8,16},{12,20},{16,8},{20,12},{24,0},{28,4},{1,25},{... | collective-permute-start | bytes 393224 | tf_op jit(solution)/shard_map/ppermute | solution.py:550
  36.8 10.3 %collective-permute-start.6 = (bf16[4,128,128]{2,1,0:T(8,128)(2,1)S(1)}, bf16[4,128,128]{2,1,0:T(8,128)(2,1)S(1)}, u32[]{:S(2)}, u32[]{:S(2)}) collective-permute-start(bf16[4,128,128]{2,1,0:T(8,128)(2,1)S(1)} %get-tuple-element.52), channel_id=1, source_target_pairs={{0,4},{4,0},{8,12},{12,8},{16,20},{20,16},{24,28},{28,24},{1,5},{5... | collective-permute-start | bytes 393224 | tf_op jit(solution)/shard_map/ppermute | solution.py:550
  37.3 12.4 %collective-permute-start.13 = (bf16[4,128,128]{2,1,0:T(8,128)(2,1)S(1)}, bf16[4,128,128]{2,1,0:T(8,128)(2,1)S(1)}, u32[]{:S(2)}, u32[]{:S(2)}) collective-permute-start(bf16[4,128,128]{2,1,0:T(8,128)(2,1)S(1)} %get-tuple-element.55.refs_1_.refs_2_), channel_id=1, source_target_pairs={{0,8},{4,12},{8,0},{12,4},{16,24},{20,28},{24,16},{28,20},{1,9},{5... | collective-permute-start | bytes 393224 | tf_op jit(solution)/shard_map/ppermute | solution.py:550
  41.4 14.7 %collective-permute-start.11 = (bf16[4,128,128]{2,1,0:T(8,128)(2,1)S(1)}, bf16[4,128,128]{2,1,0:T(8,128)(2,1)S(1)}, u32[]{:S(2)}, u32[]{:S(2)}) collective-permute-start(bf16[4,128,128]{2,1,0:T(8,128)(2,1)S(1)} %collective-permute-done.10.refs_2_), channel_id=1, source_target_pairs={{0,8},{4,12},{8,0},{12,4},{16,24},{20,28},{24,16},{28,20},{1,9},{5... | collective-permute-start | bytes 393224 | tf_op jit(solution)/shard_map/ppermute | solution.py:550
  43.1 11.1 %collective-permute-start.12 = (bf16[5,128,128]{2,1,0:T(8,128)(2,1)S(1)}, bf16[5,128,128]{2,1,0:T(8,128)(2,1)S(1)}, u32[]{:S(2)}, u32[]{:S(2)}) collective-permute-start(bf16[5,128,128]{2,1,0:T(8,128)(2,1)S(1)} %shard_map.141.refs_3_), channel_id=1, source_target_pairs={{0,8},{4,12},{8,0},{12,4},{16,24},{20,28},{24,16},{28,20},{1,9},{5... | collective-permute-start | bytes 491528 | tf_op jit(solution)/shard_map/ppermute | solution.py:550
  43.5 10.6 %collective-permute-start.8 = (bf16[5,128,128]{2,1,0:T(8,128)(2,1)S(1)}, bf16[5,128,128]{2,1,0:T(8,128)(2,1)S(1)}, u32[]{:S(2)}, u32[]{:S(2)}) collective-permute-start(bf16[5,128,128]{2,1,0:T(8,128)(2,1)S(1)} %shard_map.141.refs_3_), channel_id=1, source_target_pairs={{0,24},{4,28},{8,16},{12,20},{16,8},{20,12},{24,0},{28,4},{1,25},{... | collective-permute-start | bytes 491528 | tf_op jit(solution)/shard_map/ppermute | solution.py:550
  54.2 5.6 %collective-permute-start.9 = (bf16[5,128,128]{2,1,0:T(8,128)(2,1)S(1)}, bf16[5,128,128]{2,1,0:T(8,128)(2,1)S(1)}, u32[]{:S(2)}, u32[]{:S(2)}) collective-permute-start(bf16[5,128,128]{2,1,0:T(8,128)(2,1)S(1)} %collective-permute-done.8.refs_2_), channel_id=1, source_target_pairs={{0,8},{4,12},{8,0},{12,4},{16,24},{20,28},{24,16},{28,20},{1,9},{5... | collective-permute-start | bytes 491528 | tf_op jit(solution)/shard_map/ppermute | solution.py:550
  59.7 11.2 %copy-start = (bf16[1024,2048]{1,0:T(8,128)(2,1)S(1)}, bf16[1024,2048]{1,0:T(8,128)(2,1)}, u32[]{:S(2)}) copy-start(bf16[1024,2048]{1,0:T(8,128)(2,1)} %weight_ref.1) | copy-start | bytes 12582916
  61.7 4.8 %collective-permute-start.16 = (bf16[128,128]{1,0:T(8,128)(2,1)S(1)}, bf16[128,128]{1,0:T(8,128)(2,1)S(1)}, u32[]{:S(2)}, u32[]{:S(2)}) collective-permute-start(bf16[128,128]{1,0:T(8,128)(2,1)S(1)} %get-tuple-element.101), channel_id=1, source_target_pairs={{0,3},{1,2},{2,1},{3,0},{4,7},{5,6},{6,5},{7,4},{8,11},{9,10},{10,... | collective-permute-start | bytes 98312 | tf_op jit(solution)/shard_map/ppermute | solution.py:550
  61.8 4.8 %collective-permute-start.15 = (bf16[128,128]{1,0:T(8,128)(2,1)S(1)}, bf16[128,128]{1,0:T(8,128)(2,1)S(1)}, u32[]{:S(2)}, u32[]{:S(2)}) collective-permute-start(bf16[128,128]{1,0:T(8,128)(2,1)S(1)} %get-tuple-element.102), channel_id=1, source_target_pairs={{0,2},{1,3},{2,0},{3,1},{4,6},{5,7},{6,4},{7,5},{8,10},{9,11},{10,... | collective-permute-start | bytes 98312 | tf_op jit(solution)/shard_map/ppermute | solution.py:550
  63.4 4.8 %collective-permute-start.14 = (bf16[128,128]{1,0:T(8,128)(2,1)S(1)}, bf16[128,128]{1,0:T(8,128)(2,1)S(1)}, u32[]{:S(2)}, u32[]{:S(2)}) collective-permute-start(bf16[128,128]{1,0:T(8,128)(2,1)S(1)} %get-tuple-element.103), channel_id=1, source_target_pairs={{0,1},{1,0},{2,3},{3,2},{4,5},{5,4},{6,7},{7,6},{8,9},{9,8},{10,11... | collective-permute-start | bytes 98312 | tf_op jit(solution)/shard_map/ppermute | solution.py:550
  63.7 4.5 %collective-permute-start.20 = (bf16[128,128]{1,0:T(8,128)(2,1)S(1)}, bf16[128,128]{1,0:T(8,128)(2,1)S(1)}, u32[]{:S(2)}, u32[]{:S(2)}) collective-permute-start(bf16[128,128]{1,0:T(8,128)(2,1)S(1)} %get-tuple-element.97), channel_id=1, source_target_pairs={{0,7},{1,6},{2,5},{3,4},{4,3},{5,2},{6,1},{7,0},{8,15},{9,14},{10,... | collective-permute-start | bytes 98312 | tf_op jit(solution)/shard_map/ppermute | solution.py:560
  64.8 4.8 %collective-permute-start.19 = (bf16[128,128]{1,0:T(8,128)(2,1)S(1)}, bf16[128,128]{1,0:T(8,128)(2,1)S(1)}, u32[]{:S(2)}, u32[]{:S(2)}) collective-permute-start(bf16[128,128]{1,0:T(8,128)(2,1)S(1)} %get-tuple-element.98), channel_id=1, source_target_pairs={{0,6},{1,7},{2,4},{3,5},{4,2},{5,3},{6,0},{7,1},{8,14},{9,15},{10,... | collective-permute-start | bytes 98312 | tf_op jit(solution)/shard_map/ppermute | solution.py:560
  66.5 3.7 %collective-permute-start.18 = (bf16[128,128]{1,0:T(8,128)(2,1)S(1)}, bf16[128,128]{1,0:T(8,128)(2,1)S(1)}, u32[]{:S(2)}, u32[]{:S(2)}) collective-permute-start(bf16[128,128]{1,0:T(8,128)(2,1)S(1)} %get-tuple-element.99), channel_id=1, source_target_pairs={{0,5},{1,4},{2,7},{3,6},{4,1},{5,0},{6,3},{7,2},{8,13},{9,12},{10,... | collective-permute-start | bytes 98312 | tf_op jit(solution)/shard_map/ppermute | solution.py:560
  66.6 4.3 %collective-permute-start.17 = (bf16[128,128]{1,0:T(8,128)(2,1)S(1)}, bf16[128,128]{1,0:T(8,128)(2,1)S(1)}, u32[]{:S(2)}, u32[]{:S(2)}) collective-permute-start(bf16[128,128]{1,0:T(8,128)(2,1)S(1)} %get-tuple-element.100), channel_id=1, source_target_pairs={{0,4},{1,5},{2,6},{3,7},{4,0},{5,1},{6,2},{7,3},{8,12},{9,13},{10,... | collective-permute-start | bytes 98312 | tf_op jit(solution)/shard_map/ppermute | solution.py:560

commit v4 on v3

--- a/solution.py
+++ b/solution.py
@@ -220,11 +220,12 @@
         out_specs=jax.tree.map(lambda unused: whole_spec(), out_shape),
         scratch_shapes=list(scratch),
         cost_estimate=pl.CostEstimate(flops=flops, transcendentals=0, bytes_accessed=0),
-        compiler_params=pltpu.CompilerParams(vmem_limit_bytes=48 * 1024 * 1024),
+        compiler_params=pltpu.CompilerParams(vmem_limit_bytes=MODEST),
     )
 
 
 ROOMY = 60 * 1024 * 1024
+MODEST = 32 * 1024 * 1024
 
 
 def hbm_spec():
@@ -372,7 +373,10 @@
     side = lax.rem(lax.axis_index("sp"), kv_heads)
     for head, q_ref, kv_ref in ((1 - side, give_q, give_kv), (side, keep_q, keep_kv)):
         for i in range(q_tiles):
-            q_ref[i] = made[head, i]
+            if q_ref is keep_q:
+                q_ref[i], q_ref[q_tiles + i] = scaled_halves(made[head, i])
+            else:
+                q_ref[i] = made[head, i]
         for i in range(kv_ref.shape[0]):
             kv_ref[i] = made[head, q_tiles + i]
     keep_ctx[...] = made[side, q_tiles + len(blocks)]
@@ -390,13 +394,30 @@
     return kernel_call(merge_body, jax.ShapeDtypeStruct(near.shape, near.dtype), 2, 10**6)(near, ctx)
 
 
+def scaled_halves(tile):
+    scale = (tile.shape[-2] // 2) ** (-0.5) * LOG2E
+    wide = tile.astype(jnp.float32) * scale
+    high = wide.astype(jnp.bfloat16)
+    return high, (wide - high.astype(jnp.float32)).astype(jnp.bfloat16)
+
+
+def ready_body(q_ref, out_ref):
+    count = q_ref.shape[0]
+    for i in range(count):
+        out_ref[i], out_ref[count + i] = scaled_halves(q_ref[i])
+
+
+def ready(probes):
+    shape = jax.ShapeDtypeStruct((2 * probes.shape[0], *probes.shape[1:]), probes.dtype)
+    return kernel_call(ready_body, shape, 1, 10**6)(probes)
+
+
 def attention_body(plan, pieces, last, offset, *refs):
     q_refs, refs = refs[: len(plan)], refs[len(plan) :]
     kv_refs, refs = refs[:pieces], refs[pieces:]
     pairs = 2
     groups = 2
     span = q_refs[0].shape[1] // 2
-    scale = span ** (-0.5) * LOG2E
     halves = (0, 1)
     states = {}
     queries = {}
@@ -405,17 +426,20 @@
         if started:
             old, refs = refs[:3], refs[3:]
         for g in range(groups):
-            found = jnp.concatenate(
-                [
-                    q_ref[g * pairs + p, half * span : (half + 1) * span, :]
-                    for p in range(pairs)
-                    for half in halves
-                ],
-                axis=1,
-            )
-            blank = jnp.zeros_like(found)
-            queries[i, g, 0] = jnp.concatenate([found, blank], axis=0)
-            queries[i, g, 1] = jnp.concatenate([blank, found], axis=0)
+            high, low = [
+                jnp.concatenate(
+                    [
+                        q_ref[(level * groups + g) * pairs + p, half * span : (half + 1) * span, :]
+                        for p in range(pairs)
+                        for half in halves
+                    ],
+                    axis=1,
+                )
+                for level in halves
+            ]
+            blank = jnp.zeros_like(high)
+            queries[i, g, 0] = jnp.concatenate([high, blank, low, blank], axis=0)
+            queries[i, g, 1] = jnp.concatenate([blank, high, blank, low], axis=0)
             if started:
                 states[i, g] = tuple(ref[g] for ref in old)
             tiles += [(i, g, place) for place in wanted]
@@ -429,9 +453,10 @@
         if context:
             keys.append(ref[2 * pairs, 0:span, :])
         keys = jnp.concatenate(keys, axis=0)
+        keys = jnp.concatenate([keys, keys], axis=1)
         made = []
         for half in halves:
-            found = jnp.dot(keys, queries[i, g, half], preferred_element_type=jnp.float32) * scale
+            found = jnp.dot(keys, queries[i, g, half], preferred_element_type=jnp.float32)
             if context:
                 rows = found.shape[0] - span
                 made += [found[:rows], found[rows:] + offset * LOG2E]
@@ -628,7 +653,7 @@
         lambda *refs: projection_body(q_heads, kv_heads, *refs),
         out_shape=[
             jax.ShapeDtypeStruct((*count, *tile), jnp.bfloat16)
-            for count in ((q_tiles,), (kv_tiles,), (), (q_tiles,), (kv_tiles + 1,))
+            for count in ((2 * q_tiles,), (kv_tiles,), (), (q_tiles,), (kv_tiles + 1,))
         ],
         in_specs=[whole_spec()] * 14,
         out_specs=[whole_spec()] * 5,
@@ -638,7 +663,7 @@
             transcendentals=0,
             bytes_accessed=0,
         ),
-        compiler_params=pltpu.CompilerParams(vmem_limit_bytes=48 * 1024 * 1024),
+        compiler_params=pltpu.CompilerParams(vmem_limit_bytes=MODEST),
     )(
         latent,
         context,
@@ -657,21 +682,22 @@
     )
     offset = math.log(tok_count / (2.0 * ctx_rows))
     near = xor_move(give_kv, "sp", 1)
+    near_q = xor_move(give_q, "sp", 1)
     up = xor_move(keep_kv, "sp", 2)
     down = xor_move(keep_kv, "sp", 6)
-    near_q = xor_move(give_q, "sp", 1)
     near = merge(near, keep_ctx)
     near_down = xor_move(near, "sp", 6)
     near_up = xor_move(near, "sp", 2)
     across = xor_move(down, "sp", 2)
     near_across = xor_move(near_down, "sp", 2)
     (own,) = attend([(keep_q, None, [0])], [keep_kv], offset)
+    near_q = ready(near_q)
     own, other = attend([(keep_q, own, [1]), (near_q, None, [0, 1])], [keep_kv, near], offset)
-    for piece in (up, down, near_up, across, near_down):
+    for piece in (up, down, near_up, across):
         own, other = attend([(keep_q, own, [0]), (near_q, other, [0])], [piece], offset)
-    (own,), (other,) = attend(
-        [(keep_q, own, [0]), (near_q, other, [0])], [near_across], offset, True
-    )
+    (other,) = attend([(near_q, other, [0])], [near_down], offset)
+    ((other,),) = attend([(near_q, other, [0])], [near_across], offset, True)
+    ((own,),) = attend([(keep_q, own, [0, 1])], [near_down, near_across], offset, True)
     sent = [cross_move(other[j], j) for j in range(head_split)]
     parts = [own[0]] + [xor_move(own[j], "tp", j) for j in range(1, head_split)] + sent
     width = q_heads * CHANNEL_SPAN

time: 73 us -> 73.9 us (1.012)
  waiting for transfers between devices: 18.1 us -> 19.6 us
    ppermute x17, waiting for transfers between devices: 15.3 us -> 16.4 us  [xor_move(): return lax.ppermute(member, axis, [(i, i ^ mask) for i in range(size)])]
    pallas_call x8 -> x9, Pallas kernels: 14.1 us -> 13.6 us  [attend(): kernel_call(body, out * len(sources), len(inputs), 40 * 2 * lanes * keys...]
  transfers between devices with their start and end apart: 21 -> 21, of which waited for: 8 -> 9; matrix products, arithmetic and copies ran while one was open for 1% -> 1% of each run, Pallas kernels for 20% -> 19%
where the time goes in v4:
time: 73.9 us; the launch traced here: 73.6 us
  starting transfers between devices  27.3 us (37%)
  Pallas kernels  20 us (27%)
  waiting for transfers between devices  19.6 us (27%)
  blocking collectives  5.22 us (7%)
  local copies, waits for them, and re-layouts  0.78 us (1%)
    ppermute x17, starting transfers between devices, xor_move(): return lax.ppermute(member, axis, [(i, i ^ mask) for i in range(size)])  22.9 us
    ppermute x17, waiting for transfers between devices, xor_move(): return lax.ppermute(member, axis, [(i, i ^ mask) for i in range(size)])  16.4 us
    pallas_call x9, Pallas kernels, attend(): kernel_call(body, out * len(sources), len(inputs), 40 * 2 * lanes * keys...  13.6 us
    all_gather x1, blocking collectives, inner_device(): modulation = lax.all_gather(part, 'tp', axis=0, tiled=False)  5.22 us
    ppermute x4, starting transfers between devices, cross_move(): return lax.ppermute(member, ('sp', 'tp'), pairs)  4.39 us
    ppermute x4, waiting for transfers between devices, cross_move(): return lax.ppermute(member, ('sp', 'tp'), pairs)  3.16 us
    pallas_call x1, Pallas kernels, inner_device(): pl.pallas_call(lambda *refs: projection_body(q_heads, kv_heads, *refs), o...  2.67 us
    pallas_call x1, Pallas kernels, opening(): pl.pallas_call(opening_body, out_shape=jax.ShapeDtypeStruct((8, columns),...  2.08 us
  transfers between devices with their start and end apart: 21, of which 9 were waited for; matrix products, arithmetic and copies ran while one was open for 1% of the time, Pallas kernels for 19%

profile of v4, /device:TPU:0, one launch (start us, length us, event | category | flops | bytes accessed | tf_op | source)
XLA Modules:
  0.0 73.6 jit_solution(12559703354412165044)
XLA Ops:
  0.0 3.0 %collective-permute-start.4 = (bf16[128,2048]{1,0:T(8,128)(2,1)}, bf16[128,2048]{1,0:T(8,128)(2,1)S(1)}, u32[]{:S(2)}, u32[]{:S(2)}) collective-permute-start(bf16[128,2048]{1,0:T(8,128)(2,1)} %latent_ref.1), channel_id=1, source_target_pairs={{0,2},{1,3},{2,0},{3,1},{4,6},{5,7},{6,4},{7,5},{8,10},{9,11},{10,... | collective-permute-start | bytes 1572872 | tf_op jit(solution)/shard_map/ppermute | solution.py:575
  3.0 0.0 collective-permute-start.3
  3.0 2.1 %shard_map.136.one_ref = f32[8,512]{1,0:T(8,128)} custom-call(f32[1,2048]{1,0:T(1,128)} %bitcast.27, f32[1,2048]{1,0:T(1,128)} %bitcast.28, bf16[256,512]{1,0:T(8,128)(2,1)} %shift_hbm.1, bf16[256,512]{1,0:T(8,128)(2,1)} %scale_hbm.1, bf16[256,512]{1,0:T(8,128)(2,1)} %gate_hbm.1), custom_call_target="tpu_custom_call" | custom-call | flops 100000000 | tf_op jit(solution)/shard_map/pallas_call | solution.py:276
  5.1 2.7 %collective-permute-start = (f32[8,512]{1,0:T(8,128)}, f32[8,512]{1,0:T(8,128)S(1)}, u32[]{:S(2)}, u32[]{:S(2)}) collective-permute-start(f32[8,512]{1,0:T(8,128)} %shard_map.136.one_ref), channel_id=1, source_target_pairs={{0,16},{4,20},{8,24},{12,28},{16,0},{20,4},{24,8},{28,12},{1,17},{... | collective-permute-start | bytes 49160 | tf_op jit(solution)/shard_map/ppermute | solution.py:575
  7.7 0.1 fusion.2
  7.8 0.0 copy-start.9
  7.8 0.0 copy-start.1
  7.8 7.3 %collective-permute-done.4.refs_6_ = bf16[128,2048]{1,0:T(8,128)(2,1)S(1)} collective-permute-done((bf16[128,2048]{1,0:T(8,128)(2,1)}, bf16[128,2048]{1,0:T(8,128)(2,1)S(1)}, u32[]{:S(2)}, u32[]{:S(2)}) %collective-permute-start.4) | collective-permute-done | bytes 524320 | tf_op jit(solution)/shard_map/ppermute | solution.py:575
  15.1 0.0 collective-permute-start.5
  15.1 0.0 collective-permute-done.other_ref
  15.1 0.7 copy-done.2
  15.8 0.0 copy-start.7
  15.9 1.9 %collective-permute-start.1 = (f32[8,512]{1,0:T(8,128)S(1)}, f32[8,512]{1,0:T(8,128)S(1)}, u32[]{:S(2)}, u32[]{:S(2)}) collective-permute-start(f32[8,512]{1,0:T(8,128)S(1)} %shard_map.137.one_ref), channel_id=1, source_target_pairs={{0,8},{4,12},{8,0},{12,4},{16,24},{20,28},{24,16},{28,20},{1,9},{5... | collective-permute-start | bytes 49160 | tf_op jit(solution)/shard_map/ppermute | solution.py:575
  17.8 0.3 fusion
  18.1 1.6 %collective-permute-done.1.other_ref = f32[8,512]{1,0:T(8,128)S(1)} collective-permute-done((f32[8,512]{1,0:T(8,128)S(1)}, f32[8,512]{1,0:T(8,128)S(1)}, u32[]{:S(2)}, u32[]{:S(2)}) %collective-permute-start.1) | collective-permute-done | bytes 16416 | tf_op jit(solution)/shard_map/ppermute | solution.py:575
  19.7 1.8 %collective-permute-start.2 = (f32[8,512]{1,0:T(8,128)S(1)}, f32[8,512]{1,0:T(8,128)S(1)}, u32[]{:S(2)}, u32[]{:S(2)}) collective-permute-start(f32[8,512]{1,0:T(8,128)S(1)} %shard_map.138.one_ref), channel_id=1, source_target_pairs={{0,4},{4,0},{8,12},{12,8},{16,20},{20,16},{24,28},{28,24},{1,5},{5... | collective-permute-start | bytes 49160 | tf_op jit(solution)/shard_map/ppermute | solution.py:575
  21.5 1.9 %collective-permute-done.2.other_ref = f32[8,512]{1,0:T(8,128)S(1)} collective-permute-done((f32[8,512]{1,0:T(8,128)S(1)}, f32[8,512]{1,0:T(8,128)S(1)}, u32[]{:S(2)}, u32[]{:S(2)}) %collective-permute-start.2) | collective-permute-done | bytes 16416 | tf_op jit(solution)/shard_map/ppermute | solution.py:575
  23.4 5.2 %all-gather = f32[32,512]{1,0:T(8,128)S(1)} all-gather(f32[8,512]{1,0:T(8,128)S(1)} %shard_map.139), channel_id=2, replica_groups=mesh['sp'=8,'tp'=4] {'tp'}, dimensions={0}, use_global_device_ids=true | all-gather | bytes 81920 | tf_op jit(solution)/shard_map/all_gather | solution.py:647
  28.6 0.0 collective-permute-done.3.refs_5_
  28.6 0.0 collective-permute-done.5.refs_7_
  28.6 0.0 copy-done.8
  28.6 0.0 copy-done.9
  28.7 2.7 %shard_map.140 = (bf16[8,128,128]{2,1,0:T(8,128)(2,1)S(1)}, bf16[4,128,128]{2,1,0:T(8,128)(2,1)S(1)}, bf16[128,128]{1,0:T(8,128)(2,1)S(1)}, bf16[4,128,128]{2,1,0:T(8,128)(2,1)S(1)}, bf16[5,128,128]{2,1,0:T(8,128)(2,1)S(1)}) custom-call(bf16[128,2048]{1,0:T(8,128)(2,1)S(1)} %copy-done.1, bf16[64,2048]{1,0:T(8,128)(2,1)S(1)} %copy-done.6, ...), custom_call_target="tpu_custom_call" | custom-call | flops 2147483648 | tf_op jit(solution)/shard_map/pallas_call | solution.py:652
  31.4 1.8 %collective-permute-start.6 = (bf16[5,128,128]{2,1,0:T(8,128)(2,1)S(1)}, bf16[5,128,128]{2,1,0:T(8,128)(2,1)S(1)}, u32[]{:S(2)}, u32[]{:S(2)}) collective-permute-start(bf16[5,128,128]{2,1,0:T(8,128)(2,1)S(1)} %get-tuple-element.47), channel_id=1, source_target_pairs={{0,4},{4,0},{8,12},{12,8},{16,20},{20,16},{24,28},{28,24},{1,5},{5... | collective-permute-start | bytes 491528 | tf_op jit(solution)/shard_map/ppermute | solution.py:575
  33.2 3.6 %collective-permute-start.10 = (bf16[4,128,128]{2,1,0:T(8,128)(2,1)S(1)}, bf16[4,128,128]{2,1,0:T(8,128)(2,1)S(1)}, u32[]{:S(2)}, u32[]{:S(2)}) collective-permute-start(bf16[4,128,128]{2,1,0:T(8,128)(2,1)S(1)} %get-tuple-element.50.refs_1_.refs_2_), channel_id=1, source_target_pairs={{0,24},{4,28},{8,16},{12,20},{16,8},{20,12},{24,0},{28,4},{1,25},{... | collective-permute-start | bytes 393224 | tf_op jit(solution)/shard_map/ppermute | solution.py:575
  36.8 0.5 collective-permute-start.9
  37.3 0.0 collective-permute-start.13
  37.4 0.9 %shard_map.143 = (f32[2,1,512]{2,1,0:T(1,128)S(1)}, f32[2,1,512]{2,1,0:T(1,128)S(1)}, f32[2,64,512]{2,1,0:T(8,128)S(1)}) custom-call(bf16[8,128,128]{2,1,0:T(8,128)(2,1)S(1)} %get-tuple-element.46.refs_0_, bf16[4,128,128]{2,1,0:T(8,128)(2,1)S(1)} %get-tuple-element.50.refs_1_.refs_2_), custom_call_target="tpu_custom_call" | custom-call | flops 671088640 | tf_op jit(solution)/shard_map/pallas_call | solution.py:541
  38.2 3.2 %collective-permute-done.10.refs_2_ = bf16[4,128,128]{2,1,0:T(8,128)(2,1)S(1)} collective-permute-done((bf16[4,128,128]{2,1,0:T(8,128)(2,1)S(1)}, bf16[4,128,128]{2,1,0:T(8,128)(2,1)S(1)}, u32[]{:S(2)}, u32[]{:S(2)}) %collective-permute-start.10) | collective-permute-done | bytes 131104 | tf_op jit(solution)/shard_map/ppermute | solution.py:575
  41.4 1.6 %collective-permute-start.11 = (bf16[4,128,128]{2,1,0:T(8,128)(2,1)S(1)}, bf16[4,128,128]{2,1,0:T(8,128)(2,1)S(1)}, u32[]{:S(2)}, u32[]{:S(2)}) collective-permute-start(bf16[4,128,128]{2,1,0:T(8,128)(2,1)S(1)} %collective-permute-done.10.refs_2_), channel_id=1, source_target_pairs={{0,8},{4,12},{8,0},{12,4},{16,24},{20,28},{24,16},{28,20},{1,9},{5... | collective-permute-start | bytes 393224 | tf_op jit(solution)/shard_map/ppermute | solution.py:575
  43.1 0.0 collective-permute-done.9.q_ref
  43.1 0.0 collective-permute-done.6.near_ref
  43.1 0.1 shard_map.141.refs_3_
  43.2 0.4 collective-permute-start.12
  43.6 3.6 %collective-permute-start.7 = (bf16[5,128,128]{2,1,0:T(8,128)(2,1)S(1)}, bf16[5,128,128]{2,1,0:T(8,128)(2,1)S(1)}, u32[]{:S(2)}, u32[]{:S(2)}) collective-permute-start(bf16[5,128,128]{2,1,0:T(8,128)(2,1)S(1)} %shard_map.141.refs_3_), channel_id=1, source_target_pairs={{0,24},{4,28},{8,16},{12,20},{16,8},{20,12},{24,0},{28,4},{1,25},{... | collective-permute-start | bytes 491528 | tf_op jit(solution)/shard_map/ppermute | solution.py:575
  47.2 2.4 %shard_map.144 = (f32[2,1,512]{2,1,0:T(1,128)S(1)}, f32[2,1,512]{2,1,0:T(1,128)S(1)}, f32[2,64,512]{2,1,0:T(8,128)S(1)}, f32[2,1,512]{2,1,0:T(1,128)S(1)}, f32[2...) custom-call(bf16[8,128,128]{2,1,0:T(8,128)(2,1)S(1)} %get-tuple-element.46.refs_0_, ...), custom_call_target="tpu_custom_call" | custom-call | flops 2348810240 | tf_op jit(solution)/shard_map/pallas_call | solution.py:541
  49.6 0.0 collective-permute-done.13.refs_2_
  49.6 1.5 %shard_map.145 = (f32[2,1,512]{2,1,0:T(1,128)S(1)}, f32[2,1,512]{2,1,0:T(1,128)S(1)}, f32[2,64,512]{2,1,0:T(8,128)S(1)}, f32[2,1,512]{2,1,0:T(1,128)S(1)}, f32[2...) custom-call(bf16[8,128,128]{2,1,0:T(8,128)(2,1)S(1)} %get-tuple-element.46.refs_0_, ...), custom_call_target="tpu_custom_call" | custom-call | flops 1342177280 | tf_op jit(solution)/shard_map/pallas_call | solution.py:541
  51.1 1.5 %shard_map.146 = (f32[2,1,512]{2,1,0:T(1,128)S(1)}, f32[2,1,512]{2,1,0:T(1,128)S(1)}, f32[2,64,512]{2,1,0:T(8,128)S(1)}, f32[2,1,512]{2,1,0:T(1,128)S(1)}, f32[2...) custom-call(bf16[8,128,128]{2,1,0:T(8,128)(2,1)S(1)} %get-tuple-element.46.refs_0_, ...), custom_call_target="tpu_custom_call" | custom-call | flops 1342177280 | tf_op jit(solution)/shard_map/pallas_call | solution.py:541
  52.6 1.6 %collective-permute-done.7.refs_1_ = bf16[5,128,128]{2,1,0:T(8,128)(2,1)S(1)} collective-permute-done((bf16[5,128,128]{2,1,0:T(8,128)(2,1)S(1)}, bf16[5,128,128]{2,1,0:T(8,128)(2,1)S(1)}, u32[]{:S(2)}, u32[]{:S(2)}) %collective-permute-start.7) | collective-permute-done | bytes 163872 | tf_op jit(solution)/shard_map/ppermute | solution.py:575
  54.2 0.0 collective-permute-start.8
  54.3 0.0 collective-permute-done.12.refs_2_
  54.3 1.8 %shard_map.147 = (f32[2,1,512]{2,1,0:T(1,128)S(1)}, f32[2,1,512]{2,1,0:T(1,128)S(1)}, f32[2,64,512]{2,1,0:T(8,128)S(1)}, f32[2,1,512]{2,1,0:T(1,128)S(1)}, f32[2...) custom-call(bf16[8,128,128]{2,1,0:T(8,128)(2,1)S(1)} %get-tuple-element.46.refs_0_, ...), custom_call_target="tpu_custom_call" | custom-call | flops 1677721600 | tf_op jit(solution)/shard_map/pallas_call | solution.py:541
  56.1 0.0 collective-permute-done.11.refs_2_
  56.1 1.5 %shard_map.148 = (f32[2,1,512]{2,1,0:T(1,128)S(1)}, f32[2,1,512]{2,1,0:T(1,128)S(1)}, f32[2,64,512]{2,1,0:T(8,128)S(1)}, f32[2,1,512]{2,1,0:T(1,128)S(1)}, f32[2...) custom-call(bf16[8,128,128]{2,1,0:T(8,128)(2,1)S(1)} %get-tuple-element.46.refs_0_, ...), custom_call_target="tpu_custom_call" | custom-call | flops 1342177280 | tf_op jit(solution)/shard_map/pallas_call | solution.py:541
  57.6 1.2 %shard_map.150 = (f32[2,1,512]{2,1,0:T(1,128)S(1)}, f32[2,1,512]{2,1,0:T(1,128)S(1)}, f32[2,64,512]{2,1,0:T(8,128)S(1)}) custom-call(bf16[8,128,128]{2,1,0:T(8,128)(2,1)S(1)} %shard_map.142.refs_1_.refs_0_, bf16[5,128,128]{2,1,0:T(8,128)(2,1)S(1)} %collective-permute-done.7.refs_1_, f32[2,1,512]{2,1,0:T(1,128)S(1)} %get-tuple-element.81.refs_2_, ...), custom_call_target="tpu_custom_call" | custom-call | flops 838860800 | tf_op jit(solution)/shard_map/pallas_call | solution.py:541
  58.8 0.8 %collective-permute-done.8.refs_2_.refs_1_ = bf16[5,128,128]{2,1,0:T(8,128)(2,1)S(1)} collective-permute-done((bf16[5,128,128]{2,1,0:T(8,128)(2,1)S(1)}, bf16[5,128,128]{2,1,0:T(8,128)(2,1)S(1)}, u32[]{:S(2)}, u32[]{:S(2)}) %collective-permute-start.8) | collective-permute-done | bytes 163872 | tf_op jit(solution)/shard_map/ppermute | solution.py:575
  59.6 1.8 %shard_map.149 = bf16[4,128,128]{2,1,0:T(8,128)(2,1)S(1)} custom-call(bf16[8,128,128]{2,1,0:T(8,128)(2,1)S(1)} %get-tuple-element.46.refs_0_, bf16[5,128,128]{2,1,0:T(8,128)(2,1)S(1)} %collective-permute-done.7.refs_1_, bf16[5,128,128]{2,1,0:T(8,128)(2,1)S(1)} %collective-permute-done.8.refs_2_.refs_1_, f32[2,1,512]{2,1,0:T(1,128)S(1)} %get-tuple-element.78.refs_3_, ...), custom_call_target="tpu_custom_call" | custom-call | flops 1677721600 | tf_op jit(solution)/shard_map/pallas_call | solution.py:541
  61.4 0.1 collective-permute-start.16
  61.4 1.6 %collective-permute-start.15 = (bf16[128,128]{1,0:T(8,128)(2,1)S(1)}, bf16[128,128]{1,0:T(8,128)(2,1)S(1)}, u32[]{:S(2)}, u32[]{:S(2)}) collective-permute-start(bf16[128,128]{1,0:T(8,128)(2,1)S(1)} %get-tuple-element.92), channel_id=1, source_target_pairs={{0,2},{1,3},{2,0},{3,1},{4,6},{5,7},{6,4},{7,5},{8,10},{9,11},{10,... | collective-permute-start | bytes 98312 | tf_op jit(solution)/shard_map/ppermute | solution.py:575
  63.0 1.0 %shard_map.151 = bf16[4,128,128]{2,1,0:T(8,128)(2,1)S(1)} custom-call(bf16[8,128,128]{2,1,0:T(8,128)(2,1)S(1)} %shard_map.142.refs_1_.refs_0_, bf16[5,128,128]{2,1,0:T(8,128)(2,1)S(1)} %collective-permute-done.8.refs_2_.refs_1_, f32[2,1,512]{2,1,0:T(1,128)S(1)} %get-tuple-element.84.refs_2_, f32[2,1,512]{2,1,0:T(1,128)S(1)} %get-tuple-element.85.refs_3_, ...), custom_call_target="tpu_custom_call" | custom-call | flops 838860800 | tf_op jit(solution)/shard_map/pallas_call | solution.py:541
  64.1 0.3 collective-permute-start.14
  64.4 1.5 %collective-permute-start.20 = (bf16[128,128]{1,0:T(8,128)(2,1)S(1)}, bf16[128,128]{1,0:T(8,128)(2,1)S(1)}, u32[]{:S(2)}, u32[]{:S(2)}) collective-permute-start(bf16[128,128]{1,0:T(8,128)(2,1)S(1)} %get-tuple-element.87), channel_id=1, source_target_pairs={{0,7},{1,6},{2,5},{3,4},{4,3},{5,2},{6,1},{7,0},{8,15},{9,14},{10,... | collective-permute-start | bytes 98312 | tf_op jit(solution)/shard_map/ppermute | solution.py:585
  66.0 1.2 %collective-permute-start.19 = (bf16[128,128]{1,0:T(8,128)(2,1)S(1)}, bf16[128,128]{1,0:T(8,128)(2,1)S(1)}, u32[]{:S(2)}, u32[]{:S(2)}) collective-permute-start(bf16[128,128]{1,0:T(8,128)(2,1)S(1)} %get-tuple-element.88), channel_id=1, source_target_pairs={{0,6},{1,7},{2,4},{3,5},{4,2},{5,3},{6,0},{7,1},{8,14},{9,15},{10,... | collective-permute-start | bytes 98312 | tf_op jit(solution)/shard_map/ppermute | solution.py:585
  67.2 0.0 collective-permute-done.16.refs_3_
  67.2 0.5 collective-permute-start.18
  67.7 0.0 collective-permute-done.15.refs_2_
  67.7 1.1 %collective-permute-start.17 = (bf16[128,128]{1,0:T(8,128)(2,1)S(1)}, bf16[128,128]{1,0:T(8,128)(2,1)S(1)}, u32[]{:S(2)}, u32[]{:S(2)}) collective-permute-start(bf16[128,128]{1,0:T(8,128)(2,1)S(1)} %get-tuple-element.90), channel_id=1, source_target_pairs={{0,4},{1,5},{2,6},{3,7},{4,0},{5,1},{6,2},{7,3},{8,12},{9,13},{10,... | collective-permute-start | bytes 98312 | tf_op jit(solution)/shard_map/ppermute | solution.py:585
  68.8 0.0 collective-permute-done.14.refs_1_
  68.8 0.0 collective-permute-done.20.refs_7_
  68.8 2.0 %collective-permute-done.19.refs_6_ = bf16[128,128]{1,0:T(8,128)(2,1)S(1)} collective-permute-done((bf16[128,128]{1,0:T(8,128)(2,1)S(1)}, bf16[128,128]{1,0:T(8,128)(2,1)S(1)}, u32[]{:S(2)}, u32[]{:S(2)}) %collective-permute-start.19) | collective-permute-done | bytes 32800 | tf_op jit(solution)/shard_map/ppermute | solution.py:585
  70.8 0.4 collective-permute-done.18.refs_5_
  71.2 0.8 %collective-permute-done.17.refs_4_ = bf16[128,128]{1,0:T(8,128)(2,1)S(1)} collective-permute-done((bf16[128,128]{1,0:T(8,128)(2,1)S(1)}, bf16[128,128]{1,0:T(8,128)(2,1)S(1)}, u32[]{:S(2)}, u32[]{:S(2)}) %collective-permute-start.17) | collective-permute-done | bytes 32800 | tf_op jit(solution)/shard_map/ppermute | solution.py:585
  72.0 1.6 %shard_map.152 = bf16[128,2048]{1,0:T(8,128)(2,1)} custom-call(bf16[128,2048]{1,0:T(8,128)(2,1)S(1)} %copy-done.1, f32[4,8,512]{2,1,0:T(8,128)S(1)} %bitcast.23, bf16[1024,2048]{1,0:T(8,128)(2,1)S(1)} %copy-done, bf16[128,128]{1,0:T(8,128)(2,1)S(1)} %get-tuple-element.94.refs_0_, bf16[128,128]{1,0:T(8,128)(2,1)S(1)} %collective-permute-done.14.refs_1_, ...), custom_call_target="tpu_custom_call" | custom-call | flops 536870912 | tf_op jit(solution)/shard_map/pallas_call | solution.py:704
  (23 shorter events, 0.1 us)
Async XLA Ops:
  0.0 15.1 %collective-permute-start.4 = (bf16[128,2048]{1,0:T(8,128)(2,1)}, bf16[128,2048]{1,0:T(8,128)(2,1)S(1)}, u32[]{:S(2)}, u32[]{:S(2)}) collective-permute-start(bf16[128,2048]{1,0:T(8,128)(2,1)} %latent_ref.1), channel_id=1, source_target_pairs={{0,2},{1,3},{2,0},{3,1},{4,6},{5,7},{6,4},{7,5},{8,10},{9,11},{10,... | collective-permute-start | bytes 1572872 | tf_op jit(solution)/shard_map/ppermute | solution.py:575
  3.0 25.7 %collective-permute-start.3 = (bf16[128,2048]{1,0:T(8,128)(2,1)}, bf16[128,2048]{1,0:T(8,128)(2,1)S(1)}, u32[]{:S(2)}, u32[]{:S(2)}) collective-permute-start(bf16[128,2048]{1,0:T(8,128)(2,1)} %latent_ref.1), channel_id=1, source_target_pairs={{0,1},{1,0},{2,3},{3,2},{4,5},{5,4},{6,7},{7,6},{8,9},{9,8},{10,11... | collective-permute-start | bytes 1572872 | tf_op jit(solution)/shard_map/ppermute | solution.py:575
  5.1 10.0 %collective-permute-start = (f32[8,512]{1,0:T(8,128)}, f32[8,512]{1,0:T(8,128)S(1)}, u32[]{:S(2)}, u32[]{:S(2)}) collective-permute-start(f32[8,512]{1,0:T(8,128)} %shard_map.136.one_ref), channel_id=1, source_target_pairs={{0,16},{4,20},{8,24},{12,28},{16,0},{20,4},{24,8},{28,12},{1,17},{... | collective-permute-start | bytes 49160 | tf_op jit(solution)/shard_map/ppermute | solution.py:575
  7.8 20.8 %copy-start.8 = (f32[64]{0:T(128)S(1)}, f32[64]{0:T(128)}, u32[]{:S(2)}) copy-start(f32[64]{0:T(128)} %param.25) | copy-start | bytes 772
  7.8 20.8 %copy-start.9 = (f32[64]{0:T(128)S(1)}, f32[64]{0:T(128)}, u32[]{:S(2)}) copy-start(f32[64]{0:T(128)} %param.26) | copy-start | bytes 772
  7.8 20.8 %copy-start.1 = (bf16[128,2048]{1,0:T(8,128)(2,1)S(1)}, bf16[128,2048]{1,0:T(8,128)(2,1)}, u32[]{:S(2)}) copy-start(bf16[128,2048]{1,0:T(8,128)(2,1)} %latent_ref.1) | copy-start | bytes 1572868
  15.1 13.5 %collective-permute-start.5 = (bf16[128,2048]{1,0:T(8,128)(2,1)S(1)}, bf16[128,2048]{1,0:T(8,128)(2,1)S(1)}, u32[]{:S(2)}, u32[]{:S(2)}) collective-permute-start(bf16[128,2048]{1,0:T(8,128)(2,1)S(1)} %collective-permute-done.4.refs_6_), channel_id=1, source_target_pairs={{0,1},{1,0},{2,3},{3,2},{4,5},{5,4},{6,7},{7,6},{8,9},{9,8},{10,11... | collective-permute-start | bytes 1572872 | tf_op jit(solution)/shard_map/ppermute | solution.py:575
  15.1 0.7 copy-start.2
  15.8 12.8 %copy-start.3 = (bf16[2048,256]{1,0:T(8,128)(2,1)S(1)}, bf16[2048,256]{1,0:T(8,128)(2,1)}, u32[]{:S(2)}) copy-start(bf16[2048,256]{1,0:T(8,128)(2,1)} %refs_2_.1) | copy-start | bytes 3145732
  15.8 12.9 %copy-start.4 = (bf16[2048,128]{1,0:T(8,128)(2,1)S(1)}, bf16[2048,128]{1,0:T(8,128)(2,1)}, u32[]{:S(2)}) copy-start(bf16[2048,128]{1,0:T(8,128)(2,1)} %refs_3_.1) | copy-start | bytes 1572868
  15.8 12.9 %copy-start.5 = (bf16[2048,128]{1,0:T(8,128)(2,1)S(1)}, bf16[2048,128]{1,0:T(8,128)(2,1)}, u32[]{:S(2)}) copy-start(bf16[2048,128]{1,0:T(8,128)(2,1)} %refs_4_.1) | copy-start | bytes 1572868
  15.8 12.9 %copy-start.6 = (bf16[64,2048]{1,0:T(8,128)(2,1)S(1)}, bf16[64,2048]{1,0:T(8,128)(2,1)}, u32[]{:S(2)}) copy-start(bf16[64,2048]{1,0:T(8,128)(2,1)} %refs_1_.1) | copy-start | bytes 786436
  15.8 12.9 %copy-start.7 = (f32[2048]{0:T(1024)S(1)}, f32[2048]{0:T(1024)}, u32[]{:S(2)}) copy-start(f32[2048]{0:T(1024)} %param.18) | copy-start | bytes 24580
  15.9 3.8 %collective-permute-start.1 = (f32[8,512]{1,0:T(8,128)S(1)}, f32[8,512]{1,0:T(8,128)S(1)}, u32[]{:S(2)}, u32[]{:S(2)}) collective-permute-start(f32[8,512]{1,0:T(8,128)S(1)} %shard_map.137.one_ref), channel_id=1, source_target_pairs={{0,8},{4,12},{8,0},{12,4},{16,24},{20,28},{24,16},{28,20},{1,9},{5... | collective-permute-start | bytes 49160 | tf_op jit(solution)/shard_map/ppermute | solution.py:575
  19.7 3.7 %collective-permute-start.2 = (f32[8,512]{1,0:T(8,128)S(1)}, f32[8,512]{1,0:T(8,128)S(1)}, u32[]{:S(2)}, u32[]{:S(2)}) collective-permute-start(f32[8,512]{1,0:T(8,128)S(1)} %shard_map.138.one_ref), channel_id=1, source_target_pairs={{0,4},{4,0},{8,12},{12,8},{16,20},{20,16},{24,28},{28,24},{1,5},{5... | collective-permute-start | bytes 49160 | tf_op jit(solution)/shard_map/ppermute | solution.py:575
  31.4 11.7 %collective-permute-start.6 = (bf16[5,128,128]{2,1,0:T(8,128)(2,1)S(1)}, bf16[5,128,128]{2,1,0:T(8,128)(2,1)S(1)}, u32[]{:S(2)}, u32[]{:S(2)}) collective-permute-start(bf16[5,128,128]{2,1,0:T(8,128)(2,1)S(1)} %get-tuple-element.47), channel_id=1, source_target_pairs={{0,4},{4,0},{8,12},{12,8},{16,20},{20,16},{24,28},{28,24},{1,5},{5... | collective-permute-start | bytes 491528 | tf_op jit(solution)/shard_map/ppermute | solution.py:575
  33.2 8.2 %collective-permute-start.10 = (bf16[4,128,128]{2,1,0:T(8,128)(2,1)S(1)}, bf16[4,128,128]{2,1,0:T(8,128)(2,1)S(1)}, u32[]{:S(2)}, u32[]{:S(2)}) collective-permute-start(bf16[4,128,128]{2,1,0:T(8,128)(2,1)S(1)} %get-tuple-element.50.refs_1_.refs_2_), channel_id=1, source_target_pairs={{0,24},{4,28},{8,16},{12,20},{16,8},{20,12},{24,0},{28,4},{1,25},{... | collective-permute-start | bytes 393224 | tf_op jit(solution)/shard_map/ppermute | solution.py:575
  36.8 6.2 %collective-permute-start.9 = (bf16[4,128,128]{2,1,0:T(8,128)(2,1)S(1)}, bf16[4,128,128]{2,1,0:T(8,128)(2,1)S(1)}, u32[]{:S(2)}, u32[]{:S(2)}) collective-permute-start(bf16[4,128,128]{2,1,0:T(8,128)(2,1)S(1)} %get-tuple-element.49), channel_id=1, source_target_pairs={{0,4},{4,0},{8,12},{12,8},{16,20},{20,16},{24,28},{28,24},{1,5},{5... | collective-permute-start | bytes 393224 | tf_op jit(solution)/shard_map/ppermute | solution.py:575
  37.3 12.3 %collective-permute-start.13 = (bf16[4,128,128]{2,1,0:T(8,128)(2,1)S(1)}, bf16[4,128,128]{2,1,0:T(8,128)(2,1)S(1)}, u32[]{:S(2)}, u32[]{:S(2)}) collective-permute-start(bf16[4,128,128]{2,1,0:T(8,128)(2,1)S(1)} %get-tuple-element.50.refs_1_.refs_2_), channel_id=1, source_target_pairs={{0,8},{4,12},{8,0},{12,4},{16,24},{20,28},{24,16},{28,20},{1,9},{5... | collective-permute-start | bytes 393224 | tf_op jit(solution)/shard_map/ppermute | solution.py:575
  41.4 14.6 %collective-permute-start.11 = (bf16[4,128,128]{2,1,0:T(8,128)(2,1)S(1)}, bf16[4,128,128]{2,1,0:T(8,128)(2,1)S(1)}, u32[]{:S(2)}, u32[]{:S(2)}) collective-permute-start(bf16[4,128,128]{2,1,0:T(8,128)(2,1)S(1)} %collective-permute-done.10.refs_2_), channel_id=1, source_target_pairs={{0,8},{4,12},{8,0},{12,4},{16,24},{20,28},{24,16},{28,20},{1,9},{5... | collective-permute-start | bytes 393224 | tf_op jit(solution)/shard_map/ppermute | solution.py:575
  43.2 11.0 %collective-permute-start.12 = (bf16[5,128,128]{2,1,0:T(8,128)(2,1)S(1)}, bf16[5,128,128]{2,1,0:T(8,128)(2,1)S(1)}, u32[]{:S(2)}, u32[]{:S(2)}) collective-permute-start(bf16[5,128,128]{2,1,0:T(8,128)(2,1)S(1)} %shard_map.141.refs_3_), channel_id=1, source_target_pairs={{0,8},{4,12},{8,0},{12,4},{16,24},{20,28},{24,16},{28,20},{1,9},{5... | collective-permute-start | bytes 491528 | tf_op jit(solution)/shard_map/ppermute | solution.py:575
  43.6 10.6 %collective-permute-start.7 = (bf16[5,128,128]{2,1,0:T(8,128)(2,1)S(1)}, bf16[5,128,128]{2,1,0:T(8,128)(2,1)S(1)}, u32[]{:S(2)}, u32[]{:S(2)}) collective-permute-start(bf16[5,128,128]{2,1,0:T(8,128)(2,1)S(1)} %shard_map.141.refs_3_), channel_id=1, source_target_pairs={{0,24},{4,28},{8,16},{12,20},{16,8},{20,12},{24,0},{28,4},{1,25},{... | collective-permute-start | bytes 491528 | tf_op jit(solution)/shard_map/ppermute | solution.py:575
  54.2 5.3 %collective-permute-start.8 = (bf16[5,128,128]{2,1,0:T(8,128)(2,1)S(1)}, bf16[5,128,128]{2,1,0:T(8,128)(2,1)S(1)}, u32[]{:S(2)}, u32[]{:S(2)}) collective-permute-start(bf16[5,128,128]{2,1,0:T(8,128)(2,1)S(1)} %collective-permute-done.7.refs_1_), channel_id=1, source_target_pairs={{0,8},{4,12},{8,0},{12,4},{16,24},{20,28},{24,16},{28,20},{1,9},{5... | collective-permute-start | bytes 491528 | tf_op jit(solution)/shard_map/ppermute | solution.py:575
  59.6 12.4 %copy-start = (bf16[1024,2048]{1,0:T(8,128)(2,1)S(1)}, bf16[1024,2048]{1,0:T(8,128)(2,1)}, u32[]{:S(2)}) copy-start(bf16[1024,2048]{1,0:T(8,128)(2,1)} %weight_ref.1) | copy-start | bytes 12582916
  61.4 5.8 %collective-permute-start.16 = (bf16[128,128]{1,0:T(8,128)(2,1)S(1)}, bf16[128,128]{1,0:T(8,128)(2,1)S(1)}, u32[]{:S(2)}, u32[]{:S(2)}) collective-permute-start(bf16[128,128]{1,0:T(8,128)(2,1)S(1)} %get-tuple-element.91), channel_id=1, source_target_pairs={{0,3},{1,2},{2,1},{3,0},{4,7},{5,6},{6,5},{7,4},{8,11},{9,10},{10,... | collective-permute-start | bytes 98312 | tf_op jit(solution)/shard_map/ppermute | solution.py:575
  61.4 6.3 %collective-permute-start.15 = (bf16[128,128]{1,0:T(8,128)(2,1)S(1)}, bf16[128,128]{1,0:T(8,128)(2,1)S(1)}, u32[]{:S(2)}, u32[]{:S(2)}) collective-permute-start(bf16[128,128]{1,0:T(8,128)(2,1)S(1)} %get-tuple-element.92), channel_id=1, source_target_pairs={{0,2},{1,3},{2,0},{3,1},{4,6},{5,7},{6,4},{7,5},{8,10},{9,11},{10,... | collective-permute-start | bytes 98312 | tf_op jit(solution)/shard_map/ppermute | solution.py:575
  64.1 4.8 %collective-permute-start.14 = (bf16[128,128]{1,0:T(8,128)(2,1)S(1)}, bf16[128,128]{1,0:T(8,128)(2,1)S(1)}, u32[]{:S(2)}, u32[]{:S(2)}) collective-permute-start(bf16[128,128]{1,0:T(8,128)(2,1)S(1)} %get-tuple-element.93), channel_id=1, source_target_pairs={{0,1},{1,0},{2,3},{3,2},{4,5},{5,4},{6,7},{7,6},{8,9},{9,8},{10,11... | collective-permute-start | bytes 98312 | tf_op jit(solution)/shard_map/ppermute | solution.py:575
  64.4 4.4 %collective-permute-start.20 = (bf16[128,128]{1,0:T(8,128)(2,1)S(1)}, bf16[128,128]{1,0:T(8,128)(2,1)S(1)}, u32[]{:S(2)}, u32[]{:S(2)}) collective-permute-start(bf16[128,128]{1,0:T(8,128)(2,1)S(1)} %get-tuple-element.87), channel_id=1, source_target_pairs={{0,7},{1,6},{2,5},{3,4},{4,3},{5,2},{6,1},{7,0},{8,15},{9,14},{10,... | collective-permute-start | bytes 98312 | tf_op jit(solution)/shard_map/ppermute | solution.py:585
  66.0 4.8 %collective-permute-start.19 = (bf16[128,128]{1,0:T(8,128)(2,1)S(1)}, bf16[128,128]{1,0:T(8,128)(2,1)S(1)}, u32[]{:S(2)}, u32[]{:S(2)}) collective-permute-start(bf16[128,128]{1,0:T(8,128)(2,1)S(1)} %get-tuple-element.88), channel_id=1, source_target_pairs={{0,6},{1,7},{2,4},{3,5},{4,2},{5,3},{6,0},{7,1},{8,14},{9,15},{10,... | collective-permute-start | bytes 98312 | tf_op jit(solution)/shard_map/ppermute | solution.py:585
  67.2 4.0 %collective-permute-start.18 = (bf16[128,128]{1,0:T(8,128)(2,1)S(1)}, bf16[128,128]{1,0:T(8,128)(2,1)S(1)}, u32[]{:S(2)}, u32[]{:S(2)}) collective-permute-start(bf16[128,128]{1,0:T(8,128)(2,1)S(1)} %get-tuple-element.89), channel_id=1, source_target_pairs={{0,5},{1,4},{2,7},{3,6},{4,1},{5,0},{6,3},{7,2},{8,13},{9,12},{10,... | collective-permute-start | bytes 98312 | tf_op jit(solution)/shard_map/ppermute | solution.py:585
  67.7 4.3 %collective-permute-start.17 = (bf16[128,128]{1,0:T(8,128)(2,1)S(1)}, bf16[128,128]{1,0:T(8,128)(2,1)S(1)}, u32[]{:S(2)}, u32[]{:S(2)}) collective-permute-start(bf16[128,128]{1,0:T(8,128)(2,1)S(1)} %get-tuple-element.90), channel_id=1, source_target_pairs={{0,4},{1,5},{2,6},{3,7},{4,0},{5,1},{6,2},{7,3},{8,12},{9,13},{10,... | collective-permute-start | bytes 98312 | tf_op jit(solution)/shard_map/ppermute | solution.py:585

commit v5 on v4

--- a/solution.py
+++ b/solution.py
@@ -442,11 +442,11 @@
             queries[i, g, 1] = jnp.concatenate([blank, high, blank, low], axis=0)
             if started:
                 states[i, g] = tuple(ref[g] for ref in old)
-            tiles += [(i, g, place) for place in wanted]
-    tiles.sort(key=lambda tile: tile[2])
+            tiles += [(i, g, place, part) for place in wanted for part in halves]
+    tiles.sort(key=lambda tile: tile[2:])
 
     def scores(tile):
-        i, g, place = tile
+        i, g, place, part = tile
         ref = kv_refs[place]
         context = ref.shape[0] > 2 * pairs
         keys = [ref[p] for p in range(pairs)]
@@ -454,15 +454,11 @@
             keys.append(ref[2 * pairs, 0:span, :])
         keys = jnp.concatenate(keys, axis=0)
         keys = jnp.concatenate([keys, keys], axis=1)
-        made = []
-        for half in halves:
-            found = jnp.dot(keys, queries[i, g, half], preferred_element_type=jnp.float32)
-            if context:
-                rows = found.shape[0] - span
-                made += [found[:rows], found[rows:] + offset * LOG2E]
-            else:
-                made.append(found)
-        return jnp.concatenate(made, axis=0)
+        found = jnp.dot(keys, queries[i, g, part], preferred_element_type=jnp.float32)
+        if context:
+            rows = found.shape[0] - span
+            found = jnp.concatenate([found[:rows], found[rows:] + offset * LOG2E], axis=0)
+        return found
 
     def soften(tile, found):
         place = tile[:2]
@@ -481,12 +477,10 @@
 
     def gather(tile, shares, shrink):
         ref = kv_refs[tile[2]]
-        values = []
-        for half in halves:
-            rows = slice(half * span, (half + 1) * span)
-            values += [ref[pairs + p, rows, :] for p in range(pairs)]
-            if ref.shape[0] > 2 * pairs:
-                values.append(ref[2 * pairs, span : 2 * span, rows])
+        rows = slice(tile[3] * span, (tile[3] + 1) * span)
+        values = [ref[pairs + p, rows, :] for p in range(pairs)]
+        if ref.shape[0] > 2 * pairs:
+            values.append(ref[2 * pairs, span : 2 * span, rows])
         weighted = jnp.dot(
             jnp.concatenate(values, axis=1), shares, preferred_element_type=jnp.float32
         )
@@ -684,18 +678,22 @@
     near = xor_move(give_kv, "sp", 1)
     near_q = xor_move(give_q, "sp", 1)
     up = xor_move(keep_kv, "sp", 2)
-    down = xor_move(keep_kv, "sp", 6)
+    down = xor_move(keep_kv, "sp", 4)
     near = merge(near, keep_ctx)
-    near_down = xor_move(near, "sp", 6)
+    near_down = xor_move(near, "sp", 4)
     near_up = xor_move(near, "sp", 2)
     across = xor_move(down, "sp", 2)
     near_across = xor_move(near_down, "sp", 2)
     (own,) = attend([(keep_q, None, [0])], [keep_kv], offset)
+    (own,) = attend([(keep_q, own, [0])], [near], offset)
     near_q = ready(near_q)
-    own, other = attend([(keep_q, own, [1]), (near_q, None, [0, 1])], [keep_kv, near], offset)
-    for piece in (up, down, near_up, across):
-        own, other = attend([(keep_q, own, [0]), (near_q, other, [0])], [piece], offset)
-    (other,) = attend([(near_q, other, [0])], [near_down], offset)
+    own, other = attend(
+        [(keep_q, own, [2, 3]), (near_q, None, [0, 1, 2, 3])], [keep_kv, near, up, down], offset
+    )
+    own, other = attend(
+        [(keep_q, own, [0]), (near_q, other, [0, 1])], [near_up, near_down], offset
+    )
+    own, other = attend([(keep_q, own, [0]), (near_q, other, [0])], [across], offset)
     ((other,),) = attend([(near_q, other, [0])], [near_across], offset, True)
     ((own,),) = attend([(keep_q, own, [0, 1])], [near_down, near_across], offset, True)
     sent = [cross_move(other[j], j) for j in range(head_split)]

time: 73.9 us -> 75 us (1.015)
  starting transfers between devices: 27.3 us -> 30.3 us
  waiting for transfers between devices: 19.6 us -> 18.4 us
    ppermute x17, starting transfers between devices: 22.9 us -> 25.8 us  [xor_move(): return lax.ppermute(member, axis, [(i, i ^ mask) for i in range(size)])]
    ppermute x4, waiting for transfers between devices: 3.16 us -> 0.56 us  [cross_move(): return lax.ppermute(member, ('sp', 'tp'), pairs)]
    ppermute x17, waiting for transfers between devices: 16.4 us -> 17.8 us  [xor_move(): return lax.ppermute(member, axis, [(i, i ^ mask) for i in range(size)])]
    pallas_call x9 -> x7, Pallas kernels: 13.6 us -> 12.9 us  [attend(): kernel_call(body, out * len(sources), len(inputs), 40 * 2 * lanes * keys...]
  transfers between devices with their start and end apart: 21 -> 21, of which waited for: 9 -> 8; matrix products, arithmetic and copies ran while one was open for 1% -> 1% of each run, Pallas kernels for 19% -> 19%
where the time goes in v5:
time: 75 us; the launch traced here: 74.7 us
  starting transfers between devices  30.3 us (40%)
  Pallas kernels  19.4 us (26%)
  waiting for transfers between devices  18.4 us (25%)
  blocking collectives  5.22 us (7%)
  local copies, waits for them, and re-layouts  0.78 us (1%)
    ppermute x17, starting transfers between devices, xor_move(): return lax.ppermute(member, axis, [(i, i ^ mask) for i in range(size)])  25.8 us
    ppermute x17, waiting for transfers between devices, xor_move(): return lax.ppermute(member, axis, [(i, i ^ mask) for i in range(size)])  17.8 us
    pallas_call x7, Pallas kernels, attend(): kernel_call(body, out * len(sources), len(inputs), 40 * 2 * lanes * keys...  12.9 us
    all_gather x1, blocking collectives, inner_device(): modulation = lax.all_gather(part, 'tp', axis=0, tiled=False)  5.22 us
    ppermute x4, starting transfers between devices, cross_move(): return lax.ppermute(member, ('sp', 'tp'), pairs)  4.51 us
    pallas_call x1, Pallas kernels, inner_device(): pl.pallas_call(lambda *refs: projection_body(q_heads, kv_heads, *refs), o...  2.67 us
    pallas_call x1, Pallas kernels, opening(): pl.pallas_call(opening_body, out_shape=jax.ShapeDtypeStruct((8, columns),...  2.08 us
    pallas_call x1, Pallas kernels, inner_device(): kernel_call(output_body, jax.ShapeDtypeStruct(latent.shape, jnp.bfloat16)...  1.59 us
  transfers between devices with their start and end apart: 21, of which 8 were waited for; matrix products, arithmetic and copies ran while one was open for 1% of the time, Pallas kernels for 19%

profile of v5, /device:TPU:0, one launch (start us, length us, event | category | flops | bytes accessed | tf_op | source)
XLA Modules:
  0.0 74.7 jit_solution(11759910481036937096)
XLA Ops:
  0.0 3.0 %collective-permute-start.4 = (bf16[128,2048]{1,0:T(8,128)(2,1)}, bf16[128,2048]{1,0:T(8,128)(2,1)S(1)}, u32[]{:S(2)}, u32[]{:S(2)}) collective-permute-start(bf16[128,2048]{1,0:T(8,128)(2,1)} %latent_ref.1), channel_id=1, source_target_pairs={{0,2},{1,3},{2,0},{3,1},{4,6},{5,7},{6,4},{7,5},{8,10},{9,11},{10,... | collective-permute-start | bytes 1572872 | tf_op jit(solution)/shard_map/ppermute | solution.py:569
  3.0 0.0 collective-permute-start.3
  3.0 2.1 %shard_map.136.one_ref = f32[8,512]{1,0:T(8,128)} custom-call(f32[1,2048]{1,0:T(1,128)} %bitcast.27, f32[1,2048]{1,0:T(1,128)} %bitcast.28, bf16[256,512]{1,0:T(8,128)(2,1)} %shift_hbm.1, bf16[256,512]{1,0:T(8,128)(2,1)} %scale_hbm.1, bf16[256,512]{1,0:T(8,128)(2,1)} %gate_hbm.1), custom_call_target="tpu_custom_call" | custom-call | flops 100000000 | tf_op jit(solution)/shard_map/pallas_call | solution.py:276
  5.1 2.7 %collective-permute-start = (f32[8,512]{1,0:T(8,128)}, f32[8,512]{1,0:T(8,128)S(1)}, u32[]{:S(2)}, u32[]{:S(2)}) collective-permute-start(f32[8,512]{1,0:T(8,128)} %shard_map.136.one_ref), channel_id=1, source_target_pairs={{0,16},{4,20},{8,24},{12,28},{16,0},{20,4},{24,8},{28,12},{1,17},{... | collective-permute-start | bytes 49160 | tf_op jit(solution)/shard_map/ppermute | solution.py:569
  7.7 0.1 fusion.2
  7.8 0.0 copy-start.9
  7.8 0.0 copy-start.1
  7.8 7.3 %collective-permute-done.4.refs_6_ = bf16[128,2048]{1,0:T(8,128)(2,1)S(1)} collective-permute-done((bf16[128,2048]{1,0:T(8,128)(2,1)}, bf16[128,2048]{1,0:T(8,128)(2,1)S(1)}, u32[]{:S(2)}, u32[]{:S(2)}) %collective-permute-start.4) | collective-permute-done | bytes 524320 | tf_op jit(solution)/shard_map/ppermute | solution.py:569
  15.1 0.0 collective-permute-start.5
  15.1 0.0 collective-permute-done.other_ref
  15.1 0.7 copy-done.2
  15.8 0.0 copy-start.7
  15.9 1.9 %collective-permute-start.1 = (f32[8,512]{1,0:T(8,128)S(1)}, f32[8,512]{1,0:T(8,128)S(1)}, u32[]{:S(2)}, u32[]{:S(2)}) collective-permute-start(f32[8,512]{1,0:T(8,128)S(1)} %shard_map.137.one_ref), channel_id=1, source_target_pairs={{0,8},{4,12},{8,0},{12,4},{16,24},{20,28},{24,16},{28,20},{1,9},{5... | collective-permute-start | bytes 49160 | tf_op jit(solution)/shard_map/ppermute | solution.py:569
  17.8 0.3 fusion
  18.1 1.6 %collective-permute-done.1.other_ref = f32[8,512]{1,0:T(8,128)S(1)} collective-permute-done((f32[8,512]{1,0:T(8,128)S(1)}, f32[8,512]{1,0:T(8,128)S(1)}, u32[]{:S(2)}, u32[]{:S(2)}) %collective-permute-start.1) | collective-permute-done | bytes 16416 | tf_op jit(solution)/shard_map/ppermute | solution.py:569
  19.7 1.8 %collective-permute-start.2 = (f32[8,512]{1,0:T(8,128)S(1)}, f32[8,512]{1,0:T(8,128)S(1)}, u32[]{:S(2)}, u32[]{:S(2)}) collective-permute-start(f32[8,512]{1,0:T(8,128)S(1)} %shard_map.138.one_ref), channel_id=1, source_target_pairs={{0,4},{4,0},{8,12},{12,8},{16,20},{20,16},{24,28},{28,24},{1,5},{5... | collective-permute-start | bytes 49160 | tf_op jit(solution)/shard_map/ppermute | solution.py:569
  21.5 1.9 %collective-permute-done.2.other_ref = f32[8,512]{1,0:T(8,128)S(1)} collective-permute-done((f32[8,512]{1,0:T(8,128)S(1)}, f32[8,512]{1,0:T(8,128)S(1)}, u32[]{:S(2)}, u32[]{:S(2)}) %collective-permute-start.2) | collective-permute-done | bytes 16416 | tf_op jit(solution)/shard_map/ppermute | solution.py:569
  23.4 5.2 %all-gather = f32[32,512]{1,0:T(8,128)S(1)} all-gather(f32[8,512]{1,0:T(8,128)S(1)} %shard_map.139), channel_id=2, replica_groups=mesh['sp'=8,'tp'=4] {'tp'}, dimensions={0}, use_global_device_ids=true | all-gather | bytes 81920 | tf_op jit(solution)/shard_map/all_gather | solution.py:641
  28.6 0.0 collective-permute-done.3.refs_5_
  28.6 0.0 collective-permute-done.5.refs_7_
  28.6 0.0 copy-done.8
  28.6 0.0 copy-done.9
  28.7 0.0 copy-done.1
  28.7 2.7 %shard_map.140 = (bf16[8,128,128]{2,1,0:T(8,128)(2,1)S(1)}, bf16[4,128,128]{2,1,0:T(8,128)(2,1)S(1)}, bf16[128,128]{1,0:T(8,128)(2,1)S(1)}, bf16[4,128,128]{2,1,0:T(8,128)(2,1)S(1)}, bf16[5,128,128]{2,1,0:T(8,128)(2,1)S(1)}) custom-call(bf16[128,2048]{1,0:T(8,128)(2,1)S(1)} %copy-done.1, bf16[64,2048]{1,0:T(8,128)(2,1)S(1)} %copy-done.6, ...), custom_call_target="tpu_custom_call" | custom-call | flops 2147483648 | tf_op jit(solution)/shard_map/pallas_call | solution.py:646
  31.4 1.8 %collective-permute-start.6 = (bf16[5,128,128]{2,1,0:T(8,128)(2,1)S(1)}, bf16[5,128,128]{2,1,0:T(8,128)(2,1)S(1)}, u32[]{:S(2)}, u32[]{:S(2)}) collective-permute-start(bf16[5,128,128]{2,1,0:T(8,128)(2,1)S(1)} %get-tuple-element.35), channel_id=1, source_target_pairs={{0,4},{4,0},{8,12},{12,8},{16,20},{20,16},{24,28},{28,24},{1,5},{5... | collective-permute-start | bytes 491528 | tf_op jit(solution)/shard_map/ppermute | solution.py:569
  33.2 2.6 %collective-permute-start.10 = (bf16[4,128,128]{2,1,0:T(8,128)(2,1)S(1)}, bf16[4,128,128]{2,1,0:T(8,128)(2,1)S(1)}, u32[]{:S(2)}, u32[]{:S(2)}) collective-permute-start(bf16[4,128,128]{2,1,0:T(8,128)(2,1)S(1)} %get-tuple-element.38.refs_1_.refs_2_), channel_id=1, source_target_pairs={{0,16},{4,20},{8,24},{12,28},{16,0},{20,4},{24,8},{28,12},{1,17},{... | collective-permute-start | bytes 393224 | tf_op jit(solution)/shard_map/ppermute | solution.py:569
  35.8 0.5 collective-permute-start.9
  36.3 1.6 %collective-permute-start.13 = (bf16[4,128,128]{2,1,0:T(8,128)(2,1)S(1)}, bf16[4,128,128]{2,1,0:T(8,128)(2,1)S(1)}, u32[]{:S(2)}, u32[]{:S(2)}) collective-permute-start(bf16[4,128,128]{2,1,0:T(8,128)(2,1)S(1)} %get-tuple-element.38.refs_1_.refs_2_), channel_id=1, source_target_pairs={{0,8},{4,12},{8,0},{12,4},{16,24},{20,28},{24,16},{28,20},{1,9},{5... | collective-permute-start | bytes 393224 | tf_op jit(solution)/shard_map/ppermute | solution.py:569
  37.9 0.8 %shard_map.143 = (f32[2,1,512]{2,1,0:T(1,128)S(1)}, f32[2,1,512]{2,1,0:T(1,128)S(1)}, f32[2,64,512]{2,1,0:T(8,128)S(1)}) custom-call(bf16[8,128,128]{2,1,0:T(8,128)(2,1)S(1)} %get-tuple-element.34.refs_0_, bf16[4,128,128]{2,1,0:T(8,128)(2,1)S(1)} %get-tuple-element.38.refs_1_.refs_2_), custom_call_target="tpu_custom_call" | custom-call | flops 671088640 | tf_op jit(solution)/shard_map/pallas_call | solution.py:535
  38.8 3.7 %collective-permute-done.10.refs_5_ = bf16[4,128,128]{2,1,0:T(8,128)(2,1)S(1)} collective-permute-done((bf16[4,128,128]{2,1,0:T(8,128)(2,1)S(1)}, bf16[4,128,128]{2,1,0:T(8,128)(2,1)S(1)}, u32[]{:S(2)}, u32[]{:S(2)}) %collective-permute-start.10) | collective-permute-done | bytes 131104 | tf_op jit(solution)/shard_map/ppermute | solution.py:569
  42.5 0.6 collective-permute-start.11
  43.1 0.0 collective-permute-done.9.q_ref
  43.1 0.0 collective-permute-done.6.near_ref
  43.1 0.1 shard_map.141.refs_1_.refs_3_
  43.2 1.5 %collective-permute-start.12 = (bf16[5,128,128]{2,1,0:T(8,128)(2,1)S(1)}, bf16[5,128,128]{2,1,0:T(8,128)(2,1)S(1)}, u32[]{:S(2)}, u32[]{:S(2)}) collective-permute-start(bf16[5,128,128]{2,1,0:T(8,128)(2,1)S(1)} %shard_map.141.refs_1_.refs_3_), channel_id=1, source_target_pairs={{0,8},{4,12},{8,0},{12,4},{16,24},{20,28},{24,16},{28,20},{1,9},{5... | collective-permute-start | bytes 491528 | tf_op jit(solution)/shard_map/ppermute | solution.py:569
  44.7 2.0 %collective-permute-start.7 = (bf16[5,128,128]{2,1,0:T(8,128)(2,1)S(1)}, bf16[5,128,128]{2,1,0:T(8,128)(2,1)S(1)}, u32[]{:S(2)}, u32[]{:S(2)}) collective-permute-start(bf16[5,128,128]{2,1,0:T(8,128)(2,1)S(1)} %shard_map.141.refs_1_.refs_3_), channel_id=1, source_target_pairs={{0,16},{4,20},{8,24},{12,28},{16,0},{20,4},{24,8},{28,12},{1,17},{... | collective-permute-start | bytes 491528 | tf_op jit(solution)/shard_map/ppermute | solution.py:569
  46.7 1.0 %shard_map.144 = (f32[2,1,512]{2,1,0:T(1,128)S(1)}, f32[2,1,512]{2,1,0:T(1,128)S(1)}, f32[2,64,512]{2,1,0:T(8,128)S(1)}) custom-call(bf16[8,128,128]{2,1,0:T(8,128)(2,1)S(1)} %get-tuple-element.34.refs_0_, bf16[5,128,128]{2,1,0:T(8,128)(2,1)S(1)} %shard_map.141.refs_1_.refs_3_, f32[2,1,512]{2,1,0:T(1,128)S(1)} %get-tuple-element.39.refs_2_, ...), custom_call_target="tpu_custom_call" | custom-call | flops 838860800 | tf_op jit(solution)/shard_map/pallas_call | solution.py:535
  47.7 0.0 collective-permute-done.13.refs_4_
  47.7 3.9 %shard_map.145 = (f32[2,1,512]{2,1,0:T(1,128)S(1)}, f32[2,1,512]{2,1,0:T(1,128)S(1)}, f32[2,64,512]{2,1,0:T(8,128)S(1)}, f32[2,1,512]{2,1,0:T(1,128)S(1)}, f32[2...) custom-call(bf16[8,128,128]{2,1,0:T(8,128)(2,1)S(1)} %get-tuple-element.34.refs_0_, ...), custom_call_target="tpu_custom_call" | custom-call | flops 4194304000 | tf_op jit(solution)/shard_map/pallas_call | solution.py:535
  51.6 1.5 %collective-permute-done.7.refs_3_.refs_1_ = bf16[5,128,128]{2,1,0:T(8,128)(2,1)S(1)} collective-permute-done((bf16[5,128,128]{2,1,0:T(8,128)(2,1)S(1)}, bf16[5,128,128]{2,1,0:T(8,128)(2,1)S(1)}, u32[]{:S(2)}, u32[]{:S(2)}) %collective-permute-start.7) | collective-permute-done | bytes 163872 | tf_op jit(solution)/shard_map/ppermute | solution.py:569
  53.1 4.1 %collective-permute-start.8 = (bf16[5,128,128]{2,1,0:T(8,128)(2,1)S(1)}, bf16[5,128,128]{2,1,0:T(8,128)(2,1)S(1)}, u32[]{:S(2)}, u32[]{:S(2)}) collective-permute-start(bf16[5,128,128]{2,1,0:T(8,128)(2,1)S(1)} %collective-permute-done.7.refs_3_.refs_1_), channel_id=1, source_target_pairs={{0,8},{4,12},{8,0},{12,4},{16,24},{20,28},{24,16},{28,20},{1,9},{5... | collective-permute-start | bytes 491528 | tf_op jit(solution)/shard_map/ppermute | solution.py:569
  57.2 0.0 collective-permute-done.12.refs_2_
  57.2 2.6 %shard_map.146 = (f32[2,1,512]{2,1,0:T(1,128)S(1)}, f32[2,1,512]{2,1,0:T(1,128)S(1)}, f32[2,64,512]{2,1,0:T(8,128)S(1)}, f32[2,1,512]{2,1,0:T(1,128)S(1)}, f32[2...) custom-call(bf16[8,128,128]{2,1,0:T(8,128)(2,1)S(1)} %get-tuple-element.34.refs_0_, ...), custom_call_target="tpu_custom_call" | custom-call | flops 2516582400 | tf_op jit(solution)/shard_map/pallas_call | solution.py:535
  59.8 0.0 collective-permute-done.11.refs_2_
  59.8 1.7 %shard_map.147 = (f32[2,1,512]{2,1,0:T(1,128)S(1)}, f32[2,1,512]{2,1,0:T(1,128)S(1)}, f32[2,64,512]{2,1,0:T(8,128)S(1)}, f32[2,1,512]{2,1,0:T(1,128)S(1)}, f32[2...) custom-call(bf16[8,128,128]{2,1,0:T(8,128)(2,1)S(1)} %get-tuple-element.34.refs_0_, ...), custom_call_target="tpu_custom_call" | custom-call | flops 1342177280 | tf_op jit(solution)/shard_map/pallas_call | solution.py:535
  61.5 0.0 collective-permute-done.8.refs_2_.refs_1_
  61.5 0.0 copy-start
  61.5 1.0 %shard_map.149 = bf16[4,128,128]{2,1,0:T(8,128)(2,1)S(1)} custom-call(bf16[8,128,128]{2,1,0:T(8,128)(2,1)S(1)} %shard_map.142.refs_1_.refs_0_, bf16[5,128,128]{2,1,0:T(8,128)(2,1)S(1)} %collective-permute-done.8.refs_2_.refs_1_, f32[2,1,512]{2,1,0:T(1,128)S(1)} %get-tuple-element.60.refs_2_, f32[2,1,512]{2,1,0:T(1,128)S(1)} %get-tuple-element.61.refs_3_, ...), custom_call_target="tpu_custom_call" | custom-call | flops 838860800 | tf_op jit(solution)/shard_map/pallas_call | solution.py:535
  62.5 0.3 collective-permute-start.20
  62.8 1.5 %collective-permute-start.19 = (bf16[128,128]{1,0:T(8,128)(2,1)S(1)}, bf16[128,128]{1,0:T(8,128)(2,1)S(1)}, u32[]{:S(2)}, u32[]{:S(2)}) collective-permute-start(bf16[128,128]{1,0:T(8,128)(2,1)S(1)} %get-tuple-element.64), channel_id=1, source_target_pairs={{0,6},{1,7},{2,4},{3,5},{4,2},{5,3},{6,0},{7,1},{8,14},{9,15},{10,... | collective-permute-start | bytes 98312 | tf_op jit(solution)/shard_map/ppermute | solution.py:579
  64.3 1.8 %shard_map.148 = bf16[4,128,128]{2,1,0:T(8,128)(2,1)S(1)} custom-call(bf16[8,128,128]{2,1,0:T(8,128)(2,1)S(1)} %get-tuple-element.34.refs_0_, bf16[5,128,128]{2,1,0:T(8,128)(2,1)S(1)} %collective-permute-done.7.refs_3_.refs_1_, bf16[5,128,128]{2,1,0:T(8,128)(2,1)S(1)} %collective-permute-done.8.refs_2_.refs_1_, f32[2,1,512]{2,1,0:T(1,128)S(1)} %get-tuple-element.57.refs_3_, ...), custom_call_target="tpu_custom_call" | custom-call | flops 1677721600 | tf_op jit(solution)/shard_map/pallas_call | solution.py:535
  66.2 1.3 %collective-permute-start.18 = (bf16[128,128]{1,0:T(8,128)(2,1)S(1)}, bf16[128,128]{1,0:T(8,128)(2,1)S(1)}, u32[]{:S(2)}, u32[]{:S(2)}) collective-permute-start(bf16[128,128]{1,0:T(8,128)(2,1)S(1)} %get-tuple-element.65), channel_id=1, source_target_pairs={{0,5},{1,4},{2,7},{3,6},{4,1},{5,0},{6,3},{7,2},{8,13},{9,12},{10,... | collective-permute-start | bytes 98312 | tf_op jit(solution)/shard_map/ppermute | solution.py:579
  67.5 1.5 %collective-permute-start.17 = (bf16[128,128]{1,0:T(8,128)(2,1)S(1)}, bf16[128,128]{1,0:T(8,128)(2,1)S(1)}, u32[]{:S(2)}, u32[]{:S(2)}) collective-permute-start(bf16[128,128]{1,0:T(8,128)(2,1)S(1)} %get-tuple-element.66), channel_id=1, source_target_pairs={{0,4},{1,5},{2,6},{3,7},{4,0},{5,1},{6,2},{7,3},{8,12},{9,13},{10,... | collective-permute-start | bytes 98312 | tf_op jit(solution)/shard_map/ppermute | solution.py:579
  68.9 0.3 collective-permute-start.16
  69.2 0.0 collective-permute-done.20.refs_7_
  69.2 1.2 %collective-permute-start.15 = (bf16[128,128]{1,0:T(8,128)(2,1)S(1)}, bf16[128,128]{1,0:T(8,128)(2,1)S(1)}, u32[]{:S(2)}, u32[]{:S(2)}) collective-permute-start(bf16[128,128]{1,0:T(8,128)(2,1)S(1)} %get-tuple-element.68), channel_id=1, source_target_pairs={{0,2},{1,3},{2,0},{3,1},{4,6},{5,7},{6,4},{7,5},{8,10},{9,11},{10,... | collective-permute-start | bytes 98312 | tf_op jit(solution)/shard_map/ppermute | solution.py:569
  70.4 0.0 collective-permute-done.19.refs_6_
  70.4 0.4 collective-permute-start.14
  70.8 0.0 collective-permute-done.18.refs_5_
  70.8 0.6 collective-permute-done.17.refs_4_
  71.4 1.2 %collective-permute-done.16.refs_3_ = bf16[128,128]{1,0:T(8,128)(2,1)S(1)} collective-permute-done((bf16[128,128]{1,0:T(8,128)(2,1)S(1)}, bf16[128,128]{1,0:T(8,128)(2,1)S(1)}, u32[]{:S(2)}, u32[]{:S(2)}) %collective-permute-start.16) | collective-permute-done | bytes 32800 | tf_op jit(solution)/shard_map/ppermute | solution.py:569
  72.6 0.6 collective-permute-done.15.refs_2_
  73.1 0.0 collective-permute-done.14.refs_1_
  73.2 1.6 %shard_map.150 = bf16[128,2048]{1,0:T(8,128)(2,1)} custom-call(bf16[128,2048]{1,0:T(8,128)(2,1)S(1)} %copy-done.1, f32[4,8,512]{2,1,0:T(8,128)S(1)} %bitcast.23, bf16[1024,2048]{1,0:T(8,128)(2,1)S(1)} %copy-done, bf16[128,128]{1,0:T(8,128)(2,1)S(1)} %get-tuple-element.70.refs_0_, bf16[128,128]{1,0:T(8,128)(2,1)S(1)} %collective-permute-done.14.refs_1_, ...), custom_call_target="tpu_custom_call" | custom-call | flops 536870912 | tf_op jit(solution)/shard_map/pallas_call | solution.py:702
  (21 shorter events, 0.1 us)
Async XLA Ops:
  0.0 15.1 %collective-permute-start.4 = (bf16[128,2048]{1,0:T(8,128)(2,1)}, bf16[128,2048]{1,0:T(8,128)(2,1)S(1)}, u32[]{:S(2)}, u32[]{:S(2)}) collective-permute-start(bf16[128,2048]{1,0:T(8,128)(2,1)} %latent_ref.1), channel_id=1, source_target_pairs={{0,2},{1,3},{2,0},{3,1},{4,6},{5,7},{6,4},{7,5},{8,10},{9,11},{10,... | collective-permute-start | bytes 1572872 | tf_op jit(solution)/shard_map/ppermute | solution.py:569
  3.0 25.7 %collective-permute-start.3 = (bf16[128,2048]{1,0:T(8,128)(2,1)}, bf16[128,2048]{1,0:T(8,128)(2,1)S(1)}, u32[]{:S(2)}, u32[]{:S(2)}) collective-permute-start(bf16[128,2048]{1,0:T(8,128)(2,1)} %latent_ref.1), channel_id=1, source_target_pairs={{0,1},{1,0},{2,3},{3,2},{4,5},{5,4},{6,7},{7,6},{8,9},{9,8},{10,11... | collective-permute-start | bytes 1572872 | tf_op jit(solution)/shard_map/ppermute | solution.py:569
  5.1 10.0 %collective-permute-start = (f32[8,512]{1,0:T(8,128)}, f32[8,512]{1,0:T(8,128)S(1)}, u32[]{:S(2)}, u32[]{:S(2)}) collective-permute-start(f32[8,512]{1,0:T(8,128)} %shard_map.136.one_ref), channel_id=1, source_target_pairs={{0,16},{4,20},{8,24},{12,28},{16,0},{20,4},{24,8},{28,12},{1,17},{... | collective-permute-start | bytes 49160 | tf_op jit(solution)/shard_map/ppermute | solution.py:569
  7.8 20.8 %copy-start.8 = (f32[64]{0:T(128)S(1)}, f32[64]{0:T(128)}, u32[]{:S(2)}) copy-start(f32[64]{0:T(128)} %param.25) | copy-start | bytes 772
  7.8 20.8 %copy-start.9 = (f32[64]{0:T(128)S(1)}, f32[64]{0:T(128)}, u32[]{:S(2)}) copy-start(f32[64]{0:T(128)} %param.26) | copy-start | bytes 772
  7.8 20.8 %copy-start.1 = (bf16[128,2048]{1,0:T(8,128)(2,1)S(1)}, bf16[128,2048]{1,0:T(8,128)(2,1)}, u32[]{:S(2)}) copy-start(bf16[128,2048]{1,0:T(8,128)(2,1)} %latent_ref.1) | copy-start | bytes 1572868
  15.1 13.5 %collective-permute-start.5 = (bf16[128,2048]{1,0:T(8,128)(2,1)S(1)}, bf16[128,2048]{1,0:T(8,128)(2,1)S(1)}, u32[]{:S(2)}, u32[]{:S(2)}) collective-permute-start(bf16[128,2048]{1,0:T(8,128)(2,1)S(1)} %collective-permute-done.4.refs_6_), channel_id=1, source_target_pairs={{0,1},{1,0},{2,3},{3,2},{4,5},{5,4},{6,7},{7,6},{8,9},{9,8},{10,11... | collective-permute-start | bytes 1572872 | tf_op jit(solution)/shard_map/ppermute | solution.py:569
  15.1 0.7 copy-start.2
  15.8 12.8 %copy-start.3 = (bf16[2048,256]{1,0:T(8,128)(2,1)S(1)}, bf16[2048,256]{1,0:T(8,128)(2,1)}, u32[]{:S(2)}) copy-start(bf16[2048,256]{1,0:T(8,128)(2,1)} %refs_2_.1) | copy-start | bytes 3145732
  15.8 12.9 %copy-start.4 = (bf16[2048,128]{1,0:T(8,128)(2,1)S(1)}, bf16[2048,128]{1,0:T(8,128)(2,1)}, u32[]{:S(2)}) copy-start(bf16[2048,128]{1,0:T(8,128)(2,1)} %refs_3_.1) | copy-start | bytes 1572868
  15.8 12.9 %copy-start.5 = (bf16[2048,128]{1,0:T(8,128)(2,1)S(1)}, bf16[2048,128]{1,0:T(8,128)(2,1)}, u32[]{:S(2)}) copy-start(bf16[2048,128]{1,0:T(8,128)(2,1)} %refs_4_.1) | copy-start | bytes 1572868
  15.8 12.9 %copy-start.6 = (bf16[64,2048]{1,0:T(8,128)(2,1)S(1)}, bf16[64,2048]{1,0:T(8,128)(2,1)}, u32[]{:S(2)}) copy-start(bf16[64,2048]{1,0:T(8,128)(2,1)} %refs_1_.1) | copy-start | bytes 786436
  15.8 12.9 %copy-start.7 = (f32[2048]{0:T(1024)S(1)}, f32[2048]{0:T(1024)}, u32[]{:S(2)}) copy-start(f32[2048]{0:T(1024)} %param.18) | copy-start | bytes 24580
  15.9 3.8 %collective-permute-start.1 = (f32[8,512]{1,0:T(8,128)S(1)}, f32[8,512]{1,0:T(8,128)S(1)}, u32[]{:S(2)}, u32[]{:S(2)}) collective-permute-start(f32[8,512]{1,0:T(8,128)S(1)} %shard_map.137.one_ref), channel_id=1, source_target_pairs={{0,8},{4,12},{8,0},{12,4},{16,24},{20,28},{24,16},{28,20},{1,9},{5... | collective-permute-start | bytes 49160 | tf_op jit(solution)/shard_map/ppermute | solution.py:569
  19.7 3.7 %collective-permute-start.2 = (f32[8,512]{1,0:T(8,128)S(1)}, f32[8,512]{1,0:T(8,128)S(1)}, u32[]{:S(2)}, u32[]{:S(2)}) collective-permute-start(f32[8,512]{1,0:T(8,128)S(1)} %shard_map.138.one_ref), channel_id=1, source_target_pairs={{0,4},{4,0},{8,12},{12,8},{16,20},{20,16},{24,28},{28,24},{1,5},{5... | collective-permute-start | bytes 49160 | tf_op jit(solution)/shard_map/ppermute | solution.py:569
  31.4 11.7 %collective-permute-start.6 = (bf16[5,128,128]{2,1,0:T(8,128)(2,1)S(1)}, bf16[5,128,128]{2,1,0:T(8,128)(2,1)S(1)}, u32[]{:S(2)}, u32[]{:S(2)}) collective-permute-start(bf16[5,128,128]{2,1,0:T(8,128)(2,1)S(1)} %get-tuple-element.35), channel_id=1, source_target_pairs={{0,4},{4,0},{8,12},{12,8},{16,20},{20,16},{24,28},{28,24},{1,5},{5... | collective-permute-start | bytes 491528 | tf_op jit(solution)/shard_map/ppermute | solution.py:569
  33.2 9.3 %collective-permute-start.10 = (bf16[4,128,128]{2,1,0:T(8,128)(2,1)S(1)}, bf16[4,128,128]{2,1,0:T(8,128)(2,1)S(1)}, u32[]{:S(2)}, u32[]{:S(2)}) collective-permute-start(bf16[4,128,128]{2,1,0:T(8,128)(2,1)S(1)} %get-tuple-element.38.refs_1_.refs_2_), channel_id=1, source_target_pairs={{0,16},{4,20},{8,24},{12,28},{16,0},{20,4},{24,8},{28,12},{1,17},{... | collective-permute-start | bytes 393224 | tf_op jit(solution)/shard_map/ppermute | solution.py:569
  35.8 7.3 %collective-permute-start.9 = (bf16[4,128,128]{2,1,0:T(8,128)(2,1)S(1)}, bf16[4,128,128]{2,1,0:T(8,128)(2,1)S(1)}, u32[]{:S(2)}, u32[]{:S(2)}) collective-permute-start(bf16[4,128,128]{2,1,0:T(8,128)(2,1)S(1)} %get-tuple-element.37), channel_id=1, source_target_pairs={{0,4},{4,0},{8,12},{12,8},{16,20},{20,16},{24,28},{28,24},{1,5},{5... | collective-permute-start | bytes 393224 | tf_op jit(solution)/shard_map/ppermute | solution.py:569
  36.3 11.4 %collective-permute-start.13 = (bf16[4,128,128]{2,1,0:T(8,128)(2,1)S(1)}, bf16[4,128,128]{2,1,0:T(8,128)(2,1)S(1)}, u32[]{:S(2)}, u32[]{:S(2)}) collective-permute-start(bf16[4,128,128]{2,1,0:T(8,128)(2,1)S(1)} %get-tuple-element.38.refs_1_.refs_2_), channel_id=1, source_target_pairs={{0,8},{4,12},{8,0},{12,4},{16,24},{20,28},{24,16},{28,20},{1,9},{5... | collective-permute-start | bytes 393224 | tf_op jit(solution)/shard_map/ppermute | solution.py:569
  42.5 17.3 %collective-permute-start.11 = (bf16[4,128,128]{2,1,0:T(8,128)(2,1)S(1)}, bf16[4,128,128]{2,1,0:T(8,128)(2,1)S(1)}, u32[]{:S(2)}, u32[]{:S(2)}) collective-permute-start(bf16[4,128,128]{2,1,0:T(8,128)(2,1)S(1)} %collective-permute-done.10.refs_5_), channel_id=1, source_target_pairs={{0,8},{4,12},{8,0},{12,4},{16,24},{20,28},{24,16},{28,20},{1,9},{5... | collective-permute-start | bytes 393224 | tf_op jit(solution)/shard_map/ppermute | solution.py:569
  43.2 13.9 %collective-permute-start.12 = (bf16[5,128,128]{2,1,0:T(8,128)(2,1)S(1)}, bf16[5,128,128]{2,1,0:T(8,128)(2,1)S(1)}, u32[]{:S(2)}, u32[]{:S(2)}) collective-permute-start(bf16[5,128,128]{2,1,0:T(8,128)(2,1)S(1)} %shard_map.141.refs_1_.refs_3_), channel_id=1, source_target_pairs={{0,8},{4,12},{8,0},{12,4},{16,24},{20,28},{24,16},{28,20},{1,9},{5... | collective-permute-start | bytes 491528 | tf_op jit(solution)/shard_map/ppermute | solution.py:569
  44.7 8.4 %collective-permute-start.7 = (bf16[5,128,128]{2,1,0:T(8,128)(2,1)S(1)}, bf16[5,128,128]{2,1,0:T(8,128)(2,1)S(1)}, u32[]{:S(2)}, u32[]{:S(2)}) collective-permute-start(bf16[5,128,128]{2,1,0:T(8,128)(2,1)S(1)} %shard_map.141.refs_1_.refs_3_), channel_id=1, source_target_pairs={{0,16},{4,20},{8,24},{12,28},{16,0},{20,4},{24,8},{28,12},{1,17},{... | collective-permute-start | bytes 491528 | tf_op jit(solution)/shard_map/ppermute | solution.py:569
  53.1 8.4 %collective-permute-start.8 = (bf16[5,128,128]{2,1,0:T(8,128)(2,1)S(1)}, bf16[5,128,128]{2,1,0:T(8,128)(2,1)S(1)}, u32[]{:S(2)}, u32[]{:S(2)}) collective-permute-start(bf16[5,128,128]{2,1,0:T(8,128)(2,1)S(1)} %collective-permute-done.7.refs_3_.refs_1_), channel_id=1, source_target_pairs={{0,8},{4,12},{8,0},{12,4},{16,24},{20,28},{24,16},{28,20},{1,9},{5... | collective-permute-start | bytes 491528 | tf_op jit(solution)/shard_map/ppermute | solution.py:569
  61.5 11.7 %copy-start = (bf16[1024,2048]{1,0:T(8,128)(2,1)S(1)}, bf16[1024,2048]{1,0:T(8,128)(2,1)}, u32[]{:S(2)}) copy-start(bf16[1024,2048]{1,0:T(8,128)(2,1)} %weight_ref.1) | copy-start | bytes 12582916
  62.5 6.7 %collective-permute-start.20 = (bf16[128,128]{1,0:T(8,128)(2,1)S(1)}, bf16[128,128]{1,0:T(8,128)(2,1)S(1)}, u32[]{:S(2)}, u32[]{:S(2)}) collective-permute-start(bf16[128,128]{1,0:T(8,128)(2,1)S(1)} %get-tuple-element.63), channel_id=1, source_target_pairs={{0,7},{1,6},{2,5},{3,4},{4,3},{5,2},{6,1},{7,0},{8,15},{9,14},{10,... | collective-permute-start | bytes 98312 | tf_op jit(solution)/shard_map/ppermute | solution.py:579
  62.8 7.6 %collective-permute-start.19 = (bf16[128,128]{1,0:T(8,128)(2,1)S(1)}, bf16[128,128]{1,0:T(8,128)(2,1)S(1)}, u32[]{:S(2)}, u32[]{:S(2)}) collective-permute-start(bf16[128,128]{1,0:T(8,128)(2,1)S(1)} %get-tuple-element.64), channel_id=1, source_target_pairs={{0,6},{1,7},{2,4},{3,5},{4,2},{5,3},{6,0},{7,1},{8,14},{9,15},{10,... | collective-permute-start | bytes 98312 | tf_op jit(solution)/shard_map/ppermute | solution.py:579
  66.2 4.6 %collective-permute-start.18 = (bf16[128,128]{1,0:T(8,128)(2,1)S(1)}, bf16[128,128]{1,0:T(8,128)(2,1)S(1)}, u32[]{:S(2)}, u32[]{:S(2)}) collective-permute-start(bf16[128,128]{1,0:T(8,128)(2,1)S(1)} %get-tuple-element.65), channel_id=1, source_target_pairs={{0,5},{1,4},{2,7},{3,6},{4,1},{5,0},{6,3},{7,2},{8,13},{9,12},{10,... | collective-permute-start | bytes 98312 | tf_op jit(solution)/shard_map/ppermute | solution.py:579
  67.5 3.9 %collective-permute-start.17 = (bf16[128,128]{1,0:T(8,128)(2,1)S(1)}, bf16[128,128]{1,0:T(8,128)(2,1)S(1)}, u32[]{:S(2)}, u32[]{:S(2)}) collective-permute-start(bf16[128,128]{1,0:T(8,128)(2,1)S(1)} %get-tuple-element.66), channel_id=1, source_target_pairs={{0,4},{1,5},{2,6},{3,7},{4,0},{5,1},{6,2},{7,3},{8,12},{9,13},{10,... | collective-permute-start | bytes 98312 | tf_op jit(solution)/shard_map/ppermute | solution.py:579
  68.9 3.6 %collective-permute-start.16 = (bf16[128,128]{1,0:T(8,128)(2,1)S(1)}, bf16[128,128]{1,0:T(8,128)(2,1)S(1)}, u32[]{:S(2)}, u32[]{:S(2)}) collective-permute-start(bf16[128,128]{1,0:T(8,128)(2,1)S(1)} %get-tuple-element.67), channel_id=1, source_target_pairs={{0,3},{1,2},{2,1},{3,0},{4,7},{5,6},{6,5},{7,4},{8,11},{9,10},{10,... | collective-permute-start | bytes 98312 | tf_op jit(solution)/shard_map/ppermute | solution.py:569
  69.2 3.9 %collective-permute-start.15 = (bf16[128,128]{1,0:T(8,128)(2,1)S(1)}, bf16[128,128]{1,0:T(8,128)(2,1)S(1)}, u32[]{:S(2)}, u32[]{:S(2)}) collective-permute-start(bf16[128,128]{1,0:T(8,128)(2,1)S(1)} %get-tuple-element.68), channel_id=1, source_target_pairs={{0,2},{1,3},{2,0},{3,1},{4,6},{5,7},{6,4},{7,5},{8,10},{9,11},{10,... | collective-permute-start | bytes 98312 | tf_op jit(solution)/shard_map/ppermute | solution.py:569
  70.4 2.7 %collective-permute-start.14 = (bf16[128,128]{1,0:T(8,128)(2,1)S(1)}, bf16[128,128]{1,0:T(8,128)(2,1)S(1)}, u32[]{:S(2)}, u32[]{:S(2)}) collective-permute-start(bf16[128,128]{1,0:T(8,128)(2,1)S(1)} %get-tuple-element.69), channel_id=1, source_target_pairs={{0,1},{1,0},{2,3},{3,2},{4,5},{5,4},{6,7},{7,6},{8,9},{9,8},{10,11... | collective-permute-start | bytes 98312 | tf_op jit(solution)/shard_map/ppermute | solution.py:569

commit v6 on v5

--- a/solution.py
+++ b/solution.py
@@ -678,18 +678,16 @@
     near = xor_move(give_kv, "sp", 1)
     near_q = xor_move(give_q, "sp", 1)
     up = xor_move(keep_kv, "sp", 2)
-    down = xor_move(keep_kv, "sp", 4)
+    down = xor_move(keep_kv, "sp", 6)
     near = merge(near, keep_ctx)
-    near_down = xor_move(near, "sp", 4)
+    near_down = xor_move(near, "sp", 6)
     near_up = xor_move(near, "sp", 2)
     across = xor_move(down, "sp", 2)
     near_across = xor_move(near_down, "sp", 2)
     (own,) = attend([(keep_q, None, [0])], [keep_kv], offset)
-    (own,) = attend([(keep_q, own, [0])], [near], offset)
     near_q = ready(near_q)
-    own, other = attend(
-        [(keep_q, own, [2, 3]), (near_q, None, [0, 1, 2, 3])], [keep_kv, near, up, down], offset
-    )
+    own, other = attend([(keep_q, own, [1]), (near_q, None, [0, 1])], [keep_kv, near], offset)
+    own, other = attend([(keep_q, own, [0, 1]), (near_q, other, [0, 1])], [up, down], offset)
     own, other = attend(
         [(keep_q, own, [0]), (near_q, other, [0, 1])], [near_up, near_down], offset
     )

time: 75 us -> 73 us (0.973)
  starting transfers between devices: 30.3 us -> 27.3 us
  waiting for transfers between devices: 18.4 us -> 19.2 us
    ppermute x17, starting transfers between devices: 25.8 us -> 22.8 us  [xor_move(): return lax.ppermute(member, axis, [(i, i ^ mask) for i in range(size)])]
  transfers between devices with their start and end apart: 21 -> 21, of which waited for: 8 -> 9; matrix products, arithmetic and copies ran while one was open for 1% -> 1% of each run, Pallas kernels for 19% -> 20%
where the time goes in v6:
time: 73 us; the launch traced here: 72.7 us
  starting transfers between devices  27.3 us (37%)
  Pallas kernels  19.6 us (27%)
  waiting for transfers between devices  19.2 us (26%)
  blocking collectives  5.22 us (7%)
  local copies, waits for them, and re-layouts  0.78 us (1%)
    ppermute x17, starting transfers between devices, xor_move(): return lax.ppermute(member, axis, [(i, i ^ mask) for i in range(size)])  22.8 us
    ppermute x17, waiting for transfers between devices, xor_move(): return lax.ppermute(member, axis, [(i, i ^ mask) for i in range(size)])  18.3 us
    pallas_call x7, Pallas kernels, attend(): kernel_call(body, out * len(sources), len(inputs), 40 * 2 * lanes * keys...  13.1 us
    all_gather x1, blocking collectives, inner_device(): modulation = lax.all_gather(part, 'tp', axis=0, tiled=False)  5.22 us
    ppermute x4, starting transfers between devices, cross_move(): return lax.ppermute(member, ('sp', 'tp'), pairs)  4.51 us
    pallas_call x1, Pallas kernels, inner_device(): pl.pallas_call(lambda *refs: projection_body(q_heads, kv_heads, *refs), o...  2.67 us
    pallas_call x1, Pallas kernels, opening(): pl.pallas_call(opening_body, out_shape=jax.ShapeDtypeStruct((8, columns),...  2.08 us
    pallas_call x1, Pallas kernels, inner_device(): kernel_call(output_body, jax.ShapeDtypeStruct(latent.shape, jnp.bfloat16)...  1.59 us
  transfers between devices with their start and end apart: 21, of which 9 were waited for; matrix products, arithmetic and copies ran while one was open for 1% of the time, Pallas kernels for 20%

profile of v6, /device:TPU:0, one launch (start us, length us, event | category | flops | bytes accessed | tf_op | source)
XLA Modules:
  0.0 72.7 jit_solution(632118945475881232)
XLA Ops:
  0.0 3.0 %collective-permute-start.4 = (bf16[128,2048]{1,0:T(8,128)(2,1)}, bf16[128,2048]{1,0:T(8,128)(2,1)S(1)}, u32[]{:S(2)}, u32[]{:S(2)}) collective-permute-start(bf16[128,2048]{1,0:T(8,128)(2,1)} %latent_ref.1), channel_id=1, source_target_pairs={{0,2},{1,3},{2,0},{3,1},{4,6},{5,7},{6,4},{7,5},{8,10},{9,11},{10,... | collective-permute-start | bytes 1572872 | tf_op jit(solution)/shard_map/ppermute | solution.py:569
  3.0 0.0 collective-permute-start.3
  3.0 2.1 %shard_map.136.one_ref = f32[8,512]{1,0:T(8,128)} custom-call(f32[1,2048]{1,0:T(1,128)} %bitcast.27, f32[1,2048]{1,0:T(1,128)} %bitcast.28, bf16[256,512]{1,0:T(8,128)(2,1)} %shift_hbm.1, bf16[256,512]{1,0:T(8,128)(2,1)} %scale_hbm.1, bf16[256,512]{1,0:T(8,128)(2,1)} %gate_hbm.1), custom_call_target="tpu_custom_call" | custom-call | flops 100000000 | tf_op jit(solution)/shard_map/pallas_call | solution.py:276
  5.1 2.7 %collective-permute-start = (f32[8,512]{1,0:T(8,128)}, f32[8,512]{1,0:T(8,128)S(1)}, u32[]{:S(2)}, u32[]{:S(2)}) collective-permute-start(f32[8,512]{1,0:T(8,128)} %shard_map.136.one_ref), channel_id=1, source_target_pairs={{0,16},{4,20},{8,24},{12,28},{16,0},{20,4},{24,8},{28,12},{1,17},{... | collective-permute-start | bytes 49160 | tf_op jit(solution)/shard_map/ppermute | solution.py:569
  7.7 0.1 fusion.2
  7.8 0.0 copy-start.9
  7.8 0.0 copy-start.1
  7.8 7.3 %collective-permute-done.4.refs_6_ = bf16[128,2048]{1,0:T(8,128)(2,1)S(1)} collective-permute-done((bf16[128,2048]{1,0:T(8,128)(2,1)}, bf16[128,2048]{1,0:T(8,128)(2,1)S(1)}, u32[]{:S(2)}, u32[]{:S(2)}) %collective-permute-start.4) | collective-permute-done | bytes 524320 | tf_op jit(solution)/shard_map/ppermute | solution.py:569
  15.1 0.0 collective-permute-start.5
  15.1 0.0 collective-permute-done.other_ref
  15.1 0.7 copy-done.2
  15.8 0.0 copy-start.7
  15.9 1.9 %collective-permute-start.1 = (f32[8,512]{1,0:T(8,128)S(1)}, f32[8,512]{1,0:T(8,128)S(1)}, u32[]{:S(2)}, u32[]{:S(2)}) collective-permute-start(f32[8,512]{1,0:T(8,128)S(1)} %shard_map.137.one_ref), channel_id=1, source_target_pairs={{0,8},{4,12},{8,0},{12,4},{16,24},{20,28},{24,16},{28,20},{1,9},{5... | collective-permute-start | bytes 49160 | tf_op jit(solution)/shard_map/ppermute | solution.py:569
  17.8 0.3 fusion
  18.1 1.6 %collective-permute-done.1.other_ref = f32[8,512]{1,0:T(8,128)S(1)} collective-permute-done((f32[8,512]{1,0:T(8,128)S(1)}, f32[8,512]{1,0:T(8,128)S(1)}, u32[]{:S(2)}, u32[]{:S(2)}) %collective-permute-start.1) | collective-permute-done | bytes 16416 | tf_op jit(solution)/shard_map/ppermute | solution.py:569
  19.7 1.8 %collective-permute-start.2 = (f32[8,512]{1,0:T(8,128)S(1)}, f32[8,512]{1,0:T(8,128)S(1)}, u32[]{:S(2)}, u32[]{:S(2)}) collective-permute-start(f32[8,512]{1,0:T(8,128)S(1)} %shard_map.138.one_ref), channel_id=1, source_target_pairs={{0,4},{4,0},{8,12},{12,8},{16,20},{20,16},{24,28},{28,24},{1,5},{5... | collective-permute-start | bytes 49160 | tf_op jit(solution)/shard_map/ppermute | solution.py:569
  21.5 1.9 %collective-permute-done.2.other_ref = f32[8,512]{1,0:T(8,128)S(1)} collective-permute-done((f32[8,512]{1,0:T(8,128)S(1)}, f32[8,512]{1,0:T(8,128)S(1)}, u32[]{:S(2)}, u32[]{:S(2)}) %collective-permute-start.2) | collective-permute-done | bytes 16416 | tf_op jit(solution)/shard_map/ppermute | solution.py:569
  23.4 5.2 %all-gather = f32[32,512]{1,0:T(8,128)S(1)} all-gather(f32[8,512]{1,0:T(8,128)S(1)} %shard_map.139), channel_id=2, replica_groups=mesh['sp'=8,'tp'=4] {'tp'}, dimensions={0}, use_global_device_ids=true | all-gather | bytes 81920 | tf_op jit(solution)/shard_map/all_gather | solution.py:641
  28.6 0.0 collective-permute-done.3.refs_5_
  28.6 0.0 collective-permute-done.5.refs_7_
  28.6 0.0 copy-done.8
  28.6 0.0 copy-done.9
  28.7 0.0 copy-done.1
  28.7 0.0 copy-done.3
  28.7 2.7 %shard_map.140 = (bf16[8,128,128]{2,1,0:T(8,128)(2,1)S(1)}, bf16[4,128,128]{2,1,0:T(8,128)(2,1)S(1)}, bf16[128,128]{1,0:T(8,128)(2,1)S(1)}, bf16[4,128,128]{2,1,0:T(8,128)(2,1)S(1)}, bf16[5,128,128]{2,1,0:T(8,128)(2,1)S(1)}) custom-call(bf16[128,2048]{1,0:T(8,128)(2,1)S(1)} %copy-done.1, bf16[64,2048]{1,0:T(8,128)(2,1)S(1)} %copy-done.6, ...), custom_call_target="tpu_custom_call" | custom-call | flops 2147483648 | tf_op jit(solution)/shard_map/pallas_call | solution.py:646
  31.4 1.8 %collective-permute-start.6 = (bf16[5,128,128]{2,1,0:T(8,128)(2,1)S(1)}, bf16[5,128,128]{2,1,0:T(8,128)(2,1)S(1)}, u32[]{:S(2)}, u32[]{:S(2)}) collective-permute-start(bf16[5,128,128]{2,1,0:T(8,128)(2,1)S(1)} %get-tuple-element.38), channel_id=1, source_target_pairs={{0,4},{4,0},{8,12},{12,8},{16,20},{20,16},{24,28},{28,24},{1,5},{5... | collective-permute-start | bytes 491528 | tf_op jit(solution)/shard_map/ppermute | solution.py:569
  33.2 3.6 %collective-permute-start.10 = (bf16[4,128,128]{2,1,0:T(8,128)(2,1)S(1)}, bf16[4,128,128]{2,1,0:T(8,128)(2,1)S(1)}, u32[]{:S(2)}, u32[]{:S(2)}) collective-permute-start(bf16[4,128,128]{2,1,0:T(8,128)(2,1)S(1)} %get-tuple-element.41.refs_1_.refs_2_), channel_id=1, source_target_pairs={{0,24},{4,28},{8,16},{12,20},{16,8},{20,12},{24,0},{28,4},{1,25},{... | collective-permute-start | bytes 393224 | tf_op jit(solution)/shard_map/ppermute | solution.py:569
  36.8 0.5 collective-permute-start.9
  37.4 0.0 collective-permute-start.13
  37.4 0.9 %shard_map.143 = (f32[2,1,512]{2,1,0:T(1,128)S(1)}, f32[2,1,512]{2,1,0:T(1,128)S(1)}, f32[2,64,512]{2,1,0:T(8,128)S(1)}) custom-call(bf16[8,128,128]{2,1,0:T(8,128)(2,1)S(1)} %get-tuple-element.37.refs_0_, bf16[4,128,128]{2,1,0:T(8,128)(2,1)S(1)} %get-tuple-element.41.refs_1_.refs_2_), custom_call_target="tpu_custom_call" | custom-call | flops 671088640 | tf_op jit(solution)/shard_map/pallas_call | solution.py:535
  38.2 3.2 %collective-permute-done.10.refs_3_ = bf16[4,128,128]{2,1,0:T(8,128)(2,1)S(1)} collective-permute-done((bf16[4,128,128]{2,1,0:T(8,128)(2,1)S(1)}, bf16[4,128,128]{2,1,0:T(8,128)(2,1)S(1)}, u32[]{:S(2)}, u32[]{:S(2)}) %collective-permute-start.10) | collective-permute-done | bytes 131104 | tf_op jit(solution)/shard_map/ppermute | solution.py:569
  41.4 1.6 %collective-permute-start.11 = (bf16[4,128,128]{2,1,0:T(8,128)(2,1)S(1)}, bf16[4,128,128]{2,1,0:T(8,128)(2,1)S(1)}, u32[]{:S(2)}, u32[]{:S(2)}) collective-permute-start(bf16[4,128,128]{2,1,0:T(8,128)(2,1)S(1)} %collective-permute-done.10.refs_3_), channel_id=1, source_target_pairs={{0,8},{4,12},{8,0},{12,4},{16,24},{20,28},{24,16},{28,20},{1,9},{5... | collective-permute-start | bytes 393224 | tf_op jit(solution)/shard_map/ppermute | solution.py:569
  43.1 0.0 collective-permute-done.9.q_ref
  43.1 0.0 collective-permute-done.6.near_ref
  43.1 0.1 shard_map.141.refs_3_
  43.2 0.4 collective-permute-start.12
  43.6 3.6 %collective-permute-start.7 = (bf16[5,128,128]{2,1,0:T(8,128)(2,1)S(1)}, bf16[5,128,128]{2,1,0:T(8,128)(2,1)S(1)}, u32[]{:S(2)}, u32[]{:S(2)}) collective-permute-start(bf16[5,128,128]{2,1,0:T(8,128)(2,1)S(1)} %shard_map.141.refs_3_), channel_id=1, source_target_pairs={{0,24},{4,28},{8,16},{12,20},{16,8},{20,12},{24,0},{28,4},{1,25},{... | collective-permute-start | bytes 491528 | tf_op jit(solution)/shard_map/ppermute | solution.py:569
  47.2 2.4 %shard_map.144 = (f32[2,1,512]{2,1,0:T(1,128)S(1)}, f32[2,1,512]{2,1,0:T(1,128)S(1)}, f32[2,64,512]{2,1,0:T(8,128)S(1)}, f32[2,1,512]{2,1,0:T(1,128)S(1)}, f32[2...) custom-call(bf16[8,128,128]{2,1,0:T(8,128)(2,1)S(1)} %get-tuple-element.37.refs_0_, ...), custom_call_target="tpu_custom_call" | custom-call | flops 2348810240 | tf_op jit(solution)/shard_map/pallas_call | solution.py:535
  49.7 0.0 collective-permute-done.13.refs_2_
  49.7 2.6 %shard_map.145 = (f32[2,1,512]{2,1,0:T(1,128)S(1)}, f32[2,1,512]{2,1,0:T(1,128)S(1)}, f32[2,64,512]{2,1,0:T(8,128)S(1)}, f32[2,1,512]{2,1,0:T(1,128)S(1)}, f32[2...) custom-call(bf16[8,128,128]{2,1,0:T(8,128)(2,1)S(1)} %get-tuple-element.37.refs_0_, ...), custom_call_target="tpu_custom_call" | custom-call | flops 2684354560 | tf_op jit(solution)/shard_map/pallas_call | solution.py:535
  52.3 1.9 %collective-permute-done.7.refs_3_.refs_1_ = bf16[5,128,128]{2,1,0:T(8,128)(2,1)S(1)} collective-permute-done((bf16[5,128,128]{2,1,0:T(8,128)(2,1)S(1)}, bf16[5,128,128]{2,1,0:T(8,128)(2,1)S(1)}, u32[]{:S(2)}, u32[]{:S(2)}) %collective-permute-start.7) | collective-permute-done | bytes 163872 | tf_op jit(solution)/shard_map/ppermute | solution.py:569
  54.3 0.0 collective-permute-start.8
  54.3 0.0 collective-permute-done.12.refs_2_
  54.3 2.6 %shard_map.146 = (f32[2,1,512]{2,1,0:T(1,128)S(1)}, f32[2,1,512]{2,1,0:T(1,128)S(1)}, f32[2,64,512]{2,1,0:T(8,128)S(1)}, f32[2,1,512]{2,1,0:T(1,128)S(1)}, f32[2...) custom-call(bf16[8,128,128]{2,1,0:T(8,128)(2,1)S(1)} %get-tuple-element.37.refs_0_, ...), custom_call_target="tpu_custom_call" | custom-call | flops 2516582400 | tf_op jit(solution)/shard_map/pallas_call | solution.py:535
  56.9 0.0 collective-permute-done.11.refs_2_
  56.9 1.7 %shard_map.147 = (f32[2,1,512]{2,1,0:T(1,128)S(1)}, f32[2,1,512]{2,1,0:T(1,128)S(1)}, f32[2,64,512]{2,1,0:T(8,128)S(1)}, f32[2,1,512]{2,1,0:T(1,128)S(1)}, f32[2...) custom-call(bf16[8,128,128]{2,1,0:T(8,128)(2,1)S(1)} %get-tuple-element.37.refs_0_, ...), custom_call_target="tpu_custom_call" | custom-call | flops 1342177280 | tf_op jit(solution)/shard_map/pallas_call | solution.py:535
  58.6 1.0 %collective-permute-done.8.refs_2_.refs_1_ = bf16[5,128,128]{2,1,0:T(8,128)(2,1)S(1)} collective-permute-done((bf16[5,128,128]{2,1,0:T(8,128)(2,1)S(1)}, bf16[5,128,128]{2,1,0:T(8,128)(2,1)S(1)}, u32[]{:S(2)}, u32[]{:S(2)}) %collective-permute-start.8) | collective-permute-done | bytes 163872 | tf_op jit(solution)/shard_map/ppermute | solution.py:569
  59.6 1.0 %shard_map.149 = bf16[4,128,128]{2,1,0:T(8,128)(2,1)S(1)} custom-call(bf16[8,128,128]{2,1,0:T(8,128)(2,1)S(1)} %shard_map.142.refs_1_.refs_0_, bf16[5,128,128]{2,1,0:T(8,128)(2,1)S(1)} %collective-permute-done.8.refs_2_.refs_1_, f32[2,1,512]{2,1,0:T(1,128)S(1)} %get-tuple-element.66.refs_2_, f32[2,1,512]{2,1,0:T(1,128)S(1)} %get-tuple-element.67.refs_3_, ...), custom_call_target="tpu_custom_call" | custom-call | flops 838860800 | tf_op jit(solution)/shard_map/pallas_call | solution.py:535
  60.6 0.1 collective-permute-start.20
  60.7 1.9 %collective-permute-start.19 = (bf16[128,128]{1,0:T(8,128)(2,1)S(1)}, bf16[128,128]{1,0:T(8,128)(2,1)S(1)}, u32[]{:S(2)}, u32[]{:S(2)}) collective-permute-start(bf16[128,128]{1,0:T(8,128)(2,1)S(1)} %get-tuple-element.70), channel_id=1, source_target_pairs={{0,6},{1,7},{2,4},{3,5},{4,2},{5,3},{6,0},{7,1},{8,14},{9,15},{10,... | collective-permute-start | bytes 98312 | tf_op jit(solution)/shard_map/ppermute | solution.py:579
  62.6 1.9 %shard_map.148 = bf16[4,128,128]{2,1,0:T(8,128)(2,1)S(1)} custom-call(bf16[8,128,128]{2,1,0:T(8,128)(2,1)S(1)} %get-tuple-element.37.refs_0_, bf16[5,128,128]{2,1,0:T(8,128)(2,1)S(1)} %collective-permute-done.7.refs_3_.refs_1_, bf16[5,128,128]{2,1,0:T(8,128)(2,1)S(1)} %collective-permute-done.8.refs_2_.refs_1_, f32[2,1,512]{2,1,0:T(1,128)S(1)} %get-tuple-element.63.refs_3_, ...), custom_call_target="tpu_custom_call" | custom-call | flops 1677721600 | tf_op jit(solution)/shard_map/pallas_call | solution.py:535
  64.5 1.4 %collective-permute-start.18 = (bf16[128,128]{1,0:T(8,128)(2,1)S(1)}, bf16[128,128]{1,0:T(8,128)(2,1)S(1)}, u32[]{:S(2)}, u32[]{:S(2)}) collective-permute-start(bf16[128,128]{1,0:T(8,128)(2,1)S(1)} %get-tuple-element.71), channel_id=1, source_target_pairs={{0,5},{1,4},{2,7},{3,6},{4,1},{5,0},{6,3},{7,2},{8,13},{9,12},{10,... | collective-permute-start | bytes 98312 | tf_op jit(solution)/shard_map/ppermute | solution.py:579
  65.9 1.1 %collective-permute-start.17 = (bf16[128,128]{1,0:T(8,128)(2,1)S(1)}, bf16[128,128]{1,0:T(8,128)(2,1)S(1)}, u32[]{:S(2)}, u32[]{:S(2)}) collective-permute-start(bf16[128,128]{1,0:T(8,128)(2,1)S(1)} %get-tuple-element.72), channel_id=1, source_target_pairs={{0,4},{1,5},{2,6},{3,7},{4,0},{5,1},{6,2},{7,3},{8,12},{9,13},{10,... | collective-permute-start | bytes 98312 | tf_op jit(solution)/shard_map/ppermute | solution.py:579
  67.0 0.2 collective-permute-start.16
  67.2 0.0 collective-permute-done.20.refs_7_
  67.2 1.3 %collective-permute-start.15 = (bf16[128,128]{1,0:T(8,128)(2,1)S(1)}, bf16[128,128]{1,0:T(8,128)(2,1)S(1)}, u32[]{:S(2)}, u32[]{:S(2)}) collective-permute-start(bf16[128,128]{1,0:T(8,128)(2,1)S(1)} %get-tuple-element.74), channel_id=1, source_target_pairs={{0,2},{1,3},{2,0},{3,1},{4,6},{5,7},{6,4},{7,5},{8,10},{9,11},{10,... | collective-permute-start | bytes 98312 | tf_op jit(solution)/shard_map/ppermute | solution.py:569
  68.5 0.0 collective-permute-done.19.refs_6_
  68.5 0.4 collective-permute-start.14
  68.9 0.0 collective-permute-done.18.refs_5_
  68.9 0.9 %collective-permute-done.17.refs_4_ = bf16[128,128]{1,0:T(8,128)(2,1)S(1)} collective-permute-done((bf16[128,128]{1,0:T(8,128)(2,1)S(1)}, bf16[128,128]{1,0:T(8,128)(2,1)S(1)}, u32[]{:S(2)}, u32[]{:S(2)}) %collective-permute-start.17) | collective-permute-done | bytes 32800 | tf_op jit(solution)/shard_map/ppermute | solution.py:579
  69.8 0.9 %collective-permute-done.16.refs_3_ = bf16[128,128]{1,0:T(8,128)(2,1)S(1)} collective-permute-done((bf16[128,128]{1,0:T(8,128)(2,1)S(1)}, bf16[128,128]{1,0:T(8,128)(2,1)S(1)}, u32[]{:S(2)}, u32[]{:S(2)}) %collective-permute-start.16) | collective-permute-done | bytes 32800 | tf_op jit(solution)/shard_map/ppermute | solution.py:569
  70.7 0.5 collective-permute-done.15.refs_2_
  71.1 0.0 collective-permute-done.14.refs_1_
  71.2 1.6 %shard_map.150 = bf16[128,2048]{1,0:T(8,128)(2,1)} custom-call(bf16[128,2048]{1,0:T(8,128)(2,1)S(1)} %copy-done.1, f32[4,8,512]{2,1,0:T(8,128)S(1)} %bitcast.23, bf16[1024,2048]{1,0:T(8,128)(2,1)S(1)} %copy-done, bf16[128,128]{1,0:T(8,128)(2,1)S(1)} %get-tuple-element.76.refs_0_, bf16[128,128]{1,0:T(8,128)(2,1)S(1)} %collective-permute-done.14.refs_1_, ...), custom_call_target="tpu_custom_call" | custom-call | flops 536870912 | tf_op jit(solution)/shard_map/pallas_call | solution.py:700
  (21 shorter events, 0.1 us)
Async XLA Ops:
  0.0 15.1 %collective-permute-start.4 = (bf16[128,2048]{1,0:T(8,128)(2,1)}, bf16[128,2048]{1,0:T(8,128)(2,1)S(1)}, u32[]{:S(2)}, u32[]{:S(2)}) collective-permute-start(bf16[128,2048]{1,0:T(8,128)(2,1)} %latent_ref.1), channel_id=1, source_target_pairs={{0,2},{1,3},{2,0},{3,1},{4,6},{5,7},{6,4},{7,5},{8,10},{9,11},{10,... | collective-permute-start | bytes 1572872 | tf_op jit(solution)/shard_map/ppermute | solution.py:569
  3.0 25.7 %collective-permute-start.3 = (bf16[128,2048]{1,0:T(8,128)(2,1)}, bf16[128,2048]{1,0:T(8,128)(2,1)S(1)}, u32[]{:S(2)}, u32[]{:S(2)}) collective-permute-start(bf16[128,2048]{1,0:T(8,128)(2,1)} %latent_ref.1), channel_id=1, source_target_pairs={{0,1},{1,0},{2,3},{3,2},{4,5},{5,4},{6,7},{7,6},{8,9},{9,8},{10,11... | collective-permute-start | bytes 1572872 | tf_op jit(solution)/shard_map/ppermute | solution.py:569
  5.1 10.0 %collective-permute-start = (f32[8,512]{1,0:T(8,128)}, f32[8,512]{1,0:T(8,128)S(1)}, u32[]{:S(2)}, u32[]{:S(2)}) collective-permute-start(f32[8,512]{1,0:T(8,128)} %shard_map.136.one_ref), channel_id=1, source_target_pairs={{0,16},{4,20},{8,24},{12,28},{16,0},{20,4},{24,8},{28,12},{1,17},{... | collective-permute-start | bytes 49160 | tf_op jit(solution)/shard_map/ppermute | solution.py:569
  7.8 20.8 %copy-start.8 = (f32[64]{0:T(128)S(1)}, f32[64]{0:T(128)}, u32[]{:S(2)}) copy-start(f32[64]{0:T(128)} %param.25) | copy-start | bytes 772
  7.8 20.8 %copy-start.9 = (f32[64]{0:T(128)S(1)}, f32[64]{0:T(128)}, u32[]{:S(2)}) copy-start(f32[64]{0:T(128)} %param.26) | copy-start | bytes 772
  7.8 20.8 %copy-start.1 = (bf16[128,2048]{1,0:T(8,128)(2,1)S(1)}, bf16[128,2048]{1,0:T(8,128)(2,1)}, u32[]{:S(2)}) copy-start(bf16[128,2048]{1,0:T(8,128)(2,1)} %latent_ref.1) | copy-start | bytes 1572868
  15.1 13.5 %collective-permute-start.5 = (bf16[128,2048]{1,0:T(8,128)(2,1)S(1)}, bf16[128,2048]{1,0:T(8,128)(2,1)S(1)}, u32[]{:S(2)}, u32[]{:S(2)}) collective-permute-start(bf16[128,2048]{1,0:T(8,128)(2,1)S(1)} %collective-permute-done.4.refs_6_), channel_id=1, source_target_pairs={{0,1},{1,0},{2,3},{3,2},{4,5},{5,4},{6,7},{7,6},{8,9},{9,8},{10,11... | collective-permute-start | bytes 1572872 | tf_op jit(solution)/shard_map/ppermute | solution.py:569
  15.1 0.7 copy-start.2
  15.8 12.8 %copy-start.3 = (bf16[2048,256]{1,0:T(8,128)(2,1)S(1)}, bf16[2048,256]{1,0:T(8,128)(2,1)}, u32[]{:S(2)}) copy-start(bf16[2048,256]{1,0:T(8,128)(2,1)} %refs_2_.1) | copy-start | bytes 3145732
  15.8 12.9 %copy-start.4 = (bf16[2048,128]{1,0:T(8,128)(2,1)S(1)}, bf16[2048,128]{1,0:T(8,128)(2,1)}, u32[]{:S(2)}) copy-start(bf16[2048,128]{1,0:T(8,128)(2,1)} %refs_3_.1) | copy-start | bytes 1572868
  15.8 12.9 %copy-start.5 = (bf16[2048,128]{1,0:T(8,128)(2,1)S(1)}, bf16[2048,128]{1,0:T(8,128)(2,1)}, u32[]{:S(2)}) copy-start(bf16[2048,128]{1,0:T(8,128)(2,1)} %refs_4_.1) | copy-start | bytes 1572868
  15.8 12.9 %copy-start.6 = (bf16[64,2048]{1,0:T(8,128)(2,1)S(1)}, bf16[64,2048]{1,0:T(8,128)(2,1)}, u32[]{:S(2)}) copy-start(bf16[64,2048]{1,0:T(8,128)(2,1)} %refs_1_.1) | copy-start | bytes 786436
  15.8 12.9 %copy-start.7 = (f32[2048]{0:T(1024)S(1)}, f32[2048]{0:T(1024)}, u32[]{:S(2)}) copy-start(f32[2048]{0:T(1024)} %param.18) | copy-start | bytes 24580
  15.9 3.8 %collective-permute-start.1 = (f32[8,512]{1,0:T(8,128)S(1)}, f32[8,512]{1,0:T(8,128)S(1)}, u32[]{:S(2)}, u32[]{:S(2)}) collective-permute-start(f32[8,512]{1,0:T(8,128)S(1)} %shard_map.137.one_ref), channel_id=1, source_target_pairs={{0,8},{4,12},{8,0},{12,4},{16,24},{20,28},{24,16},{28,20},{1,9},{5... | collective-permute-start | bytes 49160 | tf_op jit(solution)/shard_map/ppermute | solution.py:569
  19.7 3.7 %collective-permute-start.2 = (f32[8,512]{1,0:T(8,128)S(1)}, f32[8,512]{1,0:T(8,128)S(1)}, u32[]{:S(2)}, u32[]{:S(2)}) collective-permute-start(f32[8,512]{1,0:T(8,128)S(1)} %shard_map.138.one_ref), channel_id=1, source_target_pairs={{0,4},{4,0},{8,12},{12,8},{16,20},{20,16},{24,28},{28,24},{1,5},{5... | collective-permute-start | bytes 49160 | tf_op jit(solution)/shard_map/ppermute | solution.py:569
  31.4 11.7 %collective-permute-start.6 = (bf16[5,128,128]{2,1,0:T(8,128)(2,1)S(1)}, bf16[5,128,128]{2,1,0:T(8,128)(2,1)S(1)}, u32[]{:S(2)}, u32[]{:S(2)}) collective-permute-start(bf16[5,128,128]{2,1,0:T(8,128)(2,1)S(1)} %get-tuple-element.38), channel_id=1, source_target_pairs={{0,4},{4,0},{8,12},{12,8},{16,20},{20,16},{24,28},{28,24},{1,5},{5... | collective-permute-start | bytes 491528 | tf_op jit(solution)/shard_map/ppermute | solution.py:569
  33.2 8.2 %collective-permute-start.10 = (bf16[4,128,128]{2,1,0:T(8,128)(2,1)S(1)}, bf16[4,128,128]{2,1,0:T(8,128)(2,1)S(1)}, u32[]{:S(2)}, u32[]{:S(2)}) collective-permute-start(bf16[4,128,128]{2,1,0:T(8,128)(2,1)S(1)} %get-tuple-element.41.refs_1_.refs_2_), channel_id=1, source_target_pairs={{0,24},{4,28},{8,16},{12,20},{16,8},{20,12},{24,0},{28,4},{1,25},{... | collective-permute-start | bytes 393224 | tf_op jit(solution)/shard_map/ppermute | solution.py:569
  36.8 6.2 %collective-permute-start.9 = (bf16[4,128,128]{2,1,0:T(8,128)(2,1)S(1)}, bf16[4,128,128]{2,1,0:T(8,128)(2,1)S(1)}, u32[]{:S(2)}, u32[]{:S(2)}) collective-permute-start(bf16[4,128,128]{2,1,0:T(8,128)(2,1)S(1)} %get-tuple-element.40), channel_id=1, source_target_pairs={{0,4},{4,0},{8,12},{12,8},{16,20},{20,16},{24,28},{28,24},{1,5},{5... | collective-permute-start | bytes 393224 | tf_op jit(solution)/shard_map/ppermute | solution.py:569
  37.4 12.3 %collective-permute-start.13 = (bf16[4,128,128]{2,1,0:T(8,128)(2,1)S(1)}, bf16[4,128,128]{2,1,0:T(8,128)(2,1)S(1)}, u32[]{:S(2)}, u32[]{:S(2)}) collective-permute-start(bf16[4,128,128]{2,1,0:T(8,128)(2,1)S(1)} %get-tuple-element.41.refs_1_.refs_2_), channel_id=1, source_target_pairs={{0,8},{4,12},{8,0},{12,4},{16,24},{20,28},{24,16},{28,20},{1,9},{5... | collective-permute-start | bytes 393224 | tf_op jit(solution)/shard_map/ppermute | solution.py:569
  41.4 15.4 %collective-permute-start.11 = (bf16[4,128,128]{2,1,0:T(8,128)(2,1)S(1)}, bf16[4,128,128]{2,1,0:T(8,128)(2,1)S(1)}, u32[]{:S(2)}, u32[]{:S(2)}) collective-permute-start(bf16[4,128,128]{2,1,0:T(8,128)(2,1)S(1)} %collective-permute-done.10.refs_3_), channel_id=1, source_target_pairs={{0,8},{4,12},{8,0},{12,4},{16,24},{20,28},{24,16},{28,20},{1,9},{5... | collective-permute-start | bytes 393224 | tf_op jit(solution)/shard_map/ppermute | solution.py:569
  43.2 11.0 %collective-permute-start.12 = (bf16[5,128,128]{2,1,0:T(8,128)(2,1)S(1)}, bf16[5,128,128]{2,1,0:T(8,128)(2,1)S(1)}, u32[]{:S(2)}, u32[]{:S(2)}) collective-permute-start(bf16[5,128,128]{2,1,0:T(8,128)(2,1)S(1)} %shard_map.141.refs_3_), channel_id=1, source_target_pairs={{0,8},{4,12},{8,0},{12,4},{16,24},{20,28},{24,16},{28,20},{1,9},{5... | collective-permute-start | bytes 491528 | tf_op jit(solution)/shard_map/ppermute | solution.py:569
  43.6 10.6 %collective-permute-start.7 = (bf16[5,128,128]{2,1,0:T(8,128)(2,1)S(1)}, bf16[5,128,128]{2,1,0:T(8,128)(2,1)S(1)}, u32[]{:S(2)}, u32[]{:S(2)}) collective-permute-start(bf16[5,128,128]{2,1,0:T(8,128)(2,1)S(1)} %shard_map.141.refs_3_), channel_id=1, source_target_pairs={{0,24},{4,28},{8,16},{12,20},{16,8},{20,12},{24,0},{28,4},{1,25},{... | collective-permute-start | bytes 491528 | tf_op jit(solution)/shard_map/ppermute | solution.py:569
  54.3 5.3 %collective-permute-start.8 = (bf16[5,128,128]{2,1,0:T(8,128)(2,1)S(1)}, bf16[5,128,128]{2,1,0:T(8,128)(2,1)S(1)}, u32[]{:S(2)}, u32[]{:S(2)}) collective-permute-start(bf16[5,128,128]{2,1,0:T(8,128)(2,1)S(1)} %collective-permute-done.7.refs_3_.refs_1_), channel_id=1, source_target_pairs={{0,8},{4,12},{8,0},{12,4},{16,24},{20,28},{24,16},{28,20},{1,9},{5... | collective-permute-start | bytes 491528 | tf_op jit(solution)/shard_map/ppermute | solution.py:569
  59.6 11.6 %copy-start = (bf16[1024,2048]{1,0:T(8,128)(2,1)S(1)}, bf16[1024,2048]{1,0:T(8,128)(2,1)}, u32[]{:S(2)}) copy-start(bf16[1024,2048]{1,0:T(8,128)(2,1)} %weight_ref.1) | copy-start | bytes 12582916
  60.6 6.6 %collective-permute-start.20 = (bf16[128,128]{1,0:T(8,128)(2,1)S(1)}, bf16[128,128]{1,0:T(8,128)(2,1)S(1)}, u32[]{:S(2)}, u32[]{:S(2)}) collective-permute-start(bf16[128,128]{1,0:T(8,128)(2,1)S(1)} %get-tuple-element.69), channel_id=1, source_target_pairs={{0,7},{1,6},{2,5},{3,4},{4,3},{5,2},{6,1},{7,0},{8,15},{9,14},{10,... | collective-permute-start | bytes 98312 | tf_op jit(solution)/shard_map/ppermute | solution.py:579
  60.7 7.8 %collective-permute-start.19 = (bf16[128,128]{1,0:T(8,128)(2,1)S(1)}, bf16[128,128]{1,0:T(8,128)(2,1)S(1)}, u32[]{:S(2)}, u32[]{:S(2)}) collective-permute-start(bf16[128,128]{1,0:T(8,128)(2,1)S(1)} %get-tuple-element.70), channel_id=1, source_target_pairs={{0,6},{1,7},{2,4},{3,5},{4,2},{5,3},{6,0},{7,1},{8,14},{9,15},{10,... | collective-permute-start | bytes 98312 | tf_op jit(solution)/shard_map/ppermute | solution.py:579
  64.5 4.4 %collective-permute-start.18 = (bf16[128,128]{1,0:T(8,128)(2,1)S(1)}, bf16[128,128]{1,0:T(8,128)(2,1)S(1)}, u32[]{:S(2)}, u32[]{:S(2)}) collective-permute-start(bf16[128,128]{1,0:T(8,128)(2,1)S(1)} %get-tuple-element.71), channel_id=1, source_target_pairs={{0,5},{1,4},{2,7},{3,6},{4,1},{5,0},{6,3},{7,2},{8,13},{9,12},{10,... | collective-permute-start | bytes 98312 | tf_op jit(solution)/shard_map/ppermute | solution.py:579
  65.9 3.9 %collective-permute-start.17 = (bf16[128,128]{1,0:T(8,128)(2,1)S(1)}, bf16[128,128]{1,0:T(8,128)(2,1)S(1)}, u32[]{:S(2)}, u32[]{:S(2)}) collective-permute-start(bf16[128,128]{1,0:T(8,128)(2,1)S(1)} %get-tuple-element.72), channel_id=1, source_target_pairs={{0,4},{1,5},{2,6},{3,7},{4,0},{5,1},{6,2},{7,3},{8,12},{9,13},{10,... | collective-permute-start | bytes 98312 | tf_op jit(solution)/shard_map/ppermute | solution.py:579
  67.0 3.6 %collective-permute-start.16 = (bf16[128,128]{1,0:T(8,128)(2,1)S(1)}, bf16[128,128]{1,0:T(8,128)(2,1)S(1)}, u32[]{:S(2)}, u32[]{:S(2)}) collective-permute-start(bf16[128,128]{1,0:T(8,128)(2,1)S(1)} %get-tuple-element.73), channel_id=1, source_target_pairs={{0,3},{1,2},{2,1},{3,0},{4,7},{5,6},{6,5},{7,4},{8,11},{9,10},{10,... | collective-permute-start | bytes 98312 | tf_op jit(solution)/shard_map/ppermute | solution.py:569
  67.2 3.9 %collective-permute-start.15 = (bf16[128,128]{1,0:T(8,128)(2,1)S(1)}, bf16[128,128]{1,0:T(8,128)(2,1)S(1)}, u32[]{:S(2)}, u32[]{:S(2)}) collective-permute-start(bf16[128,128]{1,0:T(8,128)(2,1)S(1)} %get-tuple-element.74), channel_id=1, source_target_pairs={{0,2},{1,3},{2,0},{3,1},{4,6},{5,7},{6,4},{7,5},{8,10},{9,11},{10,... | collective-permute-start | bytes 98312 | tf_op jit(solution)/shard_map/ppermute | solution.py:569
  68.5 2.6 %collective-permute-start.14 = (bf16[128,128]{1,0:T(8,128)(2,1)S(1)}, bf16[128,128]{1,0:T(8,128)(2,1)S(1)}, u32[]{:S(2)}, u32[]{:S(2)}) collective-permute-start(bf16[128,128]{1,0:T(8,128)(2,1)S(1)} %get-tuple-element.75), channel_id=1, source_target_pairs={{0,1},{1,0},{2,3},{3,2},{4,5},{5,4},{6,7},{7,6},{8,9},{9,8},{10,11... | collective-permute-start | bytes 98312 | tf_op jit(solution)/shard_map/ppermute | solution.py:569

commit v7 on v6

--- a/solution.py
+++ b/solution.py
@@ -293,12 +293,18 @@
     return field * cosine + swapped * sine
 
 
+def normed(raw, head_gain):
+    return raw * lax.rsqrt(jnp.mean(raw * raw, axis=0, keepdims=True) + epsilon) * head_gain
+
+
+def upright(ref):
+    return jnp.broadcast_to(ref[...], (8, ref.shape[1])).T[:, 0:1]
+
+
 def projection_body(
-    heads,
     kv_heads,
     own_ref,
     context_ref,
-    query_ref,
     key_ref,
     value_ref,
     core_ref,
@@ -306,19 +312,16 @@
     both_ref,
     mod_ref,
     gain_ref,
-    query_gain_ref,
     key_gain_ref,
     cosine_ref,
     sine_ref,
-    keep_q,
     keep_kv,
     keep_ctx,
-    give_q,
     give_kv,
+    hidden_out,
     made,
 ):
     span = CHANNEL_SPAN
-    group = heads // kv_heads
 
     def vector(row):
         return jnp.concatenate([mod_ref[i, row : row + 1, :] for i in range(mod_ref.shape[0])], axis=1)
@@ -330,56 +333,61 @@
         scaled = wide * lax.rsqrt(jnp.mean(wide * wide, axis=-1, keepdims=True) + epsilon)
         return (scaled * (gain * (1.0 + vector(2 + row))) + vector(row)).astype(jnp.bfloat16)
 
-    def normed(raw, head_gain):
-        return raw * lax.rsqrt(jnp.mean(raw * raw, axis=0, keepdims=True) + epsilon) * head_gain
-
-    def upright(ref):
-        return jnp.broadcast_to(ref[...], (8, span)).T[:, 0:1]
-
-    query_gain = upright(query_gain_ref)
     key_gain = upright(key_gain_ref)
     blocks = (own_ref, core_ref, far_ref, both_ref)
-    q_tiles = group * len(blocks) // 2
     waiting = {}
     for j, ref in enumerate(blocks):
         hidden = hidden_of(ref, 0)
-        cosine = cosine_ref[j]
-        sine = sine_ref[j]
+        hidden_out[j] = hidden
         rows = slice(j % 2 * span, (j % 2 + 1) * span)
-        queries = jnp.dot(hidden, query_ref[...], preferred_element_type=jnp.float32).T
-        for h in range(heads):
-            turned = turn(normed(queries[h * span : (h + 1) * span], query_gain), cosine, sine)
-            kv, g = h // group, h % group
-            made[kv, g * len(blocks) // 2 + j // 2, rows, :] = turned.astype(jnp.bfloat16)
         keys = jnp.dot(hidden, key_ref[...], preferred_element_type=jnp.float32).T
         values = jnp.dot(hidden, value_ref[...], preferred_element_type=jnp.float32).T
         for h in range(kv_heads):
             cut = slice(h * span, (h + 1) * span)
-            turned = turn(normed(keys[cut], key_gain), cosine, sine)
+            turned = turn(normed(keys[cut], key_gain), cosine_ref[j], sine_ref[j])
             if j % 2:
                 pair = jnp.concatenate([waiting[h], turned], axis=0)
-                made[h, q_tiles + j // 2] = pair.T.astype(jnp.bfloat16)
+                made[h, j // 2] = pair.T.astype(jnp.bfloat16)
             waiting[h] = turned
-            made[h, q_tiles + len(blocks) // 2 + j // 2, rows, :] = values[cut].astype(jnp.bfloat16)
+            made[h, len(blocks) // 2 + j // 2, rows, :] = values[cut].astype(jnp.bfloat16)
     hidden = hidden_of(context_ref, 1)
     keys = jnp.dot(hidden, key_ref[...], preferred_element_type=jnp.float32).T
     values = jnp.dot(hidden, value_ref[...], preferred_element_type=jnp.float32).T
     for h in range(kv_heads):
         cut = slice(h * span, (h + 1) * span)
         both = jnp.concatenate([normed(keys[cut], key_gain).T, values[cut]], axis=0)
-        made[h, q_tiles + len(blocks)] = jnp.concatenate([both, jnp.zeros_like(both)], axis=1).astype(
+        made[h, len(blocks)] = jnp.concatenate([both, jnp.zeros_like(both)], axis=1).astype(
             jnp.bfloat16
         )
     side = lax.rem(lax.axis_index("sp"), kv_heads)
-    for head, q_ref, kv_ref in ((1 - side, give_q, give_kv), (side, keep_q, keep_kv)):
-        for i in range(q_tiles):
-            if q_ref is keep_q:
-                q_ref[i], q_ref[q_tiles + i] = scaled_halves(made[head, i])
-            else:
-                q_ref[i] = made[head, i]
-        for i in range(kv_ref.shape[0]):
-            kv_ref[i] = made[head, q_tiles + i]
-    keep_ctx[...] = made[side, q_tiles + len(blocks)]
+    for i in range(give_kv.shape[0]):
+        give_kv[i] = made[1 - side, i]
+    for i in range(keep_kv.shape[0]):
+        keep_kv[i] = made[side, i]
+    keep_ctx[...] = made[side, len(blocks)]
+
+
+def probe_body(
+    kv_heads, hidden_ref, query_ref, query_gain_ref, cosine_ref, sine_ref, keep_q, give_q, made
+):
+    span = CHANNEL_SPAN
+    heads = query_ref.shape[1] // span
+    group = heads // kv_heads
+    count = hidden_ref.shape[0]
+    query_gain = upright(query_gain_ref)
+    for j in range(count):
+        rows = slice(j % 2 * span, (j % 2 + 1) * span)
+        queries = jnp.dot(hidden_ref[j], query_ref[...], preferred_element_type=jnp.float32).T
+        for h in range(heads):
+            raw = queries[h * span : (h + 1) * span]
+            turned = turn(normed(raw, query_gain), cosine_ref[j], sine_ref[j])
+            kv, g = h // group, h % group
+            made[kv, g * count // 2 + j // 2, rows, :] = turned.astype(jnp.bfloat16)
+    side = lax.rem(lax.axis_index("sp"), kv_heads)
+    q_tiles = give_q.shape[0]
+    for i in range(q_tiles):
+        give_q[i] = made[1 - side, i]
+        keep_q[i], keep_q[q_tiles + i] = scaled_halves(made[side, i])
 
 
 def merge_body(near_ref, ctx_ref, out_ref):
@@ -643,25 +651,23 @@
     q_tiles = q_heads // kv_heads * head_split // 2
     kv_tiles = head_split
     tile = (own_rows, own_rows)
-    keep_q, keep_kv, keep_ctx, give_q, give_kv = pl.pallas_call(
-        lambda *refs: projection_body(q_heads, kv_heads, *refs),
-        out_shape=[
-            jax.ShapeDtypeStruct((*count, *tile), jnp.bfloat16)
-            for count in ((2 * q_tiles,), (kv_tiles,), (), (q_tiles,), (kv_tiles + 1,))
+    keep_kv, keep_ctx, give_kv, hidden = kernel_call(
+        lambda *refs: projection_body(kv_heads, *refs),
+        [
+            jax.ShapeDtypeStruct(shape, jnp.bfloat16)
+            for shape in (
+                (kv_tiles, *tile),
+                tile,
+                (kv_tiles + 1, *tile),
+                (head_split, own_rows, depth),
+            )
         ],
-        in_specs=[whole_spec()] * 14,
-        out_specs=[whole_spec()] * 5,
-        scratch_shapes=[pltpu.VMEM((kv_heads, q_tiles + kv_tiles + 1, *tile), jnp.bfloat16)],
-        cost_estimate=pl.CostEstimate(
-            flops=4 * tok_count * depth * (q_heads + 2 * kv_heads) * CHANNEL_SPAN,
-            transcendentals=0,
-            bytes_accessed=0,
-        ),
-        compiler_params=pltpu.CompilerParams(vmem_limit_bytes=MODEST),
+        12,
+        8 * tok_count * depth * kv_heads * CHANNEL_SPAN,
+        [pltpu.VMEM((kv_heads, kv_tiles + 1, *tile), jnp.bfloat16)],
     )(
         latent,
         context,
-        query_weight,
         key_weight,
         value_weight,
         near,
@@ -669,11 +675,17 @@
         both,
         modulation,
         norm_gain.reshape(1, depth),
-        query_gain.reshape(1, CHANNEL_SPAN),
         key_gain.reshape(1, CHANNEL_SPAN),
         cosine,
         sine,
     )
+    keep_q, give_q = kernel_call(
+        lambda *refs: probe_body(kv_heads, *refs),
+        [jax.ShapeDtypeStruct((count, *tile), jnp.bfloat16) for count in (2 * q_tiles, q_tiles)],
+        5,
+        4 * tok_count * depth * q_heads * CHANNEL_SPAN,
+        [pltpu.VMEM((kv_heads, q_tiles, *tile), jnp.bfloat16)],
+    )(hidden, query_weight, query_gain.reshape(1, CHANNEL_SPAN), cosine, sine)
     offset = math.log(tok_count / (2.0 * ctx_rows))
     near = xor_move(give_kv, "sp", 1)
     near_q = xor_move(give_q, "sp", 1)

time: 73 us -> 73.2 us (level)
  starting transfers between devices: 27.3 us -> 26 us
  waiting for transfers between devices: 19.2 us -> 20.2 us
    ppermute x17, starting transfers between devices: 22.8 us -> 21.5 us  [xor_move(): return lax.ppermute(member, axis, [(i, i ^ mask) for i in range(size)])]
    pallas_call x1 -> x2, Pallas kernels: 2.67 us -> 3.12 us  [the longest x1 2.2 us: inner_device(): kernel_call(lambda *refs: projection_body(kv_heads, *refs), [jax.ShapeDty...]
  transfers between devices with their start and end apart: 21 -> 21, of which waited for: 9 -> 10; matrix products, arithmetic and copies ran while one was open for 1% -> 1% of each run, Pallas kernels for 20% -> 21%
where the time goes in v7:
time: 73.2 us; the launch traced here: 73 us
  starting transfers between devices  26 us (36%)
  waiting for transfers between devices  20.2 us (28%)
  Pallas kernels  20.1 us (27%)
  blocking collectives  5.22 us (7%)
  local copies, waits for them, and re-layouts  0.78 us (1%)
    ppermute x17, starting transfers between devices, xor_move(): return lax.ppermute(member, axis, [(i, i ^ mask) for i in range(size)])  21.5 us
    ppermute x17, waiting for transfers between devices, xor_move(): return lax.ppermute(member, axis, [(i, i ^ mask) for i in range(size)])  18.7 us
    pallas_call x7, Pallas kernels, attend(): kernel_call(body, out * len(sources), len(inputs), 40 * 2 * lanes * keys...  13.2 us
    all_gather x1, blocking collectives, inner_device(): modulation = lax.all_gather(part, 'tp', axis=0, tiled=False)  5.22 us
    ppermute x4, starting transfers between devices, cross_move(): return lax.ppermute(member, ('sp', 'tp'), pairs)  4.51 us
    pallas_call x1, Pallas kernels, inner_device(): kernel_call(lambda *refs: projection_body(kv_heads, *refs), [jax.ShapeDty...  2.2 us
    pallas_call x1, Pallas kernels, opening(): pl.pallas_call(opening_body, out_shape=jax.ShapeDtypeStruct((8, columns),...  2.08 us
    pallas_call x1, Pallas kernels, inner_device(): kernel_call(output_body, jax.ShapeDtypeStruct(latent.shape, jnp.bfloat16)...  1.6 us
  transfers between devices with their start and end apart: 21, of which 10 were waited for; matrix products, arithmetic and copies ran while one was open for 1% of the time, Pallas kernels for 21%

profile of v7, /device:TPU:0, one launch (start us, length us, event | category | flops | bytes accessed | tf_op | source)
XLA Modules:
  0.0 73.0 jit_solution(13756951995473799407)
XLA Ops:
  0.0 3.0 %collective-permute-start.4 = (bf16[128,2048]{1,0:T(8,128)(2,1)}, bf16[128,2048]{1,0:T(8,128)(2,1)S(1)}, u32[]{:S(2)}, u32[]{:S(2)}) collective-permute-start(bf16[128,2048]{1,0:T(8,128)(2,1)} %latent_ref.1), channel_id=1, source_target_pairs={{0,2},{1,3},{2,0},{3,1},{4,6},{5,7},{6,4},{7,5},{8,10},{9,11},{10,... | collective-permute-start | bytes 1572872 | tf_op jit(solution)/shard_map/ppermute | solution.py:577
  3.0 0.0 collective-permute-start.3
  3.0 2.1 %shard_map.136.one_ref = f32[8,512]{1,0:T(8,128)} custom-call(f32[1,2048]{1,0:T(1,128)} %bitcast.27, f32[1,2048]{1,0:T(1,128)} %bitcast.28, bf16[256,512]{1,0:T(8,128)(2,1)} %shift_hbm.1, bf16[256,512]{1,0:T(8,128)(2,1)} %scale_hbm.1, bf16[256,512]{1,0:T(8,128)(2,1)} %gate_hbm.1), custom_call_target="tpu_custom_call" | custom-call | flops 100000000 | tf_op jit(solution)/shard_map/pallas_call | solution.py:276
  5.1 2.7 %collective-permute-start = (f32[8,512]{1,0:T(8,128)}, f32[8,512]{1,0:T(8,128)S(1)}, u32[]{:S(2)}, u32[]{:S(2)}) collective-permute-start(f32[8,512]{1,0:T(8,128)} %shard_map.136.one_ref), channel_id=1, source_target_pairs={{0,16},{4,20},{8,24},{12,28},{16,0},{20,4},{24,8},{28,12},{1,17},{... | collective-permute-start | bytes 49160 | tf_op jit(solution)/shard_map/ppermute | solution.py:577
  7.7 0.1 fusion.2
  7.8 0.0 copy-start.1
  7.8 7.3 %collective-permute-done.4.refs_5_ = bf16[128,2048]{1,0:T(8,128)(2,1)S(1)} collective-permute-done((bf16[128,2048]{1,0:T(8,128)(2,1)}, bf16[128,2048]{1,0:T(8,128)(2,1)S(1)}, u32[]{:S(2)}, u32[]{:S(2)}) %collective-permute-start.4) | collective-permute-done | bytes 524320 | tf_op jit(solution)/shard_map/ppermute | solution.py:577
  15.1 0.0 collective-permute-start.5
  15.1 0.0 collective-permute-done.other_ref
  15.1 0.7 copy-done.2
  15.8 0.0 copy-start.3
  15.9 0.0 copy-start.9
  15.9 1.9 %collective-permute-start.1 = (f32[8,512]{1,0:T(8,128)S(1)}, f32[8,512]{1,0:T(8,128)S(1)}, u32[]{:S(2)}, u32[]{:S(2)}) collective-permute-start(f32[8,512]{1,0:T(8,128)S(1)} %shard_map.137.one_ref), channel_id=1, source_target_pairs={{0,8},{4,12},{8,0},{12,4},{16,24},{20,28},{24,16},{28,20},{1,9},{5... | collective-permute-start | bytes 49160 | tf_op jit(solution)/shard_map/ppermute | solution.py:577
  17.8 0.3 fusion
  18.1 1.6 %collective-permute-done.1.other_ref = f32[8,512]{1,0:T(8,128)S(1)} collective-permute-done((f32[8,512]{1,0:T(8,128)S(1)}, f32[8,512]{1,0:T(8,128)S(1)}, u32[]{:S(2)}, u32[]{:S(2)}) %collective-permute-start.1) | collective-permute-done | bytes 16416 | tf_op jit(solution)/shard_map/ppermute | solution.py:577
  19.7 1.8 %collective-permute-start.2 = (f32[8,512]{1,0:T(8,128)S(1)}, f32[8,512]{1,0:T(8,128)S(1)}, u32[]{:S(2)}, u32[]{:S(2)}) collective-permute-start(f32[8,512]{1,0:T(8,128)S(1)} %shard_map.138.one_ref), channel_id=1, source_target_pairs={{0,4},{4,0},{8,12},{12,8},{16,20},{20,16},{24,28},{28,24},{1,5},{5... | collective-permute-start | bytes 49160 | tf_op jit(solution)/shard_map/ppermute | solution.py:577
  21.5 1.9 %collective-permute-done.2.other_ref = f32[8,512]{1,0:T(8,128)S(1)} collective-permute-done((f32[8,512]{1,0:T(8,128)S(1)}, f32[8,512]{1,0:T(8,128)S(1)}, u32[]{:S(2)}, u32[]{:S(2)}) %collective-permute-start.2) | collective-permute-done | bytes 16416 | tf_op jit(solution)/shard_map/ppermute | solution.py:577
  23.4 5.2 %all-gather = f32[32,512]{1,0:T(8,128)S(1)} all-gather(f32[8,512]{1,0:T(8,128)S(1)} %shard_map.139), channel_id=2, replica_groups=mesh['sp'=8,'tp'=4] {'tp'}, dimensions={0}, use_global_device_ids=true | all-gather | bytes 81920 | tf_op jit(solution)/shard_map/all_gather | solution.py:649
  28.6 0.0 collective-permute-done.3.refs_4_
  28.7 0.0 collective-permute-done.5.refs_6_
  28.7 0.0 copy-done.8
  28.7 2.2 %shard_map.140 = (bf16[4,128,128]{2,1,0:T(8,128)(2,1)S(1)}, bf16[128,128]{1,0:T(8,128)(2,1)S(1)}, bf16[5,128,128]{2,1,0:T(8,128)(2,1)S(1)}, bf16[4,128,2048]{2,1,0:T(8,128)(2,1)S(1)}) custom-call(bf16[128,2048]{1,0:T(8,128)(2,1)S(1)} %copy-done.1, bf16[64,2048]{1,0:T(8,128)(2,1)S(1)} %copy-done.6, bf16[2048,128]{1,0:T(8,128)(2,1)S(1)} %copy-done.4, ...), custom_call_target="tpu_custom_call" | custom-call | flops 1073741824 | tf_op jit(solution)/shard_map/pallas_call | solution.py:654
  30.9 3.9 %collective-permute-start.10 = (bf16[4,128,128]{2,1,0:T(8,128)(2,1)S(1)}, bf16[4,128,128]{2,1,0:T(8,128)(2,1)S(1)}, u32[]{:S(2)}, u32[]{:S(2)}) collective-permute-start(bf16[4,128,128]{2,1,0:T(8,128)(2,1)S(1)} %get-tuple-element.43.refs_1_.refs_2_), channel_id=1, source_target_pairs={{0,24},{4,28},{8,16},{12,20},{16,8},{20,12},{24,0},{28,4},{1,25},{... | collective-permute-start | bytes 393224 | tf_op jit(solution)/shard_map/ppermute | solution.py:577
  34.8 1.5 %collective-permute-start.6 = (bf16[5,128,128]{2,1,0:T(8,128)(2,1)S(1)}, bf16[5,128,128]{2,1,0:T(8,128)(2,1)S(1)}, u32[]{:S(2)}, u32[]{:S(2)}) collective-permute-start(bf16[5,128,128]{2,1,0:T(8,128)(2,1)S(1)} %get-tuple-element.40), channel_id=1, source_target_pairs={{0,4},{4,0},{8,12},{12,8},{16,20},{20,16},{24,28},{28,24},{1,5},{5... | collective-permute-start | bytes 491528 | tf_op jit(solution)/shard_map/ppermute | solution.py:577
  36.3 0.0 copy-done.9
  36.3 0.9 %shard_map.141 = (bf16[8,128,128]{2,1,0:T(8,128)(2,1)S(1)}, bf16[4,128,128]{2,1,0:T(8,128)(2,1)S(1)}) custom-call(bf16[4,128,2048]{2,1,0:T(8,128)(2,1)S(1)} %get-tuple-element.38.refs_0_, bf16[2048,256]{1,0:T(8,128)(2,1)S(1)} %copy-done.3, f32[1,64]{1,0:T(1,128)S(1)} %bitcast.26, f32[4,64,128]{2,1,0:T(8,128)S(1)} %get-tuple-element.90.refs_10_.refs_3_, ...), custom_call_target="tpu_custom_call" | custom-call | flops 1073741824 | tf_op jit(solution)/shard_map/pallas_call | solution.py:682
  37.3 0.6 collective-permute-start.9
  37.9 0.0 collective-permute-start.13
  37.9 0.9 %shard_map.144 = (f32[2,1,512]{2,1,0:T(1,128)S(1)}, f32[2,1,512]{2,1,0:T(1,128)S(1)}, f32[2,64,512]{2,1,0:T(8,128)S(1)}) custom-call(bf16[8,128,128]{2,1,0:T(8,128)(2,1)S(1)} %get-tuple-element.39.refs_0_, bf16[4,128,128]{2,1,0:T(8,128)(2,1)S(1)} %get-tuple-element.43.refs_1_.refs_2_), custom_call_target="tpu_custom_call" | custom-call | flops 671088640 | tf_op jit(solution)/shard_map/pallas_call | solution.py:543
  38.7 0.2 collective-permute-done.10.refs_3_
  38.9 2.4 %collective-permute-start.11 = (bf16[4,128,128]{2,1,0:T(8,128)(2,1)S(1)}, bf16[4,128,128]{2,1,0:T(8,128)(2,1)S(1)}, u32[]{:S(2)}, u32[]{:S(2)}) collective-permute-start(bf16[4,128,128]{2,1,0:T(8,128)(2,1)S(1)} %collective-permute-done.10.refs_3_), channel_id=1, source_target_pairs={{0,8},{4,12},{8,0},{12,4},{16,24},{20,28},{24,16},{28,20},{1,9},{5... | collective-permute-start | bytes 393224 | tf_op jit(solution)/shard_map/ppermute | solution.py:577
  41.4 2.4 %collective-permute-done.9.q_ref = bf16[4,128,128]{2,1,0:T(8,128)(2,1)S(1)} collective-permute-done((bf16[4,128,128]{2,1,0:T(8,128)(2,1)S(1)}, bf16[4,128,128]{2,1,0:T(8,128)(2,1)S(1)}, u32[]{:S(2)}, u32[]{:S(2)}) %collective-permute-start.9) | collective-permute-done | bytes 131104 | tf_op jit(solution)/shard_map/ppermute | solution.py:577
  43.9 0.0 collective-permute-done.6.near_ref
  43.9 0.1 shard_map.142.refs_3_
  43.9 0.0 collective-permute-start.12
  44.0 1.0 %collective-permute-start.7 = (bf16[5,128,128]{2,1,0:T(8,128)(2,1)S(1)}, bf16[5,128,128]{2,1,0:T(8,128)(2,1)S(1)}, u32[]{:S(2)}, u32[]{:S(2)}) collective-permute-start(bf16[5,128,128]{2,1,0:T(8,128)(2,1)S(1)} %shard_map.142.refs_3_), channel_id=1, source_target_pairs={{0,24},{4,28},{8,16},{12,20},{16,8},{20,12},{24,0},{28,4},{1,25},{... | collective-permute-start | bytes 491528 | tf_op jit(solution)/shard_map/ppermute | solution.py:577
  45.0 2.4 %shard_map.145 = (f32[2,1,512]{2,1,0:T(1,128)S(1)}, f32[2,1,512]{2,1,0:T(1,128)S(1)}, f32[2,64,512]{2,1,0:T(8,128)S(1)}, f32[2,1,512]{2,1,0:T(1,128)S(1)}, f32[2...) custom-call(bf16[8,128,128]{2,1,0:T(8,128)(2,1)S(1)} %get-tuple-element.39.refs_0_, ...), custom_call_target="tpu_custom_call" | custom-call | flops 2348810240 | tf_op jit(solution)/shard_map/pallas_call | solution.py:543
  47.4 0.0 collective-permute-done.13.refs_2_
  47.4 2.6 %shard_map.146 = (f32[2,1,512]{2,1,0:T(1,128)S(1)}, f32[2,1,512]{2,1,0:T(1,128)S(1)}, f32[2,64,512]{2,1,0:T(8,128)S(1)}, f32[2,1,512]{2,1,0:T(1,128)S(1)}, f32[2...) custom-call(bf16[8,128,128]{2,1,0:T(8,128)(2,1)S(1)} %get-tuple-element.39.refs_0_, ...), custom_call_target="tpu_custom_call" | custom-call | flops 2684354560 | tf_op jit(solution)/shard_map/pallas_call | solution.py:543
  50.1 3.6 %collective-permute-done.7.refs_3_.refs_1_ = bf16[5,128,128]{2,1,0:T(8,128)(2,1)S(1)} collective-permute-done((bf16[5,128,128]{2,1,0:T(8,128)(2,1)S(1)}, bf16[5,128,128]{2,1,0:T(8,128)(2,1)S(1)}, u32[]{:S(2)}, u32[]{:S(2)}) %collective-permute-start.7) | collective-permute-done | bytes 163872 | tf_op jit(solution)/shard_map/ppermute | solution.py:577
  53.7 0.9 %collective-permute-start.8 = (bf16[5,128,128]{2,1,0:T(8,128)(2,1)S(1)}, bf16[5,128,128]{2,1,0:T(8,128)(2,1)S(1)}, u32[]{:S(2)}, u32[]{:S(2)}) collective-permute-start(bf16[5,128,128]{2,1,0:T(8,128)(2,1)S(1)} %collective-permute-done.7.refs_3_.refs_1_), channel_id=1, source_target_pairs={{0,8},{4,12},{8,0},{12,4},{16,24},{20,28},{24,16},{28,20},{1,9},{5... | collective-permute-start | bytes 491528 | tf_op jit(solution)/shard_map/ppermute | solution.py:577
  54.5 0.0 collective-permute-done.12.refs_2_
  54.5 2.6 %shard_map.147 = (f32[2,1,512]{2,1,0:T(1,128)S(1)}, f32[2,1,512]{2,1,0:T(1,128)S(1)}, f32[2,64,512]{2,1,0:T(8,128)S(1)}, f32[2,1,512]{2,1,0:T(1,128)S(1)}, f32[2...) custom-call(bf16[8,128,128]{2,1,0:T(8,128)(2,1)S(1)} %get-tuple-element.39.refs_0_, ...), custom_call_target="tpu_custom_call" | custom-call | flops 2516582400 | tf_op jit(solution)/shard_map/pallas_call | solution.py:543
  57.2 0.0 collective-permute-done.11.refs_2_
  57.2 1.7 %shard_map.148 = (f32[2,1,512]{2,1,0:T(1,128)S(1)}, f32[2,1,512]{2,1,0:T(1,128)S(1)}, f32[2,64,512]{2,1,0:T(8,128)S(1)}, f32[2,1,512]{2,1,0:T(1,128)S(1)}, f32[2...) custom-call(bf16[8,128,128]{2,1,0:T(8,128)(2,1)S(1)} %get-tuple-element.39.refs_0_, ...), custom_call_target="tpu_custom_call" | custom-call | flops 1342177280 | tf_op jit(solution)/shard_map/pallas_call | solution.py:543
  58.9 0.1 collective-permute-done.8.refs_2_.refs_1_
  59.0 1.0 %shard_map.150 = bf16[4,128,128]{2,1,0:T(8,128)(2,1)S(1)} custom-call(bf16[8,128,128]{2,1,0:T(8,128)(2,1)S(1)} %shard_map.143.refs_1_.refs_0_, bf16[5,128,128]{2,1,0:T(8,128)(2,1)S(1)} %collective-permute-done.8.refs_2_.refs_1_, f32[2,1,512]{2,1,0:T(1,128)S(1)} %get-tuple-element.68.refs_2_, f32[2,1,512]{2,1,0:T(1,128)S(1)} %get-tuple-element.69.refs_3_, ...), custom_call_target="tpu_custom_call" | custom-call | flops 838860800 | tf_op jit(solution)/shard_map/pallas_call | solution.py:543
  60.0 0.1 collective-permute-start.20
  60.1 2.5 %collective-permute-start.19 = (bf16[128,128]{1,0:T(8,128)(2,1)S(1)}, bf16[128,128]{1,0:T(8,128)(2,1)S(1)}, u32[]{:S(2)}, u32[]{:S(2)}) collective-permute-start(bf16[128,128]{1,0:T(8,128)(2,1)S(1)} %get-tuple-element.72), channel_id=1, source_target_pairs={{0,6},{1,7},{2,4},{3,5},{4,2},{5,3},{6,0},{7,1},{8,14},{9,15},{10,... | collective-permute-start | bytes 98312 | tf_op jit(solution)/shard_map/ppermute | solution.py:587
  62.6 1.9 %shard_map.149 = bf16[4,128,128]{2,1,0:T(8,128)(2,1)S(1)} custom-call(bf16[8,128,128]{2,1,0:T(8,128)(2,1)S(1)} %get-tuple-element.39.refs_0_, bf16[5,128,128]{2,1,0:T(8,128)(2,1)S(1)} %collective-permute-done.7.refs_3_.refs_1_, bf16[5,128,128]{2,1,0:T(8,128)(2,1)S(1)} %collective-permute-done.8.refs_2_.refs_1_, f32[2,1,512]{2,1,0:T(1,128)S(1)} %get-tuple-element.65.refs_3_, ...), custom_call_target="tpu_custom_call" | custom-call | flops 1677721600 | tf_op jit(solution)/shard_map/pallas_call | solution.py:543
  64.5 1.4 %collective-permute-start.18 = (bf16[128,128]{1,0:T(8,128)(2,1)S(1)}, bf16[128,128]{1,0:T(8,128)(2,1)S(1)}, u32[]{:S(2)}, u32[]{:S(2)}) collective-permute-start(bf16[128,128]{1,0:T(8,128)(2,1)S(1)} %get-tuple-element.73), channel_id=1, source_target_pairs={{0,5},{1,4},{2,7},{3,6},{4,1},{5,0},{6,3},{7,2},{8,13},{9,12},{10,... | collective-permute-start | bytes 98312 | tf_op jit(solution)/shard_map/ppermute | solution.py:587
  65.9 0.5 collective-permute-start.17
  66.5 0.8 %collective-permute-start.16 = (bf16[128,128]{1,0:T(8,128)(2,1)S(1)}, bf16[128,128]{1,0:T(8,128)(2,1)S(1)}, u32[]{:S(2)}, u32[]{:S(2)}) collective-permute-start(bf16[128,128]{1,0:T(8,128)(2,1)S(1)} %get-tuple-element.75), channel_id=1, source_target_pairs={{0,3},{1,2},{2,1},{3,0},{4,7},{5,6},{6,5},{7,4},{8,11},{9,10},{10,... | collective-permute-start | bytes 98312 | tf_op jit(solution)/shard_map/ppermute | solution.py:577
  67.2 0.0 collective-permute-done.20.refs_7_
  67.2 0.8 %collective-permute-start.15 = (bf16[128,128]{1,0:T(8,128)(2,1)S(1)}, bf16[128,128]{1,0:T(8,128)(2,1)S(1)}, u32[]{:S(2)}, u32[]{:S(2)}) collective-permute-start(bf16[128,128]{1,0:T(8,128)(2,1)S(1)} %get-tuple-element.76), channel_id=1, source_target_pairs={{0,2},{1,3},{2,0},{3,1},{4,6},{5,7},{6,4},{7,5},{8,10},{9,11},{10,... | collective-permute-start | bytes 98312 | tf_op jit(solution)/shard_map/ppermute | solution.py:577
  68.1 0.0 collective-permute-done.19.refs_6_
  68.1 0.2 collective-permute-start.14
  68.3 0.0 collective-permute-done.18.refs_5_
  68.3 1.5 %collective-permute-done.17.refs_4_ = bf16[128,128]{1,0:T(8,128)(2,1)S(1)} collective-permute-done((bf16[128,128]{1,0:T(8,128)(2,1)S(1)}, bf16[128,128]{1,0:T(8,128)(2,1)S(1)}, u32[]{:S(2)}, u32[]{:S(2)}) %collective-permute-start.17) | collective-permute-done | bytes 32800 | tf_op jit(solution)/shard_map/ppermute | solution.py:587
  69.8 0.1 collective-permute-done.16.refs_3_
  70.0 1.4 %collective-permute-done.15.refs_2_ = bf16[128,128]{1,0:T(8,128)(2,1)S(1)} collective-permute-done((bf16[128,128]{1,0:T(8,128)(2,1)S(1)}, bf16[128,128]{1,0:T(8,128)(2,1)S(1)}, u32[]{:S(2)}, u32[]{:S(2)}) %collective-permute-start.15) | collective-permute-done | bytes 32800 | tf_op jit(solution)/shard_map/ppermute | solution.py:577
  71.4 0.0 collective-permute-done.14.refs_1_
  71.4 0.0 copy-done
  71.4 1.6 %shard_map.151 = bf16[128,2048]{1,0:T(8,128)(2,1)} custom-call(bf16[128,2048]{1,0:T(8,128)(2,1)S(1)} %copy-done.1, f32[4,8,512]{2,1,0:T(8,128)S(1)} %bitcast.23, bf16[1024,2048]{1,0:T(8,128)(2,1)S(1)} %copy-done, bf16[128,128]{1,0:T(8,128)(2,1)S(1)} %get-tuple-element.78.refs_0_, bf16[128,128]{1,0:T(8,128)(2,1)S(1)} %collective-permute-done.14.refs_1_, ...), custom_call_target="tpu_custom_call" | custom-call | flops 536870912 | tf_op jit(solution)/shard_map/pallas_call | solution.py:712
  (22 shorter events, 0.1 us)
Async XLA Ops:
  0.0 15.1 %collective-permute-start.4 = (bf16[128,2048]{1,0:T(8,128)(2,1)}, bf16[128,2048]{1,0:T(8,128)(2,1)S(1)}, u32[]{:S(2)}, u32[]{:S(2)}) collective-permute-start(bf16[128,2048]{1,0:T(8,128)(2,1)} %latent_ref.1), channel_id=1, source_target_pairs={{0,2},{1,3},{2,0},{3,1},{4,6},{5,7},{6,4},{7,5},{8,10},{9,11},{10,... | collective-permute-start | bytes 1572872 | tf_op jit(solution)/shard_map/ppermute | solution.py:577
  3.0 25.7 %collective-permute-start.3 = (bf16[128,2048]{1,0:T(8,128)(2,1)}, bf16[128,2048]{1,0:T(8,128)(2,1)S(1)}, u32[]{:S(2)}, u32[]{:S(2)}) collective-permute-start(bf16[128,2048]{1,0:T(8,128)(2,1)} %latent_ref.1), channel_id=1, source_target_pairs={{0,1},{1,0},{2,3},{3,2},{4,5},{5,4},{6,7},{7,6},{8,9},{9,8},{10,11... | collective-permute-start | bytes 1572872 | tf_op jit(solution)/shard_map/ppermute | solution.py:577
  5.1 10.0 %collective-permute-start = (f32[8,512]{1,0:T(8,128)}, f32[8,512]{1,0:T(8,128)S(1)}, u32[]{:S(2)}, u32[]{:S(2)}) collective-permute-start(f32[8,512]{1,0:T(8,128)} %shard_map.136.one_ref), channel_id=1, source_target_pairs={{0,16},{4,20},{8,24},{12,28},{16,0},{20,4},{24,8},{28,12},{1,17},{... | collective-permute-start | bytes 49160 | tf_op jit(solution)/shard_map/ppermute | solution.py:577
  7.8 20.9 %copy-start.8 = (f32[64]{0:T(128)S(1)}, f32[64]{0:T(128)}, u32[]{:S(2)}) copy-start(f32[64]{0:T(128)} %param.26) | copy-start | bytes 772
  7.8 20.8 %copy-start.1 = (bf16[128,2048]{1,0:T(8,128)(2,1)S(1)}, bf16[128,2048]{1,0:T(8,128)(2,1)}, u32[]{:S(2)}) copy-start(bf16[128,2048]{1,0:T(8,128)(2,1)} %latent_ref.1) | copy-start | bytes 1572868
  15.1 13.6 %collective-permute-start.5 = (bf16[128,2048]{1,0:T(8,128)(2,1)S(1)}, bf16[128,2048]{1,0:T(8,128)(2,1)S(1)}, u32[]{:S(2)}, u32[]{:S(2)}) collective-permute-start(bf16[128,2048]{1,0:T(8,128)(2,1)S(1)} %collective-permute-done.4.refs_5_), channel_id=1, source_target_pairs={{0,1},{1,0},{2,3},{3,2},{4,5},{5,4},{6,7},{7,6},{8,9},{9,8},{10,11... | collective-permute-start | bytes 1572872 | tf_op jit(solution)/shard_map/ppermute | solution.py:577
  15.1 0.7 copy-start.2
  15.8 12.8 %copy-start.4 = (bf16[2048,128]{1,0:T(8,128)(2,1)S(1)}, bf16[2048,128]{1,0:T(8,128)(2,1)}, u32[]{:S(2)}) copy-start(bf16[2048,128]{1,0:T(8,128)(2,1)} %refs_2_.1) | copy-start | bytes 1572868
  15.8 12.9 %copy-start.5 = (bf16[2048,128]{1,0:T(8,128)(2,1)S(1)}, bf16[2048,128]{1,0:T(8,128)(2,1)}, u32[]{:S(2)}) copy-start(bf16[2048,128]{1,0:T(8,128)(2,1)} %refs_3_.1) | copy-start | bytes 1572868
  15.8 12.9 %copy-start.6 = (bf16[64,2048]{1,0:T(8,128)(2,1)S(1)}, bf16[64,2048]{1,0:T(8,128)(2,1)}, u32[]{:S(2)}) copy-start(bf16[64,2048]{1,0:T(8,128)(2,1)} %refs_1_.2) | copy-start | bytes 786436
  15.8 12.9 %copy-start.7 = (f32[2048]{0:T(1024)S(1)}, f32[2048]{0:T(1024)}, u32[]{:S(2)}) copy-start(f32[2048]{0:T(1024)} %param.18) | copy-start | bytes 24580
  15.8 20.5 %copy-start.3 = (bf16[2048,256]{1,0:T(8,128)(2,1)S(1)}, bf16[2048,256]{1,0:T(8,128)(2,1)}, u32[]{:S(2)}) copy-start(bf16[2048,256]{1,0:T(8,128)(2,1)} %refs_1_.3) | copy-start | bytes 3145732
  15.9 20.5 %copy-start.9 = (f32[64]{0:T(128)S(1)}, f32[64]{0:T(128)}, u32[]{:S(2)}) copy-start(f32[64]{0:T(128)} %param.25) | copy-start | bytes 772
  15.9 3.8 %collective-permute-start.1 = (f32[8,512]{1,0:T(8,128)S(1)}, f32[8,512]{1,0:T(8,128)S(1)}, u32[]{:S(2)}, u32[]{:S(2)}) collective-permute-start(f32[8,512]{1,0:T(8,128)S(1)} %shard_map.137.one_ref), channel_id=1, source_target_pairs={{0,8},{4,12},{8,0},{12,4},{16,24},{20,28},{24,16},{28,20},{1,9},{5... | collective-permute-start | bytes 49160 | tf_op jit(solution)/shard_map/ppermute | solution.py:577
  19.7 3.7 %collective-permute-start.2 = (f32[8,512]{1,0:T(8,128)S(1)}, f32[8,512]{1,0:T(8,128)S(1)}, u32[]{:S(2)}, u32[]{:S(2)}) collective-permute-start(f32[8,512]{1,0:T(8,128)S(1)} %shard_map.138.one_ref), channel_id=1, source_target_pairs={{0,4},{4,0},{8,12},{12,8},{16,20},{20,16},{24,28},{28,24},{1,5},{5... | collective-permute-start | bytes 49160 | tf_op jit(solution)/shard_map/ppermute | solution.py:577
  30.9 8.0 %collective-permute-start.10 = (bf16[4,128,128]{2,1,0:T(8,128)(2,1)S(1)}, bf16[4,128,128]{2,1,0:T(8,128)(2,1)S(1)}, u32[]{:S(2)}, u32[]{:S(2)}) collective-permute-start(bf16[4,128,128]{2,1,0:T(8,128)(2,1)S(1)} %get-tuple-element.43.refs_1_.refs_2_), channel_id=1, source_target_pairs={{0,24},{4,28},{8,16},{12,20},{16,8},{20,12},{24,0},{28,4},{1,25},{... | collective-permute-start | bytes 393224 | tf_op jit(solution)/shard_map/ppermute | solution.py:577
  34.8 9.0 %collective-permute-start.6 = (bf16[5,128,128]{2,1,0:T(8,128)(2,1)S(1)}, bf16[5,128,128]{2,1,0:T(8,128)(2,1)S(1)}, u32[]{:S(2)}, u32[]{:S(2)}) collective-permute-start(bf16[5,128,128]{2,1,0:T(8,128)(2,1)S(1)} %get-tuple-element.40), channel_id=1, source_target_pairs={{0,4},{4,0},{8,12},{12,8},{16,20},{20,16},{24,28},{28,24},{1,5},{5... | collective-permute-start | bytes 491528 | tf_op jit(solution)/shard_map/ppermute | solution.py:577
  37.3 6.5 %collective-permute-start.9 = (bf16[4,128,128]{2,1,0:T(8,128)(2,1)S(1)}, bf16[4,128,128]{2,1,0:T(8,128)(2,1)S(1)}, u32[]{:S(2)}, u32[]{:S(2)}) collective-permute-start(bf16[4,128,128]{2,1,0:T(8,128)(2,1)S(1)} %get-tuple-element.42), channel_id=1, source_target_pairs={{0,4},{4,0},{8,12},{12,8},{16,20},{20,16},{24,28},{28,24},{1,5},{5... | collective-permute-start | bytes 393224 | tf_op jit(solution)/shard_map/ppermute | solution.py:577
  37.9 9.6 %collective-permute-start.13 = (bf16[4,128,128]{2,1,0:T(8,128)(2,1)S(1)}, bf16[4,128,128]{2,1,0:T(8,128)(2,1)S(1)}, u32[]{:S(2)}, u32[]{:S(2)}) collective-permute-start(bf16[4,128,128]{2,1,0:T(8,128)(2,1)S(1)} %get-tuple-element.43.refs_1_.refs_2_), channel_id=1, source_target_pairs={{0,8},{4,12},{8,0},{12,4},{16,24},{20,28},{24,16},{28,20},{1,9},{5... | collective-permute-start | bytes 393224 | tf_op jit(solution)/shard_map/ppermute | solution.py:577
  38.9 18.2 %collective-permute-start.11 = (bf16[4,128,128]{2,1,0:T(8,128)(2,1)S(1)}, bf16[4,128,128]{2,1,0:T(8,128)(2,1)S(1)}, u32[]{:S(2)}, u32[]{:S(2)}) collective-permute-start(bf16[4,128,128]{2,1,0:T(8,128)(2,1)S(1)} %collective-permute-done.10.refs_3_), channel_id=1, source_target_pairs={{0,8},{4,12},{8,0},{12,4},{16,24},{20,28},{24,16},{28,20},{1,9},{5... | collective-permute-start | bytes 393224 | tf_op jit(solution)/shard_map/ppermute | solution.py:577
  43.9 10.6 %collective-permute-start.12 = (bf16[5,128,128]{2,1,0:T(8,128)(2,1)S(1)}, bf16[5,128,128]{2,1,0:T(8,128)(2,1)S(1)}, u32[]{:S(2)}, u32[]{:S(2)}) collective-permute-start(bf16[5,128,128]{2,1,0:T(8,128)(2,1)S(1)} %shard_map.142.refs_3_), channel_id=1, source_target_pairs={{0,8},{4,12},{8,0},{12,4},{16,24},{20,28},{24,16},{28,20},{1,9},{5... | collective-permute-start | bytes 491528 | tf_op jit(solution)/shard_map/ppermute | solution.py:577
  44.0 9.7 %collective-permute-start.7 = (bf16[5,128,128]{2,1,0:T(8,128)(2,1)S(1)}, bf16[5,128,128]{2,1,0:T(8,128)(2,1)S(1)}, u32[]{:S(2)}, u32[]{:S(2)}) collective-permute-start(bf16[5,128,128]{2,1,0:T(8,128)(2,1)S(1)} %shard_map.142.refs_3_), channel_id=1, source_target_pairs={{0,24},{4,28},{8,16},{12,20},{16,8},{20,12},{24,0},{28,4},{1,25},{... | collective-permute-start | bytes 491528 | tf_op jit(solution)/shard_map/ppermute | solution.py:577
  53.7 5.3 %collective-permute-start.8 = (bf16[5,128,128]{2,1,0:T(8,128)(2,1)S(1)}, bf16[5,128,128]{2,1,0:T(8,128)(2,1)S(1)}, u32[]{:S(2)}, u32[]{:S(2)}) collective-permute-start(bf16[5,128,128]{2,1,0:T(8,128)(2,1)S(1)} %collective-permute-done.7.refs_3_.refs_1_), channel_id=1, source_target_pairs={{0,8},{4,12},{8,0},{12,4},{16,24},{20,28},{24,16},{28,20},{1,9},{5... | collective-permute-start | bytes 491528 | tf_op jit(solution)/shard_map/ppermute | solution.py:577
  59.0 12.4 %copy-start = (bf16[1024,2048]{1,0:T(8,128)(2,1)S(1)}, bf16[1024,2048]{1,0:T(8,128)(2,1)}, u32[]{:S(2)}) copy-start(bf16[1024,2048]{1,0:T(8,128)(2,1)} %weight_ref.1) | copy-start | bytes 12582916
  60.0 7.2 %collective-permute-start.20 = (bf16[128,128]{1,0:T(8,128)(2,1)S(1)}, bf16[128,128]{1,0:T(8,128)(2,1)S(1)}, u32[]{:S(2)}, u32[]{:S(2)}) collective-permute-start(bf16[128,128]{1,0:T(8,128)(2,1)S(1)} %get-tuple-element.71), channel_id=1, source_target_pairs={{0,7},{1,6},{2,5},{3,4},{4,3},{5,2},{6,1},{7,0},{8,15},{9,14},{10,... | collective-permute-start | bytes 98312 | tf_op jit(solution)/shard_map/ppermute | solution.py:587
  60.1 8.0 %collective-permute-start.19 = (bf16[128,128]{1,0:T(8,128)(2,1)S(1)}, bf16[128,128]{1,0:T(8,128)(2,1)S(1)}, u32[]{:S(2)}, u32[]{:S(2)}) collective-permute-start(bf16[128,128]{1,0:T(8,128)(2,1)S(1)} %get-tuple-element.72), channel_id=1, source_target_pairs={{0,6},{1,7},{2,4},{3,5},{4,2},{5,3},{6,0},{7,1},{8,14},{9,15},{10,... | collective-permute-start | bytes 98312 | tf_op jit(solution)/shard_map/ppermute | solution.py:587
  64.5 3.8 %collective-permute-start.18 = (bf16[128,128]{1,0:T(8,128)(2,1)S(1)}, bf16[128,128]{1,0:T(8,128)(2,1)S(1)}, u32[]{:S(2)}, u32[]{:S(2)}) collective-permute-start(bf16[128,128]{1,0:T(8,128)(2,1)S(1)} %get-tuple-element.73), channel_id=1, source_target_pairs={{0,5},{1,4},{2,7},{3,6},{4,1},{5,0},{6,3},{7,2},{8,13},{9,12},{10,... | collective-permute-start | bytes 98312 | tf_op jit(solution)/shard_map/ppermute | solution.py:587
  65.9 3.9 %collective-permute-start.17 = (bf16[128,128]{1,0:T(8,128)(2,1)S(1)}, bf16[128,128]{1,0:T(8,128)(2,1)S(1)}, u32[]{:S(2)}, u32[]{:S(2)}) collective-permute-start(bf16[128,128]{1,0:T(8,128)(2,1)S(1)} %get-tuple-element.74), channel_id=1, source_target_pairs={{0,4},{1,5},{2,6},{3,7},{4,0},{5,1},{6,2},{7,3},{8,12},{9,13},{10,... | collective-permute-start | bytes 98312 | tf_op jit(solution)/shard_map/ppermute | solution.py:587
  66.5 3.5 %collective-permute-start.16 = (bf16[128,128]{1,0:T(8,128)(2,1)S(1)}, bf16[128,128]{1,0:T(8,128)(2,1)S(1)}, u32[]{:S(2)}, u32[]{:S(2)}) collective-permute-start(bf16[128,128]{1,0:T(8,128)(2,1)S(1)} %get-tuple-element.75), channel_id=1, source_target_pairs={{0,3},{1,2},{2,1},{3,0},{4,7},{5,6},{6,5},{7,4},{8,11},{9,10},{10,... | collective-permute-start | bytes 98312 | tf_op jit(solution)/shard_map/ppermute | solution.py:577
  67.2 4.1 %collective-permute-start.15 = (bf16[128,128]{1,0:T(8,128)(2,1)S(1)}, bf16[128,128]{1,0:T(8,128)(2,1)S(1)}, u32[]{:S(2)}, u32[]{:S(2)}) collective-permute-start(bf16[128,128]{1,0:T(8,128)(2,1)S(1)} %get-tuple-element.76), channel_id=1, source_target_pairs={{0,2},{1,3},{2,0},{3,1},{4,6},{5,7},{6,4},{7,5},{8,10},{9,11},{10,... | collective-permute-start | bytes 98312 | tf_op jit(solution)/shard_map/ppermute | solution.py:577
  68.1 3.3 %collective-permute-start.14 = (bf16[128,128]{1,0:T(8,128)(2,1)S(1)}, bf16[128,128]{1,0:T(8,128)(2,1)S(1)}, u32[]{:S(2)}, u32[]{:S(2)}) collective-permute-start(bf16[128,128]{1,0:T(8,128)(2,1)S(1)} %get-tuple-element.77), channel_id=1, source_target_pairs={{0,1},{1,0},{2,3},{3,2},{4,5},{5,4},{6,7},{7,6},{8,9},{9,8},{10,11... | collective-permute-start | bytes 98312 | tf_op jit(solution)/shard_map/ppermute | solution.py:577

commit v8 on v7

--- a/solution.py
+++ b/solution.py
@@ -269,6 +269,24 @@
     return kernel_call(combine_body, jax.ShapeDtypeStruct(one.shape, one.dtype), 2, flops)(
         one, other
     )
+
+
+def stash_body(source, target, sem):
+    copy = pltpu.make_async_copy(source, target, sem)
+    copy.start()
+    copy.wait()
+
+
+def stash(member):
+    return pl.pallas_call(
+        stash_body,
+        out_shape=jax.ShapeDtypeStruct(member.shape, member.dtype),
+        in_specs=[hbm_spec()],
+        out_specs=whole_spec(),
+        scratch_shapes=[pltpu.SemaphoreType.DMA],
+        cost_estimate=pl.CostEstimate(flops=10**6, transcendentals=0, bytes_accessed=0),
+        compiler_params=pltpu.CompilerParams(vmem_limit_bytes=MODEST),
+    )(member)
 
 
 def opening(first, second, *weights):
@@ -643,6 +661,8 @@
     mask = seq_split // 2
     while mask:
         other = xor_move(part, "sp", mask)
+        if 2 * mask == seq_split:
+            part = stash(part)
         part = combine(part, other, 10**11 if 2 * mask == seq_split else 10**6)
         mask //= 2
     both = xor_move(far, "tp", 1)
@@ -703,9 +723,11 @@
     own, other = attend(
         [(keep_q, own, [0]), (near_q, other, [0, 1])], [near_up, near_down], offset
     )
-    own, other = attend([(keep_q, own, [0]), (near_q, other, [0])], [across], offset)
+    own, other = attend(
+        [(keep_q, own, [0, 1]), (near_q, other, [0])], [across, near_down], offset
+    )
     ((other,),) = attend([(near_q, other, [0])], [near_across], offset, True)
-    ((own,),) = attend([(keep_q, own, [0, 1])], [near_down, near_across], offset, True)
+    ((own,),) = attend([(keep_q, own, [0])], [near_across], offset, True)
     sent = [cross_move(other[j], j) for j in range(head_split)]
     parts = [own[0]] + [xor_move(own[j], "tp", j) for j in range(1, head_split)] + sent
     width = q_heads * CHANNEL_SPAN

time: 73.2 us -> 72.4 us (0.989)
  waiting for transfers between devices: 20.2 us -> 19.3 us
    ppermute x17, waiting for transfers between devices: 18.7 us -> 17.8 us  [xor_move(): return lax.ppermute(member, axis, [(i, i ^ mask) for i in range(size)])]
  transfers between devices with their start and end apart: 21 -> 21, of which waited for: 10 -> 9; matrix products, arithmetic and copies ran while one was open for 1% -> 1% of each run, Pallas kernels for 21% -> 21%
where the time goes in v8:
time: 72.4 us; the launch traced here: 72.1 us
  starting transfers between devices  26 us (36%)
  Pallas kernels  20 us (28%)
  waiting for transfers between devices  19.3 us (27%)
  blocking collectives  5.22 us (7%)
  local copies, waits for them, and re-layouts  0.79 us (1%)
    ppermute x17, starting transfers between devices, xor_move(): return lax.ppermute(member, axis, [(i, i ^ mask) for i in range(size)])  21.5 us
    ppermute x17, waiting for transfers between devices, xor_move(): return lax.ppermute(member, axis, [(i, i ^ mask) for i in range(size)])  17.8 us
    pallas_call x7, Pallas kernels, attend(): kernel_call(body, out * len(sources), len(inputs), 40 * 2 * lanes * keys...  13.1 us
    all_gather x1, blocking collectives, inner_device(): modulation = lax.all_gather(part, 'tp', axis=0, tiled=False)  5.22 us
    ppermute x4, starting transfers between devices, cross_move(): return lax.ppermute(member, ('sp', 'tp'), pairs)  4.52 us
    pallas_call x1, Pallas kernels, inner_device(): kernel_call(lambda *refs: projection_body(kv_heads, *refs), [jax.ShapeDty...  2.19 us
    pallas_call x1, Pallas kernels, opening(): pl.pallas_call(opening_body, out_shape=jax.ShapeDtypeStruct((8, columns),...  2.08 us
    pallas_call x1, Pallas kernels, inner_device(): kernel_call(output_body, jax.ShapeDtypeStruct(latent.shape, jnp.bfloat16)...  1.59 us
  transfers between devices with their start and end apart: 21, of which 9 were waited for; matrix products, arithmetic and copies ran while one was open for 1% of the time, Pallas kernels for 21%

profile of v8, /device:TPU:0, one launch (start us, length us, event | category | flops | bytes accessed | tf_op | source)
XLA Modules:
  0.0 72.1 jit_solution(5936654937742726980)
XLA Ops:
  0.0 3.0 %collective-permute-start.4 = (bf16[128,2048]{1,0:T(8,128)(2,1)}, bf16[128,2048]{1,0:T(8,128)(2,1)S(1)}, u32[]{:S(2)}, u32[]{:S(2)}) collective-permute-start(bf16[128,2048]{1,0:T(8,128)(2,1)} %latent_ref.1), channel_id=1, source_target_pairs={{0,2},{1,3},{2,0},{3,1},{4,6},{5,7},{6,4},{7,5},{8,10},{9,11},{10,... | collective-permute-start | bytes 1572872 | tf_op jit(solution)/shard_map/ppermute | solution.py:595
  3.0 0.0 collective-permute-start.3
  3.0 2.1 %shard_map.136.source = f32[8,512]{1,0:T(8,128)} custom-call(f32[1,2048]{1,0:T(1,128)} %bitcast.27, f32[1,2048]{1,0:T(1,128)} %bitcast.28, bf16[256,512]{1,0:T(8,128)(2,1)} %shift_hbm.1, bf16[256,512]{1,0:T(8,128)(2,1)} %scale_hbm.1, bf16[256,512]{1,0:T(8,128)(2,1)} %gate_hbm.1), custom_call_target="tpu_custom_call" | custom-call | flops 100000000 | tf_op jit(solution)/shard_map/pallas_call | solution.py:294
  5.1 2.7 %collective-permute-start = (f32[8,512]{1,0:T(8,128)}, f32[8,512]{1,0:T(8,128)S(1)}, u32[]{:S(2)}, u32[]{:S(2)}) collective-permute-start(f32[8,512]{1,0:T(8,128)} %shard_map.136.source), channel_id=1, source_target_pairs={{0,16},{4,20},{8,24},{12,28},{16,0},{20,4},{24,8},{28,12},{1,17},{... | collective-permute-start | bytes 49160 | tf_op jit(solution)/shard_map/ppermute | solution.py:595
  7.7 0.1 fusion.2
  7.8 0.7 copy-done.2
  8.6 0.0 copy-start.1
  8.6 0.0 copy-start.4
  8.6 0.0 copy-start.5
  8.6 0.0 copy-start.6
  8.6 0.0 copy-start.7
  8.6 0.0 copy-start.8
  8.6 6.5 %collective-permute-done.4.refs_5_ = bf16[128,2048]{1,0:T(8,128)(2,1)S(1)} collective-permute-done((bf16[128,2048]{1,0:T(8,128)(2,1)}, bf16[128,2048]{1,0:T(8,128)(2,1)S(1)}, u32[]{:S(2)}, u32[]{:S(2)}) %collective-permute-start.4) | collective-permute-done | bytes 524320 | tf_op jit(solution)/shard_map/ppermute | solution.py:595
  15.1 0.0 collective-permute-start.5
  15.1 0.0 collective-permute-done.other_ref
  15.1 0.0 copy-start.3
  15.1 0.0 copy-start.9
  15.1 1.9 %collective-permute-start.1 = (f32[8,512]{1,0:T(8,128)S(1)}, f32[8,512]{1,0:T(8,128)S(1)}, u32[]{:S(2)}, u32[]{:S(2)}) collective-permute-start(f32[8,512]{1,0:T(8,128)S(1)} %shard_map.138.one_ref), channel_id=1, source_target_pairs={{0,8},{4,12},{8,0},{12,4},{16,24},{20,28},{24,16},{28,20},{1,9},{5... | collective-permute-start | bytes 49160 | tf_op jit(solution)/shard_map/ppermute | solution.py:595
  17.0 0.3 fusion
  17.3 1.6 %collective-permute-done.1.other_ref = f32[8,512]{1,0:T(8,128)S(1)} collective-permute-done((f32[8,512]{1,0:T(8,128)S(1)}, f32[8,512]{1,0:T(8,128)S(1)}, u32[]{:S(2)}, u32[]{:S(2)}) %collective-permute-start.1) | collective-permute-done | bytes 16416 | tf_op jit(solution)/shard_map/ppermute | solution.py:595
  18.9 1.8 %collective-permute-start.2 = (f32[8,512]{1,0:T(8,128)S(1)}, f32[8,512]{1,0:T(8,128)S(1)}, u32[]{:S(2)}, u32[]{:S(2)}) collective-permute-start(f32[8,512]{1,0:T(8,128)S(1)} %shard_map.139.one_ref), channel_id=1, source_target_pairs={{0,4},{4,0},{8,12},{12,8},{16,20},{20,16},{24,28},{28,24},{1,5},{5... | collective-permute-start | bytes 49160 | tf_op jit(solution)/shard_map/ppermute | solution.py:595
  20.7 1.9 %collective-permute-done.2.other_ref = f32[8,512]{1,0:T(8,128)S(1)} collective-permute-done((f32[8,512]{1,0:T(8,128)S(1)}, f32[8,512]{1,0:T(8,128)S(1)}, u32[]{:S(2)}, u32[]{:S(2)}) %collective-permute-start.2) | collective-permute-done | bytes 16416 | tf_op jit(solution)/shard_map/ppermute | solution.py:595
  22.7 5.2 %all-gather = f32[32,512]{1,0:T(8,128)S(1)} all-gather(f32[8,512]{1,0:T(8,128)S(1)} %shard_map.140), channel_id=2, replica_groups=mesh['sp'=8,'tp'=4] {'tp'}, dimensions={0}, use_global_device_ids=true | all-gather | bytes 81920 | tf_op jit(solution)/shard_map/all_gather | solution.py:669
  27.9 0.0 collective-permute-done.3.refs_4_
  27.9 0.0 collective-permute-done.5.refs_6_
  28.0 2.2 %shard_map.141 = (bf16[4,128,128]{2,1,0:T(8,128)(2,1)S(1)}, bf16[128,128]{1,0:T(8,128)(2,1)S(1)}, bf16[5,128,128]{2,1,0:T(8,128)(2,1)S(1)}, bf16[4,128,2048]{2,1,0:T(8,128)(2,1)S(1)}) custom-call(bf16[128,2048]{1,0:T(8,128)(2,1)S(1)} %copy-done.1, bf16[64,2048]{1,0:T(8,128)(2,1)S(1)} %copy-done.6, bf16[2048,128]{1,0:T(8,128)(2,1)S(1)} %copy-done.4, ...), custom_call_target="tpu_custom_call" | custom-call | flops 1073741824 | tf_op jit(solution)/shard_map/pallas_call | solution.py:674
  30.2 3.9 %collective-permute-start.10 = (bf16[4,128,128]{2,1,0:T(8,128)(2,1)S(1)}, bf16[4,128,128]{2,1,0:T(8,128)(2,1)S(1)}, u32[]{:S(2)}, u32[]{:S(2)}) collective-permute-start(bf16[4,128,128]{2,1,0:T(8,128)(2,1)S(1)} %get-tuple-element.43.refs_1_.refs_2_), channel_id=1, source_target_pairs={{0,24},{4,28},{8,16},{12,20},{16,8},{20,12},{24,0},{28,4},{1,25},{... | collective-permute-start | bytes 393224 | tf_op jit(solution)/shard_map/ppermute | solution.py:595
  34.1 1.5 %collective-permute-start.6 = (bf16[5,128,128]{2,1,0:T(8,128)(2,1)S(1)}, bf16[5,128,128]{2,1,0:T(8,128)(2,1)S(1)}, u32[]{:S(2)}, u32[]{:S(2)}) collective-permute-start(bf16[5,128,128]{2,1,0:T(8,128)(2,1)S(1)} %get-tuple-element.40), channel_id=1, source_target_pairs={{0,4},{4,0},{8,12},{12,8},{16,20},{20,16},{24,28},{28,24},{1,5},{5... | collective-permute-start | bytes 491528 | tf_op jit(solution)/shard_map/ppermute | solution.py:595
  35.6 0.9 %shard_map.142 = (bf16[8,128,128]{2,1,0:T(8,128)(2,1)S(1)}, bf16[4,128,128]{2,1,0:T(8,128)(2,1)S(1)}) custom-call(bf16[4,128,2048]{2,1,0:T(8,128)(2,1)S(1)} %get-tuple-element.38.refs_0_, bf16[2048,256]{1,0:T(8,128)(2,1)S(1)} %copy-done.3, f32[1,64]{1,0:T(1,128)S(1)} %bitcast.26, f32[4,64,128]{2,1,0:T(8,128)S(1)} %get-tuple-element.90.refs_10_.refs_3_, ...), custom_call_target="tpu_custom_call" | custom-call | flops 1073741824 | tf_op jit(solution)/shard_map/pallas_call | solution.py:702
  36.5 0.6 collective-permute-start.9
  37.1 0.0 collective-permute-start.13
  37.1 0.9 %shard_map.145 = (f32[2,1,512]{2,1,0:T(1,128)S(1)}, f32[2,1,512]{2,1,0:T(1,128)S(1)}, f32[2,64,512]{2,1,0:T(8,128)S(1)}) custom-call(bf16[8,128,128]{2,1,0:T(8,128)(2,1)S(1)} %get-tuple-element.39.refs_0_, bf16[4,128,128]{2,1,0:T(8,128)(2,1)S(1)} %get-tuple-element.43.refs_1_.refs_2_), custom_call_target="tpu_custom_call" | custom-call | flops 671088640 | tf_op jit(solution)/shard_map/pallas_call | solution.py:561
  38.0 0.2 collective-permute-done.10.refs_3_
  38.2 2.4 %collective-permute-start.11 = (bf16[4,128,128]{2,1,0:T(8,128)(2,1)S(1)}, bf16[4,128,128]{2,1,0:T(8,128)(2,1)S(1)}, u32[]{:S(2)}, u32[]{:S(2)}) collective-permute-start(bf16[4,128,128]{2,1,0:T(8,128)(2,1)S(1)} %collective-permute-done.10.refs_3_), channel_id=1, source_target_pairs={{0,8},{4,12},{8,0},{12,4},{16,24},{20,28},{24,16},{28,20},{1,9},{5... | collective-permute-start | bytes 393224 | tf_op jit(solution)/shard_map/ppermute | solution.py:595
  40.6 2.4 %collective-permute-done.9.q_ref = bf16[4,128,128]{2,1,0:T(8,128)(2,1)S(1)} collective-permute-done((bf16[4,128,128]{2,1,0:T(8,128)(2,1)S(1)}, bf16[4,128,128]{2,1,0:T(8,128)(2,1)S(1)}, u32[]{:S(2)}, u32[]{:S(2)}) %collective-permute-start.9) | collective-permute-done | bytes 131104 | tf_op jit(solution)/shard_map/ppermute | solution.py:595
  43.1 0.0 collective-permute-done.6.near_ref
  43.1 0.1 shard_map.143.refs_3_
  43.2 0.0 collective-permute-start.12
  43.2 1.0 %collective-permute-start.7 = (bf16[5,128,128]{2,1,0:T(8,128)(2,1)S(1)}, bf16[5,128,128]{2,1,0:T(8,128)(2,1)S(1)}, u32[]{:S(2)}, u32[]{:S(2)}) collective-permute-start(bf16[5,128,128]{2,1,0:T(8,128)(2,1)S(1)} %shard_map.143.refs_3_), channel_id=1, source_target_pairs={{0,24},{4,28},{8,16},{12,20},{16,8},{20,12},{24,0},{28,4},{1,25},{... | collective-permute-start | bytes 491528 | tf_op jit(solution)/shard_map/ppermute | solution.py:595
  44.2 2.4 %shard_map.146 = (f32[2,1,512]{2,1,0:T(1,128)S(1)}, f32[2,1,512]{2,1,0:T(1,128)S(1)}, f32[2,64,512]{2,1,0:T(8,128)S(1)}, f32[2,1,512]{2,1,0:T(1,128)S(1)}, f32[2...) custom-call(bf16[8,128,128]{2,1,0:T(8,128)(2,1)S(1)} %get-tuple-element.39.refs_0_, ...), custom_call_target="tpu_custom_call" | custom-call | flops 2348810240 | tf_op jit(solution)/shard_map/pallas_call | solution.py:561
  46.7 0.0 collective-permute-done.13.refs_2_
  46.7 2.6 %shard_map.147 = (f32[2,1,512]{2,1,0:T(1,128)S(1)}, f32[2,1,512]{2,1,0:T(1,128)S(1)}, f32[2,64,512]{2,1,0:T(8,128)S(1)}, f32[2,1,512]{2,1,0:T(1,128)S(1)}, f32[2...) custom-call(bf16[8,128,128]{2,1,0:T(8,128)(2,1)S(1)} %get-tuple-element.39.refs_0_, ...), custom_call_target="tpu_custom_call" | custom-call | flops 2684354560 | tf_op jit(solution)/shard_map/pallas_call | solution.py:561
  49.4 3.6 %collective-permute-done.7.refs_3_ = bf16[5,128,128]{2,1,0:T(8,128)(2,1)S(1)} collective-permute-done((bf16[5,128,128]{2,1,0:T(8,128)(2,1)S(1)}, bf16[5,128,128]{2,1,0:T(8,128)(2,1)S(1)}, u32[]{:S(2)}, u32[]{:S(2)}) %collective-permute-start.7) | collective-permute-done | bytes 163872 | tf_op jit(solution)/shard_map/ppermute | solution.py:595
  52.9 0.9 %collective-permute-start.8 = (bf16[5,128,128]{2,1,0:T(8,128)(2,1)S(1)}, bf16[5,128,128]{2,1,0:T(8,128)(2,1)S(1)}, u32[]{:S(2)}, u32[]{:S(2)}) collective-permute-start(bf16[5,128,128]{2,1,0:T(8,128)(2,1)S(1)} %collective-permute-done.7.refs_3_), channel_id=1, source_target_pairs={{0,8},{4,12},{8,0},{12,4},{16,24},{20,28},{24,16},{28,20},{1,9},{5... | collective-permute-start | bytes 491528 | tf_op jit(solution)/shard_map/ppermute | solution.py:595
  53.8 0.0 collective-permute-done.12.refs_2_
  53.8 2.6 %shard_map.148 = (f32[2,1,512]{2,1,0:T(1,128)S(1)}, f32[2,1,512]{2,1,0:T(1,128)S(1)}, f32[2,64,512]{2,1,0:T(8,128)S(1)}, f32[2,1,512]{2,1,0:T(1,128)S(1)}, f32[2...) custom-call(bf16[8,128,128]{2,1,0:T(8,128)(2,1)S(1)} %get-tuple-element.39.refs_0_, ...), custom_call_target="tpu_custom_call" | custom-call | flops 2516582400 | tf_op jit(solution)/shard_map/pallas_call | solution.py:561
  56.4 0.0 collective-permute-done.11.refs_2_
  56.4 2.5 %shard_map.149 = (f32[2,1,512]{2,1,0:T(1,128)S(1)}, f32[2,1,512]{2,1,0:T(1,128)S(1)}, f32[2,64,512]{2,1,0:T(8,128)S(1)}, f32[2,1,512]{2,1,0:T(1,128)S(1)}, f32[2...) custom-call(bf16[8,128,128]{2,1,0:T(8,128)(2,1)S(1)} %get-tuple-element.39.refs_0_, ...), custom_call_target="tpu_custom_call" | custom-call | flops 2181038080 | tf_op jit(solution)/shard_map/pallas_call | solution.py:561
  58.9 0.0 copy-start
  58.9 1.0 %shard_map.151 = bf16[4,128,128]{2,1,0:T(8,128)(2,1)S(1)} custom-call(bf16[8,128,128]{2,1,0:T(8,128)(2,1)S(1)} %shard_map.144.refs_1_.refs_0_, bf16[5,128,128]{2,1,0:T(8,128)(2,1)S(1)} %collective-permute-done.8.refs_1_, f32[2,1,512]{2,1,0:T(1,128)S(1)} %get-tuple-element.68.refs_2_, f32[2,1,512]{2,1,0:T(1,128)S(1)} %get-tuple-element.69.refs_3_, ...), custom_call_target="tpu_custom_call" | custom-call | flops 838860800 | tf_op jit(solution)/shard_map/pallas_call | solution.py:561
  60.0 0.1 collective-permute-start.20
  60.1 2.5 %collective-permute-start.19 = (bf16[128,128]{1,0:T(8,128)(2,1)S(1)}, bf16[128,128]{1,0:T(8,128)(2,1)S(1)}, u32[]{:S(2)}, u32[]{:S(2)}) collective-permute-start(bf16[128,128]{1,0:T(8,128)(2,1)S(1)} %get-tuple-element.72), channel_id=1, source_target_pairs={{0,6},{1,7},{2,4},{3,5},{4,2},{5,3},{6,0},{7,1},{8,14},{9,15},{10,... | collective-permute-start | bytes 98312 | tf_op jit(solution)/shard_map/ppermute | solution.py:605
  62.6 1.0 %shard_map.150 = bf16[4,128,128]{2,1,0:T(8,128)(2,1)S(1)} custom-call(bf16[8,128,128]{2,1,0:T(8,128)(2,1)S(1)} %get-tuple-element.39.refs_0_, bf16[5,128,128]{2,1,0:T(8,128)(2,1)S(1)} %collective-permute-done.8.refs_1_, f32[2,1,512]{2,1,0:T(1,128)S(1)} %get-tuple-element.65.refs_2_, f32[2,1,512]{2,1,0:T(1,128)S(1)} %get-tuple-element.66.refs_3_, ...), custom_call_target="tpu_custom_call" | custom-call | flops 838860800 | tf_op jit(solution)/shard_map/pallas_call | solution.py:561
  63.7 1.4 %collective-permute-start.18 = (bf16[128,128]{1,0:T(8,128)(2,1)S(1)}, bf16[128,128]{1,0:T(8,128)(2,1)S(1)}, u32[]{:S(2)}, u32[]{:S(2)}) collective-permute-start(bf16[128,128]{1,0:T(8,128)(2,1)S(1)} %get-tuple-element.73), channel_id=1, source_target_pairs={{0,5},{1,4},{2,7},{3,6},{4,1},{5,0},{6,3},{7,2},{8,13},{9,12},{10,... | collective-permute-start | bytes 98312 | tf_op jit(solution)/shard_map/ppermute | solution.py:605
  65.1 0.5 collective-permute-start.17
  65.6 0.8 %collective-permute-start.16 = (bf16[128,128]{1,0:T(8,128)(2,1)S(1)}, bf16[128,128]{1,0:T(8,128)(2,1)S(1)}, u32[]{:S(2)}, u32[]{:S(2)}) collective-permute-start(bf16[128,128]{1,0:T(8,128)(2,1)S(1)} %get-tuple-element.75), channel_id=1, source_target_pairs={{0,3},{1,2},{2,1},{3,0},{4,7},{5,6},{6,5},{7,4},{8,11},{9,10},{10,... | collective-permute-start | bytes 98312 | tf_op jit(solution)/shard_map/ppermute | solution.py:595
  66.4 0.0 collective-permute-done.20.refs_7_
  66.4 0.8 %collective-permute-start.15 = (bf16[128,128]{1,0:T(8,128)(2,1)S(1)}, bf16[128,128]{1,0:T(8,128)(2,1)S(1)}, u32[]{:S(2)}, u32[]{:S(2)}) collective-permute-start(bf16[128,128]{1,0:T(8,128)(2,1)S(1)} %get-tuple-element.76), channel_id=1, source_target_pairs={{0,2},{1,3},{2,0},{3,1},{4,6},{5,7},{6,4},{7,5},{8,10},{9,11},{10,... | collective-permute-start | bytes 98312 | tf_op jit(solution)/shard_map/ppermute | solution.py:595
  67.2 0.0 collective-permute-done.19.refs_6_
  67.2 0.2 collective-permute-start.14
  67.4 1.6 %collective-permute-done.17.refs_4_ = bf16[128,128]{1,0:T(8,128)(2,1)S(1)} collective-permute-done((bf16[128,128]{1,0:T(8,128)(2,1)S(1)}, bf16[128,128]{1,0:T(8,128)(2,1)S(1)}, u32[]{:S(2)}, u32[]{:S(2)}) %collective-permute-start.17) | collective-permute-done | bytes 32800 | tf_op jit(solution)/shard_map/ppermute | solution.py:605
  69.0 0.1 collective-permute-done.16.refs_3_
  69.1 1.4 %collective-permute-done.15.refs_2_ = bf16[128,128]{1,0:T(8,128)(2,1)S(1)} collective-permute-done((bf16[128,128]{1,0:T(8,128)(2,1)S(1)}, bf16[128,128]{1,0:T(8,128)(2,1)S(1)}, u32[]{:S(2)}, u32[]{:S(2)}) %collective-permute-start.15) | collective-permute-done | bytes 32800 | tf_op jit(solution)/shard_map/ppermute | solution.py:595
  70.5 1.6 %shard_map.152 = bf16[128,2048]{1,0:T(8,128)(2,1)} custom-call(bf16[128,2048]{1,0:T(8,128)(2,1)S(1)} %copy-done.1, f32[4,8,512]{2,1,0:T(8,128)S(1)} %bitcast.23, bf16[1024,2048]{1,0:T(8,128)(2,1)S(1)} %copy-done, bf16[128,128]{1,0:T(8,128)(2,1)S(1)} %get-tuple-element.78.refs_0_, bf16[128,128]{1,0:T(8,128)(2,1)S(1)} %collective-permute-done.14.refs_1_, ...), custom_call_target="tpu_custom_call" | custom-call | flops 536870912 | tf_op jit(solution)/shard_map/pallas_call | solution.py:734
  (23 shorter events, 0.2 us)
Async XLA Ops:
  0.0 15.1 %collective-permute-start.4 = (bf16[128,2048]{1,0:T(8,128)(2,1)}, bf16[128,2048]{1,0:T(8,128)(2,1)S(1)}, u32[]{:S(2)}, u32[]{:S(2)}) collective-permute-start(bf16[128,2048]{1,0:T(8,128)(2,1)} %latent_ref.1), channel_id=1, source_target_pairs={{0,2},{1,3},{2,0},{3,1},{4,6},{5,7},{6,4},{7,5},{8,10},{9,11},{10,... | collective-permute-start | bytes 1572872 | tf_op jit(solution)/shard_map/ppermute | solution.py:595
  3.0 24.9 %collective-permute-start.3 = (bf16[128,2048]{1,0:T(8,128)(2,1)}, bf16[128,2048]{1,0:T(8,128)(2,1)S(1)}, u32[]{:S(2)}, u32[]{:S(2)}) collective-permute-start(bf16[128,2048]{1,0:T(8,128)(2,1)} %latent_ref.1), channel_id=1, source_target_pairs={{0,1},{1,0},{2,3},{3,2},{4,5},{5,4},{6,7},{7,6},{8,9},{9,8},{10,11... | collective-permute-start | bytes 1572872 | tf_op jit(solution)/shard_map/ppermute | solution.py:595
  5.1 10.0 %collective-permute-start = (f32[8,512]{1,0:T(8,128)}, f32[8,512]{1,0:T(8,128)S(1)}, u32[]{:S(2)}, u32[]{:S(2)}) collective-permute-start(f32[8,512]{1,0:T(8,128)} %shard_map.136.source), channel_id=1, source_target_pairs={{0,16},{4,20},{8,24},{12,28},{16,0},{20,4},{24,8},{28,12},{1,17},{... | collective-permute-start | bytes 49160 | tf_op jit(solution)/shard_map/ppermute | solution.py:595
  7.8 0.7 %copy-start.2 = (f32[8,512]{1,0:T(8,128)S(1)}, f32[8,512]{1,0:T(8,128)}, u32[]{:S(2)}) copy-start(f32[8,512]{1,0:T(8,128)} %shard_map.136.source) | copy-start | bytes 49156
  8.6 19.4 %copy-start.1 = (bf16[128,2048]{1,0:T(8,128)(2,1)S(1)}, bf16[128,2048]{1,0:T(8,128)(2,1)}, u32[]{:S(2)}) copy-start(bf16[128,2048]{1,0:T(8,128)(2,1)} %latent_ref.1) | copy-start | bytes 1572868
  8.6 19.4 %copy-start.4 = (bf16[2048,128]{1,0:T(8,128)(2,1)S(1)}, bf16[2048,128]{1,0:T(8,128)(2,1)}, u32[]{:S(2)}) copy-start(bf16[2048,128]{1,0:T(8,128)(2,1)} %refs_2_.1) | copy-start | bytes 1572868
  8.6 19.4 %copy-start.5 = (bf16[2048,128]{1,0:T(8,128)(2,1)S(1)}, bf16[2048,128]{1,0:T(8,128)(2,1)}, u32[]{:S(2)}) copy-start(bf16[2048,128]{1,0:T(8,128)(2,1)} %refs_3_.1) | copy-start | bytes 1572868
  8.6 19.4 %copy-start.6 = (bf16[64,2048]{1,0:T(8,128)(2,1)S(1)}, bf16[64,2048]{1,0:T(8,128)(2,1)}, u32[]{:S(2)}) copy-start(bf16[64,2048]{1,0:T(8,128)(2,1)} %refs_1_.2) | copy-start | bytes 786436
  8.6 19.4 %copy-start.7 = (f32[2048]{0:T(1024)S(1)}, f32[2048]{0:T(1024)}, u32[]{:S(2)}) copy-start(f32[2048]{0:T(1024)} %param.18) | copy-start | bytes 24580
  8.6 19.3 %copy-start.8 = (f32[64]{0:T(128)S(1)}, f32[64]{0:T(128)}, u32[]{:S(2)}) copy-start(f32[64]{0:T(128)} %param.26) | copy-start | bytes 772
  15.1 12.8 %collective-permute-start.5 = (bf16[128,2048]{1,0:T(8,128)(2,1)S(1)}, bf16[128,2048]{1,0:T(8,128)(2,1)S(1)}, u32[]{:S(2)}, u32[]{:S(2)}) collective-permute-start(bf16[128,2048]{1,0:T(8,128)(2,1)S(1)} %collective-permute-done.4.refs_5_), channel_id=1, source_target_pairs={{0,1},{1,0},{2,3},{3,2},{4,5},{5,4},{6,7},{7,6},{8,9},{9,8},{10,11... | collective-permute-start | bytes 1572872 | tf_op jit(solution)/shard_map/ppermute | solution.py:595
  15.1 20.5 %copy-start.3 = (bf16[2048,256]{1,0:T(8,128)(2,1)S(1)}, bf16[2048,256]{1,0:T(8,128)(2,1)}, u32[]{:S(2)}) copy-start(bf16[2048,256]{1,0:T(8,128)(2,1)} %refs_1_.3) | copy-start | bytes 3145732
  15.1 20.5 %copy-start.9 = (f32[64]{0:T(128)S(1)}, f32[64]{0:T(128)}, u32[]{:S(2)}) copy-start(f32[64]{0:T(128)} %param.25) | copy-start | bytes 772
  15.1 3.8 %collective-permute-start.1 = (f32[8,512]{1,0:T(8,128)S(1)}, f32[8,512]{1,0:T(8,128)S(1)}, u32[]{:S(2)}, u32[]{:S(2)}) collective-permute-start(f32[8,512]{1,0:T(8,128)S(1)} %shard_map.138.one_ref), channel_id=1, source_target_pairs={{0,8},{4,12},{8,0},{12,4},{16,24},{20,28},{24,16},{28,20},{1,9},{5... | collective-permute-start | bytes 49160 | tf_op jit(solution)/shard_map/ppermute | solution.py:595
  18.9 3.7 %collective-permute-start.2 = (f32[8,512]{1,0:T(8,128)S(1)}, f32[8,512]{1,0:T(8,128)S(1)}, u32[]{:S(2)}, u32[]{:S(2)}) collective-permute-start(f32[8,512]{1,0:T(8,128)S(1)} %shard_map.139.one_ref), channel_id=1, source_target_pairs={{0,4},{4,0},{8,12},{12,8},{16,20},{20,16},{24,28},{28,24},{1,5},{5... | collective-permute-start | bytes 49160 | tf_op jit(solution)/shard_map/ppermute | solution.py:595
  30.2 8.0 %collective-permute-start.10 = (bf16[4,128,128]{2,1,0:T(8,128)(2,1)S(1)}, bf16[4,128,128]{2,1,0:T(8,128)(2,1)S(1)}, u32[]{:S(2)}, u32[]{:S(2)}) collective-permute-start(bf16[4,128,128]{2,1,0:T(8,128)(2,1)S(1)} %get-tuple-element.43.refs_1_.refs_2_), channel_id=1, source_target_pairs={{0,24},{4,28},{8,16},{12,20},{16,8},{20,12},{24,0},{28,4},{1,25},{... | collective-permute-start | bytes 393224 | tf_op jit(solution)/shard_map/ppermute | solution.py:595
  34.1 9.0 %collective-permute-start.6 = (bf16[5,128,128]{2,1,0:T(8,128)(2,1)S(1)}, bf16[5,128,128]{2,1,0:T(8,128)(2,1)S(1)}, u32[]{:S(2)}, u32[]{:S(2)}) collective-permute-start(bf16[5,128,128]{2,1,0:T(8,128)(2,1)S(1)} %get-tuple-element.40), channel_id=1, source_target_pairs={{0,4},{4,0},{8,12},{12,8},{16,20},{20,16},{24,28},{28,24},{1,5},{5... | collective-permute-start | bytes 491528 | tf_op jit(solution)/shard_map/ppermute | solution.py:595
  36.5 6.5 %collective-permute-start.9 = (bf16[4,128,128]{2,1,0:T(8,128)(2,1)S(1)}, bf16[4,128,128]{2,1,0:T(8,128)(2,1)S(1)}, u32[]{:S(2)}, u32[]{:S(2)}) collective-permute-start(bf16[4,128,128]{2,1,0:T(8,128)(2,1)S(1)} %get-tuple-element.42), channel_id=1, source_target_pairs={{0,4},{4,0},{8,12},{12,8},{16,20},{20,16},{24,28},{28,24},{1,5},{5... | collective-permute-start | bytes 393224 | tf_op jit(solution)/shard_map/ppermute | solution.py:595
  37.1 9.6 %collective-permute-start.13 = (bf16[4,128,128]{2,1,0:T(8,128)(2,1)S(1)}, bf16[4,128,128]{2,1,0:T(8,128)(2,1)S(1)}, u32[]{:S(2)}, u32[]{:S(2)}) collective-permute-start(bf16[4,128,128]{2,1,0:T(8,128)(2,1)S(1)} %get-tuple-element.43.refs_1_.refs_2_), channel_id=1, source_target_pairs={{0,8},{4,12},{8,0},{12,4},{16,24},{20,28},{24,16},{28,20},{1,9},{5... | collective-permute-start | bytes 393224 | tf_op jit(solution)/shard_map/ppermute | solution.py:595
  38.2 18.2 %collective-permute-start.11 = (bf16[4,128,128]{2,1,0:T(8,128)(2,1)S(1)}, bf16[4,128,128]{2,1,0:T(8,128)(2,1)S(1)}, u32[]{:S(2)}, u32[]{:S(2)}) collective-permute-start(bf16[4,128,128]{2,1,0:T(8,128)(2,1)S(1)} %collective-permute-done.10.refs_3_), channel_id=1, source_target_pairs={{0,8},{4,12},{8,0},{12,4},{16,24},{20,28},{24,16},{28,20},{1,9},{5... | collective-permute-start | bytes 393224 | tf_op jit(solution)/shard_map/ppermute | solution.py:595
  43.2 10.6 %collective-permute-start.12 = (bf16[5,128,128]{2,1,0:T(8,128)(2,1)S(1)}, bf16[5,128,128]{2,1,0:T(8,128)(2,1)S(1)}, u32[]{:S(2)}, u32[]{:S(2)}) collective-permute-start(bf16[5,128,128]{2,1,0:T(8,128)(2,1)S(1)} %shard_map.143.refs_3_), channel_id=1, source_target_pairs={{0,8},{4,12},{8,0},{12,4},{16,24},{20,28},{24,16},{28,20},{1,9},{5... | collective-permute-start | bytes 491528 | tf_op jit(solution)/shard_map/ppermute | solution.py:595
  43.2 9.7 %collective-permute-start.7 = (bf16[5,128,128]{2,1,0:T(8,128)(2,1)S(1)}, bf16[5,128,128]{2,1,0:T(8,128)(2,1)S(1)}, u32[]{:S(2)}, u32[]{:S(2)}) collective-permute-start(bf16[5,128,128]{2,1,0:T(8,128)(2,1)S(1)} %shard_map.143.refs_3_), channel_id=1, source_target_pairs={{0,24},{4,28},{8,16},{12,20},{16,8},{20,12},{24,0},{28,4},{1,25},{... | collective-permute-start | bytes 491528 | tf_op jit(solution)/shard_map/ppermute | solution.py:595
  52.9 6.0 %collective-permute-start.8 = (bf16[5,128,128]{2,1,0:T(8,128)(2,1)S(1)}, bf16[5,128,128]{2,1,0:T(8,128)(2,1)S(1)}, u32[]{:S(2)}, u32[]{:S(2)}) collective-permute-start(bf16[5,128,128]{2,1,0:T(8,128)(2,1)S(1)} %collective-permute-done.7.refs_3_), channel_id=1, source_target_pairs={{0,8},{4,12},{8,0},{12,4},{16,24},{20,28},{24,16},{28,20},{1,9},{5... | collective-permute-start | bytes 491528 | tf_op jit(solution)/shard_map/ppermute | solution.py:595
  58.9 11.6 %copy-start = (bf16[1024,2048]{1,0:T(8,128)(2,1)S(1)}, bf16[1024,2048]{1,0:T(8,128)(2,1)}, u32[]{:S(2)}) copy-start(bf16[1024,2048]{1,0:T(8,128)(2,1)} %weight_ref.1) | copy-start | bytes 12582916
  60.0 6.4 %collective-permute-start.20 = (bf16[128,128]{1,0:T(8,128)(2,1)S(1)}, bf16[128,128]{1,0:T(8,128)(2,1)S(1)}, u32[]{:S(2)}, u32[]{:S(2)}) collective-permute-start(bf16[128,128]{1,0:T(8,128)(2,1)S(1)} %get-tuple-element.71), channel_id=1, source_target_pairs={{0,7},{1,6},{2,5},{3,4},{4,3},{5,2},{6,1},{7,0},{8,15},{9,14},{10,... | collective-permute-start | bytes 98312 | tf_op jit(solution)/shard_map/ppermute | solution.py:605
  60.1 7.2 %collective-permute-start.19 = (bf16[128,128]{1,0:T(8,128)(2,1)S(1)}, bf16[128,128]{1,0:T(8,128)(2,1)S(1)}, u32[]{:S(2)}, u32[]{:S(2)}) collective-permute-start(bf16[128,128]{1,0:T(8,128)(2,1)S(1)} %get-tuple-element.72), channel_id=1, source_target_pairs={{0,6},{1,7},{2,4},{3,5},{4,2},{5,3},{6,0},{7,1},{8,14},{9,15},{10,... | collective-permute-start | bytes 98312 | tf_op jit(solution)/shard_map/ppermute | solution.py:605
  63.7 3.8 %collective-permute-start.18 = (bf16[128,128]{1,0:T(8,128)(2,1)S(1)}, bf16[128,128]{1,0:T(8,128)(2,1)S(1)}, u32[]{:S(2)}, u32[]{:S(2)}) collective-permute-start(bf16[128,128]{1,0:T(8,128)(2,1)S(1)} %get-tuple-element.73), channel_id=1, source_target_pairs={{0,5},{1,4},{2,7},{3,6},{4,1},{5,0},{6,3},{7,2},{8,13},{9,12},{10,... | collective-permute-start | bytes 98312 | tf_op jit(solution)/shard_map/ppermute | solution.py:605
  65.1 3.9 %collective-permute-start.17 = (bf16[128,128]{1,0:T(8,128)(2,1)S(1)}, bf16[128,128]{1,0:T(8,128)(2,1)S(1)}, u32[]{:S(2)}, u32[]{:S(2)}) collective-permute-start(bf16[128,128]{1,0:T(8,128)(2,1)S(1)} %get-tuple-element.74), channel_id=1, source_target_pairs={{0,4},{1,5},{2,6},{3,7},{4,0},{5,1},{6,2},{7,3},{8,12},{9,13},{10,... | collective-permute-start | bytes 98312 | tf_op jit(solution)/shard_map/ppermute | solution.py:605
  65.6 3.5 %collective-permute-start.16 = (bf16[128,128]{1,0:T(8,128)(2,1)S(1)}, bf16[128,128]{1,0:T(8,128)(2,1)S(1)}, u32[]{:S(2)}, u32[]{:S(2)}) collective-permute-start(bf16[128,128]{1,0:T(8,128)(2,1)S(1)} %get-tuple-element.75), channel_id=1, source_target_pairs={{0,3},{1,2},{2,1},{3,0},{4,7},{5,6},{6,5},{7,4},{8,11},{9,10},{10,... | collective-permute-start | bytes 98312 | tf_op jit(solution)/shard_map/ppermute | solution.py:595
  66.4 4.1 %collective-permute-start.15 = (bf16[128,128]{1,0:T(8,128)(2,1)S(1)}, bf16[128,128]{1,0:T(8,128)(2,1)S(1)}, u32[]{:S(2)}, u32[]{:S(2)}) collective-permute-start(bf16[128,128]{1,0:T(8,128)(2,1)S(1)} %get-tuple-element.76), channel_id=1, source_target_pairs={{0,2},{1,3},{2,0},{3,1},{4,6},{5,7},{6,4},{7,5},{8,10},{9,11},{10,... | collective-permute-start | bytes 98312 | tf_op jit(solution)/shard_map/ppermute | solution.py:595
  67.2 3.3 %collective-permute-start.14 = (bf16[128,128]{1,0:T(8,128)(2,1)S(1)}, bf16[128,128]{1,0:T(8,128)(2,1)S(1)}, u32[]{:S(2)}, u32[]{:S(2)}) collective-permute-start(bf16[128,128]{1,0:T(8,128)(2,1)S(1)} %get-tuple-element.77), channel_id=1, source_target_pairs={{0,1},{1,0},{2,3},{3,2},{4,5},{5,4},{6,7},{7,6},{8,9},{9,8},{10,11... | collective-permute-start | bytes 98312 | tf_op jit(solution)/shard_map/ppermute | solution.py:595
